TPU v7x, 768 devices: a whole 4x8x12 slice. The times are simulated.
768 devices in a mesh: rep: 3 (over z_hi), fs: 32 (over z_lo, y), tp: 8 (over x, core).
Axes of the slice: x: 4, y: 8, z: 12 (z_hi: 3, z_lo: 4; z = z_hi * 4 + z_lo), core: 2. Of those that a mesh axis runs over, the one named last changes fastest.
Arguments:
- out_grad: bfloat16 [24576, 2048], P(('rep', 'fs'), 'tp'), may hold values from -6 to 6
- gate_lin: bfloat16 [24576, 5632], P(('rep', 'fs'), 'tp'), may hold values from -6 to 6
- up_lin: bfloat16 [24576, 5632], P(('rep', 'fs'), 'tp'), may hold values from -6 to 6
- conv_weight: bfloat16 [3, 5632], replicated, may hold values from -3.5 to 3.5
- gate_weight: bfloat16 [2048, 5632], P('fs', 'tp'), may hold values from -0.125 to 0.125
- up_weight: bfloat16 [2048, 5632], P('fs', 'tp'), may hold values from -0.125 to 0.125
- down_weight: bfloat16 [5632, 2048], P('tp', 'fs'), may hold values from -0.078125 to 0.078125
Outputs:
- input_grad: bfloat16 [24576, 2048], P(('rep', 'fs'), 'tp')
- conv_grad: float32 [3, 5632], replicated
All inputs are finite; a program needn't handle non-finite values.
Results may differ from a plain program's by a relative error of at most 0.015.
Values may be sent and summed in bfloat16 or wider, within the bound.
No kernel may reach another device: no remote copies, remote signals or barrier semaphores. Data moves between devices by JAX's collectives and lax.ppermute only.
A program may use at most 64 MiB of HBM per device.

v0:
```python
import math

import jax
import jax.numpy as jnp
from jax import lax
from jax.sharding import Mesh
from jax.sharding import PartitionSpec as P


Z_ALL = ("rep", "zk", "zp")
SEQ_AXES = ("zk", "zp", "y")
TP = ("x", "core")
GROUP = ("zp", "x", "core")
ROWS = ("rep", "zk", "zp", "y")
PAD = 264


def shifted(value, axis, by):
    count = lax.axis_size(axis)
    return lax.ppermute(value, axis, [(i, (i + by) % count) for i in range(count)])


def to_next(value, axis, by):
    count = lax.axis_size(axis)
    pairs = [(i, i + by) for i in range(count) if 0 <= i + by < count]
    return lax.ppermute(value, axis, pairs)


def swapped(value, axis, bit):
    return lax.ppermute(value, axis, [(i, i ^ bit) for i in range(lax.axis_size(axis))])


def sent_to_all(value, axis):
    peers = lax.axis_size(axis)
    return lax.all_to_all(
        jnp.broadcast_to(value[None], (peers, *value.shape)), axis, 0, 0, tiled=True
    )


def halves_of(value, second):
    half = value.shape[-1] // 2
    left, right = value[..., :half], value[..., half:]
    return jnp.where(second, right, left), jnp.where(second, left, right)


def gathered_z(own, other):
    relative = [
        own, shifted(other, Z_ALL, -1), shifted(own, Z_ALL, 2), shifted(other, Z_ALL, 1)
    ]
    count = len(relative)
    at = lax.axis_index(("zk", "zp"))
    return jnp.stack(
        [lax.select_n((place - at) % count, *relative) for place in range(count)], axis=1
    )


def gathered_y(block):
    pieces = [(0, 0, block)]
    half = block.shape[1] // 2
    up = down = block
    for k in range(1, 4):
        up = shifted(up, "y", 1)
        down = shifted(down, "y", -1)
        pieces += [(-k, 0, up), (k, 0, down)]
    pieces.append((4, 0, shifted(up[:, :half], "y", 1)))
    pieces.append((4, half, shifted(down[:, half:], "y", -1)))
    count, y_at = lax.axis_size("y"), lax.axis_index("y")
    parts, z_count, share, columns = block.shape
    whole = jnp.zeros((parts, z_count, count, share, columns), block.dtype)
    for k, first, piece in pieces:
        whole = lax.dynamic_update_slice(
            whole, piece[:, :, None], (0, first, (y_at + k) % count, 0, 0)
        )
    return whole.reshape(parts, -1, columns)


def gelu_parts(gate):
    normal_cdf = 0.5 * (1.0 + jax.scipy.special.erf(gate * (1.0 / math.sqrt(2.0))))
    density = jnp.exp(-0.5 * gate * gate) * (1.0 / math.sqrt(2.0 * math.pi))
    return (gate * normal_cdf, normal_cdf + gate * density)


def block_gradients(out_grad, gate_lin, up_lin, conv_weight, gate_weight, up_weight, down_weight):
    rows, columns = gate_lin.shape
    width = out_grad.shape[1]
    half = columns // 2
    second = lax.axis_index("zp") == 1

    own, other = halves_of(jnp.stack([down_weight.T, gate_weight, up_weight]), second)
    block = gathered_z(own, other)
    block, out_grad, gate_lin, up_lin = lax.optimization_barrier(
        (block, out_grad, gate_lin, up_lin)
    )
    down_full, gate_full, up_full = gathered_y(block)

    spare = ((0, 0), (0, columns - width))
    last = jnp.concatenate([gate_lin[-2:], up_lin[-1:], jnp.pad(out_grad[-1:], spare)])
    lead = jnp.concatenate([gate_lin[:2], up_lin[:1], jnp.pad(out_grad[:1], spare)])
    before = to_next(last, SEQ_AXES, 1)
    after = to_next(lead, SEQ_AXES, -1)
    grads = jnp.concatenate(
        [
            before[3:, :width],
            out_grad,
            after[3:, :width],
            jnp.zeros((PAD - rows - 2, width), out_grad.dtype),
        ]
    )
    grads = sent_to_all(grads, GROUP).reshape(2, -1, PAD, width)
    grads = grads.transpose(0, 2, 1, 3).reshape(2 * PAD, -1)

    saved = jnp.concatenate(
        [before[:2], gate_lin, after[:2], before[2:3], up_lin, after[2:3]]
    )
    kept, sent = halves_of(saved, second)
    came = swapped(sent, "zp", 1)
    pair = jnp.stack([jnp.where(second, came, kept), jnp.where(second, kept, came)])
    pair = pair.astype(jnp.float32)
    linear, up_ext = pair[:, : rows + 4], pair[:, rows + 4 :]
    start = lax.axis_index(TP) * columns + jnp.where(second, half, 0)
    taps = lax.dynamic_slice_in_dim(conv_weight, start, half, 1).astype(jnp.float32)

    gate = taps[0] * linear[:, :-2] + taps[1] * linear[:, 1:-1] + taps[2] * linear[:, 2:]
    gelu_value, gelu_slope = gelu_parts(gate)

    act_grad = jnp.dot(grads, down_full, preferred_element_type=jnp.float32)
    act_grad = act_grad.reshape(2, PAD, half)[:, : rows + 2]
    gate_grad = act_grad * up_ext * gelu_slope
    up_grad = (act_grad * gelu_value)[:, 1:-1].astype(jnp.bfloat16)
    own_grad = gate_grad[:, 1:-1]
    linear_grad = (
        taps[0] * gate_grad[:, 2:] + taps[1] * own_grad + taps[2] * gate_grad[:, :-2]
    ).astype(jnp.bfloat16)

    conv = jnp.stack(
        [jnp.sum(own_grad * linear[:, 1 + k : 1 + k + rows], axis=(0, 1)) for k in range(3)]
    )
    conv = sent_to_all(conv, Z_ALL)
    conv = conv.reshape(-1, 2, 3, half).sum(axis=0).transpose(1, 0, 2).reshape(3, columns)
    contract = (((1,), (1,)), ((), ()))
    product = lax.dot_general(
        linear_grad.reshape(-1, half), gate_full, contract, preferred_element_type=jnp.float32
    ) + lax.dot_general(
        up_grad.reshape(-1, half), up_full, contract, preferred_element_type=jnp.float32
    )
    product = product.astype(jnp.bfloat16).reshape(2, rows, -1, width)
    product = product.transpose(0, 2, 1, 3).reshape(-1, rows, width)
    conv, product = lax.optimization_barrier((conv, product))
    arrived = lax.all_to_all(product, GROUP, 0, 0, tiled=True)
    input_grad = arrived.astype(jnp.float32).sum(axis=0).astype(jnp.bfloat16)
    for bit in (1, 2, 4):
        conv = conv + swapped(conv, "y", bit)
    conv = conv[None]
    for axis, bit in (("core", 1), ("x", 1), ("x", 2)):
        low = lax.axis_index(axis) & bit == 0
        peer = swapped(conv, axis, bit)
        conv = jnp.concatenate([jnp.where(low, conv, peer), jnp.where(low, peer, conv)])
    conv_grad = conv.transpose(1, 0, 2).reshape(3, -1)
    return (input_grad, conv_grad)


def solution(mesh):
    finer = Mesh(
        mesh.devices.reshape(mesh.shape["rep"], 2, 2, 8, 4, 2),
        ("rep", "zk", "zp", "y", "x", "core"),
    )
    return jax.shard_map(
        block_gradients,
        mesh=finer,
        in_specs=(
            P(ROWS, TP),
            P(ROWS, TP),
            P(ROWS, TP),
            P(),
            P(SEQ_AXES, TP),
            P(SEQ_AXES, TP),
            P(TP, SEQ_AXES),
        ),
        out_specs=(P(ROWS, TP), P()),
        check_vma=False,
    )
```

profile of v0, /device:TPU:1, one launch (start us, length us, event | category | flops | bytes accessed | tf_op | source)
XLA Modules:
  0.0 203.6 jit_solution(2529014050315000189)
XLA Ops:
  0.7 1.1 pad_maximum_fusion.1
  1.7 0.1 broadcast_select_fusion.2
  1.9 15.1 %collective-permute-start = (bf16[3,64,352]{2,1,0:T(8,128)(2,1)S(1)}, bf16[3,64,352]{2,1,0:T(8,128)(2,1)S(1)}, u32[]{:S(2)}, u32[]{:S(2)}) collective-permute-start(bf16[3,64,352]{2,1,0:T(8,128)(2,1)S(1)} %get-tuple-element.36), channel_id=1, source_target_pairs={{0,704},{64,0},{128,64},{192,128},{256,192},{320,256},{384,320},{4... | collective-permute-start | bytes 405512 | tf_op jit(solution)/shard_map/ppermute | solution.py:20
  17.0 1.9 collective-permute-start.1
  18.9 1.9 collective-permute-start.2
  20.9 8.7 %collective-permute-done.1 = bf16[3,64,352]{2,1,0:T(8,128)(2,1)S(1)} collective-permute-done((bf16[3,64,352]{2,1,0:T(8,128)(2,1)S(1)}, bf16[3,64,352]{2,1,0:T(8,128)(2,1)S(1)}, u32[]{:S(2)}, u32[]{:S(2)}) %collective-permute-start.1) | collective-permute-done | bytes 135200 | tf_op jit(solution)/shard_map/ppermute | solution.py:20
  29.7 0.3 collective-permute-done.2
  30.1 0.1 pad_maximum_fusion
  30.2 1.2 copy.81
  31.4 0.2 copy.82
  31.7 1.3 collective-permute-start.4
  33.0 4.0 %collective-permute-start.3 = (bf16[4,704]{1,0:T(4,128)(2,1)S(1)}, bf16[4,704]{1,0:T(4,128)(2,1)S(1)}, u32[]{:S(2)}, u32[]{:S(2)}) collective-permute-start(bf16[4,704]{1,0:T(4,128)(2,1)S(1)} %fusion.18), channel_id=1, source_target_pairs={{0,8},{8,16},{16,24},{24,32},{32,40},{40,48},{48,56},{56,64},{64,7... | collective-permute-start | bytes 16904 | tf_op jit(solution)/shard_map/ppermute | solution.py:26
  37.1 0.7 collective-permute-done.3
  37.9 1.5 broadcast_in_dim.49
  39.3 13.4 %all-to-all-start = ((bf16[16,264,256]{2,1,0:T(8,128)(2,1)}), bf16[16,264,256]{2,1,0:T(8,128)(2,1)}, u32[]{:S(2)}, u32[]{:S(2)}) async-start(bf16[16,264,256]{2,1,0:T(8,128)(2,1)} %broadcast_in_dim.49), calls=%async_computation | async-start | bytes 4325376 | tf_op jit(solution)/shard_map/all_to_all | solution.py:35
  52.7 0.8 dynamic-slice_convert_fusion
  53.5 1.9 collective-permute-start.5
  55.4 4.6 %collective-permute-start.6 = (bf16[3,4,64,352]{3,2,0,1:T(8,128)(2,1)S(1)}, bf16[3,4,64,352]{3,2,0,1:T(8,128)(2,1)S(1)}, u32[]{:S(2)}, u32[]{:S(2)}) collective-permute-start(bf16[3,4,64,352]{3,2,0,1:T(8,128)(2,1)S(1)} %pad_maximum_fusion), channel_id=1, source_target_pairs={{0,56},{8,0},{16,8},{24,16},{32,24},{40,32},{48,40},{56,48},{1,57}... | collective-permute-start | bytes 1622024 | tf_op jit(solution)/shard_map/ppermute | solution.py:20
  60.0 2.8 %concatenate.24 = bf16[518,704]{1,0:T(8,128)(2,1)S(1)} concatenate(bf16[2,704]{1,0:T(2,128)(2,1)S(1)} %slice.158, bf16[256,704]{1,0:T(8,128)(2,1)S(1)} %copy.81, bf16[2,704]{1,0:T(2,128)(2,1)S(1)} %slice.159, bf16[1,704]{1,0:T(2,128)(2,1)S(1)} %slice.160, bf16[256,704]{1,0:T(8,128)(2,1)S(1)} %copy.82, bf16[1,704]{1,0:T(2,128)(2,1)S(1)} %slice.161), dimensions={0} | concatenate | bytes 1458688 | tf_op jit(solution)/shard_map/concatenate | solution.py:112
  62.8 0.2 broadcast_select_fusion.1
  63.0 3.3 %collective-permute-start.13 = (bf16[518,352]{1,0:T(8,128)(2,1)S(1)}, bf16[518,352]{1,0:T(8,128)(2,1)}, u32[]{:S(2)}, u32[]{:S(2)}) collective-permute-start(bf16[518,352]{1,0:T(8,128)(2,1)S(1)} %broadcast_select_fusion.1), channel_id=1, source_target_pairs={{0,64},{64,0},{1,65},{65,1},{2,66},{66,2},{3,67},{67,3},{4,68},{68... | collective-permute-start | bytes 1094024 | tf_op jit(solution)/shard_map/ppermute | solution.py:30
  66.4 0.8 broadcast_in_dim.50
  67.2 0.1 copy_dynamic-update-slice_fusion.6
  67.3 20.4 %collective-permute-done.13 = bf16[518,352]{1,0:T(8,128)(2,1)} collective-permute-done((bf16[518,352]{1,0:T(8,128)(2,1)S(1)}, bf16[518,352]{1,0:T(8,128)(2,1)}, u32[]{:S(2)}, u32[]{:S(2)}) %collective-permute-start.13) | collective-permute-done | bytes 364704 | tf_op jit(solution)/shard_map/ppermute | solution.py:30
  87.7 1.2 select_bitcast_fusion.1
  88.9 1.9 collective-permute-start.7
  90.8 4.6 %collective-permute-start.8 = (bf16[3,4,64,352]{3,2,0,1:T(8,128)(2,1)S(1)}, bf16[3,4,64,352]{3,2,0,1:T(8,128)(2,1)S(1)}, u32[]{:S(2)}, u32[]{:S(2)}) collective-permute-start(bf16[3,4,64,352]{3,2,0,1:T(8,128)(2,1)S(1)} %collective-permute-done.6), channel_id=1, source_target_pairs={{0,56},{8,0},{16,8},{24,16},{32,24},{40,32},{48,40},{56,48},{1,57}... | collective-permute-start | bytes 1622024 | tf_op jit(solution)/shard_map/ppermute | solution.py:20
  95.4 0.2 maximum_convert_fusion
  95.6 1.6 add_multiply_fusion
  97.2 8.6 %collective-permute-done.7 = bf16[3,4,64,352]{3,2,0,1:T(8,128)(2,1)S(1)} collective-permute-done((bf16[3,4,64,352]{3,2,0,1:T(8,128)(2,1)S(1)}, bf16[3,4,64,352]{3,2,0,1:T(8,128)(2,1)S(1)}, u32[]{:S(2)}, u32[]{:S(2)}) %collective-permute-start.7) | collective-permute-done | bytes 540704 | tf_op jit(solution)/shard_map/ppermute | solution.py:20
  105.9 1.9 collective-permute-start.9
  107.8 4.6 %collective-permute-start.10 = (bf16[3,4,64,352]{3,2,0,1:T(8,128)(2,1)S(1)}, bf16[3,4,64,352]{3,2,0,1:T(8,128)(2,1)S(1)}, u32[]{:S(2)}, u32[]{:S(2)}) collective-permute-start(bf16[3,4,64,352]{3,2,0,1:T(8,128)(2,1)S(1)} %collective-permute-done.8), channel_id=1, source_target_pairs={{0,56},{8,0},{16,8},{24,16},{32,24},{40,32},{48,40},{56,48},{1,57}... | collective-permute-start | bytes 1622024 | tf_op jit(solution)/shard_map/ppermute | solution.py:20
  112.8 9.3 %collective-permute-done.9 = bf16[3,4,64,352]{3,2,0,1:T(8,128)(2,1)S(1)} collective-permute-done((bf16[3,4,64,352]{3,2,0,1:T(8,128)(2,1)S(1)}, bf16[3,4,64,352]{3,2,0,1:T(8,128)(2,1)S(1)}, u32[]{:S(2)}, u32[]{:S(2)}) %collective-permute-start.9) | collective-permute-done | bytes 540704 | tf_op jit(solution)/shard_map/ppermute | solution.py:20
  122.1 1.9 collective-permute-start.11
  124.1 4.6 %collective-permute-start.12 = (bf16[3,2,64,352]{3,2,0,1:T(8,128)(2,1)S(1)}, bf16[3,2,64,352]{3,2,0,1:T(8,128)(2,1)S(1)}, u32[]{:S(2)}, u32[]{:S(2)}) collective-permute-start(bf16[3,2,64,352]{3,2,0,1:T(8,128)(2,1)S(1)} %slice.157), channel_id=1, source_target_pairs={{0,56},{8,0},{16,8},{24,16},{32,24},{40,32},{48,40},{56,48},{1,57}... | collective-permute-start | bytes 811016 | tf_op jit(solution)/shard_map/ppermute | solution.py:20
  128.9 2.2 %collective-permute-done.11 = bf16[3,2,64,352]{3,2,0,1:T(8,128)(2,1)S(1)} collective-permute-done((bf16[3,2,64,352]{3,2,0,1:T(8,128)(2,1)S(1)}, bf16[3,2,64,352]{3,2,0,1:T(8,128)(2,1)S(1)}, u32[]{:S(2)}, u32[]{:S(2)}) %collective-permute-start.11) | collective-permute-done | bytes 270368 | tf_op jit(solution)/shard_map/ppermute | solution.py:20
  131.1 1.2 collective-permute-done.12
  132.3 2.2 %fusion.21 = (bf16[1,4,8,64,352]{4,3,2,1,0:T(8,128)(2,1)}, bf16[1,4,8,64,352]{4,3,2,1,0:T(8,128)(2,1)S(1)}, bf16[1,4,8,64,352]{4,3,2,1,0:T(8,128)(2,1)}) fusion(bf16[3,4,8,64,352]{4,3,2,1,0:T(8,128)(2,1)S(1)} %copy_dynamic-update-slice_fusion.7), kind=kLoop, calls=%fused_computation.74 | loop fusion | bytes 8650752 | tf_op jit(solution)/shard_map/unstack | solution.py:94
  134.6 2.0 copy.107
  136.6 0.3 copy-done.4
  136.9 1.5 fusion.6
  138.4 1.7 fusion.15
  140.1 0.6 broadcast_in_dim.60
  140.8 4.7 %all-to-all-start.1 = ((f32[12,3,352]{2,1,0:T(4,128)}), f32[12,3,352]{2,1,0:T(4,128)S(1)}, u32[]{:S(2)}, u32[]{:S(2)}) async-start(f32[12,3,352]{2,1,0:T(4,128)} %broadcast_in_dim.60), calls=%async_computation.1 | async-start | bytes 147456 | tf_op jit(solution)/shard_map/all_to_all | solution.py:35
  145.5 2.3 %fusion.25 = f32[512,2048]{1,0:T(8,128)S(1)} fusion(bf16[512,352]{1,0:T(8,128)(2,1)} %bitcast.81, bf16[2048,352]{1,0:T(8,128)(2,1)S(1)} %bitcast.77), kind=kOutput, calls=%fused_computation.78 | convolution fusion | flops 738197504 | bytes 5996544 | tf_op jit(solution)/shard_map/dot_general | solution.py:141
  147.8 1.3 add_convert_fusion
  149.1 0.7 copy.108
  149.8 1.8 copy.100
  151.6 3.6 %all-to-all-done.1 = f32[12,3,352]{2,1,0:T(4,128)S(1)} async-done(((f32[12,3,352]{2,1,0:T(4,128)}), f32[12,3,352]{2,1,0:T(4,128)S(1)}, u32[]{:S(2)}, u32[]{:S(2)}) %all-to-all-start.1) | async-done | bytes 50720 | tf_op jit(solution)/shard_map/all_to_all | solution.py:35
  155.3 10.5 %all-to-all-start.2 = ((bf16[16,256,256]{2,1,0:T(8,128)(2,1)}), bf16[16,256,256]{2,1,0:T(8,128)(2,1)S(1)}, u32[]{:S(2)}, u32[]{:S(2)}) async-start(bf16[16,256,256]{2,1,0:T(8,128)(2,1)} %bitcast.30), calls=%async_computation.2 | async-start | bytes 4194304 | tf_op jit(solution)/shard_map/all_to_all | solution.py:149
  165.8 1.9 collective-permute-start.14
  167.7 2.8 %collective-permute-done.14 = f32[3,704]{1,0:T(4,128)S(1)} collective-permute-done((f32[3,704]{1,0:T(4,128)S(1)}, f32[3,704]{1,0:T(4,128)S(1)}, u32[]{:S(2)}, u32[]{:S(2)}) %collective-permute-start.14) | collective-permute-done | bytes 8480 | tf_op jit(solution)/shard_map/ppermute | solution.py:30
  170.5 4.4 %collective-permute-start.15 = (f32[3,704]{1,0:T(4,128)S(1)}, f32[3,704]{1,0:T(4,128)S(1)}, u32[]{:S(2)}, u32[]{:S(2)}) collective-permute-start(f32[3,704]{1,0:T(4,128)S(1)} %add.173), channel_id=1, source_target_pairs={{0,16},{8,24},{16,0},{24,8},{32,48},{40,56},{48,32},{56,40},{1,17}... | collective-permute-start | bytes 25352 | tf_op jit(solution)/shard_map/ppermute | solution.py:30
  174.9 1.4 collective-permute-done.15
  176.3 4.6 %collective-permute-start.16 = (f32[3,704]{1,0:T(4,128)S(1)}, f32[3,704]{1,0:T(4,128)S(1)}, u32[]{:S(2)}, u32[]{:S(2)}) collective-permute-start(f32[3,704]{1,0:T(4,128)S(1)} %add.174), channel_id=1, source_target_pairs={{0,32},{8,40},{16,48},{24,56},{32,0},{40,8},{48,16},{56,24},{1,33}... | collective-permute-start | bytes 25352 | tf_op jit(solution)/shard_map/ppermute | solution.py:30
  180.9 3.7 %collective-permute-done.16 = f32[3,704]{1,0:T(4,128)S(1)} collective-permute-done((f32[3,704]{1,0:T(4,128)S(1)}, f32[3,704]{1,0:T(4,128)S(1)}, u32[]{:S(2)}, u32[]{:S(2)}) %collective-permute-start.16) | collective-permute-done | bytes 8480 | tf_op jit(solution)/shard_map/ppermute | solution.py:30
  184.6 4.7 %collective-permute-start.17 = (f32[1,3,704]{2,1,0:T(4,128)S(1)}, f32[1,3,704]{2,1,0:T(4,128)S(1)}, u32[]{:S(2)}, u32[]{:S(2)}) collective-permute-start(f32[1,3,704]{2,1,0:T(4,128)S(1)} %add_bitcast_fusion), channel_id=1, source_target_pairs={{0,1},{1,0},{2,3},{3,2},{4,5},{5,4},{6,7},{7,6},{8,9},{9,8},{10,11... | collective-permute-start | bytes 25352 | tf_op jit(solution)/shard_map/ppermute | solution.py:30
  189.4 0.8 collective-permute-done.17
  190.2 4.0 %collective-permute-start.18 = (f32[2,3,704]{2,1,0:T(4,128)S(1)}, f32[2,3,704]{2,1,0:T(4,128)S(1)}, u32[]{:S(2)}, u32[]{:S(2)}) collective-permute-start(f32[2,3,704]{2,1,0:T(4,128)S(1)} %pad_maximum_fusion.3), channel_id=1, source_target_pairs={{0,2},{2,0},{4,6},{6,4},{1,3},{3,1},{5,7},{7,5},{8,10},{10,8},{12,... | collective-permute-start | bytes 50696 | tf_op jit(solution)/shard_map/ppermute | solution.py:30
  194.2 1.2 collective-permute-done.18
  195.4 4.4 %collective-permute-start.19 = (f32[4,3,704]{2,1,0:T(4,128)S(1)}, f32[4,3,704]{2,1,0:T(4,128)S(1)}, u32[]{:S(2)}, u32[]{:S(2)}) collective-permute-start(f32[4,3,704]{2,1,0:T(4,128)S(1)} %pad_maximum_fusion.2), channel_id=1, source_target_pairs={{0,4},{2,6},{4,0},{6,2},{1,5},{3,7},{5,1},{7,3},{8,12},{10,14},{12... | collective-permute-start | bytes 101384 | tf_op jit(solution)/shard_map/ppermute | solution.py:30
  199.9 1.9 collective-permute-done.19
  201.9 0.7 reshape.51
  202.6 1.0 reduce_sum.52
  (64 shorter events, 1.6 us)
Async XLA Ops:
  0.6 31.0 %copy-start.6 = (bf16[256,256]{1,0:T(8,128)(2,1)S(1)}, bf16[256,256]{1,0:T(8,128)(2,1)}, u32[]{:S(2)}) copy-start(bf16[256,256]{1,0:T(8,128)(2,1)} %param.7) | copy-start | bytes 393220
  0.6 30.8 %copy-start.5 = (bf16[256,704]{0,1:T(8,128)(2,1)S(1)}, bf16[256,704]{0,1:T(8,128)(2,1)}, u32[]{:S(2)}) copy-start(bf16[256,704]{0,1:T(8,128)(2,1)} %param.9) | copy-start | bytes 1081348
  1.9 19.1 %collective-permute-start = (bf16[3,64,352]{2,1,0:T(8,128)(2,1)S(1)}, bf16[3,64,352]{2,1,0:T(8,128)(2,1)S(1)}, u32[]{:S(2)}, u32[]{:S(2)}) collective-permute-start(bf16[3,64,352]{2,1,0:T(8,128)(2,1)S(1)} %get-tuple-element.36), channel_id=1, source_target_pairs={{0,704},{64,0},{128,64},{192,128},{256,192},{320,256},{384,320},{4... | collective-permute-start | bytes 405512 | tf_op jit(solution)/shard_map/ppermute | solution.py:20
  17.0 12.7 %collective-permute-start.1 = (bf16[3,64,352]{2,1,0:T(8,128)(2,1)S(1)}, bf16[3,64,352]{2,1,0:T(8,128)(2,1)S(1)}, u32[]{:S(2)}, u32[]{:S(2)}) collective-permute-start(bf16[3,64,352]{2,1,0:T(8,128)(2,1)S(1)} %get-tuple-element.37), channel_id=1, source_target_pairs={{0,128},{64,192},{128,256},{192,320},{256,384},{320,448},{384,512}... | collective-permute-start | bytes 405512 | tf_op jit(solution)/shard_map/ppermute | solution.py:20
  18.9 11.1 %collective-permute-start.2 = (bf16[3,64,352]{2,1,0:T(8,128)(2,1)S(1)}, bf16[3,64,352]{2,1,0:T(8,128)(2,1)S(1)}, u32[]{:S(2)}, u32[]{:S(2)}) collective-permute-start(bf16[3,64,352]{2,1,0:T(8,128)(2,1)S(1)} %get-tuple-element.36), channel_id=1, source_target_pairs={{0,64},{64,128},{128,192},{192,256},{256,320},{320,384},{384,448},... | collective-permute-start | bytes 405512 | tf_op jit(solution)/shard_map/ppermute | solution.py:20
  31.7 5.4 %collective-permute-start.4 = (bf16[4,704]{1,0:T(4,128)(2,1)S(1)}, bf16[4,704]{1,0:T(4,128)(2,1)S(1)}, u32[]{:S(2)}, u32[]{:S(2)}) collective-permute-start(bf16[4,704]{1,0:T(4,128)(2,1)S(1)} %fusion.19), channel_id=1, source_target_pairs={{8,0},{16,8},{24,16},{32,24},{40,32},{48,40},{56,48},{64,56},{72,6... | collective-permute-start | bytes 16904 | tf_op jit(solution)/shard_map/ppermute | solution.py:26
  33.0 4.8 %collective-permute-start.3 = (bf16[4,704]{1,0:T(4,128)(2,1)S(1)}, bf16[4,704]{1,0:T(4,128)(2,1)S(1)}, u32[]{:S(2)}, u32[]{:S(2)}) collective-permute-start(bf16[4,704]{1,0:T(4,128)(2,1)S(1)} %fusion.18), channel_id=1, source_target_pairs={{0,8},{8,16},{16,24},{24,32},{32,40},{40,48},{48,56},{56,64},{64,7... | collective-permute-start | bytes 16904 | tf_op jit(solution)/shard_map/ppermute | solution.py:26
  39.3 95.2 %all-to-all-start = ((bf16[16,264,256]{2,1,0:T(8,128)(2,1)}), bf16[16,264,256]{2,1,0:T(8,128)(2,1)}, u32[]{:S(2)}, u32[]{:S(2)}) async-start(bf16[16,264,256]{2,1,0:T(8,128)(2,1)} %broadcast_in_dim.49), calls=%async_computation | async-start | bytes 4325376 | tf_op jit(solution)/shard_map/all_to_all | solution.py:35
  53.5 35.4 %collective-permute-start.5 = (bf16[3,4,64,352]{3,2,0,1:T(8,128)(2,1)S(1)}, bf16[3,4,64,352]{3,2,0,1:T(8,128)(2,1)S(1)}, u32[]{:S(2)}, u32[]{:S(2)}) collective-permute-start(bf16[3,4,64,352]{3,2,0,1:T(8,128)(2,1)S(1)} %pad_maximum_fusion), channel_id=1, source_target_pairs={{0,8},{8,16},{16,24},{24,32},{32,40},{40,48},{48,56},{56,0},{1,9},... | collective-permute-start | bytes 1622024 | tf_op jit(solution)/shard_map/ppermute | solution.py:20
  55.4 35.4 %collective-permute-start.6 = (bf16[3,4,64,352]{3,2,0,1:T(8,128)(2,1)S(1)}, bf16[3,4,64,352]{3,2,0,1:T(8,128)(2,1)S(1)}, u32[]{:S(2)}, u32[]{:S(2)}) collective-permute-start(bf16[3,4,64,352]{3,2,0,1:T(8,128)(2,1)S(1)} %pad_maximum_fusion), channel_id=1, source_target_pairs={{0,56},{8,0},{16,8},{24,16},{32,24},{40,32},{48,40},{56,48},{1,57}... | collective-permute-start | bytes 1622024 | tf_op jit(solution)/shard_map/ppermute | solution.py:20
  63.0 24.7 %collective-permute-start.13 = (bf16[518,352]{1,0:T(8,128)(2,1)S(1)}, bf16[518,352]{1,0:T(8,128)(2,1)}, u32[]{:S(2)}, u32[]{:S(2)}) collective-permute-start(bf16[518,352]{1,0:T(8,128)(2,1)S(1)} %broadcast_select_fusion.1), channel_id=1, source_target_pairs={{0,64},{64,0},{1,65},{65,1},{2,66},{66,2},{3,67},{67,3},{4,68},{68... | collective-permute-start | bytes 1094024 | tf_op jit(solution)/shard_map/ppermute | solution.py:30
  88.9 17.0 %collective-permute-start.7 = (bf16[3,4,64,352]{3,2,0,1:T(8,128)(2,1)S(1)}, bf16[3,4,64,352]{3,2,0,1:T(8,128)(2,1)S(1)}, u32[]{:S(2)}, u32[]{:S(2)}) collective-permute-start(bf16[3,4,64,352]{3,2,0,1:T(8,128)(2,1)S(1)} %collective-permute-done.5), channel_id=1, source_target_pairs={{0,8},{8,16},{16,24},{24,32},{32,40},{40,48},{48,56},{56,0},{1,9},... | collective-permute-start | bytes 1622024 | tf_op jit(solution)/shard_map/ppermute | solution.py:20
  90.8 17.0 %collective-permute-start.8 = (bf16[3,4,64,352]{3,2,0,1:T(8,128)(2,1)S(1)}, bf16[3,4,64,352]{3,2,0,1:T(8,128)(2,1)S(1)}, u32[]{:S(2)}, u32[]{:S(2)}) collective-permute-start(bf16[3,4,64,352]{3,2,0,1:T(8,128)(2,1)S(1)} %collective-permute-done.6), channel_id=1, source_target_pairs={{0,56},{8,0},{16,8},{24,16},{32,24},{40,32},{48,40},{56,48},{1,57}... | collective-permute-start | bytes 1622024 | tf_op jit(solution)/shard_map/ppermute | solution.py:20
  105.9 16.2 %collective-permute-start.9 = (bf16[3,4,64,352]{3,2,0,1:T(8,128)(2,1)S(1)}, bf16[3,4,64,352]{3,2,0,1:T(8,128)(2,1)S(1)}, u32[]{:S(2)}, u32[]{:S(2)}) collective-permute-start(bf16[3,4,64,352]{3,2,0,1:T(8,128)(2,1)S(1)} %collective-permute-done.7), channel_id=1, source_target_pairs={{0,8},{8,16},{16,24},{24,32},{32,40},{40,48},{48,56},{56,0},{1,9},... | collective-permute-start | bytes 1622024 | tf_op jit(solution)/shard_map/ppermute | solution.py:20
  107.8 16.2 %collective-permute-start.10 = (bf16[3,4,64,352]{3,2,0,1:T(8,128)(2,1)S(1)}, bf16[3,4,64,352]{3,2,0,1:T(8,128)(2,1)S(1)}, u32[]{:S(2)}, u32[]{:S(2)}) collective-permute-start(bf16[3,4,64,352]{3,2,0,1:T(8,128)(2,1)S(1)} %collective-permute-done.8), channel_id=1, source_target_pairs={{0,56},{8,0},{16,8},{24,16},{32,24},{40,32},{48,40},{56,48},{1,57}... | collective-permute-start | bytes 1622024 | tf_op jit(solution)/shard_map/ppermute | solution.py:20
  122.1 9.0 %collective-permute-start.11 = (bf16[3,2,64,352]{3,2,0,1:T(8,128)(2,1)S(1)}, bf16[3,2,64,352]{3,2,0,1:T(8,128)(2,1)S(1)}, u32[]{:S(2)}, u32[]{:S(2)}) collective-permute-start(bf16[3,2,64,352]{3,2,0,1:T(8,128)(2,1)S(1)} %slice.156), channel_id=1, source_target_pairs={{0,8},{8,16},{16,24},{24,32},{32,40},{40,48},{48,56},{56,0},{1,9},... | collective-permute-start | bytes 811016 | tf_op jit(solution)/shard_map/ppermute | solution.py:20
  124.1 8.2 %collective-permute-start.12 = (bf16[3,2,64,352]{3,2,0,1:T(8,128)(2,1)S(1)}, bf16[3,2,64,352]{3,2,0,1:T(8,128)(2,1)S(1)}, u32[]{:S(2)}, u32[]{:S(2)}) collective-permute-start(bf16[3,2,64,352]{3,2,0,1:T(8,128)(2,1)S(1)} %slice.157), channel_id=1, source_target_pairs={{0,56},{8,0},{16,8},{24,16},{32,24},{40,32},{48,40},{56,48},{1,57}... | collective-permute-start | bytes 811016 | tf_op jit(solution)/shard_map/ppermute | solution.py:20
  134.6 2.0 %copy-start.2 = (f32[2,258,352]{2,1,0:T(8,128)S(1)}, f32[2,258,352]{2,1,0:T(8,128)}, u32[]{:S(2)}) copy-start(f32[2,258,352]{2,1,0:T(8,128)} %get-tuple-element.21) | copy-start | bytes 2179588
  134.6 2.3 %copy-start.4 = (bf16[1,4,8,64,352]{4,3,2,1,0:T(8,128)(2,1)S(1)}, bf16[1,4,8,64,352]{4,3,2,1,0:T(8,128)(2,1)}, u32[]{:S(2)}) copy-start(bf16[1,4,8,64,352]{4,3,2,1,0:T(8,128)(2,1)} %get-tuple-element.24) | copy-start | bytes 4325380
  136.9 1.5 copy-start.1
  140.1 7.7 %copy-start = (bf16[1,4,8,64,352]{4,3,2,1,0:T(8,128)(2,1)S(1)}, bf16[1,4,8,64,352]{4,3,2,1,0:T(8,128)(2,1)}, u32[]{:S(2)}) copy-start(bf16[1,4,8,64,352]{4,3,2,1,0:T(8,128)(2,1)} %get-tuple-element.22) | copy-start | bytes 4325380
  140.8 14.4 %all-to-all-start.1 = ((f32[12,3,352]{2,1,0:T(4,128)}), f32[12,3,352]{2,1,0:T(4,128)S(1)}, u32[]{:S(2)}, u32[]{:S(2)}) async-start(f32[12,3,352]{2,1,0:T(4,128)} %broadcast_in_dim.60), calls=%async_computation.1 | async-start | bytes 147456 | tf_op jit(solution)/shard_map/all_to_all | solution.py:35
  145.5 2.4 %copy-start.3 = (bf16[2,256,352]{2,1,0:T(8,128)(2,1)S(1)}, bf16[2,256,352]{2,1,0:T(8,128)(2,1)}, u32[]{:S(2)}) copy-start(bf16[2,256,352]{2,1,0:T(8,128)(2,1)} %get-tuple-element.48) | copy-start | bytes 1081348
  155.3 47.3 %all-to-all-start.2 = ((bf16[16,256,256]{2,1,0:T(8,128)(2,1)}), bf16[16,256,256]{2,1,0:T(8,128)(2,1)S(1)}, u32[]{:S(2)}, u32[]{:S(2)}) async-start(bf16[16,256,256]{2,1,0:T(8,128)(2,1)} %bitcast.30), calls=%async_computation.2 | async-start | bytes 4194304 | tf_op jit(solution)/shard_map/all_to_all | solution.py:149
  165.8 4.7 %collective-permute-start.14 = (f32[3,704]{1,0:T(4,128)S(1)}, f32[3,704]{1,0:T(4,128)S(1)}, u32[]{:S(2)}, u32[]{:S(2)}) collective-permute-start(f32[3,704]{1,0:T(4,128)S(1)} %reshape.46), channel_id=1, source_target_pairs={{0,8},{8,0},{16,24},{24,16},{32,40},{40,32},{48,56},{56,48},{1,9},... | collective-permute-start | bytes 25352 | tf_op jit(solution)/shard_map/ppermute | solution.py:30
  170.5 5.8 %collective-permute-start.15 = (f32[3,704]{1,0:T(4,128)S(1)}, f32[3,704]{1,0:T(4,128)S(1)}, u32[]{:S(2)}, u32[]{:S(2)}) collective-permute-start(f32[3,704]{1,0:T(4,128)S(1)} %add.173), channel_id=1, source_target_pairs={{0,16},{8,24},{16,0},{24,8},{32,48},{40,56},{48,32},{56,40},{1,17}... | collective-permute-start | bytes 25352 | tf_op jit(solution)/shard_map/ppermute | solution.py:30
  176.3 8.3 %collective-permute-start.16 = (f32[3,704]{1,0:T(4,128)S(1)}, f32[3,704]{1,0:T(4,128)S(1)}, u32[]{:S(2)}, u32[]{:S(2)}) collective-permute-start(f32[3,704]{1,0:T(4,128)S(1)} %add.174), channel_id=1, source_target_pairs={{0,32},{8,40},{16,48},{24,56},{32,0},{40,8},{48,16},{56,24},{1,33}... | collective-permute-start | bytes 25352 | tf_op jit(solution)/shard_map/ppermute | solution.py:30
  184.6 5.6 %collective-permute-start.17 = (f32[1,3,704]{2,1,0:T(4,128)S(1)}, f32[1,3,704]{2,1,0:T(4,128)S(1)}, u32[]{:S(2)}, u32[]{:S(2)}) collective-permute-start(f32[1,3,704]{2,1,0:T(4,128)S(1)} %add_bitcast_fusion), channel_id=1, source_target_pairs={{0,1},{1,0},{2,3},{3,2},{4,5},{5,4},{6,7},{7,6},{8,9},{9,8},{10,11... | collective-permute-start | bytes 25352 | tf_op jit(solution)/shard_map/ppermute | solution.py:30
  190.2 5.2 %collective-permute-start.18 = (f32[2,3,704]{2,1,0:T(4,128)S(1)}, f32[2,3,704]{2,1,0:T(4,128)S(1)}, u32[]{:S(2)}, u32[]{:S(2)}) collective-permute-start(f32[2,3,704]{2,1,0:T(4,128)S(1)} %pad_maximum_fusion.3), channel_id=1, source_target_pairs={{0,2},{2,0},{4,6},{6,4},{1,3},{3,1},{5,7},{7,5},{8,10},{10,8},{12,... | collective-permute-start | bytes 50696 | tf_op jit(solution)/shard_map/ppermute | solution.py:30
  195.4 6.3 %collective-permute-start.19 = (f32[4,3,704]{2,1,0:T(4,128)S(1)}, f32[4,3,704]{2,1,0:T(4,128)S(1)}, u32[]{:S(2)}, u32[]{:S(2)}) collective-permute-start(f32[4,3,704]{2,1,0:T(4,128)S(1)} %pad_maximum_fusion.2), channel_id=1, source_target_pairs={{0,4},{2,6},{4,0},{6,2},{1,5},{3,7},{5,1},{7,3},{8,12},{10,14},{12... | collective-permute-start | bytes 101384 | tf_op jit(solution)/shard_map/ppermute | solution.py:30
where the time goes:
time: 206 us; the launch traced here: 204 us
  starting transfers between devices  106 us (51%)
  waiting for transfers between devices  66.7 us (32%)
  local copies, waits for them, and re-layouts  16 us (8%)
  other arithmetic  8.24 us (4%)
  matrix products  5.11 us (2%)
    ppermute x11, starting transfers between devices, shifted(): lax.ppermute(value, axis, [(i, (i + by) % count) for i in range(count)])  44.9 us
    ppermute x7, waiting for transfers between devices, swapped(): lax.ppermute(value, axis, [(i, i ^ bit) for i in range(lax.axis_size(axis...  32.1 us
    ppermute x11, waiting for transfers between devices, shifted(): lax.ppermute(value, axis, [(i, (i + by) % count) for i in range(count)])  30.3 us
    ppermute x7, starting transfers between devices, swapped(): lax.ppermute(value, axis, [(i, i ^ bit) for i in range(lax.axis_size(axis...  27.3 us
    all_to_all x2, starting transfers between devices, sent_to_all(): lax.all_to_all(jnp.broadcast_to(value[None], (peers, *value.shape)), axis...  18.1 us
    all_to_all x1, starting transfers between devices, block_gradients(): arrived = lax.all_to_all(product, GROUP, 0, 0, tiled=True)  10.5 us
    ppermute x2, starting transfers between devices, to_next(): return lax.ppermute(value, axis, pairs)  5.28 us
  transfers between devices with their start and end apart: 23, of which 15 were waited for; matrix products, arithmetic and copies ran while one was open for 9% of the time, Pallas kernels for 0%

commit v1 on v0

--- a/solution.py
+++ b/solution.py
@@ -3,6 +3,8 @@
 import jax
 import jax.numpy as jnp
 from jax import lax
+from jax.experimental import pallas as pl
+from jax.experimental.pallas import tpu as pltpu
 from jax.sharding import Mesh
 from jax.sharding import PartitionSpec as P
 
@@ -44,9 +46,7 @@
 
 
 def gathered_z(own, other):
-    relative = [
-        own, shifted(other, Z_ALL, -1), shifted(own, Z_ALL, 2), shifted(other, Z_ALL, 1)
-    ]
+    relative = [own, shifted(other, Z_ALL, -1), shifted(own, Z_ALL, 2), shifted(other, Z_ALL, 1)]
     count = len(relative)
     at = lax.axis_index(("zk", "zp"))
     return jnp.stack(
@@ -55,6 +55,10 @@
 
 
 def gathered_y(block):
+    count, y_at = lax.axis_size("y"), lax.axis_index("y")
+    parts, z_count, share, columns = block.shape
+    whole = jnp.zeros((parts, z_count, count, share, columns), block.dtype)
+    block, whole = lax.optimization_barrier((block, whole))
     pieces = [(0, 0, block)]
     half = block.shape[1] // 2
     up = down = block
@@ -64,9 +68,6 @@
         pieces += [(-k, 0, up), (k, 0, down)]
     pieces.append((4, 0, shifted(up[:, :half], "y", 1)))
     pieces.append((4, half, shifted(down[:, half:], "y", -1)))
-    count, y_at = lax.axis_size("y"), lax.axis_index("y")
-    parts, z_count, share, columns = block.shape
-    whole = jnp.zeros((parts, z_count, count, share, columns), block.dtype)
     for k, first, piece in pieces:
         whole = lax.dynamic_update_slice(
             whole, piece[:, :, None], (0, first, (y_at + k) % count, 0, 0)
@@ -80,6 +81,104 @@
     return (gate * normal_cdf, normal_cdf + gate * density)
 
 
+def hidden_kernel(grads, down, slope, value, linear, taps, linear_out, up_out, conv_out):
+    peers, padded, width = grads.shape
+    rows = linear_out.shape[1]
+    act = jnp.zeros(slope.shape[1:], jnp.float32)
+    for t in range(peers):
+        act += jnp.dot(
+            grads[t], down[0, t * width : (t + 1) * width], preferred_element_type=jnp.float32
+        )
+    grad = act * slope[0]
+
+    def ahead(value, by):
+        return pltpu.roll(value, padded - by, 0)
+
+    linear_grad = (
+        taps[0:1] * ahead(grad, 2) + taps[1:2] * ahead(grad, 1) + taps[2:3] * grad
+    )
+    linear_out[0] = linear_grad[:rows].astype(jnp.bfloat16)
+    up_out[0] = ahead(act * value[0], 1)[:rows].astype(jnp.bfloat16)
+    at = lax.broadcasted_iota(jnp.int32, grad.shape, 0)
+    own = jnp.where((at >= 1) & (at <= rows), grad, 0.0)
+    near = linear[0]
+    sums = jnp.concatenate(
+        [
+            jnp.sum(own * (near if k == 0 else ahead(near, k)), axis=0, keepdims=True)
+            for k in range(3)
+        ]
+    )
+    first = pl.program_id(0) == 0
+
+    @pl.when(first)
+    def _():
+        conv_out[...] = sums
+
+    @pl.when(jnp.logical_not(first))
+    def _():
+        conv_out[...] += sums
+
+
+def hidden_gradients(grads, weights, slope, value, linear, taps):
+    peers, padded, width = grads.shape
+    _, depth, half = weights.shape
+    rows = width
+    saved = pl.BlockSpec((1, padded, half), lambda b: (b, 0, 0))
+    made = pl.BlockSpec((1, rows, half), lambda b: (b, 0, 0))
+    return pl.pallas_call(
+        hidden_kernel,
+        grid=(2,),
+        in_specs=[
+            pl.BlockSpec((peers // 2, padded, width), lambda b: (b, 0, 0)),
+            pl.BlockSpec((1, depth, half), lambda b: (0, 0, 0)),
+            saved,
+            saved,
+            saved,
+            pl.BlockSpec((3, half), lambda b: (0, 0)),
+        ],
+        out_specs=[made, made, pl.BlockSpec((3, half), lambda b: (0, 0))],
+        out_shape=[
+            jax.ShapeDtypeStruct((2, rows, half), jnp.bfloat16),
+            jax.ShapeDtypeStruct((2, rows, half), jnp.bfloat16),
+            jax.ShapeDtypeStruct((3, half), jnp.float32),
+        ],
+    )(grads, weights, slope, value, linear, taps)
+
+
+def output_kernel(linear_grad, up_grad, gate, up, out):
+    width = out.shape[3]
+    contract = (((1,), (1,)), ((), ()))
+    for t in range(out.shape[1]):
+        span = slice(t * width, (t + 1) * width)
+        for b in range(2):
+            part = lax.dot_general(
+                linear_grad[b], gate[0, span], contract, preferred_element_type=jnp.float32
+            ) + lax.dot_general(
+                up_grad[b], up[0, span], contract, preferred_element_type=jnp.float32
+            )
+            out[b, t] = part.astype(jnp.bfloat16)
+
+
+def output_partials(linear_grad, up_grad, weights, width):
+    _, rows, half = linear_grad.shape
+    peers = weights.shape[1] // width
+    steps = 4
+    whole = pl.BlockSpec((2, rows, half), lambda i: (0, 0, 0))
+    product = pl.pallas_call(
+        output_kernel,
+        grid=(steps,),
+        in_specs=[
+            whole,
+            whole,
+            pl.BlockSpec((1, weights.shape[1] // steps, half), lambda i: (1, i, 0)),
+            pl.BlockSpec((1, weights.shape[1] // steps, half), lambda i: (2, i, 0)),
+        ],
+        out_specs=pl.BlockSpec((2, peers // steps, rows, width), lambda i: (0, i, 0, 0)),
+        out_shape=jax.ShapeDtypeStruct((2, peers, rows, width), jnp.bfloat16),
+    )(linear_grad, up_grad, weights, weights)
+    return product.reshape(2 * peers, rows, width)
+
+
 def block_gradients(out_grad, gate_lin, up_lin, conv_weight, gate_weight, up_weight, down_weight):
     rows, columns = gate_lin.shape
     width = out_grad.shape[1]
@@ -87,11 +186,7 @@
     second = lax.axis_index("zp") == 1
 
     own, other = halves_of(jnp.stack([down_weight.T, gate_weight, up_weight]), second)
-    block = gathered_z(own, other)
-    block, out_grad, gate_lin, up_lin = lax.optimization_barrier(
-        (block, out_grad, gate_lin, up_lin)
-    )
-    down_full, gate_full, up_full = gathered_y(block)
+    weights = gathered_y(gathered_z(own, other))
 
     spare = ((0, 0), (0, columns - width))
     last = jnp.concatenate([gate_lin[-2:], up_lin[-1:], jnp.pad(out_grad[-1:], spare)])
@@ -106,8 +201,7 @@
             jnp.zeros((PAD - rows - 2, width), out_grad.dtype),
         ]
     )
-    grads = sent_to_all(grads, GROUP).reshape(2, -1, PAD, width)
-    grads = grads.transpose(0, 2, 1, 3).reshape(2 * PAD, -1)
+    grads = sent_to_all(grads, GROUP)
 
     saved = jnp.concatenate(
         [before[:2], gate_lin, after[:2], before[2:3], up_lin, after[2:3]]
@@ -123,38 +217,36 @@
     gate = taps[0] * linear[:, :-2] + taps[1] * linear[:, 1:-1] + taps[2] * linear[:, 2:]
     gelu_value, gelu_slope = gelu_parts(gate)
 
-    act_grad = jnp.dot(grads, down_full, preferred_element_type=jnp.float32)
-    act_grad = act_grad.reshape(2, PAD, half)[:, : rows + 2]
-    gate_grad = act_grad * up_ext * gelu_slope
-    up_grad = (act_grad * gelu_value)[:, 1:-1].astype(jnp.bfloat16)
-    own_grad = gate_grad[:, 1:-1]
-    linear_grad = (
-        taps[0] * gate_grad[:, 2:] + taps[1] * own_grad + taps[2] * gate_grad[:, :-2]
-    ).astype(jnp.bfloat16)
-
-    conv = jnp.stack(
-        [jnp.sum(own_grad * linear[:, 1 + k : 1 + k + rows], axis=(0, 1)) for k in range(3)]
-    )
-    conv = sent_to_all(conv, Z_ALL)
-    conv = conv.reshape(-1, 2, 3, half).sum(axis=0).transpose(1, 0, 2).reshape(3, columns)
-    contract = (((1,), (1,)), ((), ()))
-    product = lax.dot_general(
-        linear_grad.reshape(-1, half), gate_full, contract, preferred_element_type=jnp.float32
-    ) + lax.dot_general(
-        up_grad.reshape(-1, half), up_full, contract, preferred_element_type=jnp.float32
-    )
-    product = product.astype(jnp.bfloat16).reshape(2, rows, -1, width)
-    product = product.transpose(0, 2, 1, 3).reshape(-1, rows, width)
-    conv, product = lax.optimization_barrier((conv, product))
+    tail = ((0, 0), (0, PAD - rows - 2), (0, 0))
+    linear_grad, up_grad, conv = hidden_gradients(
+        grads,
+        weights,
+        jnp.pad(up_ext * gelu_slope, tail),
+        jnp.pad(gelu_value, tail),
+        jnp.pad(linear, ((0, 0), (0, PAD - rows - 4), (0, 0))),
+        taps,
+    )
+    one, two = shifted(conv, "rep", 1), shifted(conv, "rep", 2)
+    product = output_partials(linear_grad, up_grad, weights, width)
     arrived = lax.all_to_all(product, GROUP, 0, 0, tiled=True)
     input_grad = arrived.astype(jnp.float32).sum(axis=0).astype(jnp.bfloat16)
-    for bit in (1, 2, 4):
-        conv = conv + swapped(conv, "y", bit)
-    conv = conv[None]
-    for axis, bit in (("core", 1), ("x", 1), ("x", 2)):
-        low = lax.axis_index(axis) & bit == 0
-        peer = swapped(conv, axis, bit)
-        conv = jnp.concatenate([jnp.where(low, conv, peer), jnp.where(low, peer, conv)])
+    rep_at, rep_count = lax.axis_index("rep"), lax.axis_size("rep")
+    conv = sum(lax.select_n((rep_at - k) % rep_count, conv, one, two) for k in range(rep_count))
+    near = conv + swapped(conv, "zk", 1)
+    pair_swap = [(i, i ^ 1) for i in range(4)]
+    both_swap = [(i, i ^ 3) for i in range(4)]
+    far = lax.ppermute(conv, ("zk", "zp"), pair_swap) + lax.ppermute(conv, ("zk", "zp"), both_swap)
+    conv = jnp.concatenate(
+        [jnp.where(second, far, near), jnp.where(second, near, far)], axis=1
+    )
+    conv = (conv + swapped(conv, "y", 1)) + (swapped(conv, "y", 2) + swapped(conv, "y", 3))
+    conv = conv + swapped(conv, "y", 4)
+    low = lax.axis_index("core") == 0
+    peer = swapped(conv, "core", 1)
+    conv = jnp.stack([jnp.where(low, conv, peer), jnp.where(low, peer, conv)])
+    peers = [conv] + [swapped(conv, "x", k) for k in range(1, 4)]
+    x_at = lax.axis_index("x")
+    conv = jnp.concatenate([lax.select_n(x_at ^ k, *peers) for k in range(4)])
     conv_grad = conv.transpose(1, 0, 2).reshape(3, -1)
     return (input_grad, conv_grad)
 

time: 206 us -> 239 us (1.16)
  starting transfers between devices: 106 us -> 119 us
  Pallas kernels: 0 us -> 11 us
  waiting for transfers between devices: 66.7 us -> 75.2 us
  local copies, waits for them, and re-layouts: 16 us -> 23.4 us
  matrix products: 5.11 us -> 0 us
    ppermute x11 -> x13, waiting for transfers between devices: 30.3 us -> 57.9 us  [shifted(): lax.ppermute(value, axis, [(i, (i + by) % count) for i in range(count)])]
    ppermute x7 -> x10, waiting for transfers between devices: 32.1 us -> 14.3 us  [swapped(): lax.ppermute(value, axis, [(i, i ^ bit) for i in range(lax.axis_size(axis...]
    pallas_call x0 -> x2, Pallas kernels: none -> 11 us  [the longest x1 5.81 us: output_partials(): pl.pallas_call(output_kernel, grid=(steps,), in_specs=[whole, whole, pl.B...]
    ppermute x7 -> x10, starting transfers between devices: 27.3 us -> 37.6 us  [swapped(): lax.ppermute(value, axis, [(i, i ^ bit) for i in range(lax.axis_size(axis...]
    dynamic_update_slice x9, local copies, waits for them, and re-layouts: 0.87 us -> 7.87 us  [gathered_y(): lax.dynamic_update_slice(whole, piece[:, :, None], (0, first, (y_at + k)...]
    ppermute x0 -> x2, starting transfers between devices: none -> 6.9 us  [the longest x1 4.98 us: block_gradients(): lax.ppermute(conv, ('zk', 'zp'), both_swap)]
    all_to_all x2 -> x1, starting transfers between devices: 18.1 us -> 12.4 us  [sent_to_all(): lax.all_to_all(jnp.broadcast_to(value[None], (peers, *value.shape)), axis...]
    dot_general x3 -> x0, matrix products: 5.11 us -> none  [the longest x1 2.33 us: block_gradients(): lax.dot_general(linear_grad.reshape(-1, half), gate_full, contract, prefe...]
  transfers between devices with their start and end apart: 23 -> 29, of which waited for: 15 -> 14; matrix products, arithmetic and copies ran while one was open for 9% -> 10% of each run, Pallas kernels for 0% -> 0%
where the time goes in v1:
time: 239 us; the launch traced here: 238 us
  starting transfers between devices  119 us (50%)
  waiting for transfers between devices  75.2 us (31%)
  local copies, waits for them, and re-layouts  23.4 us (10%)
  Pallas kernels  11 us (5%)
  other arithmetic  7.48 us (3%)
    ppermute x13, waiting for transfers between devices, shifted(): lax.ppermute(value, axis, [(i, (i + by) % count) for i in range(count)])  57.9 us
    ppermute x13, starting transfers between devices, shifted(): lax.ppermute(value, axis, [(i, (i + by) % count) for i in range(count)])  49.2 us
    ppermute x10, starting transfers between devices, swapped(): lax.ppermute(value, axis, [(i, i ^ bit) for i in range(lax.axis_size(axis...  37.6 us
    ppermute x10, waiting for transfers between devices, swapped(): lax.ppermute(value, axis, [(i, i ^ bit) for i in range(lax.axis_size(axis...  14.3 us
    all_to_all x1, starting transfers between devices, sent_to_all(): lax.all_to_all(jnp.broadcast_to(value[None], (peers, *value.shape)), axis...  12.4 us
    dynamic_update_slice x9, local copies, waits for them, and re-layouts, gathered_y(): lax.dynamic_update_slice(whole, piece[:, :, None], (0, first, (y_at + k)...  7.87 us
    all_to_all x1, starting transfers between devices, block_gradients(): arrived = lax.all_to_all(product, GROUP, 0, 0, tiled=True)  7.81 us
    pallas_call x1, Pallas kernels, output_partials(): pl.pallas_call(output_kernel, grid=(steps,), in_specs=[whole, whole, pl.B...  5.81 us
  transfers between devices with their start and end apart: 29, of which 14 were waited for; matrix products, arithmetic and copies ran while one was open for 10% of the time, Pallas kernels for 0%

profile of v1, /device:TPU:1, one launch (start us, length us, event | category | flops | bytes accessed | tf_op | source)
XLA Modules:
  0.0 237.8 jit_solution(7977169587115673734)
XLA Ops:
  0.7 1.2 copy.24
  1.9 1.2 copy.25
  3.1 0.8 fusion.15
  3.9 4.0 %collective-permute-start = (bf16[4,704]{1,0:T(4,128)(2,1)S(1)}, bf16[4,704]{1,0:T(4,128)(2,1)S(1)}, u32[]{:S(2)}, u32[]{:S(2)}) collective-permute-start(bf16[4,704]{1,0:T(4,128)(2,1)S(1)} %fusion.9), channel_id=1, source_target_pairs={{0,8},{8,16},{16,24},{24,32},{32,40},{40,48},{48,56},{56,64},{64,7... | collective-permute-start | bytes 16904 | tf_op jit(solution)/shard_map/ppermute | solution.py:28
  7.9 1.3 collective-permute-start.1
  9.3 3.0 %collective-permute-done.1 = bf16[4,704]{1,0:T(4,128)(2,1)S(1)} collective-permute-done((bf16[4,704]{1,0:T(4,128)(2,1)S(1)}, bf16[4,704]{1,0:T(4,128)(2,1)S(1)}, u32[]{:S(2)}, u32[]{:S(2)}) %collective-permute-start.1) | collective-permute-done | bytes 5664 | tf_op jit(solution)/shard_map/ppermute | solution.py:28
  12.3 1.0 maximum_maximum_fusion
  13.3 1.5 broadcast_in_dim.40
  14.9 12.4 %all-to-all-start = ((bf16[16,264,256]{2,1,0:T(8,128)(2,1)}), bf16[16,264,256]{2,1,0:T(8,128)(2,1)S(1)}, u32[]{:S(2)}, u32[]{:S(2)}) async-start(bf16[16,264,256]{2,1,0:T(8,128)(2,1)} %broadcast_in_dim.40), calls=%async_computation | async-start | bytes 4325376 | tf_op jit(solution)/shard_map/all_to_all | solution.py:37
  28.1 9.7 %collective-permute-start.2 = (bf16[3,64,352]{2,1,0:T(8,128)(2,1)}, bf16[3,64,352]{2,1,0:T(8,128)(2,1)}, u32[]{:S(2)}, u32[]{:S(2)}) collective-permute-start(bf16[3,64,352]{2,1,0:T(8,128)(2,1)} %get-tuple-element.27), channel_id=1, source_target_pairs={{0,704},{64,0},{128,64},{192,128},{256,192},{320,256},{384,320},{4... | collective-permute-start | bytes 405512 | tf_op jit(solution)/shard_map/ppermute | solution.py:22
  37.8 1.9 collective-permute-start.4
  39.7 1.9 collective-permute-start.3
  42.7 3.6 %concatenate.21 = bf16[518,704]{1,0:T(8,128)(2,1)S(1)} concatenate(bf16[2,704]{1,0:T(2,128)(2,1)S(1)} %slice.118, bf16[256,704]{1,0:T(8,128)(2,1)S(1)} %copy.24, bf16[2,704]{1,0:T(2,128)(2,1)S(1)} %slice.119, bf16[1,704]{1,0:T(2,128)(2,1)S(1)} %slice.120, bf16[256,704]{1,0:T(8,128)(2,1)} %copy-done.1, bf16[1,704]{1,0:T(2,128)(2,1)S(1)} %slice.121), dimensions={0} | concatenate | bytes 1458688 | tf_op jit(solution)/shard_map/concatenate | solution.py:206
  46.5 1.9 collective-permute-start.13
  48.5 8.5 %collective-permute-done.2 = bf16[3,64,352]{2,1,0:T(8,128)(2,1)} collective-permute-done((bf16[3,64,352]{2,1,0:T(8,128)(2,1)}, bf16[3,64,352]{2,1,0:T(8,128)(2,1)}, u32[]{:S(2)}, u32[]{:S(2)}) %collective-permute-start.2) | collective-permute-done | bytes 135200 | tf_op jit(solution)/shard_map/ppermute | solution.py:22
  56.9 12.7 %collective-permute-done.3 = bf16[3,64,352]{2,1,0:T(8,128)(2,1)} collective-permute-done((bf16[3,64,352]{2,1,0:T(8,128)(2,1)S(1)}, bf16[3,64,352]{2,1,0:T(8,128)(2,1)}, u32[]{:S(2)}, u32[]{:S(2)}) %collective-permute-start.3) | collective-permute-done | bytes 135200 | tf_op jit(solution)/shard_map/ppermute | solution.py:22
  69.6 1.2 select_bitcast_fusion.5
  70.9 2.9 %collective-permute-start.5 = (bf16[3,4,64,352]{3,2,0,1:T(8,128)(2,1)S(1)}, bf16[3,4,64,352]{3,2,0,1:T(8,128)(2,1)S(1)}, u32[]{:S(2)}, u32[]{:S(2)}) collective-permute-start(bf16[3,4,64,352]{3,2,0,1:T(8,128)(2,1)S(1)} %pad_maximum_fusion), channel_id=1, source_target_pairs={{0,8},{8,16},{16,24},{24,32},{32,40},{40,48},{48,56},{56,0},{1,9},... | collective-permute-start | bytes 1622024 | tf_op jit(solution)/shard_map/ppermute | solution.py:22
  73.8 4.1 %collective-permute-start.6 = (bf16[3,4,64,352]{3,2,0,1:T(8,128)(2,1)S(1)}, bf16[3,4,64,352]{3,2,0,1:T(8,128)(2,1)S(1)}, u32[]{:S(2)}, u32[]{:S(2)}) collective-permute-start(bf16[3,4,64,352]{3,2,0,1:T(8,128)(2,1)S(1)} %pad_maximum_fusion), channel_id=1, source_target_pairs={{0,56},{8,0},{16,8},{24,16},{32,24},{40,32},{48,40},{56,48},{1,57}... | collective-permute-start | bytes 1622024 | tf_op jit(solution)/shard_map/ppermute | solution.py:22
  77.9 2.9 %broadcast_in_dim.41 = bf16[3,4,8,64,352]{4,3,2,1,0:T(8,128)(2,1)} broadcast(bf16[]{:T(256)} %constant.111.clone.1), dimensions={} | broadcast | bytes 4325378 | tf_op jit(solution)/shard_map/broadcast_in_dim | solution.py:60
  80.9 0.9 copy_dynamic-update-slice_fusion.6
  82.5 6.4 %collective-permute-done.5 = bf16[3,4,64,352]{3,2,0,1:T(8,128)(2,1)S(1)} collective-permute-done((bf16[3,4,64,352]{3,2,0,1:T(8,128)(2,1)S(1)}, bf16[3,4,64,352]{3,2,0,1:T(8,128)(2,1)S(1)}, u32[]{:S(2)}, u32[]{:S(2)}) %collective-permute-start.5) | collective-permute-done | bytes 540704 | tf_op jit(solution)/shard_map/ppermute | solution.py:22
  88.9 1.9 collective-permute-start.7
  90.9 4.6 %collective-permute-start.8 = (bf16[3,4,64,352]{3,2,0,1:T(8,128)(2,1)S(1)}, bf16[3,4,64,352]{3,2,0,1:T(8,128)(2,1)S(1)}, u32[]{:S(2)}, u32[]{:S(2)}) collective-permute-start(bf16[3,4,64,352]{3,2,0,1:T(8,128)(2,1)S(1)} %collective-permute-done.6), channel_id=1, source_target_pairs={{0,56},{8,0},{16,8},{24,16},{32,24},{40,32},{48,40},{56,48},{1,57}... | collective-permute-start | bytes 1622024 | tf_op jit(solution)/shard_map/ppermute | solution.py:22
  95.8 1.0 pad.20.slope
  96.8 1.0 pad.21.value
  97.8 1.0 slice_select_fusion.linear
  98.8 0.9 copy_dynamic-update-slice_fusion.5
  99.7 5.8 %collective-permute-done.7 = bf16[3,4,64,352]{3,2,0,1:T(8,128)(2,1)S(1)} collective-permute-done((bf16[3,4,64,352]{3,2,0,1:T(8,128)(2,1)S(1)}, bf16[3,4,64,352]{3,2,0,1:T(8,128)(2,1)S(1)}, u32[]{:S(2)}, u32[]{:S(2)}) %collective-permute-start.7) | collective-permute-done | bytes 540704 | tf_op jit(solution)/shard_map/ppermute | solution.py:22
  105.6 1.9 collective-permute-start.9
  107.5 4.6 %collective-permute-start.10 = (bf16[3,4,64,352]{3,2,0,1:T(8,128)(2,1)S(1)}, bf16[3,4,64,352]{3,2,0,1:T(8,128)(2,1)S(1)}, u32[]{:S(2)}, u32[]{:S(2)}) collective-permute-start(bf16[3,4,64,352]{3,2,0,1:T(8,128)(2,1)S(1)} %collective-permute-done.8), channel_id=1, source_target_pairs={{0,56},{8,0},{16,8},{24,16},{32,24},{40,32},{48,40},{56,48},{1,57}... | collective-permute-start | bytes 1622024 | tf_op jit(solution)/shard_map/ppermute | solution.py:22
  112.1 0.9 copy_dynamic-update-slice_fusion.4
  113.0 0.9 copy_dynamic-update-slice_fusion.3
  113.9 0.9 copy_dynamic-update-slice_fusion.2
  114.8 6.6 %collective-permute-done.9 = bf16[3,4,64,352]{3,2,0,1:T(8,128)(2,1)S(1)} collective-permute-done((bf16[3,4,64,352]{3,2,0,1:T(8,128)(2,1)S(1)}, bf16[3,4,64,352]{3,2,0,1:T(8,128)(2,1)S(1)}, u32[]{:S(2)}, u32[]{:S(2)}) %collective-permute-start.9) | collective-permute-done | bytes 540704 | tf_op jit(solution)/shard_map/ppermute | solution.py:22
  121.4 1.9 collective-permute-start.11
  123.4 4.6 %collective-permute-start.12 = (bf16[3,2,64,352]{3,2,0,1:T(8,128)(2,1)S(1)}, bf16[3,2,64,352]{3,2,0,1:T(8,128)(2,1)S(1)}, u32[]{:S(2)}, u32[]{:S(2)}) collective-permute-start(bf16[3,2,64,352]{3,2,0,1:T(8,128)(2,1)S(1)} %slice.117), channel_id=1, source_target_pairs={{0,56},{8,0},{16,8},{24,16},{32,24},{40,32},{48,40},{56,48},{1,57}... | collective-permute-start | bytes 811016 | tf_op jit(solution)/shard_map/ppermute | solution.py:22
  127.9 0.9 copy_dynamic-update-slice_fusion.1
  128.8 0.9 copy_dynamic-update-slice_fusion
  130.1 0.8 copy_dynamic-update-slice_fusion.8
  132.3 1.4 copy-done
  133.7 5.2 %shard_map.86 = (bf16[2,256,352]{2,1,0:T(8,128)(2,1)}, bf16[2,256,352]{2,1,0:T(8,128)(2,1)}, f32[3,352]{1,0:T(4,128)}) custom-call(bf16[16,264,256]{2,1,0:T(8,128)(2,1)} %copy-done, bf16[3,2048,352]{2,1,0:T(8,128)(2,1)} %bitcast.17.down.gate.up, f32[2,264,352]{2,1,0:T(8,128)} %pad.20.slope, f32[2,264,352]{2,1,0:T(8,128)} %pad.21.value, ...), custom_call_target="tpu_custom_call" | custom-call | tf_op jit(solution)/shard_map/pallas_call | solution.py:128
  138.9 5.8 %shard_map.87 = bf16[2,8,256,256]{3,2,1,0:T(8,128)(2,1)} custom-call(bf16[2,256,352]{2,1,0:T(8,128)(2,1)} %get-tuple-element.9.linear_grad, bf16[2,256,352]{2,1,0:T(8,128)(2,1)} %get-tuple-element.10.up_grad, bf16[3,2048,352]{2,1,0:T(8,128)(2,1)} %bitcast.17.down.gate.up, bf16[3,2048,352]{2,1,0:T(8,128)(2,1)} %bitcast.17.down.gate.up), custom_call_target="tpu_custom_call" | custom-call | tf_op jit(solution)/shard_map/pallas_call | solution.py:167
  144.7 7.8 %all-to-all-start.1 = ((bf16[16,256,256]{2,1,0:T(8,128)(2,1)}), bf16[16,256,256]{2,1,0:T(8,128)(2,1)S(1)}, u32[]{:S(2)}, u32[]{:S(2)}) async-start(bf16[16,256,256]{2,1,0:T(8,128)(2,1)} %bitcast.52), calls=%async_computation.1 | async-start | bytes 4194304 | tf_op jit(solution)/shard_map/all_to_all | solution.py:231
  152.5 1.9 collective-permute-start.14
  154.4 7.3 %collective-permute-start.15 = (f32[3,352]{1,0:T(4,128)S(1)}, f32[3,352]{1,0:T(4,128)S(1)}, u32[]{:S(2)}, u32[]{:S(2)}) collective-permute-start(f32[3,352]{1,0:T(4,128)S(1)} %copy-done.6), channel_id=1, source_target_pairs={{0,512},{256,0},{512,256},{1,513},{257,1},{513,257},{2,514},{258,2... | collective-permute-start | bytes 12680 | tf_op jit(solution)/shard_map/ppermute | solution.py:22
  161.8 17.0 %collective-permute-done.14 = f32[3,352]{1,0:T(4,128)S(1)} collective-permute-done((f32[3,352]{1,0:T(4,128)S(1)}, f32[3,352]{1,0:T(4,128)S(1)}, u32[]{:S(2)}, u32[]{:S(2)}) %collective-permute-start.14) | collective-permute-done | bytes 4256 | tf_op jit(solution)/shard_map/ppermute | solution.py:22
  178.8 1.9 collective-permute-start.16
  180.7 5.0 %collective-permute-start.17 = (f32[3,352]{1,0:T(4,128)S(1)}, f32[3,352]{1,0:T(4,128)S(1)}, u32[]{:S(2)}, u32[]{:S(2)}) collective-permute-start(f32[3,352]{1,0:T(4,128)S(1)} %select_add_fusion), channel_id=1, source_target_pairs={{0,192},{64,128},{128,64},{192,0},{1,193},{65,129},{129,65},{193,1... | collective-permute-start | bytes 12680 | tf_op jit(solution)/shard_map/ppermute | solution.py:238
  185.7 1.9 collective-permute-start.18
  187.6 3.3 %collective-permute-done.18 = f32[3,352]{1,0:T(4,128)S(1)} collective-permute-done((f32[3,352]{1,0:T(4,128)S(1)}, f32[3,352]{1,0:T(4,128)S(1)}, u32[]{:S(2)}, u32[]{:S(2)}) %collective-permute-start.18) | collective-permute-done | bytes 4256 | tf_op jit(solution)/shard_map/ppermute | solution.py:32
  191.1 1.9 collective-permute-start.19
  193.0 6.5 %collective-permute-start.20 = (f32[3,704]{1,0:T(4,128)S(1)}, f32[3,704]{1,0:T(4,128)S(1)}, u32[]{:S(2)}, u32[]{:S(2)}) collective-permute-start(f32[3,704]{1,0:T(4,128)S(1)} %pad_maximum_fusion.3), channel_id=1, source_target_pairs={{0,16},{8,24},{16,0},{24,8},{32,48},{40,56},{48,32},{56,40},{1,17}... | collective-permute-start | bytes 25352 | tf_op jit(solution)/shard_map/ppermute | solution.py:32
  199.4 1.9 collective-permute-start.21
  201.4 4.3 %collective-permute-done.21 = f32[3,704]{1,0:T(4,128)S(1)} collective-permute-done((f32[3,704]{1,0:T(4,128)S(1)}, f32[3,704]{1,0:T(4,128)S(1)}, u32[]{:S(2)}, u32[]{:S(2)}) %collective-permute-start.21) | collective-permute-done | bytes 8480 | tf_op jit(solution)/shard_map/ppermute | solution.py:32
  205.8 3.9 %collective-permute-start.22 = (f32[3,704]{1,0:T(4,128)S(1)}, f32[3,704]{1,0:T(4,128)S(1)}, u32[]{:S(2)}, u32[]{:S(2)}) collective-permute-start(f32[3,704]{1,0:T(4,128)S(1)} %add_add_fusion), channel_id=1, source_target_pairs={{0,32},{8,40},{16,48},{24,56},{32,0},{40,8},{48,16},{56,24},{1,33}... | collective-permute-start | bytes 25352 | tf_op jit(solution)/shard_map/ppermute | solution.py:32
  209.7 4.4 %collective-permute-done.22 = f32[3,704]{1,0:T(4,128)S(1)} collective-permute-done((f32[3,704]{1,0:T(4,128)S(1)}, f32[3,704]{1,0:T(4,128)S(1)}, u32[]{:S(2)}, u32[]{:S(2)}) %collective-permute-start.22) | collective-permute-done | bytes 8480 | tf_op jit(solution)/shard_map/ppermute | solution.py:32
  214.1 7.6 %collective-permute-start.23 = (f32[3,704]{1,0:T(4,128)S(1)}, f32[3,704]{1,0:T(4,128)S(1)}, u32[]{:S(2)}, u32[]{:S(2)}) collective-permute-start(f32[3,704]{1,0:T(4,128)S(1)} %add.201), channel_id=1, source_target_pairs={{0,1},{1,0},{2,3},{3,2},{4,5},{5,4},{6,7},{7,6},{8,9},{9,8},{10,11... | collective-permute-start | bytes 25352 | tf_op jit(solution)/shard_map/ppermute | solution.py:32
  221.7 0.8 collective-permute-done.23
  222.5 5.8 %collective-permute-start.24 = (f32[2,3,704]{2,1,0:T(4,128)S(1)}, f32[2,3,704]{2,1,0:T(4,128)S(1)}, u32[]{:S(2)}, u32[]{:S(2)}) collective-permute-start(f32[2,3,704]{2,1,0:T(4,128)S(1)} %pad_maximum_fusion.2), channel_id=1, source_target_pairs={{0,2},{2,0},{4,6},{6,4},{1,3},{3,1},{5,7},{7,5},{8,10},{10,8},{12,... | collective-permute-start | bytes 50696 | tf_op jit(solution)/shard_map/ppermute | solution.py:32
  228.3 1.9 collective-permute-start.25
  230.2 4.3 %collective-permute-start.26 = (f32[2,3,704]{2,1,0:T(4,128)S(1)}, f32[2,3,704]{2,1,0:T(4,128)S(1)}, u32[]{:S(2)}, u32[]{:S(2)}) collective-permute-start(f32[2,3,704]{2,1,0:T(4,128)S(1)} %pad_maximum_fusion.2), channel_id=1, source_target_pairs={{0,6},{2,4},{4,2},{6,0},{1,7},{3,5},{5,3},{7,1},{8,14},{10,12},{12... | collective-permute-start | bytes 50696 | tf_op jit(solution)/shard_map/ppermute | solution.py:32
  234.6 1.4 collective-permute-done.26
  236.8 1.0 reduce_sum.12
  (69 shorter events, 6.2 us)
Async XLA Ops:
  0.6 26.6 %copy-start.4 = (bf16[704,64]{0,1:T(8,128)(2,1)S(1)}, bf16[704,64]{0,1:T(8,128)(2,1)}, u32[]{:S(2)}) copy-start(bf16[704,64]{0,1:T(8,128)(2,1)} %param.13) | copy-start | bytes 270340
  0.6 26.6 %copy-start.3 = (bf16[64,704]{1,0:T(8,128)(2,1)S(1)}, bf16[64,704]{1,0:T(8,128)(2,1)}, u32[]{:S(2)}) copy-start(bf16[64,704]{1,0:T(8,128)(2,1)} %param.11) | copy-start | bytes 270340
  0.7 26.6 %copy-start.2 = (bf16[64,704]{1,0:T(8,128)(2,1)S(1)}, bf16[64,704]{1,0:T(8,128)(2,1)}, u32[]{:S(2)}) copy-start(bf16[64,704]{1,0:T(8,128)(2,1)} %param.12) | copy-start | bytes 270340
  3.0 11.8 %copy-start.1 = (bf16[256,704]{1,0:T(8,128)(2,1)}, bf16[256,704]{1,0:T(8,128)(2,1)S(1)}, u32[]{:S(2)}) copy-start(bf16[256,704]{1,0:T(8,128)(2,1)S(1)} %copy.25) | copy-start | bytes 1081348
  3.9 5.4 %collective-permute-start = (bf16[4,704]{1,0:T(4,128)(2,1)S(1)}, bf16[4,704]{1,0:T(4,128)(2,1)S(1)}, u32[]{:S(2)}, u32[]{:S(2)}) collective-permute-start(bf16[4,704]{1,0:T(4,128)(2,1)S(1)} %fusion.9), channel_id=1, source_target_pairs={{0,8},{8,16},{16,24},{24,32},{32,40},{40,48},{48,56},{56,64},{64,7... | collective-permute-start | bytes 16904 | tf_op jit(solution)/shard_map/ppermute | solution.py:28
  7.9 4.4 %collective-permute-start.1 = (bf16[4,704]{1,0:T(4,128)(2,1)S(1)}, bf16[4,704]{1,0:T(4,128)(2,1)S(1)}, u32[]{:S(2)}, u32[]{:S(2)}) collective-permute-start(bf16[4,704]{1,0:T(4,128)(2,1)S(1)} %fusion.10), channel_id=1, source_target_pairs={{8,0},{16,8},{24,16},{32,24},{40,32},{48,40},{56,48},{64,56},{72,6... | collective-permute-start | bytes 16904 | tf_op jit(solution)/shard_map/ppermute | solution.py:28
  14.9 117.5 %all-to-all-start = ((bf16[16,264,256]{2,1,0:T(8,128)(2,1)}), bf16[16,264,256]{2,1,0:T(8,128)(2,1)S(1)}, u32[]{:S(2)}, u32[]{:S(2)}) async-start(bf16[16,264,256]{2,1,0:T(8,128)(2,1)} %broadcast_in_dim.40), calls=%async_computation | async-start | bytes 4325376 | tf_op jit(solution)/shard_map/all_to_all | solution.py:37
  28.1 28.8 %collective-permute-start.2 = (bf16[3,64,352]{2,1,0:T(8,128)(2,1)}, bf16[3,64,352]{2,1,0:T(8,128)(2,1)}, u32[]{:S(2)}, u32[]{:S(2)}) collective-permute-start(bf16[3,64,352]{2,1,0:T(8,128)(2,1)} %get-tuple-element.27), channel_id=1, source_target_pairs={{0,704},{64,0},{128,64},{192,128},{256,192},{320,256},{384,320},{4... | collective-permute-start | bytes 405512 | tf_op jit(solution)/shard_map/ppermute | solution.py:22
  37.8 31.8 %collective-permute-start.4 = (bf16[3,64,352]{2,1,0:T(8,128)(2,1)}, bf16[3,64,352]{2,1,0:T(8,128)(2,1)}, u32[]{:S(2)}, u32[]{:S(2)}) collective-permute-start(bf16[3,64,352]{2,1,0:T(8,128)(2,1)} %get-tuple-element.27), channel_id=1, source_target_pairs={{0,64},{64,128},{128,192},{192,256},{256,320},{320,384},{384,448},... | collective-permute-start | bytes 405512 | tf_op jit(solution)/shard_map/ppermute | solution.py:22
  39.7 29.9 %collective-permute-start.3 = (bf16[3,64,352]{2,1,0:T(8,128)(2,1)S(1)}, bf16[3,64,352]{2,1,0:T(8,128)(2,1)}, u32[]{:S(2)}, u32[]{:S(2)}) collective-permute-start(bf16[3,64,352]{2,1,0:T(8,128)(2,1)S(1)} %get-tuple-element.28), channel_id=1, source_target_pairs={{0,128},{64,192},{128,256},{192,320},{256,384},{320,448},{384,512}... | collective-permute-start | bytes 405512 | tf_op jit(solution)/shard_map/ppermute | solution.py:22
  42.6 38.2 %copy-start.5 = (f32[3,352]{1,0:T(4,128)}, f32[3,352]{1,0:T(4,128)S(1)}, u32[]{:S(2)}) copy-start(f32[3,352]{1,0:T(4,128)S(1)} %dynamic-slice_convert_fusion.taps) | copy-start | bytes 12676
  46.5 35.2 %collective-permute-start.13 = (bf16[518,352]{1,0:T(8,128)(2,1)S(1)}, bf16[518,352]{1,0:T(8,128)(2,1)S(1)}, u32[]{:S(2)}, u32[]{:S(2)}) collective-permute-start(bf16[518,352]{1,0:T(8,128)(2,1)S(1)} %broadcast_select_fusion.1), channel_id=1, source_target_pairs={{0,64},{64,0},{1,65},{65,1},{2,66},{66,2},{3,67},{67,3},{4,68},{68... | collective-permute-start | bytes 1094024 | tf_op jit(solution)/shard_map/ppermute | solution.py:32
  70.9 18.0 %collective-permute-start.5 = (bf16[3,4,64,352]{3,2,0,1:T(8,128)(2,1)S(1)}, bf16[3,4,64,352]{3,2,0,1:T(8,128)(2,1)S(1)}, u32[]{:S(2)}, u32[]{:S(2)}) collective-permute-start(bf16[3,4,64,352]{3,2,0,1:T(8,128)(2,1)S(1)} %pad_maximum_fusion), channel_id=1, source_target_pairs={{0,8},{8,16},{16,24},{24,32},{32,40},{40,48},{48,56},{56,0},{1,9},... | collective-permute-start | bytes 1622024 | tf_op jit(solution)/shard_map/ppermute | solution.py:22
  73.8 17.0 %collective-permute-start.6 = (bf16[3,4,64,352]{3,2,0,1:T(8,128)(2,1)S(1)}, bf16[3,4,64,352]{3,2,0,1:T(8,128)(2,1)S(1)}, u32[]{:S(2)}, u32[]{:S(2)}) collective-permute-start(bf16[3,4,64,352]{3,2,0,1:T(8,128)(2,1)S(1)} %pad_maximum_fusion), channel_id=1, source_target_pairs={{0,56},{8,0},{16,8},{24,16},{32,24},{40,32},{48,40},{56,48},{1,57}... | collective-permute-start | bytes 1622024 | tf_op jit(solution)/shard_map/ppermute | solution.py:22
  82.1 15.6 %copy-start.7 = (pred[264]{0:T(512)(128)(4,1)S(1)}, pred[264]{0:T(512)(128)(4,1)}, u32[]{:S(2)}) copy-start(pred[264]{0:T(512)(128)(4,1)} %constant.135.clone.1) | copy-start | bytes 796
  88.9 16.6 %collective-permute-start.7 = (bf16[3,4,64,352]{3,2,0,1:T(8,128)(2,1)S(1)}, bf16[3,4,64,352]{3,2,0,1:T(8,128)(2,1)S(1)}, u32[]{:S(2)}, u32[]{:S(2)}) collective-permute-start(bf16[3,4,64,352]{3,2,0,1:T(8,128)(2,1)S(1)} %collective-permute-done.5), channel_id=1, source_target_pairs={{0,8},{8,16},{16,24},{24,32},{32,40},{40,48},{48,56},{56,0},{1,9},... | collective-permute-start | bytes 1622024 | tf_op jit(solution)/shard_map/ppermute | solution.py:22
  90.9 16.6 %collective-permute-start.8 = (bf16[3,4,64,352]{3,2,0,1:T(8,128)(2,1)S(1)}, bf16[3,4,64,352]{3,2,0,1:T(8,128)(2,1)S(1)}, u32[]{:S(2)}, u32[]{:S(2)}) collective-permute-start(bf16[3,4,64,352]{3,2,0,1:T(8,128)(2,1)S(1)} %collective-permute-done.6), channel_id=1, source_target_pairs={{0,56},{8,0},{16,8},{24,16},{32,24},{40,32},{48,40},{56,48},{1,57}... | collective-permute-start | bytes 1622024 | tf_op jit(solution)/shard_map/ppermute | solution.py:22
  105.6 15.8 %collective-permute-start.9 = (bf16[3,4,64,352]{3,2,0,1:T(8,128)(2,1)S(1)}, bf16[3,4,64,352]{3,2,0,1:T(8,128)(2,1)S(1)}, u32[]{:S(2)}, u32[]{:S(2)}) collective-permute-start(bf16[3,4,64,352]{3,2,0,1:T(8,128)(2,1)S(1)} %collective-permute-done.7), channel_id=1, source_target_pairs={{0,8},{8,16},{16,24},{24,32},{32,40},{40,48},{48,56},{56,0},{1,9},... | collective-permute-start | bytes 1622024 | tf_op jit(solution)/shard_map/ppermute | solution.py:22
  107.5 15.8 %collective-permute-start.10 = (bf16[3,4,64,352]{3,2,0,1:T(8,128)(2,1)S(1)}, bf16[3,4,64,352]{3,2,0,1:T(8,128)(2,1)S(1)}, u32[]{:S(2)}, u32[]{:S(2)}) collective-permute-start(bf16[3,4,64,352]{3,2,0,1:T(8,128)(2,1)S(1)} %collective-permute-done.8), channel_id=1, source_target_pairs={{0,56},{8,0},{16,8},{24,16},{32,24},{40,32},{48,40},{56,48},{1,57}... | collective-permute-start | bytes 1622024 | tf_op jit(solution)/shard_map/ppermute | solution.py:22
  121.4 8.7 %collective-permute-start.11 = (bf16[3,2,64,352]{3,2,0,1:T(8,128)(2,1)S(1)}, bf16[3,2,64,352]{3,2,0,1:T(8,128)(2,1)S(1)}, u32[]{:S(2)}, u32[]{:S(2)}) collective-permute-start(bf16[3,2,64,352]{3,2,0,1:T(8,128)(2,1)S(1)} %slice.116), channel_id=1, source_target_pairs={{0,8},{8,16},{16,24},{24,32},{32,40},{40,48},{48,56},{56,0},{1,9},... | collective-permute-start | bytes 811016 | tf_op jit(solution)/shard_map/ppermute | solution.py:22
  123.4 8.2 %collective-permute-start.12 = (bf16[3,2,64,352]{3,2,0,1:T(8,128)(2,1)S(1)}, bf16[3,2,64,352]{3,2,0,1:T(8,128)(2,1)S(1)}, u32[]{:S(2)}, u32[]{:S(2)}) collective-permute-start(bf16[3,2,64,352]{3,2,0,1:T(8,128)(2,1)S(1)} %slice.117), channel_id=1, source_target_pairs={{0,56},{8,0},{16,8},{24,16},{32,24},{40,32},{48,40},{56,48},{1,57}... | collective-permute-start | bytes 811016 | tf_op jit(solution)/shard_map/ppermute | solution.py:22
  132.3 1.4 copy-start
  138.9 13.6 %copy-start.6 = (f32[3,352]{1,0:T(4,128)S(1)}, f32[3,352]{1,0:T(4,128)}, u32[]{:S(2)}) copy-start(f32[3,352]{1,0:T(4,128)} %get-tuple-element.11) | copy-start | bytes 12676
  144.7 92.2 %all-to-all-start.1 = ((bf16[16,256,256]{2,1,0:T(8,128)(2,1)}), bf16[16,256,256]{2,1,0:T(8,128)(2,1)S(1)}, u32[]{:S(2)}, u32[]{:S(2)}) async-start(bf16[16,256,256]{2,1,0:T(8,128)(2,1)} %bitcast.52), calls=%async_computation.1 | async-start | bytes 4194304 | tf_op jit(solution)/shard_map/all_to_all | solution.py:231
  152.5 26.3 %collective-permute-start.14 = (f32[3,352]{1,0:T(4,128)S(1)}, f32[3,352]{1,0:T(4,128)S(1)}, u32[]{:S(2)}, u32[]{:S(2)}) collective-permute-start(f32[3,352]{1,0:T(4,128)S(1)} %copy-done.6), channel_id=1, source_target_pairs={{0,256},{256,512},{512,0},{1,257},{257,513},{513,1},{2,258},{258,5... | collective-permute-start | bytes 12680 | tf_op jit(solution)/shard_map/ppermute | solution.py:22
  154.4 24.3 %collective-permute-start.15 = (f32[3,352]{1,0:T(4,128)S(1)}, f32[3,352]{1,0:T(4,128)S(1)}, u32[]{:S(2)}, u32[]{:S(2)}) collective-permute-start(f32[3,352]{1,0:T(4,128)S(1)} %copy-done.6), channel_id=1, source_target_pairs={{0,512},{256,0},{512,256},{1,513},{257,1},{513,257},{2,514},{258,2... | collective-permute-start | bytes 12680 | tf_op jit(solution)/shard_map/ppermute | solution.py:22
  178.8 8.8 %collective-permute-start.16 = (f32[3,352]{1,0:T(4,128)S(1)}, f32[3,352]{1,0:T(4,128)S(1)}, u32[]{:S(2)}, u32[]{:S(2)}) collective-permute-start(f32[3,352]{1,0:T(4,128)S(1)} %select_add_fusion), channel_id=1, source_target_pairs={{0,64},{64,0},{128,192},{192,128},{1,65},{65,1},{129,193},{193,129... | collective-permute-start | bytes 12680 | tf_op jit(solution)/shard_map/ppermute | solution.py:238
  180.7 6.9 %collective-permute-start.17 = (f32[3,352]{1,0:T(4,128)S(1)}, f32[3,352]{1,0:T(4,128)S(1)}, u32[]{:S(2)}, u32[]{:S(2)}) collective-permute-start(f32[3,352]{1,0:T(4,128)S(1)} %select_add_fusion), channel_id=1, source_target_pairs={{0,192},{64,128},{128,64},{192,0},{1,193},{65,129},{129,65},{193,1... | collective-permute-start | bytes 12680 | tf_op jit(solution)/shard_map/ppermute | solution.py:238
  185.7 5.3 %collective-permute-start.18 = (f32[3,352]{1,0:T(4,128)S(1)}, f32[3,352]{1,0:T(4,128)S(1)}, u32[]{:S(2)}, u32[]{:S(2)}) collective-permute-start(f32[3,352]{1,0:T(4,128)S(1)} %select_add_fusion), channel_id=1, source_target_pairs={{0,128},{128,0},{1,129},{129,1},{2,130},{130,2},{3,131},{131,3},{4... | collective-permute-start | bytes 12680 | tf_op jit(solution)/shard_map/ppermute | solution.py:32
  191.1 10.3 %collective-permute-start.19 = (f32[3,704]{1,0:T(4,128)S(1)}, f32[3,704]{1,0:T(4,128)S(1)}, u32[]{:S(2)}, u32[]{:S(2)}) collective-permute-start(f32[3,704]{1,0:T(4,128)S(1)} %pad_maximum_fusion.3), channel_id=1, source_target_pairs={{0,8},{8,0},{16,24},{24,16},{32,40},{40,32},{48,56},{56,48},{1,9},... | collective-permute-start | bytes 25352 | tf_op jit(solution)/shard_map/ppermute | solution.py:32
  193.0 8.4 %collective-permute-start.20 = (f32[3,704]{1,0:T(4,128)S(1)}, f32[3,704]{1,0:T(4,128)S(1)}, u32[]{:S(2)}, u32[]{:S(2)}) collective-permute-start(f32[3,704]{1,0:T(4,128)S(1)} %pad_maximum_fusion.3), channel_id=1, source_target_pairs={{0,16},{8,24},{16,0},{24,8},{32,48},{40,56},{48,32},{56,40},{1,17}... | collective-permute-start | bytes 25352 | tf_op jit(solution)/shard_map/ppermute | solution.py:32
  199.4 6.2 %collective-permute-start.21 = (f32[3,704]{1,0:T(4,128)S(1)}, f32[3,704]{1,0:T(4,128)S(1)}, u32[]{:S(2)}, u32[]{:S(2)}) collective-permute-start(f32[3,704]{1,0:T(4,128)S(1)} %pad_maximum_fusion.3), channel_id=1, source_target_pairs={{0,24},{8,16},{16,8},{24,0},{32,56},{40,48},{48,40},{56,32},{1,25}... | collective-permute-start | bytes 25352 | tf_op jit(solution)/shard_map/ppermute | solution.py:32
  205.8 8.3 %collective-permute-start.22 = (f32[3,704]{1,0:T(4,128)S(1)}, f32[3,704]{1,0:T(4,128)S(1)}, u32[]{:S(2)}, u32[]{:S(2)}) collective-permute-start(f32[3,704]{1,0:T(4,128)S(1)} %add_add_fusion), channel_id=1, source_target_pairs={{0,32},{8,40},{16,48},{24,56},{32,0},{40,8},{48,16},{56,24},{1,33}... | collective-permute-start | bytes 25352 | tf_op jit(solution)/shard_map/ppermute | solution.py:32
  214.1 8.4 %collective-permute-start.23 = (f32[3,704]{1,0:T(4,128)S(1)}, f32[3,704]{1,0:T(4,128)S(1)}, u32[]{:S(2)}, u32[]{:S(2)}) collective-permute-start(f32[3,704]{1,0:T(4,128)S(1)} %add.201), channel_id=1, source_target_pairs={{0,1},{1,0},{2,3},{3,2},{4,5},{5,4},{6,7},{7,6},{8,9},{9,8},{10,11... | collective-permute-start | bytes 25352 | tf_op jit(solution)/shard_map/ppermute | solution.py:32
  222.5 12.0 %collective-permute-start.24 = (f32[2,3,704]{2,1,0:T(4,128)S(1)}, f32[2,3,704]{2,1,0:T(4,128)S(1)}, u32[]{:S(2)}, u32[]{:S(2)}) collective-permute-start(f32[2,3,704]{2,1,0:T(4,128)S(1)} %pad_maximum_fusion.2), channel_id=1, source_target_pairs={{0,2},{2,0},{4,6},{6,4},{1,3},{3,1},{5,7},{7,5},{8,10},{10,8},{12,... | collective-permute-start | bytes 50696 | tf_op jit(solution)/shard_map/ppermute | solution.py:32
  228.3 6.3 %collective-permute-start.25 = (f32[2,3,704]{2,1,0:T(4,128)S(1)}, f32[2,3,704]{2,1,0:T(4,128)S(1)}, u32[]{:S(2)}, u32[]{:S(2)}) collective-permute-start(f32[2,3,704]{2,1,0:T(4,128)S(1)} %pad_maximum_fusion.2), channel_id=1, source_target_pairs={{0,4},{2,6},{4,0},{6,2},{1,5},{3,7},{5,1},{7,3},{8,12},{10,14},{12... | collective-permute-start | bytes 50696 | tf_op jit(solution)/shard_map/ppermute | solution.py:32
  230.2 5.8 %collective-permute-start.26 = (f32[2,3,704]{2,1,0:T(4,128)S(1)}, f32[2,3,704]{2,1,0:T(4,128)S(1)}, u32[]{:S(2)}, u32[]{:S(2)}) collective-permute-start(f32[2,3,704]{2,1,0:T(4,128)S(1)} %pad_maximum_fusion.2), channel_id=1, source_target_pairs={{0,6},{2,4},{4,2},{6,0},{1,7},{3,5},{5,3},{7,1},{8,14},{10,12},{12... | collective-permute-start | bytes 50696 | tf_op jit(solution)/shard_map/ppermute | solution.py:32

commit v2 on v1

--- a/solution.py
+++ b/solution.py
@@ -55,24 +55,26 @@
 
 
 def gathered_y(block):
-    count, y_at = lax.axis_size("y"), lax.axis_index("y")
-    parts, z_count, share, columns = block.shape
-    whole = jnp.zeros((parts, z_count, count, share, columns), block.dtype)
-    block, whole = lax.optimization_barrier((block, whole))
-    pieces = [(0, 0, block)]
     half = block.shape[1] // 2
+    pieces = {0: block}
     up = down = block
     for k in range(1, 4):
         up = shifted(up, "y", 1)
         down = shifted(down, "y", -1)
-        pieces += [(-k, 0, up), (k, 0, down)]
-    pieces.append((4, 0, shifted(up[:, :half], "y", 1)))
-    pieces.append((4, half, shifted(down[:, half:], "y", -1)))
-    for k, first, piece in pieces:
+        pieces[-k], pieces[k] = up, down
+    ends = [(0, shifted(up[:, :half], "y", 1)), (half, shifted(down[:, half:], "y", -1))]
+    count, y_at = lax.axis_size("y"), lax.axis_index("y")
+    parts, z_count, share, columns = block.shape
+    base = -2
+    whole = jnp.broadcast_to(
+        pieces[base][:, :, None], (parts, z_count, count, share, columns)
+    )
+    placed = [(k, 0, piece) for k, piece in pieces.items() if k != base]
+    for k, first, piece in placed + [(4, first, piece) for first, piece in ends]:
         whole = lax.dynamic_update_slice(
             whole, piece[:, :, None], (0, first, (y_at + k) % count, 0, 0)
         )
-    return whole.reshape(parts, -1, columns)
+    return whole.reshape(parts, -1, columns), pieces[3]
 
 
 def gelu_parts(gate):
@@ -186,7 +188,7 @@
     second = lax.axis_index("zp") == 1
 
     own, other = halves_of(jnp.stack([down_weight.T, gate_weight, up_weight]), second)
-    weights = gathered_y(gathered_z(own, other))
+    weights, late = gathered_y(gathered_z(own, other))
 
     spare = ((0, 0), (0, columns - width))
     last = jnp.concatenate([gate_lin[-2:], up_lin[-1:], jnp.pad(out_grad[-1:], spare)])
@@ -203,14 +205,14 @@
     )
     grads = sent_to_all(grads, GROUP)
 
-    saved = jnp.concatenate(
-        [before[:2], gate_lin, after[:2], before[2:3], up_lin, after[2:3]]
-    )
-    kept, sent = halves_of(saved, second)
+    kept, sent = halves_of(jnp.concatenate([gate_lin, up_lin, before, after]), second)
     came = swapped(sent, "zp", 1)
+    kept, came, _ = lax.optimization_barrier((kept, came, late))
     pair = jnp.stack([jnp.where(second, came, kept), jnp.where(second, kept, came)])
     pair = pair.astype(jnp.float32)
-    linear, up_ext = pair[:, : rows + 4], pair[:, rows + 4 :]
+    edge = pair[:, 2 * rows :]
+    linear = jnp.concatenate([edge[:, :2], pair[:, :rows], edge[:, 4:6]], axis=1)
+    up_ext = jnp.concatenate([edge[:, 2:3], pair[:, rows : 2 * rows], edge[:, 6:7]], axis=1)
     start = lax.axis_index(TP) * columns + jnp.where(second, half, 0)
     taps = lax.dynamic_slice_in_dim(conv_weight, start, half, 1).astype(jnp.float32)
 
@@ -226,27 +228,18 @@
         jnp.pad(linear, ((0, 0), (0, PAD - rows - 4), (0, 0))),
         taps,
     )
-    one, two = shifted(conv, "rep", 1), shifted(conv, "rep", 2)
+    conv = sent_to_all(conv, Z_ALL)
+    conv = conv.reshape(-1, 2, 3, half).sum(axis=0).transpose(1, 0, 2).reshape(3, columns)
     product = output_partials(linear_grad, up_grad, weights, width)
     arrived = lax.all_to_all(product, GROUP, 0, 0, tiled=True)
     input_grad = arrived.astype(jnp.float32).sum(axis=0).astype(jnp.bfloat16)
-    rep_at, rep_count = lax.axis_index("rep"), lax.axis_size("rep")
-    conv = sum(lax.select_n((rep_at - k) % rep_count, conv, one, two) for k in range(rep_count))
-    near = conv + swapped(conv, "zk", 1)
-    pair_swap = [(i, i ^ 1) for i in range(4)]
-    both_swap = [(i, i ^ 3) for i in range(4)]
-    far = lax.ppermute(conv, ("zk", "zp"), pair_swap) + lax.ppermute(conv, ("zk", "zp"), both_swap)
-    conv = jnp.concatenate(
-        [jnp.where(second, far, near), jnp.where(second, near, far)], axis=1
-    )
-    conv = (conv + swapped(conv, "y", 1)) + (swapped(conv, "y", 2) + swapped(conv, "y", 3))
-    conv = conv + swapped(conv, "y", 4)
-    low = lax.axis_index("core") == 0
-    peer = swapped(conv, "core", 1)
-    conv = jnp.stack([jnp.where(low, conv, peer), jnp.where(low, peer, conv)])
-    peers = [conv] + [swapped(conv, "x", k) for k in range(1, 4)]
-    x_at = lax.axis_index("x")
-    conv = jnp.concatenate([lax.select_n(x_at ^ k, *peers) for k in range(4)])
+    for bit in (1, 2, 4):
+        conv = conv + swapped(conv, "y", bit)
+    conv = conv[None]
+    for axis, bit in (("core", 1), ("x", 1), ("x", 2)):
+        low = lax.axis_index(axis) & bit == 0
+        peer = swapped(conv, axis, bit)
+        conv = jnp.concatenate([jnp.where(low, conv, peer), jnp.where(low, peer, conv)])
     conv_grad = conv.transpose(1, 0, 2).reshape(3, -1)
     return (input_grad, conv_grad)
 

time: 239 us -> 212 us (0.89)
  starting transfers between devices: 119 us -> 102 us
  waiting for transfers between devices: 75.2 us -> 61.8 us
  local copies, waits for them, and re-layouts: 23.4 us -> 26.3 us
    ppermute x13 -> x11, waiting for transfers between devices: 57.9 us -> 42.6 us  [shifted(): lax.ppermute(value, axis, [(i, (i + by) % count) for i in range(count)])]
    ppermute x10 -> x7, starting transfers between devices: 37.6 us -> 23 us  [swapped(): lax.ppermute(value, axis, [(i, i ^ bit) for i in range(lax.axis_size(axis...]
    all_to_all x1 -> x2, starting transfers between devices: 12.4 us -> 20.1 us  [sent_to_all(): lax.all_to_all(jnp.broadcast_to(value[None], (peers, *value.shape)), axis...]
    ppermute x2 -> x0, starting transfers between devices: 6.9 us -> none  [the longest x1 4.98 us: block_gradients(): lax.ppermute(conv, ('zk', 'zp'), both_swap)]
    ppermute x13 -> x11, starting transfers between devices: 49.2 us -> 42.8 us  [shifted(): lax.ppermute(value, axis, [(i, (i + by) % count) for i in range(count)])]
    all_to_all x1 -> x2, waiting for transfers between devices: 0.01 us -> 3.88 us  [sent_to_all(): lax.all_to_all(jnp.broadcast_to(value[None], (peers, *value.shape)), axis...]
    concatenate x1 -> x0, local copies, waits for them, and re-layouts: 3.63 us -> none  [block_gradients(): jnp.concatenate([before[:2], gate_lin, after[:2], before[2:3], up_lin, af...]
    dynamic_update_slice x9 -> x8, local copies, waits for them, and re-layouts: 7.87 us -> 10.2 us  [gathered_y(): lax.dynamic_update_slice(whole, piece[:, :, None], (0, first, (y_at + k)...]
  transfers between devices with their start and end apart: 29 -> 23, of which waited for: 14 -> 11; matrix products, arithmetic and copies ran while one was open for 10% -> 11% of each run, Pallas kernels for 0% -> 3%
where the time goes in v2:
time: 212 us; the launch traced here: 209 us
  starting transfers between devices  102 us (48%)
  waiting for transfers between devices  61.8 us (29%)
  local copies, waits for them, and re-layouts  26.3 us (12%)
  Pallas kernels  11 us (5%)
  other arithmetic  6.79 us (3%)
    ppermute x11, starting transfers between devices, shifted(): lax.ppermute(value, axis, [(i, (i + by) % count) for i in range(count)])  42.8 us
    ppermute x11, waiting for transfers between devices, shifted(): lax.ppermute(value, axis, [(i, (i + by) % count) for i in range(count)])  42.6 us
    ppermute x7, starting transfers between devices, swapped(): lax.ppermute(value, axis, [(i, i ^ bit) for i in range(lax.axis_size(axis...  23 us
    all_to_all x2, starting transfers between devices, sent_to_all(): lax.all_to_all(jnp.broadcast_to(value[None], (peers, *value.shape)), axis...  20.1 us
    ppermute x7, waiting for transfers between devices, swapped(): lax.ppermute(value, axis, [(i, i ^ bit) for i in range(lax.axis_size(axis...  14.6 us
    dynamic_update_slice x8, local copies, waits for them, and re-layouts, gathered_y(): lax.dynamic_update_slice(whole, piece[:, :, None], (0, first, (y_at + k)...  10.2 us
    all_to_all x1, starting transfers between devices, block_gradients(): arrived = lax.all_to_all(product, GROUP, 0, 0, tiled=True)  9.95 us
    ppermute x2, starting transfers between devices, to_next(): return lax.ppermute(value, axis, pairs)  5.94 us
  transfers between devices with their start and end apart: 23, of which 11 were waited for; matrix products, arithmetic and copies ran while one was open for 11% of the time, Pallas kernels for 3%

profile of v2, /device:TPU:1, one launch (start us, length us, event | category | flops | bytes accessed | tf_op | source)
XLA Modules:
  0.0 208.9 jit_solution(4866866598442437864)
XLA Ops:
  0.7 0.8 fusion.16
  1.4 1.2 copy.58
  2.6 1.2 copy.57
  3.8 1.3 collective-permute-start.1
  5.1 4.6 %collective-permute-start = (bf16[4,704]{1,0:T(4,128)(2,1)S(1)}, bf16[4,704]{1,0:T(4,128)(2,1)S(1)}, u32[]{:S(2)}, u32[]{:S(2)}) collective-permute-start(bf16[4,704]{1,0:T(4,128)(2,1)S(1)} %fusion.9), channel_id=1, source_target_pairs={{0,8},{8,16},{16,24},{24,32},{32,40},{40,48},{48,56},{56,64},{64,7... | collective-permute-start | bytes 16904 | tf_op jit(solution)/shard_map/ppermute | solution.py:28
  9.9 0.7 collective-permute-done
  10.5 0.6 copy-done.5
  11.1 1.0 maximum_maximum_fusion
  12.1 1.5 broadcast_in_dim.49
  13.7 14.5 %all-to-all-start = ((bf16[16,264,256]{2,1,0:T(8,128)(2,1)}), bf16[16,264,256]{2,1,0:T(8,128)(2,1)S(1)}, u32[]{:S(2)}, u32[]{:S(2)}) async-start(bf16[16,264,256]{2,1,0:T(8,128)(2,1)} %broadcast_in_dim.49), calls=%async_computation | async-start | bytes 4325376 | tf_op jit(solution)/shard_map/all_to_all | solution.py:37
  28.2 0.8 broadcast_select_fusion.2
  29.0 4.4 %collective-permute-start.3 = (bf16[3,64,352]{2,1,0:T(8,128)(2,1)S(1)}, bf16[3,64,352]{2,1,0:T(8,128)(2,1)S(1)}, u32[]{:S(2)}, u32[]{:S(2)}) collective-permute-start(bf16[3,64,352]{2,1,0:T(8,128)(2,1)S(1)} %get-tuple-element.38), channel_id=1, source_target_pairs={{0,128},{64,192},{128,256},{192,320},{256,384},{320,448},{384,512}... | collective-permute-start | bytes 405512 | tf_op jit(solution)/shard_map/ppermute | solution.py:22
  33.3 3.3 %collective-permute-start.4 = (bf16[3,64,352]{2,1,0:T(8,128)(2,1)}, bf16[3,64,352]{2,1,0:T(8,128)(2,1)S(1)}, u32[]{:S(2)}, u32[]{:S(2)}) collective-permute-start(bf16[3,64,352]{2,1,0:T(8,128)(2,1)} %get-tuple-element.37), channel_id=1, source_target_pairs={{0,64},{64,128},{128,192},{192,256},{256,320},{320,384},{384,448},... | collective-permute-start | bytes 405512 | tf_op jit(solution)/shard_map/ppermute | solution.py:22
  36.6 9.2 %collective-permute-start.2 = (bf16[3,64,352]{2,1,0:T(8,128)(2,1)}, bf16[3,64,352]{2,1,0:T(8,128)(2,1)S(1)}, u32[]{:S(2)}, u32[]{:S(2)}) collective-permute-start(bf16[3,64,352]{2,1,0:T(8,128)(2,1)} %get-tuple-element.37), channel_id=1, source_target_pairs={{0,704},{64,0},{128,64},{192,128},{256,192},{320,256},{384,320},{4... | collective-permute-start | bytes 405512 | tf_op jit(solution)/shard_map/ppermute | solution.py:22
  45.9 25.2 %collective-permute-done.3 = bf16[3,64,352]{2,1,0:T(8,128)(2,1)S(1)} collective-permute-done((bf16[3,64,352]{2,1,0:T(8,128)(2,1)S(1)}, bf16[3,64,352]{2,1,0:T(8,128)(2,1)S(1)}, u32[]{:S(2)}, u32[]{:S(2)}) %collective-permute-start.3) | collective-permute-done | bytes 135200 | tf_op jit(solution)/shard_map/ppermute | solution.py:22
  71.2 1.0 fusion.11
  72.2 1.9 collective-permute-start.5
  74.1 4.6 %collective-permute-start.7 = (bf16[3,4,64,352]{3,2,0,1:T(8,128)(2,1)}, bf16[3,4,64,352]{3,2,0,1:T(8,128)(2,1)}, u32[]{:S(2)}, u32[]{:S(2)}) collective-permute-start(bf16[3,4,64,352]{3,2,0,1:T(8,128)(2,1)} %get-tuple-element.28), channel_id=1, source_target_pairs={{0,56},{8,0},{16,8},{24,16},{32,24},{40,32},{48,40},{56,48},{1,57}... | collective-permute-start | bytes 1622024 | tf_op jit(solution)/shard_map/ppermute | solution.py:22
  78.7 11.0 %collective-permute-done.5 = bf16[3,4,64,352]{3,2,0,1:T(8,128)(2,1)} collective-permute-done((bf16[3,4,64,352]{3,2,0,1:T(8,128)(2,1)}, bf16[3,4,64,352]{3,2,0,1:T(8,128)(2,1)}, u32[]{:S(2)}, u32[]{:S(2)}) %collective-permute-start.5) | collective-permute-done | bytes 540704 | tf_op jit(solution)/shard_map/ppermute | solution.py:22
  89.7 1.9 collective-permute-start.6
  91.7 4.6 %collective-permute-start.8 = (bf16[3,4,64,352]{3,2,0,1:T(8,128)(2,1)}, bf16[3,4,64,352]{3,2,0,1:T(8,128)(2,1)}, u32[]{:S(2)}, u32[]{:S(2)}) collective-permute-start(bf16[3,4,64,352]{3,2,0,1:T(8,128)(2,1)} %collective-permute-done.7), channel_id=1, source_target_pairs={{0,56},{8,0},{16,8},{24,16},{32,24},{40,32},{48,40},{56,48},{1,57}... | collective-permute-start | bytes 1622024 | tf_op jit(solution)/shard_map/ppermute | solution.py:22
  96.3 0.8 dynamic-slice_convert_fusion.taps
  97.1 0.8 pad_maximum_fusion.1
  98.1 1.9 collective-permute-start.13
  100.0 6.4 %collective-permute-done.6 = bf16[3,4,64,352]{3,2,0,1:T(8,128)(2,1)} collective-permute-done((bf16[3,4,64,352]{3,2,0,1:T(8,128)(2,1)}, bf16[3,4,64,352]{3,2,0,1:T(8,128)(2,1)}, u32[]{:S(2)}, u32[]{:S(2)}) %collective-permute-start.6) | collective-permute-done | bytes 540704 | tf_op jit(solution)/shard_map/ppermute | solution.py:22
  106.4 1.1 copy.61
  107.5 1.9 collective-permute-start.9
  109.5 4.6 %collective-permute-start.10 = (bf16[3,4,64,352]{3,2,0,1:T(8,128)(2,1)}, bf16[3,4,64,352]{3,2,0,1:T(8,128)(2,1)S(1)}, u32[]{:S(2)}, u32[]{:S(2)}) collective-permute-start(bf16[3,4,64,352]{3,2,0,1:T(8,128)(2,1)} %collective-permute-done.8), channel_id=1, source_target_pairs={{0,56},{8,0},{16,8},{24,16},{32,24},{40,32},{48,40},{56,48},{1,57}... | collective-permute-start | bytes 1622024 | tf_op jit(solution)/shard_map/ppermute | solution.py:22
  114.1 2.9 %broadcast_in_dim.50 = bf16[3,4,8,64,352]{4,3,2,1,0:T(8,128)(2,1)} broadcast(bf16[3,4,64,352]{3,2,1,0:T(8,128)(2,1)S(1)} %copy.61), dimensions={0,1,3,4} | broadcast | bytes 4866048 | tf_op jit(solution)/shard_map/broadcast_in_dim | solution.py:69
  117.0 1.0 copy_dynamic-update-slice_fusion.5
  118.0 1.9 copy_dynamic-update-slice_fusion.4
  119.9 2.0 copy_dynamic-update-slice_fusion.3
  121.9 2.1 copy_dynamic-update-slice_fusion.2
  124.0 1.9 collective-permute-start.11
  125.9 4.6 %collective-permute-start.12 = (bf16[3,2,64,352]{3,2,0,1:T(8,128)(2,1)S(1)}, bf16[3,2,64,352]{3,2,0,1:T(8,128)(2,1)S(1)}, u32[]{:S(2)}, u32[]{:S(2)}) collective-permute-start(bf16[3,2,64,352]{3,2,0,1:T(8,128)(2,1)S(1)} %slice.114), channel_id=1, source_target_pairs={{0,56},{8,0},{16,8},{24,16},{32,24},{40,32},{48,40},{56,48},{1,57}... | collective-permute-start | bytes 811016 | tf_op jit(solution)/shard_map/ppermute | solution.py:22
  131.0 0.7 fusion.12
  131.7 0.9 copy_dynamic-update-slice_fusion.1
  132.6 0.9 copy_dynamic-update-slice_fusion
  133.5 1.0 pad.22.linear
  134.5 1.0 pad.20.slope
  135.4 1.0 pad.21.value
  136.4 0.7 copy_dynamic-update-slice_fusion.7
  137.2 0.8 copy_dynamic-update-slice_fusion.6
  138.0 1.4 copy-done
  139.3 5.2 %shard_map.86 = (bf16[2,256,352]{2,1,0:T(8,128)(2,1)}, bf16[2,256,352]{2,1,0:T(8,128)(2,1)}, f32[3,352]{1,0:T(4,128)}) custom-call(bf16[16,264,256]{2,1,0:T(8,128)(2,1)} %copy-done, bf16[3,2048,352]{2,1,0:T(8,128)(2,1)} %bitcast.16.down.gate.up, f32[2,264,352]{2,1,0:T(8,128)} %pad.20.slope, f32[2,264,352]{2,1,0:T(8,128)} %pad.21.value, ...), custom_call_target="tpu_custom_call" | custom-call | tf_op jit(solution)/shard_map/pallas_call | solution.py:130
  144.5 1.3 broadcast_in_dim.59
  145.9 5.6 %all-to-all-start.2 = ((f32[12,3,352]{2,1,0:T(4,128)}), f32[12,3,352]{2,1,0:T(4,128)S(1)}, u32[]{:S(2)}, u32[]{:S(2)}) async-start(f32[12,3,352]{2,1,0:T(4,128)} %broadcast_in_dim.59), calls=%async_computation.2 | async-start | bytes 147456 | tf_op jit(solution)/shard_map/all_to_all | solution.py:37
  151.5 5.9 %shard_map.87 = bf16[2,8,256,256]{3,2,1,0:T(8,128)(2,1)} custom-call(bf16[2,256,352]{2,1,0:T(8,128)(2,1)} %get-tuple-element.9.linear_grad, bf16[2,256,352]{2,1,0:T(8,128)(2,1)} %get-tuple-element.10.up_grad, bf16[3,2048,352]{2,1,0:T(8,128)(2,1)} %bitcast.16.down.gate.up, bf16[3,2048,352]{2,1,0:T(8,128)(2,1)} %bitcast.16.down.gate.up), custom_call_target="tpu_custom_call" | custom-call | tf_op jit(solution)/shard_map/pallas_call | solution.py:169
  157.3 3.9 %all-to-all-done.2 = f32[12,3,352]{2,1,0:T(4,128)S(1)} async-done(((f32[12,3,352]{2,1,0:T(4,128)}), f32[12,3,352]{2,1,0:T(4,128)S(1)}, u32[]{:S(2)}, u32[]{:S(2)}) %all-to-all-start.2) | async-done | bytes 50720 | tf_op jit(solution)/shard_map/all_to_all | solution.py:37
  161.2 9.9 %all-to-all-start.1 = ((bf16[16,256,256]{2,1,0:T(8,128)(2,1)}), bf16[16,256,256]{2,1,0:T(8,128)(2,1)S(1)}, u32[]{:S(2)}, u32[]{:S(2)}) async-start(bf16[16,256,256]{2,1,0:T(8,128)(2,1)} %bitcast.50), calls=%async_computation.1 | async-start | bytes 4194304 | tf_op jit(solution)/shard_map/all_to_all | solution.py:234
  171.3 1.9 collective-permute-start.14
  173.2 2.8 %collective-permute-done.14 = f32[3,704]{1,0:T(4,128)S(1)} collective-permute-done((f32[3,704]{1,0:T(4,128)S(1)}, f32[3,704]{1,0:T(4,128)S(1)}, u32[]{:S(2)}, u32[]{:S(2)}) %collective-permute-start.14) | collective-permute-done | bytes 8480 | tf_op jit(solution)/shard_map/ppermute | solution.py:32
  176.0 1.9 collective-permute-start.15
  177.9 3.7 %collective-permute-done.15 = f32[3,704]{1,0:T(4,128)S(1)} collective-permute-done((f32[3,704]{1,0:T(4,128)S(1)}, f32[3,704]{1,0:T(4,128)S(1)}, u32[]{:S(2)}, u32[]{:S(2)}) %collective-permute-start.15) | collective-permute-done | bytes 8480 | tf_op jit(solution)/shard_map/ppermute | solution.py:32
  181.6 4.0 %collective-permute-start.16 = (f32[3,704]{1,0:T(4,128)S(1)}, f32[3,704]{1,0:T(4,128)S(1)}, u32[]{:S(2)}, u32[]{:S(2)}) collective-permute-start(f32[3,704]{1,0:T(4,128)S(1)} %add.156), channel_id=1, source_target_pairs={{0,32},{8,40},{16,48},{24,56},{32,0},{40,8},{48,16},{56,24},{1,33}... | collective-permute-start | bytes 25352 | tf_op jit(solution)/shard_map/ppermute | solution.py:32
  185.7 4.3 %collective-permute-done.16 = f32[3,704]{1,0:T(4,128)S(1)} collective-permute-done((f32[3,704]{1,0:T(4,128)S(1)}, f32[3,704]{1,0:T(4,128)S(1)}, u32[]{:S(2)}, u32[]{:S(2)}) %collective-permute-start.16) | collective-permute-done | bytes 8480 | tf_op jit(solution)/shard_map/ppermute | solution.py:32
  190.0 4.9 %collective-permute-start.17 = (f32[1,3,704]{2,1,0:T(4,128)S(1)}, f32[1,3,704]{2,1,0:T(4,128)S(1)}, u32[]{:S(2)}, u32[]{:S(2)}) collective-permute-start(f32[1,3,704]{2,1,0:T(4,128)S(1)} %add_bitcast_fusion), channel_id=1, source_target_pairs={{0,1},{1,0},{2,3},{3,2},{4,5},{5,4},{6,7},{7,6},{8,9},{9,8},{10,11... | collective-permute-start | bytes 25352 | tf_op jit(solution)/shard_map/ppermute | solution.py:32
  194.9 0.8 collective-permute-done.17
  195.7 3.9 %collective-permute-start.18 = (f32[2,3,704]{2,1,0:T(4,128)S(1)}, f32[2,3,704]{2,1,0:T(4,128)S(1)}, u32[]{:S(2)}, u32[]{:S(2)}) collective-permute-start(f32[2,3,704]{2,1,0:T(4,128)S(1)} %pad_maximum_fusion.5), channel_id=1, source_target_pairs={{0,2},{2,0},{4,6},{6,4},{1,3},{3,1},{5,7},{7,5},{8,10},{10,8},{12,... | collective-permute-start | bytes 50696 | tf_op jit(solution)/shard_map/ppermute | solution.py:32
  199.6 1.2 collective-permute-done.18
  200.8 4.6 %collective-permute-start.19 = (f32[4,3,704]{2,1,0:T(4,128)S(1)}, f32[4,3,704]{2,1,0:T(4,128)S(1)}, u32[]{:S(2)}, u32[]{:S(2)}) collective-permute-start(f32[4,3,704]{2,1,0:T(4,128)S(1)} %pad_maximum_fusion.4), channel_id=1, source_target_pairs={{0,4},{2,6},{4,0},{6,2},{1,5},{3,7},{5,1},{7,3},{8,12},{10,14},{12... | collective-permute-start | bytes 101384 | tf_op jit(solution)/shard_map/ppermute | solution.py:32
  205.4 1.8 collective-permute-done.19
  207.2 0.7 reshape.29
  208.0 1.0 reduce_sum.21
  (55 shorter events, 1.3 us)
Async XLA Ops:
  0.6 27.5 %copy-start.1 = (bf16[64,704]{1,0:T(8,128)(2,1)S(1)}, bf16[64,704]{1,0:T(8,128)(2,1)}, u32[]{:S(2)}) copy-start(bf16[64,704]{1,0:T(8,128)(2,1)} %param.12) | copy-start | bytes 270340
  0.6 27.5 %copy-start.2 = (bf16[64,704]{1,0:T(8,128)(2,1)S(1)}, bf16[64,704]{1,0:T(8,128)(2,1)}, u32[]{:S(2)}) copy-start(bf16[64,704]{1,0:T(8,128)(2,1)} %param.11) | copy-start | bytes 270340
  0.7 27.5 %copy-start.3 = (bf16[704,64]{0,1:T(8,128)(2,1)S(1)}, bf16[704,64]{0,1:T(8,128)(2,1)}, u32[]{:S(2)}) copy-start(bf16[704,64]{0,1:T(8,128)(2,1)} %param.13) | copy-start | bytes 270340
  3.8 6.1 %collective-permute-start.1 = (bf16[4,704]{1,0:T(4,128)(2,1)S(1)}, bf16[4,704]{1,0:T(4,128)(2,1)S(1)}, u32[]{:S(2)}, u32[]{:S(2)}) collective-permute-start(bf16[4,704]{1,0:T(4,128)(2,1)S(1)} %fusion.10), channel_id=1, source_target_pairs={{8,0},{16,8},{24,16},{32,24},{40,32},{48,40},{56,48},{64,56},{72,6... | collective-permute-start | bytes 16904 | tf_op jit(solution)/shard_map/ppermute | solution.py:28
  5.1 5.4 %collective-permute-start = (bf16[4,704]{1,0:T(4,128)(2,1)S(1)}, bf16[4,704]{1,0:T(4,128)(2,1)S(1)}, u32[]{:S(2)}, u32[]{:S(2)}) collective-permute-start(bf16[4,704]{1,0:T(4,128)(2,1)S(1)} %fusion.9), channel_id=1, source_target_pairs={{0,8},{8,16},{16,24},{24,32},{32,40},{40,48},{48,56},{56,64},{64,7... | collective-permute-start | bytes 16904 | tf_op jit(solution)/shard_map/ppermute | solution.py:28
  10.5 0.6 copy-start.5
  13.7 124.3 %all-to-all-start = ((bf16[16,264,256]{2,1,0:T(8,128)(2,1)}), bf16[16,264,256]{2,1,0:T(8,128)(2,1)S(1)}, u32[]{:S(2)}, u32[]{:S(2)}) async-start(bf16[16,264,256]{2,1,0:T(8,128)(2,1)} %broadcast_in_dim.49), calls=%async_computation | async-start | bytes 4325376 | tf_op jit(solution)/shard_map/all_to_all | solution.py:37
  29.0 42.1 %collective-permute-start.3 = (bf16[3,64,352]{2,1,0:T(8,128)(2,1)S(1)}, bf16[3,64,352]{2,1,0:T(8,128)(2,1)S(1)}, u32[]{:S(2)}, u32[]{:S(2)}) collective-permute-start(bf16[3,64,352]{2,1,0:T(8,128)(2,1)S(1)} %get-tuple-element.38), channel_id=1, source_target_pairs={{0,128},{64,192},{128,256},{192,320},{256,384},{320,448},{384,512}... | collective-permute-start | bytes 405512 | tf_op jit(solution)/shard_map/ppermute | solution.py:22
  33.3 37.8 %collective-permute-start.4 = (bf16[3,64,352]{2,1,0:T(8,128)(2,1)}, bf16[3,64,352]{2,1,0:T(8,128)(2,1)S(1)}, u32[]{:S(2)}, u32[]{:S(2)}) collective-permute-start(bf16[3,64,352]{2,1,0:T(8,128)(2,1)} %get-tuple-element.37), channel_id=1, source_target_pairs={{0,64},{64,128},{128,192},{192,256},{256,320},{320,384},{384,448},... | collective-permute-start | bytes 405512 | tf_op jit(solution)/shard_map/ppermute | solution.py:22
  36.6 34.5 %collective-permute-start.2 = (bf16[3,64,352]{2,1,0:T(8,128)(2,1)}, bf16[3,64,352]{2,1,0:T(8,128)(2,1)S(1)}, u32[]{:S(2)}, u32[]{:S(2)}) collective-permute-start(bf16[3,64,352]{2,1,0:T(8,128)(2,1)} %get-tuple-element.37), channel_id=1, source_target_pairs={{0,704},{64,0},{128,64},{192,128},{256,192},{320,256},{384,320},{4... | collective-permute-start | bytes 405512 | tf_op jit(solution)/shard_map/ppermute | solution.py:22
  72.2 17.5 %collective-permute-start.5 = (bf16[3,4,64,352]{3,2,0,1:T(8,128)(2,1)}, bf16[3,4,64,352]{3,2,0,1:T(8,128)(2,1)}, u32[]{:S(2)}, u32[]{:S(2)}) collective-permute-start(bf16[3,4,64,352]{3,2,0,1:T(8,128)(2,1)} %get-tuple-element.28), channel_id=1, source_target_pairs={{0,8},{8,16},{16,24},{24,32},{32,40},{40,48},{48,56},{56,0},{1,9},... | collective-permute-start | bytes 1622024 | tf_op jit(solution)/shard_map/ppermute | solution.py:22
  74.1 17.5 %collective-permute-start.7 = (bf16[3,4,64,352]{3,2,0,1:T(8,128)(2,1)}, bf16[3,4,64,352]{3,2,0,1:T(8,128)(2,1)}, u32[]{:S(2)}, u32[]{:S(2)}) collective-permute-start(bf16[3,4,64,352]{3,2,0,1:T(8,128)(2,1)} %get-tuple-element.28), channel_id=1, source_target_pairs={{0,56},{8,0},{16,8},{24,16},{32,24},{40,32},{48,40},{56,48},{1,57}... | collective-permute-start | bytes 1622024 | tf_op jit(solution)/shard_map/ppermute | solution.py:22
  89.7 16.7 %collective-permute-start.6 = (bf16[3,4,64,352]{3,2,0,1:T(8,128)(2,1)}, bf16[3,4,64,352]{3,2,0,1:T(8,128)(2,1)}, u32[]{:S(2)}, u32[]{:S(2)}) collective-permute-start(bf16[3,4,64,352]{3,2,0,1:T(8,128)(2,1)} %collective-permute-done.5), channel_id=1, source_target_pairs={{0,8},{8,16},{16,24},{24,32},{32,40},{40,48},{48,56},{56,0},{1,9},... | collective-permute-start | bytes 1622024 | tf_op jit(solution)/shard_map/ppermute | solution.py:22
  91.7 17.8 %collective-permute-start.8 = (bf16[3,4,64,352]{3,2,0,1:T(8,128)(2,1)}, bf16[3,4,64,352]{3,2,0,1:T(8,128)(2,1)}, u32[]{:S(2)}, u32[]{:S(2)}) collective-permute-start(bf16[3,4,64,352]{3,2,0,1:T(8,128)(2,1)} %collective-permute-done.7), channel_id=1, source_target_pairs={{0,56},{8,0},{16,8},{24,16},{32,24},{40,32},{48,40},{56,48},{1,57}... | collective-permute-start | bytes 1622024 | tf_op jit(solution)/shard_map/ppermute | solution.py:22
  97.0 20.0 %copy-start.4 = (f32[3,352]{1,0:T(4,128)}, f32[3,352]{1,0:T(4,128)S(1)}, u32[]{:S(2)}) copy-start(f32[3,352]{1,0:T(4,128)S(1)} %dynamic-slice_convert_fusion.taps) | copy-start | bytes 12676
  98.1 32.5 %collective-permute-start.13 = (bf16[520,352]{1,0:T(8,128)(2,1)S(1)}, bf16[520,352]{1,0:T(8,128)(2,1)S(1)}, u32[]{:S(2)}, u32[]{:S(2)}) collective-permute-start(bf16[520,352]{1,0:T(8,128)(2,1)S(1)} %get-tuple-element.25), channel_id=1, source_target_pairs={{0,64},{64,0},{1,65},{65,1},{2,66},{66,2},{3,67},{67,3},{4,68},{68... | collective-permute-start | bytes 1098248 | tf_op jit(solution)/shard_map/ppermute | solution.py:32
  107.5 16.4 %collective-permute-start.9 = (bf16[3,4,64,352]{3,2,0,1:T(8,128)(2,1)}, bf16[3,4,64,352]{3,2,0,1:T(8,128)(2,1)S(1)}, u32[]{:S(2)}, u32[]{:S(2)}) collective-permute-start(bf16[3,4,64,352]{3,2,0,1:T(8,128)(2,1)} %collective-permute-done.6), channel_id=1, source_target_pairs={{0,8},{8,16},{16,24},{24,32},{32,40},{40,48},{48,56},{56,0},{1,9},... | collective-permute-start | bytes 1622024 | tf_op jit(solution)/shard_map/ppermute | solution.py:22
  109.5 16.4 %collective-permute-start.10 = (bf16[3,4,64,352]{3,2,0,1:T(8,128)(2,1)}, bf16[3,4,64,352]{3,2,0,1:T(8,128)(2,1)S(1)}, u32[]{:S(2)}, u32[]{:S(2)}) collective-permute-start(bf16[3,4,64,352]{3,2,0,1:T(8,128)(2,1)} %collective-permute-done.8), channel_id=1, source_target_pairs={{0,56},{8,0},{16,8},{24,16},{32,24},{40,32},{48,40},{56,48},{1,57}... | collective-permute-start | bytes 1622024 | tf_op jit(solution)/shard_map/ppermute | solution.py:22
  124.0 12.5 %collective-permute-start.11 = (bf16[3,2,64,352]{3,2,0,1:T(8,128)(2,1)S(1)}, bf16[3,2,64,352]{3,2,0,1:T(8,128)(2,1)S(1)}, u32[]{:S(2)}, u32[]{:S(2)}) collective-permute-start(bf16[3,2,64,352]{3,2,0,1:T(8,128)(2,1)S(1)} %slice.113), channel_id=1, source_target_pairs={{0,8},{8,16},{16,24},{24,32},{32,40},{40,48},{48,56},{56,0},{1,9},... | collective-permute-start | bytes 811016 | tf_op jit(solution)/shard_map/ppermute | solution.py:22
  125.9 11.2 %collective-permute-start.12 = (bf16[3,2,64,352]{3,2,0,1:T(8,128)(2,1)S(1)}, bf16[3,2,64,352]{3,2,0,1:T(8,128)(2,1)S(1)}, u32[]{:S(2)}, u32[]{:S(2)}) collective-permute-start(bf16[3,2,64,352]{3,2,0,1:T(8,128)(2,1)S(1)} %slice.114), channel_id=1, source_target_pairs={{0,56},{8,0},{16,8},{24,16},{32,24},{40,32},{48,40},{56,48},{1,57}... | collective-permute-start | bytes 811016 | tf_op jit(solution)/shard_map/ppermute | solution.py:22
  138.0 1.4 copy-start
  145.9 15.4 %all-to-all-start.2 = ((f32[12,3,352]{2,1,0:T(4,128)}), f32[12,3,352]{2,1,0:T(4,128)S(1)}, u32[]{:S(2)}, u32[]{:S(2)}) async-start(f32[12,3,352]{2,1,0:T(4,128)} %broadcast_in_dim.59), calls=%async_computation.2 | async-start | bytes 147456 | tf_op jit(solution)/shard_map/all_to_all | solution.py:37
  161.2 46.8 %all-to-all-start.1 = ((bf16[16,256,256]{2,1,0:T(8,128)(2,1)}), bf16[16,256,256]{2,1,0:T(8,128)(2,1)S(1)}, u32[]{:S(2)}, u32[]{:S(2)}) async-start(bf16[16,256,256]{2,1,0:T(8,128)(2,1)} %bitcast.50), calls=%async_computation.1 | async-start | bytes 4194304 | tf_op jit(solution)/shard_map/all_to_all | solution.py:234
  171.3 4.7 %collective-permute-start.14 = (f32[3,704]{1,0:T(4,128)S(1)}, f32[3,704]{1,0:T(4,128)S(1)}, u32[]{:S(2)}, u32[]{:S(2)}) collective-permute-start(f32[3,704]{1,0:T(4,128)S(1)} %reshape.28), channel_id=1, source_target_pairs={{0,8},{8,0},{16,24},{24,16},{32,40},{40,32},{48,56},{56,48},{1,9},... | collective-permute-start | bytes 25352 | tf_op jit(solution)/shard_map/ppermute | solution.py:32
  176.0 5.6 %collective-permute-start.15 = (f32[3,704]{1,0:T(4,128)S(1)}, f32[3,704]{1,0:T(4,128)S(1)}, u32[]{:S(2)}, u32[]{:S(2)}) collective-permute-start(f32[3,704]{1,0:T(4,128)S(1)} %add.155), channel_id=1, source_target_pairs={{0,16},{8,24},{16,0},{24,8},{32,48},{40,56},{48,32},{56,40},{1,17}... | collective-permute-start | bytes 25352 | tf_op jit(solution)/shard_map/ppermute | solution.py:32
  181.6 8.3 %collective-permute-start.16 = (f32[3,704]{1,0:T(4,128)S(1)}, f32[3,704]{1,0:T(4,128)S(1)}, u32[]{:S(2)}, u32[]{:S(2)}) collective-permute-start(f32[3,704]{1,0:T(4,128)S(1)} %add.156), channel_id=1, source_target_pairs={{0,32},{8,40},{16,48},{24,56},{32,0},{40,8},{48,16},{56,24},{1,33}... | collective-permute-start | bytes 25352 | tf_op jit(solution)/shard_map/ppermute | solution.py:32
  190.0 5.7 %collective-permute-start.17 = (f32[1,3,704]{2,1,0:T(4,128)S(1)}, f32[1,3,704]{2,1,0:T(4,128)S(1)}, u32[]{:S(2)}, u32[]{:S(2)}) collective-permute-start(f32[1,3,704]{2,1,0:T(4,128)S(1)} %add_bitcast_fusion), channel_id=1, source_target_pairs={{0,1},{1,0},{2,3},{3,2},{4,5},{5,4},{6,7},{7,6},{8,9},{9,8},{10,11... | collective-permute-start | bytes 25352 | tf_op jit(solution)/shard_map/ppermute | solution.py:32
  195.7 5.1 %collective-permute-start.18 = (f32[2,3,704]{2,1,0:T(4,128)S(1)}, f32[2,3,704]{2,1,0:T(4,128)S(1)}, u32[]{:S(2)}, u32[]{:S(2)}) collective-permute-start(f32[2,3,704]{2,1,0:T(4,128)S(1)} %pad_maximum_fusion.5), channel_id=1, source_target_pairs={{0,2},{2,0},{4,6},{6,4},{1,3},{3,1},{5,7},{7,5},{8,10},{10,8},{12,... | collective-permute-start | bytes 50696 | tf_op jit(solution)/shard_map/ppermute | solution.py:32
  200.8 6.3 %collective-permute-start.19 = (f32[4,3,704]{2,1,0:T(4,128)S(1)}, f32[4,3,704]{2,1,0:T(4,128)S(1)}, u32[]{:S(2)}, u32[]{:S(2)}) collective-permute-start(f32[4,3,704]{2,1,0:T(4,128)S(1)} %pad_maximum_fusion.4), channel_id=1, source_target_pairs={{0,4},{2,6},{4,0},{6,2},{1,5},{3,7},{5,1},{7,3},{8,12},{10,14},{12... | collective-permute-start | bytes 101384 | tf_op jit(solution)/shard_map/ppermute | solution.py:32

commit v3 on v2

--- a/solution.py
+++ b/solution.py
@@ -54,27 +54,39 @@
     )
 
 
+def placed(pieces, base, count, y_at):
+    first = pieces.pop(base)[0][1]
+    outer, share, columns = first.shape
+    whole = jnp.broadcast_to(first[:, None], (outer, count, share, columns))
+    for k, parts in pieces.items():
+        for start, part in parts:
+            whole = lax.dynamic_update_slice(whole, part[:, None], (start, (y_at + k) % count, 0, 0))
+    return whole
+
+
 def gathered_y(block):
-    half = block.shape[1] // 2
-    pieces = {0: block}
-    up = down = block
-    for k in range(1, 4):
-        up = shifted(up, "y", 1)
-        down = shifted(down, "y", -1)
-        pieces[-k], pieces[k] = up, down
-    ends = [(0, shifted(up[:, :half], "y", 1)), (half, shifted(down[:, half:], "y", -1))]
+    _, z_count, share, columns = block.shape
+    own_down, own_rest = block[0], block[1:].reshape(-1, share, columns)
+    rest, mid = own_rest.shape[0], z_count // 2
+    downs, rests = {0: [(0, own_down)]}, {0: [(0, own_rest)]}
+    up, low = shifted(own_down, "y", 1), shifted(own_down, "y", -1)
+    downs[-1], downs[1] = [(0, up)], [(0, low)]
+    up = jnp.concatenate([own_rest, up])
+    low = jnp.concatenate([own_rest, low[mid:], low[:mid]])
+    for k in (2, 3):
+        up, low = shifted(up, "y", 1), shifted(low, "y", -1)
+        downs[-k] = [(0, up[rest:])]
+        downs[k] = [(mid, low[rest : rest + mid]), (0, low[rest + mid :])]
+        rests[1 - k], rests[k - 1] = [(0, up[:rest])], [(0, low[:rest])]
+    late = low
+    up, low = shifted(up[: rest + mid], "y", 1), shifted(low[: rest + mid], "y", -1)
+    downs[4] = [(0, up[rest:]), (mid, low[rest:])]
+    rests[-3], rests[3] = [(0, up[:rest])], [(0, low[:rest])]
+    rests[4] = [(0, shifted(up[:z_count], "y", 1)), (z_count, shifted(low[z_count:rest], "y", -1))]
     count, y_at = lax.axis_size("y"), lax.axis_index("y")
-    parts, z_count, share, columns = block.shape
-    base = -2
-    whole = jnp.broadcast_to(
-        pieces[base][:, :, None], (parts, z_count, count, share, columns)
-    )
-    placed = [(k, 0, piece) for k, piece in pieces.items() if k != base]
-    for k, first, piece in placed + [(4, first, piece) for first, piece in ends]:
-        whole = lax.dynamic_update_slice(
-            whole, piece[:, :, None], (0, first, (y_at + k) % count, 0, 0)
-        )
-    return whole.reshape(parts, -1, columns), pieces[3]
+    down_full = placed(downs, -1, count, y_at).reshape(1, -1, columns)
+    rest_full = placed(rests, -1, count, y_at).reshape(rest // z_count, -1, columns)
+    return down_full, rest_full, late
 
 
 def gelu_parts(gate):
@@ -172,8 +184,8 @@
         in_specs=[
             whole,
             whole,
+            pl.BlockSpec((1, weights.shape[1] // steps, half), lambda i: (0, i, 0)),
             pl.BlockSpec((1, weights.shape[1] // steps, half), lambda i: (1, i, 0)),
-            pl.BlockSpec((1, weights.shape[1] // steps, half), lambda i: (2, i, 0)),
         ],
         out_specs=pl.BlockSpec((2, peers // steps, rows, width), lambda i: (0, i, 0, 0)),
         out_shape=jax.ShapeDtypeStruct((2, peers, rows, width), jnp.bfloat16),
@@ -188,7 +200,7 @@
     second = lax.axis_index("zp") == 1
 
     own, other = halves_of(jnp.stack([down_weight.T, gate_weight, up_weight]), second)
-    weights, late = gathered_y(gathered_z(own, other))
+    down_full, rest_full, late = gathered_y(gathered_z(own, other))
 
     spare = ((0, 0), (0, columns - width))
     last = jnp.concatenate([gate_lin[-2:], up_lin[-1:], jnp.pad(out_grad[-1:], spare)])
@@ -222,7 +234,7 @@
     tail = ((0, 0), (0, PAD - rows - 2), (0, 0))
     linear_grad, up_grad, conv = hidden_gradients(
         grads,
-        weights,
+        down_full,
         jnp.pad(up_ext * gelu_slope, tail),
         jnp.pad(gelu_value, tail),
         jnp.pad(linear, ((0, 0), (0, PAD - rows - 4), (0, 0))),
@@ -230,7 +242,7 @@
     )
     conv = sent_to_all(conv, Z_ALL)
     conv = conv.reshape(-1, 2, 3, half).sum(axis=0).transpose(1, 0, 2).reshape(3, columns)
-    product = output_partials(linear_grad, up_grad, weights, width)
+    product = output_partials(linear_grad, up_grad, rest_full, width)
     arrived = lax.all_to_all(product, GROUP, 0, 0, tiled=True)
     input_grad = arrived.astype(jnp.float32).sum(axis=0).astype(jnp.bfloat16)
     for bit in (1, 2, 4):

time: 212 us -> 182 us (0.86)
  waiting for transfers between devices: 61.8 us -> 42.3 us
  local copies, waits for them, and re-layouts: 26.3 us -> 14.1 us
  starting transfers between devices: 102 us -> 106 us
    ppermute x11 -> x13, waiting for transfers between devices: 42.6 us -> 24.6 us  [shifted(): lax.ppermute(value, axis, [(i, (i + by) % count) for i in range(count)])]
    dynamic_update_slice x8 -> x17, local copies, waits for them, and re-layouts: 10.2 us -> 0.74 us  [placed(): lax.dynamic_update_slice(whole, part[:, None], (start, (y_at + k) % count...]
    ppermute x11 -> x13, starting transfers between devices: 42.8 us -> 50.2 us  [shifted(): lax.ppermute(value, axis, [(i, (i + by) % count) for i in range(count)])]
    all_to_all x2, starting transfers between devices: 20.1 us -> 17.5 us  [sent_to_all(): lax.all_to_all(jnp.broadcast_to(value[None], (peers, *value.shape)), axis...]
    broadcast_in_dim x1 -> x2, local copies, waits for them, and re-layouts: 2.94 us -> 0.74 us  [placed(): whole = jnp.broadcast_to(first[:, None], (outer, count, share, columns))]
    unnamed x15 -> x13, local copies, waits for them, and re-layouts: 4.31 us -> 4.13 us
  transfers between devices with their start and end apart: 23 -> 25, of which waited for: 11 -> 12; matrix products, arithmetic and copies ran while one was open for 11% -> 8% of each run, Pallas kernels for 3% -> 6%
where the time goes in v3:
time: 182 us; the launch traced here: 180 us
  starting transfers between devices  106 us (58%)
  waiting for transfers between devices  42.3 us (23%)
  local copies, waits for them, and re-layouts  14.1 us (8%)
  Pallas kernels  11 us (6%)
  other arithmetic  4.96 us (3%)
    ppermute x13, starting transfers between devices, shifted(): lax.ppermute(value, axis, [(i, (i + by) % count) for i in range(count)])  50.2 us
    ppermute x13, waiting for transfers between devices, shifted(): lax.ppermute(value, axis, [(i, (i + by) % count) for i in range(count)])  24.6 us
    ppermute x7, starting transfers between devices, swapped(): lax.ppermute(value, axis, [(i, i ^ bit) for i in range(lax.axis_size(axis...  23.4 us
    all_to_all x2, starting transfers between devices, sent_to_all(): lax.all_to_all(jnp.broadcast_to(value[None], (peers, *value.shape)), axis...  17.5 us
    ppermute x7, waiting for transfers between devices, swapped(): lax.ppermute(value, axis, [(i, i ^ bit) for i in range(lax.axis_size(axis...  15.5 us
    all_to_all x1, starting transfers between devices, block_gradients(): arrived = lax.all_to_all(product, GROUP, 0, 0, tiled=True)  9.59 us
    pallas_call x1, Pallas kernels, output_partials(): pl.pallas_call(output_kernel, grid=(steps,), in_specs=[whole, whole, pl.B...  5.81 us
    ppermute x2, starting transfers between devices, to_next(): return lax.ppermute(value, axis, pairs)  5.28 us
  transfers between devices with their start and end apart: 25, of which 12 were waited for; matrix products, arithmetic and copies ran while one was open for 8% of the time, Pallas kernels for 6%

profile of v3, /device:TPU:1, one launch (start us, length us, event | category | flops | bytes accessed | tf_op | source)
XLA Modules:
  0.0 179.7 jit_solution(3098566422672748595)
XLA Ops:
  0.7 1.1 pad_maximum_fusion.7
  1.7 0.1 broadcast_select_fusion.2
  1.9 4.8 %collective-permute-start.4 = (bf16[3,64,352]{2,1,0:T(8,128)(2,1)S(1)}, bf16[3,64,352]{2,1,0:T(8,128)(2,1)S(1)}, u32[]{:S(2)}, u32[]{:S(2)}) collective-permute-start(bf16[3,64,352]{2,1,0:T(8,128)(2,1)S(1)} %get-tuple-element.37), channel_id=1, source_target_pairs={{0,64},{64,128},{128,192},{192,256},{256,320},{320,384},{384,448},... | collective-permute-start | bytes 405512 | tf_op jit(solution)/shard_map/ppermute | solution.py:22
  6.7 12.2 %collective-permute-start.2 = (bf16[3,64,352]{2,1,0:T(8,128)(2,1)S(1)}, bf16[3,64,352]{2,1,0:T(8,128)(2,1)S(1)}, u32[]{:S(2)}, u32[]{:S(2)}) collective-permute-start(bf16[3,64,352]{2,1,0:T(8,128)(2,1)S(1)} %get-tuple-element.37), channel_id=1, source_target_pairs={{0,704},{64,0},{128,64},{192,128},{256,192},{320,256},{384,320},{4... | collective-permute-start | bytes 405512 | tf_op jit(solution)/shard_map/ppermute | solution.py:22
  18.9 0.7 fusion.32
  19.6 1.2 copy.116
  20.8 0.2 copy.115
  21.0 1.3 collective-permute-start.1
  22.4 4.0 %collective-permute-start = (bf16[4,704]{1,0:T(4,128)(2,1)S(1)}, bf16[4,704]{1,0:T(4,128)(2,1)S(1)}, u32[]{:S(2)}, u32[]{:S(2)}) collective-permute-start(bf16[4,704]{1,0:T(4,128)(2,1)S(1)} %fusion.23), channel_id=1, source_target_pairs={{0,8},{8,16},{16,24},{24,32},{32,40},{40,48},{48,56},{56,64},{64,7... | collective-permute-start | bytes 16904 | tf_op jit(solution)/shard_map/ppermute | solution.py:28
  26.4 1.9 %collective-permute-start.3 = (bf16[3,64,352]{2,1,0:T(8,128)(2,1)S(1)}, bf16[3,64,352]{2,1,0:T(8,128)(2,1)S(1)}, u32[]{:S(2)}, u32[]{:S(2)}) collective-permute-start(bf16[3,64,352]{2,1,0:T(8,128)(2,1)S(1)} %get-tuple-element.38), channel_id=1, source_target_pairs={{0,128},{64,192},{128,256},{192,320},{256,384},{320,448},{384,512}... | collective-permute-start | bytes 405512 | tf_op jit(solution)/shard_map/ppermute | solution.py:22
  28.4 0.8 fusion.25.taps
  29.4 0.1 maximum_maximum_fusion
  29.5 1.5 broadcast_in_dim.79
  31.0 12.4 %all-to-all-start = ((bf16[16,264,256]{2,1,0:T(8,128)(2,1)}), bf16[16,264,256]{2,1,0:T(8,128)(2,1)}, u32[]{:S(2)}, u32[]{:S(2)}) async-start(bf16[16,264,256]{2,1,0:T(8,128)(2,1)} %broadcast_in_dim.79), calls=%async_computation | async-start | bytes 4325376 | tf_op jit(solution)/shard_map/all_to_all | solution.py:37
  43.5 0.1 select_bitcast_fusion.5
  43.6 1.9 %collective-permute-start.6 = (bf16[4,64,352]{2,1,0:T(8,128)(2,1)S(1)}, bf16[4,64,352]{2,1,0:T(8,128)(2,1)S(1)}, u32[]{:S(2)}, u32[]{:S(2)}) collective-permute-start(bf16[4,64,352]{2,1,0:T(8,128)(2,1)S(1)} %fusion.26), channel_id=1, source_target_pairs={{0,56},{8,0},{16,8},{24,16},{32,24},{40,32},{48,40},{56,48},{1,57}... | collective-permute-start | bytes 540680 | tf_op jit(solution)/shard_map/ppermute | solution.py:22
  45.7 3.4 %collective-permute-start.5 = (bf16[4,64,352]{2,1,0:T(8,128)(2,1)S(1)}, bf16[4,64,352]{2,1,0:T(8,128)(2,1)S(1)}, u32[]{:S(2)}, u32[]{:S(2)}) collective-permute-start(bf16[4,64,352]{2,1,0:T(8,128)(2,1)S(1)} %fusion.26), channel_id=1, source_target_pairs={{0,8},{8,16},{16,24},{24,32},{32,40},{40,48},{48,56},{56,0},{1,9},... | collective-permute-start | bytes 540680 | tf_op jit(solution)/shard_map/ppermute | solution.py:22
  49.1 2.8 %collective-permute-done.6 = bf16[4,64,352]{2,1,0:T(8,128)(2,1)S(1)} collective-permute-done((bf16[4,64,352]{2,1,0:T(8,128)(2,1)S(1)}, bf16[4,64,352]{2,1,0:T(8,128)(2,1)S(1)}, u32[]{:S(2)}, u32[]{:S(2)}) %collective-permute-start.6) | collective-permute-done | bytes 180256 | tf_op jit(solution)/shard_map/ppermute | solution.py:22
  52.0 3.2 %collective-permute-done.5 = bf16[4,64,352]{2,1,0:T(8,128)(2,1)S(1)} collective-permute-done((bf16[4,64,352]{2,1,0:T(8,128)(2,1)S(1)}, bf16[4,64,352]{2,1,0:T(8,128)(2,1)S(1)}, u32[]{:S(2)}, u32[]{:S(2)}) %collective-permute-start.5) | collective-permute-done | bytes 180256 | tf_op jit(solution)/shard_map/ppermute | solution.py:22
  55.2 0.2 fusion.7
  55.4 1.9 %collective-permute-start.7 = (bf16[12,64,352]{2,1,0:T(8,128)(2,1)S(1)}, bf16[12,64,352]{2,1,0:T(8,128)(2,1)S(1)}, u32[]{:S(2)}, u32[]{:S(2)}) collective-permute-start(bf16[12,64,352]{2,1,0:T(8,128)(2,1)S(1)} %get-tuple-element.32), channel_id=1, source_target_pairs={{0,8},{8,16},{16,24},{24,32},{32,40},{40,48},{48,56},{56,0},{1,9},... | collective-permute-start | bytes 1622024 | tf_op jit(solution)/shard_map/ppermute | solution.py:22
  57.3 4.6 %collective-permute-start.8 = (bf16[12,64,352]{2,1,0:T(8,128)(2,1)S(1)}, bf16[12,64,352]{2,1,0:T(8,128)(2,1)S(1)}, u32[]{:S(2)}, u32[]{:S(2)}) collective-permute-start(bf16[12,64,352]{2,1,0:T(8,128)(2,1)S(1)} %get-tuple-element.31), channel_id=1, source_target_pairs={{0,56},{8,0},{16,8},{24,16},{32,24},{40,32},{48,40},{56,48},{1,57}... | collective-permute-start | bytes 1622024 | tf_op jit(solution)/shard_map/ppermute | solution.py:22
  61.9 0.2 broadcast_select_fusion
  62.1 3.0 %collective-permute-start.13 = (bf16[520,352]{1,0:T(8,128)(2,1)S(1)}, bf16[520,352]{1,0:T(8,128)(2,1)S(1)}, u32[]{:S(2)}, u32[]{:S(2)}) collective-permute-start(bf16[520,352]{1,0:T(8,128)(2,1)S(1)} %get-tuple-element.25), channel_id=1, source_target_pairs={{0,64},{64,0},{1,65},{65,1},{2,66},{66,2},{3,67},{67,3},{4,68},{68... | collective-permute-start | bytes 1098248 | tf_op jit(solution)/shard_map/ppermute | solution.py:32
  65.1 0.2 broadcast_in_dim.80
  65.4 7.1 %collective-permute-done.7 = bf16[12,64,352]{2,1,0:T(8,128)(2,1)S(1)} collective-permute-done((bf16[12,64,352]{2,1,0:T(8,128)(2,1)S(1)}, bf16[12,64,352]{2,1,0:T(8,128)(2,1)S(1)}, u32[]{:S(2)}, u32[]{:S(2)}) %collective-permute-start.7) | collective-permute-done | bytes 540704 | tf_op jit(solution)/shard_map/ppermute | solution.py:22
  72.5 1.9 %collective-permute-start.9 = (bf16[12,64,352]{2,1,0:T(8,128)(2,1)S(1)}, bf16[12,64,352]{2,1,0:T(8,128)(2,1)S(1)}, u32[]{:S(2)}, u32[]{:S(2)}) collective-permute-start(bf16[12,64,352]{2,1,0:T(8,128)(2,1)S(1)} %collective-permute-done.7), channel_id=1, source_target_pairs={{0,8},{8,16},{16,24},{24,32},{32,40},{40,48},{48,56},{56,0},{1,9},... | collective-permute-start | bytes 1622024 | tf_op jit(solution)/shard_map/ppermute | solution.py:22
  74.5 4.6 %collective-permute-start.10 = (bf16[12,64,352]{2,1,0:T(8,128)(2,1)S(1)}, bf16[12,64,352]{2,1,0:T(8,128)(2,1)S(1)}, u32[]{:S(2)}, u32[]{:S(2)}) collective-permute-start(bf16[12,64,352]{2,1,0:T(8,128)(2,1)S(1)} %collective-permute-done.8), channel_id=1, source_target_pairs={{0,56},{8,0},{16,8},{24,16},{32,24},{40,32},{48,40},{56,48},{1,57}... | collective-permute-start | bytes 1622024 | tf_op jit(solution)/shard_map/ppermute | solution.py:22
  79.2 0.5 broadcast_in_dim.90
  79.9 9.0 %collective-permute-done.9 = bf16[12,64,352]{2,1,0:T(8,128)(2,1)S(1)} collective-permute-done((bf16[12,64,352]{2,1,0:T(8,128)(2,1)S(1)}, bf16[12,64,352]{2,1,0:T(8,128)(2,1)S(1)}, u32[]{:S(2)}, u32[]{:S(2)}) %collective-permute-start.9) | collective-permute-done | bytes 540704 | tf_op jit(solution)/shard_map/ppermute | solution.py:22
  88.9 1.9 %collective-permute-start.11 = (bf16[10,64,352]{2,1,0:T(8,128)(2,1)S(1)}, bf16[10,64,352]{2,1,0:T(8,128)(2,1)S(1)}, u32[]{:S(2)}, u32[]{:S(2)}) collective-permute-start(bf16[10,64,352]{2,1,0:T(8,128)(2,1)S(1)} %slice.201), channel_id=1, source_target_pairs={{0,8},{8,16},{16,24},{24,32},{32,40},{40,48},{48,56},{56,0},{1,9},... | collective-permute-start | bytes 1351688 | tf_op jit(solution)/shard_map/ppermute | solution.py:22
  90.9 4.6 %collective-permute-start.12 = (bf16[10,64,352]{2,1,0:T(8,128)(2,1)S(1)}, bf16[10,64,352]{2,1,0:T(8,128)(2,1)S(1)}, u32[]{:S(2)}, u32[]{:S(2)}) collective-permute-start(bf16[10,64,352]{2,1,0:T(8,128)(2,1)S(1)} %slice.203), channel_id=1, source_target_pairs={{0,56},{8,0},{16,8},{24,16},{32,24},{40,32},{48,40},{56,48},{1,57}... | collective-permute-start | bytes 1351688 | tf_op jit(solution)/shard_map/ppermute | solution.py:22
  95.6 0.2 maximum_convert_fusion
  95.8 0.1 fusion.28
  96.0 1.0 pad.22.linear
  97.0 0.7 fusion.27
  97.7 1.0 pad.20.slope
  98.7 0.9 pad.21.value
  99.9 2.4 %collective-permute-done.11 = bf16[10,64,352]{2,1,0:T(8,128)(2,1)S(1)} collective-permute-done((bf16[10,64,352]{2,1,0:T(8,128)(2,1)S(1)}, bf16[10,64,352]{2,1,0:T(8,128)(2,1)S(1)}, u32[]{:S(2)}, u32[]{:S(2)}) %collective-permute-start.11) | collective-permute-done | bytes 450592 | tf_op jit(solution)/shard_map/ppermute | solution.py:22
  102.3 1.9 %collective-permute-start.14 = (bf16[4,64,352]{2,1,0:T(8,128)(2,1)S(1)}, bf16[4,64,352]{2,1,0:T(8,128)(2,1)S(1)}, u32[]{:S(2)}, u32[]{:S(2)}) collective-permute-start(bf16[4,64,352]{2,1,0:T(8,128)(2,1)S(1)} %slice.219), channel_id=1, source_target_pairs={{0,8},{8,16},{16,24},{24,32},{32,40},{40,48},{48,56},{56,0},{1,9},... | collective-permute-start | bytes 540680 | tf_op jit(solution)/shard_map/ppermute | solution.py:22
  104.3 0.7 slice.220
  105.0 4.6 %collective-permute-start.15 = (bf16[4,64,352]{2,1,0:T(8,128)(2,1)}, bf16[4,64,352]{2,1,0:T(8,128)(2,1)S(1)}, u32[]{:S(2)}, u32[]{:S(2)}) collective-permute-start(bf16[4,64,352]{2,1,0:T(8,128)(2,1)} %slice.220), channel_id=1, source_target_pairs={{0,56},{8,0},{16,8},{24,16},{32,24},{40,32},{48,40},{56,48},{1,57}... | collective-permute-start | bytes 540680 | tf_op jit(solution)/shard_map/ppermute | solution.py:22
  109.8 1.2 copy-done.1
  111.0 5.2 %shard_map.86 = (bf16[2,256,352]{2,1,0:T(8,128)(2,1)}, bf16[2,256,352]{2,1,0:T(8,128)(2,1)}, f32[3,352]{1,0:T(4,128)}) custom-call(bf16[16,264,256]{2,1,0:T(8,128)(2,1)} %all-to-all-done.grads, bf16[1,2048,352]{2,1,0:T(8,128)(2,1)} %bitcast.137, f32[2,264,352]{2,1,0:T(8,128)} %pad.20.slope, f32[2,264,352]{2,1,0:T(8,128)} %pad.21.value, ...), custom_call_target="tpu_custom_call" | custom-call | tf_op jit(solution)/shard_map/pallas_call | solution.py:142
  116.2 1.3 broadcast_in_dim.98
  117.5 5.0 %all-to-all-start.2 = ((f32[12,3,352]{2,1,0:T(4,128)}), f32[12,3,352]{2,1,0:T(4,128)S(1)}, u32[]{:S(2)}, u32[]{:S(2)}) async-start(f32[12,3,352]{2,1,0:T(4,128)} %broadcast_in_dim.98), calls=%async_computation.2 | async-start | bytes 147456 | tf_op jit(solution)/shard_map/all_to_all | solution.py:37
  122.6 1.6 copy-done
  124.2 5.8 %shard_map.87 = bf16[2,8,256,256]{3,2,1,0:T(8,128)(2,1)} custom-call(bf16[2,256,352]{2,1,0:T(8,128)(2,1)} %get-tuple-element.9.linear_grad, bf16[2,256,352]{2,1,0:T(8,128)(2,1)} %get-tuple-element.10.up_grad, bf16[2,2048,352]{2,1,0:T(8,128)(2,1)} %bitcast.134, bf16[2,2048,352]{2,1,0:T(8,128)(2,1)} %bitcast.135), custom_call_target="tpu_custom_call" | custom-call | tf_op jit(solution)/shard_map/pallas_call | solution.py:181
  130.0 2.2 %all-to-all-done.2 = f32[12,3,352]{2,1,0:T(4,128)S(1)} async-done(((f32[12,3,352]{2,1,0:T(4,128)}), f32[12,3,352]{2,1,0:T(4,128)S(1)}, u32[]{:S(2)}, u32[]{:S(2)}) %all-to-all-start.2) | async-done | bytes 50720 | tf_op jit(solution)/shard_map/all_to_all | solution.py:37
  132.3 9.6 %all-to-all-start.1 = ((bf16[16,256,256]{2,1,0:T(8,128)(2,1)}), bf16[16,256,256]{2,1,0:T(8,128)(2,1)S(1)}, u32[]{:S(2)}, u32[]{:S(2)}) async-start(bf16[16,256,256]{2,1,0:T(8,128)(2,1)} %bitcast.136), calls=%async_computation.1 | async-start | bytes 4194304 | tf_op jit(solution)/shard_map/all_to_all | solution.py:246
  142.0 1.9 %collective-permute-start.16 = (f32[3,704]{1,0:T(4,128)S(1)}, f32[3,704]{1,0:T(4,128)S(1)}, u32[]{:S(2)}, u32[]{:S(2)}) collective-permute-start(f32[3,704]{1,0:T(4,128)S(1)} %reshape.37), channel_id=1, source_target_pairs={{0,8},{8,0},{16,24},{24,16},{32,40},{40,32},{48,56},{56,48},{1,9},... | collective-permute-start | bytes 25352 | tf_op jit(solution)/shard_map/ppermute | solution.py:32
  143.9 2.8 %collective-permute-done.16 = f32[3,704]{1,0:T(4,128)S(1)} collective-permute-done((f32[3,704]{1,0:T(4,128)S(1)}, f32[3,704]{1,0:T(4,128)S(1)}, u32[]{:S(2)}, u32[]{:S(2)}) %collective-permute-start.16) | collective-permute-done | bytes 8480 | tf_op jit(solution)/shard_map/ppermute | solution.py:32
  146.7 1.9 %collective-permute-start.17 = (f32[3,704]{1,0:T(4,128)S(1)}, f32[3,704]{1,0:T(4,128)S(1)}, u32[]{:S(2)}, u32[]{:S(2)}) collective-permute-start(f32[3,704]{1,0:T(4,128)S(1)} %add.184), channel_id=1, source_target_pairs={{0,16},{8,24},{16,0},{24,8},{32,48},{40,56},{48,32},{56,40},{1,17}... | collective-permute-start | bytes 25352 | tf_op jit(solution)/shard_map/ppermute | solution.py:32
  148.6 3.7 %collective-permute-done.17 = f32[3,704]{1,0:T(4,128)S(1)} collective-permute-done((f32[3,704]{1,0:T(4,128)S(1)}, f32[3,704]{1,0:T(4,128)S(1)}, u32[]{:S(2)}, u32[]{:S(2)}) %collective-permute-start.17) | collective-permute-done | bytes 8480 | tf_op jit(solution)/shard_map/ppermute | solution.py:32
  152.3 3.7 %collective-permute-start.18 = (f32[3,704]{1,0:T(4,128)S(1)}, f32[3,704]{1,0:T(4,128)S(1)}, u32[]{:S(2)}, u32[]{:S(2)}) collective-permute-start(f32[3,704]{1,0:T(4,128)S(1)} %add.185), channel_id=1, source_target_pairs={{0,32},{8,40},{16,48},{24,56},{32,0},{40,8},{48,16},{56,24},{1,33}... | collective-permute-start | bytes 25352 | tf_op jit(solution)/shard_map/ppermute | solution.py:32
  156.0 4.7 %collective-permute-done.18 = f32[3,704]{1,0:T(4,128)S(1)} collective-permute-done((f32[3,704]{1,0:T(4,128)S(1)}, f32[3,704]{1,0:T(4,128)S(1)}, u32[]{:S(2)}, u32[]{:S(2)}) %collective-permute-start.18) | collective-permute-done | bytes 8480 | tf_op jit(solution)/shard_map/ppermute | solution.py:32
  160.7 5.0 %collective-permute-start.19 = (f32[1,3,704]{2,1,0:T(4,128)S(1)}, f32[1,3,704]{2,1,0:T(4,128)S(1)}, u32[]{:S(2)}, u32[]{:S(2)}) collective-permute-start(f32[1,3,704]{2,1,0:T(4,128)S(1)} %add_bitcast_fusion), channel_id=1, source_target_pairs={{0,1},{1,0},{2,3},{3,2},{4,5},{5,4},{6,7},{7,6},{8,9},{9,8},{10,11... | collective-permute-start | bytes 25352 | tf_op jit(solution)/shard_map/ppermute | solution.py:32
  165.7 0.8 collective-permute-done.19
  166.5 3.4 %collective-permute-start.20 = (f32[2,3,704]{2,1,0:T(4,128)S(1)}, f32[2,3,704]{2,1,0:T(4,128)S(1)}, u32[]{:S(2)}, u32[]{:S(2)}) collective-permute-start(f32[2,3,704]{2,1,0:T(4,128)S(1)} %pad_maximum_fusion.10), channel_id=1, source_target_pairs={{0,2},{2,0},{4,6},{6,4},{1,3},{3,1},{5,7},{7,5},{8,10},{10,8},{12,... | collective-permute-start | bytes 50696 | tf_op jit(solution)/shard_map/ppermute | solution.py:32
  169.9 1.6 collective-permute-done.20
  171.6 4.5 %collective-permute-start.21 = (f32[4,3,704]{2,1,0:T(4,128)S(1)}, f32[4,3,704]{2,1,0:T(4,128)S(1)}, u32[]{:S(2)}, u32[]{:S(2)}) collective-permute-start(f32[4,3,704]{2,1,0:T(4,128)S(1)} %pad_maximum_fusion.9), channel_id=1, source_target_pairs={{0,4},{2,6},{4,0},{6,2},{1,5},{3,7},{5,1},{7,3},{8,12},{10,14},{12... | collective-permute-start | bytes 101384 | tf_op jit(solution)/shard_map/ppermute | solution.py:32
  176.1 1.9 %collective-permute-done.21 = f32[4,3,704]{2,1,0:T(4,128)S(1)} collective-permute-done((f32[4,3,704]{2,1,0:T(4,128)S(1)}, f32[4,3,704]{2,1,0:T(4,128)S(1)}, u32[]{:S(2)}, u32[]{:S(2)}) %collective-permute-start.21) | collective-permute-done | bytes 33824 | tf_op jit(solution)/shard_map/ppermute | solution.py:32
  178.0 0.7 reshape.38
  178.8 1.0 reduce_sum.21
  (73 shorter events, 1.8 us)
Async XLA Ops:
  0.6 28.8 %copy-start.3 = (bf16[256,256]{1,0:T(8,128)(2,1)S(1)}, bf16[256,256]{1,0:T(8,128)(2,1)}, u32[]{:S(2)}) copy-start(bf16[256,256]{1,0:T(8,128)(2,1)} %param.7) | copy-start | bytes 393220
  0.6 20.2 %copy-start.2 = (bf16[256,704]{0,1:T(8,128)(2,1)S(1)}, bf16[256,704]{0,1:T(8,128)(2,1)}, u32[]{:S(2)}) copy-start(bf16[256,704]{0,1:T(8,128)(2,1)} %param.8) | copy-start | bytes 1081348
  1.9 41.6 %collective-permute-start.4 = (bf16[3,64,352]{2,1,0:T(8,128)(2,1)S(1)}, bf16[3,64,352]{2,1,0:T(8,128)(2,1)S(1)}, u32[]{:S(2)}, u32[]{:S(2)}) collective-permute-start(bf16[3,64,352]{2,1,0:T(8,128)(2,1)S(1)} %get-tuple-element.37), channel_id=1, source_target_pairs={{0,64},{64,128},{128,192},{192,256},{256,320},{320,384},{384,448},... | collective-permute-start | bytes 405512 | tf_op jit(solution)/shard_map/ppermute | solution.py:22
  6.7 36.8 %collective-permute-start.2 = (bf16[3,64,352]{2,1,0:T(8,128)(2,1)S(1)}, bf16[3,64,352]{2,1,0:T(8,128)(2,1)S(1)}, u32[]{:S(2)}, u32[]{:S(2)}) collective-permute-start(bf16[3,64,352]{2,1,0:T(8,128)(2,1)S(1)} %get-tuple-element.37), channel_id=1, source_target_pairs={{0,704},{64,0},{128,64},{192,128},{256,192},{320,256},{384,320},{4... | collective-permute-start | bytes 405512 | tf_op jit(solution)/shard_map/ppermute | solution.py:22
  21.0 8.3 %collective-permute-start.1 = (bf16[4,704]{1,0:T(4,128)(2,1)S(1)}, bf16[4,704]{1,0:T(4,128)(2,1)S(1)}, u32[]{:S(2)}, u32[]{:S(2)}) collective-permute-start(bf16[4,704]{1,0:T(4,128)(2,1)S(1)} %fusion.24), channel_id=1, source_target_pairs={{8,0},{16,8},{24,16},{32,24},{40,32},{48,40},{56,48},{64,56},{72,6... | collective-permute-start | bytes 16904 | tf_op jit(solution)/shard_map/ppermute | solution.py:28
  22.4 7.0 %collective-permute-start = (bf16[4,704]{1,0:T(4,128)(2,1)S(1)}, bf16[4,704]{1,0:T(4,128)(2,1)S(1)}, u32[]{:S(2)}, u32[]{:S(2)}) collective-permute-start(bf16[4,704]{1,0:T(4,128)(2,1)S(1)} %fusion.23), channel_id=1, source_target_pairs={{0,8},{8,16},{16,24},{24,32},{32,40},{40,48},{48,56},{56,64},{64,7... | collective-permute-start | bytes 16904 | tf_op jit(solution)/shard_map/ppermute | solution.py:28
  26.4 17.1 %collective-permute-start.3 = (bf16[3,64,352]{2,1,0:T(8,128)(2,1)S(1)}, bf16[3,64,352]{2,1,0:T(8,128)(2,1)S(1)}, u32[]{:S(2)}, u32[]{:S(2)}) collective-permute-start(bf16[3,64,352]{2,1,0:T(8,128)(2,1)S(1)} %get-tuple-element.38), channel_id=1, source_target_pairs={{0,128},{64,192},{128,256},{192,320},{256,384},{320,448},{384,512}... | collective-permute-start | bytes 405512 | tf_op jit(solution)/shard_map/ppermute | solution.py:22
  29.2 1.8 %copy-start.4 = (f32[3,352]{1,0:T(4,128)}, f32[3,352]{1,0:T(4,128)S(1)}, u32[]{:S(2)}) copy-start(f32[3,352]{1,0:T(4,128)S(1)} %fusion.25.taps) | copy-start | bytes 12676
  31.0 79.9 %all-to-all-start = ((bf16[16,264,256]{2,1,0:T(8,128)(2,1)}), bf16[16,264,256]{2,1,0:T(8,128)(2,1)}, u32[]{:S(2)}, u32[]{:S(2)}) async-start(bf16[16,264,256]{2,1,0:T(8,128)(2,1)} %broadcast_in_dim.79), calls=%async_computation | async-start | bytes 4325376 | tf_op jit(solution)/shard_map/all_to_all | solution.py:37
  43.6 8.3 %collective-permute-start.6 = (bf16[4,64,352]{2,1,0:T(8,128)(2,1)S(1)}, bf16[4,64,352]{2,1,0:T(8,128)(2,1)S(1)}, u32[]{:S(2)}, u32[]{:S(2)}) collective-permute-start(bf16[4,64,352]{2,1,0:T(8,128)(2,1)S(1)} %fusion.26), channel_id=1, source_target_pairs={{0,56},{8,0},{16,8},{24,16},{32,24},{40,32},{48,40},{56,48},{1,57}... | collective-permute-start | bytes 540680 | tf_op jit(solution)/shard_map/ppermute | solution.py:22
  45.7 9.5 %collective-permute-start.5 = (bf16[4,64,352]{2,1,0:T(8,128)(2,1)S(1)}, bf16[4,64,352]{2,1,0:T(8,128)(2,1)S(1)}, u32[]{:S(2)}, u32[]{:S(2)}) collective-permute-start(bf16[4,64,352]{2,1,0:T(8,128)(2,1)S(1)} %fusion.26), channel_id=1, source_target_pairs={{0,8},{8,16},{16,24},{24,32},{32,40},{40,48},{48,56},{56,0},{1,9},... | collective-permute-start | bytes 540680 | tf_op jit(solution)/shard_map/ppermute | solution.py:22
  55.4 17.2 %collective-permute-start.7 = (bf16[12,64,352]{2,1,0:T(8,128)(2,1)S(1)}, bf16[12,64,352]{2,1,0:T(8,128)(2,1)S(1)}, u32[]{:S(2)}, u32[]{:S(2)}) collective-permute-start(bf16[12,64,352]{2,1,0:T(8,128)(2,1)S(1)} %get-tuple-element.32), channel_id=1, source_target_pairs={{0,8},{8,16},{16,24},{24,32},{32,40},{40,48},{48,56},{56,0},{1,9},... | collective-permute-start | bytes 1622024 | tf_op jit(solution)/shard_map/ppermute | solution.py:22
  57.3 17.2 %collective-permute-start.8 = (bf16[12,64,352]{2,1,0:T(8,128)(2,1)S(1)}, bf16[12,64,352]{2,1,0:T(8,128)(2,1)S(1)}, u32[]{:S(2)}, u32[]{:S(2)}) collective-permute-start(bf16[12,64,352]{2,1,0:T(8,128)(2,1)S(1)} %get-tuple-element.31), channel_id=1, source_target_pairs={{0,56},{8,0},{16,8},{24,16},{32,24},{40,32},{48,40},{56,48},{1,57}... | collective-permute-start | bytes 1622024 | tf_op jit(solution)/shard_map/ppermute | solution.py:22
  62.1 33.5 %collective-permute-start.13 = (bf16[520,352]{1,0:T(8,128)(2,1)S(1)}, bf16[520,352]{1,0:T(8,128)(2,1)S(1)}, u32[]{:S(2)}, u32[]{:S(2)}) collective-permute-start(bf16[520,352]{1,0:T(8,128)(2,1)S(1)} %get-tuple-element.25), channel_id=1, source_target_pairs={{0,64},{64,0},{1,65},{65,1},{2,66},{66,2},{3,67},{67,3},{4,68},{68... | collective-permute-start | bytes 1098248 | tf_op jit(solution)/shard_map/ppermute | solution.py:32
  72.5 16.3 %collective-permute-start.9 = (bf16[12,64,352]{2,1,0:T(8,128)(2,1)S(1)}, bf16[12,64,352]{2,1,0:T(8,128)(2,1)S(1)}, u32[]{:S(2)}, u32[]{:S(2)}) collective-permute-start(bf16[12,64,352]{2,1,0:T(8,128)(2,1)S(1)} %collective-permute-done.7), channel_id=1, source_target_pairs={{0,8},{8,16},{16,24},{24,32},{32,40},{40,48},{48,56},{56,0},{1,9},... | collective-permute-start | bytes 1622024 | tf_op jit(solution)/shard_map/ppermute | solution.py:22
  74.5 16.3 %collective-permute-start.10 = (bf16[12,64,352]{2,1,0:T(8,128)(2,1)S(1)}, bf16[12,64,352]{2,1,0:T(8,128)(2,1)S(1)}, u32[]{:S(2)}, u32[]{:S(2)}) collective-permute-start(bf16[12,64,352]{2,1,0:T(8,128)(2,1)S(1)} %collective-permute-done.8), channel_id=1, source_target_pairs={{0,56},{8,0},{16,8},{24,16},{32,24},{40,32},{48,40},{56,48},{1,57}... | collective-permute-start | bytes 1622024 | tf_op jit(solution)/shard_map/ppermute | solution.py:22
  88.9 13.4 %collective-permute-start.11 = (bf16[10,64,352]{2,1,0:T(8,128)(2,1)S(1)}, bf16[10,64,352]{2,1,0:T(8,128)(2,1)S(1)}, u32[]{:S(2)}, u32[]{:S(2)}) collective-permute-start(bf16[10,64,352]{2,1,0:T(8,128)(2,1)S(1)} %slice.201), channel_id=1, source_target_pairs={{0,8},{8,16},{16,24},{24,32},{32,40},{40,48},{48,56},{56,0},{1,9},... | collective-permute-start | bytes 1351688 | tf_op jit(solution)/shard_map/ppermute | solution.py:22
  90.9 13.3 %collective-permute-start.12 = (bf16[10,64,352]{2,1,0:T(8,128)(2,1)S(1)}, bf16[10,64,352]{2,1,0:T(8,128)(2,1)S(1)}, u32[]{:S(2)}, u32[]{:S(2)}) collective-permute-start(bf16[10,64,352]{2,1,0:T(8,128)(2,1)S(1)} %slice.203), channel_id=1, source_target_pairs={{0,56},{8,0},{16,8},{24,16},{32,24},{40,32},{48,40},{56,48},{1,57}... | collective-permute-start | bytes 1351688 | tf_op jit(solution)/shard_map/ppermute | solution.py:22
  102.3 8.6 %collective-permute-start.14 = (bf16[4,64,352]{2,1,0:T(8,128)(2,1)S(1)}, bf16[4,64,352]{2,1,0:T(8,128)(2,1)S(1)}, u32[]{:S(2)}, u32[]{:S(2)}) collective-permute-start(bf16[4,64,352]{2,1,0:T(8,128)(2,1)S(1)} %slice.219), channel_id=1, source_target_pairs={{0,8},{8,16},{16,24},{24,32},{32,40},{40,48},{48,56},{56,0},{1,9},... | collective-permute-start | bytes 540680 | tf_op jit(solution)/shard_map/ppermute | solution.py:22
  105.0 17.6 %collective-permute-start.15 = (bf16[4,64,352]{2,1,0:T(8,128)(2,1)}, bf16[4,64,352]{2,1,0:T(8,128)(2,1)S(1)}, u32[]{:S(2)}, u32[]{:S(2)}) collective-permute-start(bf16[4,64,352]{2,1,0:T(8,128)(2,1)} %slice.220), channel_id=1, source_target_pairs={{0,56},{8,0},{16,8},{24,16},{32,24},{40,32},{48,40},{56,48},{1,57}... | collective-permute-start | bytes 540680 | tf_op jit(solution)/shard_map/ppermute | solution.py:22
  109.7 1.2 copy-start.1
  117.5 14.8 %all-to-all-start.2 = ((f32[12,3,352]{2,1,0:T(4,128)}), f32[12,3,352]{2,1,0:T(4,128)S(1)}, u32[]{:S(2)}, u32[]{:S(2)}) async-start(f32[12,3,352]{2,1,0:T(4,128)} %broadcast_in_dim.98), calls=%async_computation.2 | async-start | bytes 147456 | tf_op jit(solution)/shard_map/all_to_all | solution.py:37
  122.6 1.6 copy-start
  132.3 46.5 %all-to-all-start.1 = ((bf16[16,256,256]{2,1,0:T(8,128)(2,1)}), bf16[16,256,256]{2,1,0:T(8,128)(2,1)S(1)}, u32[]{:S(2)}, u32[]{:S(2)}) async-start(bf16[16,256,256]{2,1,0:T(8,128)(2,1)} %bitcast.136), calls=%async_computation.1 | async-start | bytes 4194304 | tf_op jit(solution)/shard_map/all_to_all | solution.py:246
  142.0 4.7 %collective-permute-start.16 = (f32[3,704]{1,0:T(4,128)S(1)}, f32[3,704]{1,0:T(4,128)S(1)}, u32[]{:S(2)}, u32[]{:S(2)}) collective-permute-start(f32[3,704]{1,0:T(4,128)S(1)} %reshape.37), channel_id=1, source_target_pairs={{0,8},{8,0},{16,24},{24,16},{32,40},{40,32},{48,56},{56,48},{1,9},... | collective-permute-start | bytes 25352 | tf_op jit(solution)/shard_map/ppermute | solution.py:32
  146.7 5.6 %collective-permute-start.17 = (f32[3,704]{1,0:T(4,128)S(1)}, f32[3,704]{1,0:T(4,128)S(1)}, u32[]{:S(2)}, u32[]{:S(2)}) collective-permute-start(f32[3,704]{1,0:T(4,128)S(1)} %add.184), channel_id=1, source_target_pairs={{0,16},{8,24},{16,0},{24,8},{32,48},{40,56},{48,32},{56,40},{1,17}... | collective-permute-start | bytes 25352 | tf_op jit(solution)/shard_map/ppermute | solution.py:32
  152.3 8.3 %collective-permute-start.18 = (f32[3,704]{1,0:T(4,128)S(1)}, f32[3,704]{1,0:T(4,128)S(1)}, u32[]{:S(2)}, u32[]{:S(2)}) collective-permute-start(f32[3,704]{1,0:T(4,128)S(1)} %add.185), channel_id=1, source_target_pairs={{0,32},{8,40},{16,48},{24,56},{32,0},{40,8},{48,16},{56,24},{1,33}... | collective-permute-start | bytes 25352 | tf_op jit(solution)/shard_map/ppermute | solution.py:32
  160.7 5.8 %collective-permute-start.19 = (f32[1,3,704]{2,1,0:T(4,128)S(1)}, f32[1,3,704]{2,1,0:T(4,128)S(1)}, u32[]{:S(2)}, u32[]{:S(2)}) collective-permute-start(f32[1,3,704]{2,1,0:T(4,128)S(1)} %add_bitcast_fusion), channel_id=1, source_target_pairs={{0,1},{1,0},{2,3},{3,2},{4,5},{5,4},{6,7},{7,6},{8,9},{9,8},{10,11... | collective-permute-start | bytes 25352 | tf_op jit(solution)/shard_map/ppermute | solution.py:32
  166.5 5.1 %collective-permute-start.20 = (f32[2,3,704]{2,1,0:T(4,128)S(1)}, f32[2,3,704]{2,1,0:T(4,128)S(1)}, u32[]{:S(2)}, u32[]{:S(2)}) collective-permute-start(f32[2,3,704]{2,1,0:T(4,128)S(1)} %pad_maximum_fusion.10), channel_id=1, source_target_pairs={{0,2},{2,0},{4,6},{6,4},{1,3},{3,1},{5,7},{7,5},{8,10},{10,8},{12,... | collective-permute-start | bytes 50696 | tf_op jit(solution)/shard_map/ppermute | solution.py:32
  171.6 6.3 %collective-permute-start.21 = (f32[4,3,704]{2,1,0:T(4,128)S(1)}, f32[4,3,704]{2,1,0:T(4,128)S(1)}, u32[]{:S(2)}, u32[]{:S(2)}) collective-permute-start(f32[4,3,704]{2,1,0:T(4,128)S(1)} %pad_maximum_fusion.9), channel_id=1, source_target_pairs={{0,4},{2,6},{4,0},{6,2},{1,5},{3,7},{5,1},{7,3},{8,12},{10,14},{12... | collective-permute-start | bytes 101384 | tf_op jit(solution)/shard_map/ppermute | solution.py:32

commit v4 on v2

--- a/solution.py
+++ b/solution.py
@@ -15,6 +15,7 @@
 GROUP = ("zp", "x", "core")
 ROWS = ("rep", "zk", "zp", "y")
 PAD = 264
+PIECES = 9
 
 
 def shifted(value, axis, by):
@@ -45,36 +46,37 @@
     return jnp.where(second, right, left), jnp.where(second, left, right)
 
 
+def crossed(value, axis, by):
+    names = axis if isinstance(axis, tuple) else (axis,)
+    count = lax.axis_size(names)
+    pairs = [
+        (2 * i + core, 2 * ((i + step) % count) + core)
+        for i in range(count)
+        for core, step in enumerate((by, -by))
+    ]
+    return lax.ppermute(value, (*names, "core"), pairs)
+
+
 def gathered_z(own, other):
-    relative = [own, shifted(other, Z_ALL, -1), shifted(own, Z_ALL, 2), shifted(other, Z_ALL, 1)]
+    relative = [own, shifted(other, Z_ALL, -1), crossed(own, Z_ALL, 2), shifted(other, Z_ALL, 1)]
     count = len(relative)
     at = lax.axis_index(("zk", "zp"))
-    return jnp.stack(
-        [lax.select_n((place - at) % count, *relative) for place in range(count)], axis=1
-    )
+    return jnp.stack([lax.select_n((place - at) % count, *relative) for place in range(count)])
 
 
 def gathered_y(block):
-    half = block.shape[1] // 2
-    pieces = {0: block}
-    up = down = block
+    mid = block.shape[0] // 2
+    pieces, steps = [block], [0]
+    one = two = block
     for k in range(1, 4):
-        up = shifted(up, "y", 1)
-        down = shifted(down, "y", -1)
-        pieces[-k], pieces[k] = up, down
-    ends = [(0, shifted(up[:, :half], "y", 1)), (half, shifted(down[:, half:], "y", -1))]
-    count, y_at = lax.axis_size("y"), lax.axis_index("y")
-    parts, z_count, share, columns = block.shape
-    base = -2
-    whole = jnp.broadcast_to(
-        pieces[base][:, :, None], (parts, z_count, count, share, columns)
-    )
-    placed = [(k, 0, piece) for k, piece in pieces.items() if k != base]
-    for k, first, piece in placed + [(4, first, piece) for first, piece in ends]:
-        whole = lax.dynamic_update_slice(
-            whole, piece[:, :, None], (0, first, (y_at + k) % count, 0, 0)
-        )
-    return whole.reshape(parts, -1, columns), pieces[3]
+        one, two = crossed(one, "y", 1), crossed(two, "y", -1)
+        pieces += [one, two]
+        steps += [-k, k]
+    pieces += [crossed(one[:mid], "y", 1), crossed(two[mid:], "y", -1)]
+    sign = 1 - 2 * lax.axis_index("core")
+    count = lax.axis_size("y")
+    places = (lax.axis_index("y") + sign * jnp.array(steps + [4, 4], jnp.int32)) % count
+    return pieces, places.astype(jnp.int32), one
 
 
 def gelu_parts(gate):
@@ -83,13 +85,30 @@
     return (gate * normal_cdf, normal_cdf + gate * density)
 
 
-def hidden_kernel(grads, down, slope, value, linear, taps, linear_out, up_out, conv_out):
+def hidden_kernel(places, *refs):
+    pieces, refs = refs[:PIECES], refs[PIECES:]
+    grads, slope, value, linear, taps, linear_out, up_out, conv_out, down = refs
     peers, padded, width = grads.shape
     rows = linear_out.shape[1]
+    z_count, y_count, share, half = down.shape
+    first = pl.program_id(0) == 0
+
+    @pl.when(first)
+    def _():
+        start = 0
+        for at, piece in enumerate(pieces):
+            depth = piece.shape[0]
+            down[start : start + depth, pl.ds(places[at], 1)] = piece[...]
+            start = (start + depth) % z_count
+
+    per_tp = width // share
     act = jnp.zeros(slope.shape[1:], jnp.float32)
     for t in range(peers):
+        z, y = divmod(t * per_tp, y_count)
         act += jnp.dot(
-            grads[t], down[0, t * width : (t + 1) * width], preferred_element_type=jnp.float32
+            grads[t],
+            down[z, y : y + per_tp].reshape(width, half),
+            preferred_element_type=jnp.float32,
         )
     grad = act * slope[0]
 
@@ -110,7 +129,6 @@
             for k in range(3)
         ]
     )
-    first = pl.program_id(0) == 0
 
     @pl.when(first)
     def _():
@@ -121,63 +139,92 @@
         conv_out[...] += sums
 
 
-def hidden_gradients(grads, weights, slope, value, linear, taps):
+def hidden_gradients(pieces, places, grads, slope, value, linear, taps):
     peers, padded, width = grads.shape
-    _, depth, half = weights.shape
+    z_count, _, share, half = pieces[0].shape
+    y_count = peers // 2 * width // share // z_count
     rows = width
-    saved = pl.BlockSpec((1, padded, half), lambda b: (b, 0, 0))
-    made = pl.BlockSpec((1, rows, half), lambda b: (b, 0, 0))
+    saved = pl.BlockSpec((1, padded, half), lambda b, at: (b, 0, 0))
+    made = pl.BlockSpec((1, rows, half), lambda b, at: (b, 0, 0))
+    small = pl.BlockSpec((3, half), lambda b, at: (0, 0))
     return pl.pallas_call(
         hidden_kernel,
-        grid=(2,),
-        in_specs=[
-            pl.BlockSpec((peers // 2, padded, width), lambda b: (b, 0, 0)),
-            pl.BlockSpec((1, depth, half), lambda b: (0, 0, 0)),
-            saved,
-            saved,
-            saved,
-            pl.BlockSpec((3, half), lambda b: (0, 0)),
-        ],
-        out_specs=[made, made, pl.BlockSpec((3, half), lambda b: (0, 0))],
+        grid_spec=pltpu.PrefetchScalarGridSpec(
+            num_scalar_prefetch=1,
+            grid=(2,),
+            in_specs=[
+                pl.BlockSpec((piece.shape[0], 1, share, half), lambda b, at: (0, 2, 0, 0))
+                for piece in pieces
+            ]
+            + [
+                pl.BlockSpec((peers // 2, padded, width), lambda b, at: (b, 0, 0)),
+                saved,
+                saved,
+                saved,
+                small,
+            ],
+            out_specs=[made, made, small],
+            scratch_shapes=[pltpu.VMEM((z_count, y_count, share, half), jnp.bfloat16)],
+        ),
         out_shape=[
             jax.ShapeDtypeStruct((2, rows, half), jnp.bfloat16),
             jax.ShapeDtypeStruct((2, rows, half), jnp.bfloat16),
             jax.ShapeDtypeStruct((3, half), jnp.float32),
         ],
-    )(grads, weights, slope, value, linear, taps)
-
-
-def output_kernel(linear_grad, up_grad, gate, up, out):
+    )(places, *pieces, grads, slope, value, linear, taps)
+
+
+def output_kernel(places, *refs):
+    pieces, (linear_grad, up_grad, out, both) = refs[:PIECES], refs[PIECES:]
+    _, _, share, half = both.shape
     width = out.shape[3]
+    per_tp = width // share
+    z = pl.program_id(0)
+    split = pl.num_programs(0) // 2
+
+    def place(at):
+        both[:, pl.ds(places[at], 1)] = pieces[at][0][:, None]
+
+    for at in range(PIECES - 2):
+        place(at)
+    pl.when(z < split)(lambda: place(PIECES - 2))
+    pl.when(z >= split)(lambda: place(PIECES - 1))
     contract = (((1,), (1,)), ((), ()))
     for t in range(out.shape[1]):
-        span = slice(t * width, (t + 1) * width)
+        gate, up = (
+            both[part, t * per_tp : (t + 1) * per_tp].reshape(width, half) for part in range(2)
+        )
         for b in range(2):
             part = lax.dot_general(
-                linear_grad[b], gate[0, span], contract, preferred_element_type=jnp.float32
+                linear_grad[b], gate, contract, preferred_element_type=jnp.float32
             ) + lax.dot_general(
-                up_grad[b], up[0, span], contract, preferred_element_type=jnp.float32
+                up_grad[b], up, contract, preferred_element_type=jnp.float32
             )
             out[b, t] = part.astype(jnp.bfloat16)
 
 
-def output_partials(linear_grad, up_grad, weights, width):
+def output_partials(pieces, places, linear_grad, up_grad, width):
     _, rows, half = linear_grad.shape
-    peers = weights.shape[1] // width
-    steps = 4
-    whole = pl.BlockSpec((2, rows, half), lambda i: (0, 0, 0))
+    z_count, _, share, _ = pieces[0].shape
+    mid = pieces[-1].shape[0]
+    y_count = 8
+    peers = z_count * y_count * share // width
+    whole = pl.BlockSpec((2, rows, half), lambda i, at: (0, 0, 0))
+    maps = [lambda i, at: (i, 0, 0, 0)] * (PIECES - 2) + [
+        lambda i, at: (jnp.minimum(i, mid - 1), 0, 0, 0),
+        lambda i, at: (jnp.maximum(i - mid, 0), 0, 0, 0),
+    ]
     product = pl.pallas_call(
         output_kernel,
-        grid=(steps,),
-        in_specs=[
-            whole,
-            whole,
-            pl.BlockSpec((1, weights.shape[1] // steps, half), lambda i: (1, i, 0)),
-            pl.BlockSpec((1, weights.shape[1] // steps, half), lambda i: (2, i, 0)),
-        ],
-        out_specs=pl.BlockSpec((2, peers // steps, rows, width), lambda i: (0, i, 0, 0)),
+        grid_spec=pltpu.PrefetchScalarGridSpec(
+            num_scalar_prefetch=1,
+            grid=(z_count,),
+            in_specs=[pl.BlockSpec((1, 2, share, half), m) for m in maps] + [whole, whole],
+            out_specs=pl.BlockSpec((2, peers // z_count, rows, width), lambda i, at: (0, i, 0, 0)),
+            scratch_shapes=[pltpu.VMEM((2, y_count, share, half), jnp.bfloat16)],
+        ),
         out_shape=jax.ShapeDtypeStruct((2, peers, rows, width), jnp.bfloat16),
-    )(linear_grad, up_grad, weights, weights)
+    )(places, *pieces, linear_grad, up_grad)
     return product.reshape(2 * peers, rows, width)
 
 
@@ -187,8 +234,8 @@
     half = columns // 2
     second = lax.axis_index("zp") == 1
 
-    own, other = halves_of(jnp.stack([down_weight.T, gate_weight, up_weight]), second)
-    weights, late = gathered_y(gathered_z(own, other))
+    own, other = halves_of(jnp.stack([gate_weight, up_weight, down_weight.T]), second)
+    pieces, places, late = gathered_y(gathered_z(own, other))
 
     spare = ((0, 0), (0, columns - width))
     last = jnp.concatenate([gate_lin[-2:], up_lin[-1:], jnp.pad(out_grad[-1:], spare)])
@@ -221,8 +268,9 @@
 
     tail = ((0, 0), (0, PAD - rows - 2), (0, 0))
     linear_grad, up_grad, conv = hidden_gradients(
+        pieces,
+        places,
         grads,
-        weights,
         jnp.pad(up_ext * gelu_slope, tail),
         jnp.pad(gelu_value, tail),
         jnp.pad(linear, ((0, 0), (0, PAD - rows - 4), (0, 0))),
@@ -230,7 +278,7 @@
     )
     conv = sent_to_all(conv, Z_ALL)
     conv = conv.reshape(-1, 2, 3, half).sum(axis=0).transpose(1, 0, 2).reshape(3, columns)
-    product = output_partials(linear_grad, up_grad, weights, width)
+    product = output_partials(pieces, places, linear_grad, up_grad, width)
     arrived = lax.all_to_all(product, GROUP, 0, 0, tiled=True)
     input_grad = arrived.astype(jnp.float32).sum(axis=0).astype(jnp.bfloat16)
     for bit in (1, 2, 4):

time: 212 us -> 209 us (0.986)
  starting transfers between devices: 102 us -> 128 us
  waiting for transfers between devices: 61.8 us -> 43.6 us
  local copies, waits for them, and re-layouts: 26.3 us -> 13.2 us
    ppermute x0 -> x9, starting transfers between devices: none -> 41.1 us  [crossed(): return lax.ppermute(value, (*names, 'core'), pairs)]
    ppermute x11 -> x2, starting transfers between devices: 42.8 us -> 6.49 us  [shifted(): lax.ppermute(value, axis, [(i, (i + by) % count) for i in range(count)])]
    ppermute x11 -> x2, waiting for transfers between devices: 42.6 us -> 13.8 us  [shifted(): lax.ppermute(value, axis, [(i, (i + by) % count) for i in range(count)])]
    all_to_all x2, starting transfers between devices: 20.1 us -> 36.6 us  [sent_to_all(): lax.all_to_all(jnp.broadcast_to(value[None], (peers, *value.shape)), axis...]
    ppermute x0 -> x9, waiting for transfers between devices: none -> 13.7 us  [crossed(): return lax.ppermute(value, (*names, 'core'), pairs)]
    dynamic_update_slice x8 -> x0, local copies, waits for them, and re-layouts: 10.2 us -> none  [gathered_y(): lax.dynamic_update_slice(whole, piece[:, :, None], (0, first, (y_at + k)...]
    ppermute x7, starting transfers between devices: 23 us -> 29.4 us  [swapped(): lax.ppermute(value, axis, [(i, i ^ bit) for i in range(lax.axis_size(axis...]
    broadcast_in_dim x1 -> x0, local copies, waits for them, and re-layouts: 2.94 us -> none  [gathered_y(): jnp.broadcast_to(pieces[base][:, :, None], (parts, z_count, count, share,...]
  transfers between devices with their start and end apart: 23 -> 23, of which waited for: 11 -> 15; matrix products, arithmetic and copies ran while one was open for 11% -> 5% of each run, Pallas kernels for 3% -> 3%
where the time goes in v4:
time: 209 us; the launch traced here: 206 us
  starting transfers between devices  128 us (61%)
  waiting for transfers between devices  43.6 us (21%)
  local copies, waits for them, and re-layouts  13.2 us (6%)
  Pallas kernels  12.9 us (6%)
  other arithmetic  7.31 us (3%)
    ppermute x9, starting transfers between devices, crossed(): return lax.ppermute(value, (*names, 'core'), pairs)  41.1 us
    all_to_all x2, starting transfers between devices, sent_to_all(): lax.all_to_all(jnp.broadcast_to(value[None], (peers, *value.shape)), axis...  36.6 us
    ppermute x7, starting transfers between devices, swapped(): lax.ppermute(value, axis, [(i, i ^ bit) for i in range(lax.axis_size(axis...  29.4 us
    ppermute x2, waiting for transfers between devices, shifted(): lax.ppermute(value, axis, [(i, (i + by) % count) for i in range(count)])  13.8 us
    ppermute x9, waiting for transfers between devices, crossed(): return lax.ppermute(value, (*names, 'core'), pairs)  13.7 us
    ppermute x7, waiting for transfers between devices, swapped(): lax.ppermute(value, axis, [(i, i ^ bit) for i in range(lax.axis_size(axis...  12.7 us
    all_to_all x1, starting transfers between devices, block_gradients(): arrived = lax.all_to_all(product, GROUP, 0, 0, tiled=True)  8.69 us
    pallas_call x1, Pallas kernels, output_partials(): pl.pallas_call(output_kernel, grid_spec=pltpu.PrefetchScalarGridSpec(num_...  7.03 us
  transfers between devices with their start and end apart: 23, of which 15 were waited for; matrix products, arithmetic and copies ran while one was open for 5% of the time, Pallas kernels for 3%

profile of v4, /device:TPU:1, one launch (start us, length us, event | category | flops | bytes accessed | tf_op | source)
XLA Modules:
  0.0 206.4 jit_solution(9579643937120080233)
XLA Ops:
  0.6 0.8 fusion.16
  1.4 1.2 copy.32
  2.6 1.3 copy.31
  3.9 1.3 collective-permute-start.12
  5.3 4.6 %collective-permute-start.11 = (bf16[4,704]{1,0:T(4,128)(2,1)S(1)}, bf16[4,704]{1,0:T(4,128)(2,1)S(1)}, u32[]{:S(2)}, u32[]{:S(2)}) collective-permute-start(bf16[4,704]{1,0:T(4,128)(2,1)S(1)} %fusion.9), channel_id=1, source_target_pairs={{0,8},{8,16},{16,24},{24,32},{32,40},{40,48},{48,56},{56,64},{64,7... | collective-permute-start | bytes 16904 | tf_op jit(solution)/shard_map/ppermute | solution.py:29
  10.0 0.7 collective-permute-done.11
  10.8 1.5 broadcast_in_dim.9
  12.3 14.6 %all-to-all-start = ((bf16[16,264,256]{2,1,0:T(8,128)(2,1)}), bf16[16,264,256]{2,1,0:T(8,128)(2,1)S(1)}, u32[]{:S(2)}, u32[]{:S(2)}) async-start(bf16[16,264,256]{2,1,0:T(8,128)(2,1)} %broadcast_in_dim.9), calls=%async_computation | async-start | bytes 4325376 | tf_op jit(solution)/shard_map/all_to_all | solution.py:38
  27.0 0.1 broadcast_select_fusion.2
  27.1 12.8 %collective-permute-start.1 = (bf16[3,64,352]{2,1,0:T(8,128)(2,1)S(1)}, bf16[3,64,352]{2,1,0:T(8,128)(2,1)S(1)}, u32[]{:S(2)}, u32[]{:S(2)}) collective-permute-start(bf16[3,64,352]{2,1,0:T(8,128)(2,1)S(1)} %get-tuple-element.36), channel_id=1, source_target_pairs={{0,128},{1,641},{64,192},{65,705},{128,256},{129,1},{192,320},{193... | collective-permute-start | bytes 405512 | tf_op jit(solution)/shard_map/ppermute | solution.py:57
  40.0 3.3 %collective-permute-start.2 = (bf16[3,64,352]{2,1,0:T(8,128)(2,1)S(1)}, bf16[3,64,352]{2,1,0:T(8,128)(2,1)S(1)}, u32[]{:S(2)}, u32[]{:S(2)}) collective-permute-start(bf16[3,64,352]{2,1,0:T(8,128)(2,1)S(1)} %get-tuple-element.35), channel_id=1, source_target_pairs={{0,64},{64,128},{128,192},{192,256},{256,320},{320,384},{384,448},... | collective-permute-start | bytes 405512 | tf_op jit(solution)/shard_map/ppermute | solution.py:23
  43.2 3.2 %collective-permute-start = (bf16[3,64,352]{2,1,0:T(8,128)(2,1)S(1)}, bf16[3,64,352]{2,1,0:T(8,128)(2,1)S(1)}, u32[]{:S(2)}, u32[]{:S(2)}) collective-permute-start(bf16[3,64,352]{2,1,0:T(8,128)(2,1)S(1)} %get-tuple-element.35), channel_id=1, source_target_pairs={{0,704},{64,0},{128,64},{192,128},{256,192},{320,256},{384,320},{4... | collective-permute-start | bytes 405512 | tf_op jit(solution)/shard_map/ppermute | solution.py:23
  46.6 9.7 %collective-permute-done.2 = bf16[3,64,352]{2,1,0:T(8,128)(2,1)S(1)} collective-permute-done((bf16[3,64,352]{2,1,0:T(8,128)(2,1)S(1)}, bf16[3,64,352]{2,1,0:T(8,128)(2,1)S(1)}, u32[]{:S(2)}, u32[]{:S(2)}) %collective-permute-start.2) | collective-permute-done | bytes 135200 | tf_op jit(solution)/shard_map/ppermute | solution.py:23
  56.3 4.1 %collective-permute-done = bf16[3,64,352]{2,1,0:T(8,128)(2,1)S(1)} collective-permute-done((bf16[3,64,352]{2,1,0:T(8,128)(2,1)S(1)}, bf16[3,64,352]{2,1,0:T(8,128)(2,1)S(1)}, u32[]{:S(2)}, u32[]{:S(2)}) %collective-permute-start) | collective-permute-done | bytes 135200 | tf_op jit(solution)/shard_map/ppermute | solution.py:23
  60.3 0.1 select_bitcast_fusion.5
  60.5 0.1 pad_maximum_fusion.2.refs_0_
  60.6 1.9 collective-permute-start.3
  62.5 3.9 %collective-permute-start.4 = (bf16[4,3,64,352]{3,2,1,0:T(8,128)(2,1)S(1)}, bf16[4,3,64,352]{3,2,1,0:T(8,128)(2,1)}, u32[]{:S(2)}, u32[]{:S(2)}) collective-permute-start(bf16[4,3,64,352]{3,2,1,0:T(8,128)(2,1)S(1)} %pad_maximum_fusion.2.refs_0_), channel_id=1, source_target_pairs={{0,56},{1,9},{8,0},{9,17},{16,8},{17,25},{24,16},{25,33},{32,24},{... | collective-permute-start | bytes 1622024 | tf_op jit(solution)/shard_map/ppermute | solution.py:57
  66.5 5.3 %collective-permute-done.3.refs_1_ = bf16[4,3,64,352]{3,2,1,0:T(8,128)(2,1)S(1)} collective-permute-done((bf16[4,3,64,352]{3,2,1,0:T(8,128)(2,1)S(1)}, bf16[4,3,64,352]{3,2,1,0:T(8,128)(2,1)S(1)}, u32[]{:S(2)}, u32[]{:S(2)}) %collective-permute-start.3) | collective-permute-done | bytes 540704 | tf_op jit(solution)/shard_map/ppermute | solution.py:57
  71.8 2.6 %collective-permute-start.5 = (bf16[4,3,64,352]{3,2,1,0:T(8,128)(2,1)S(1)}, bf16[4,3,64,352]{3,2,1,0:T(8,128)(2,1)}, u32[]{:S(2)}, u32[]{:S(2)}) collective-permute-start(bf16[4,3,64,352]{3,2,1,0:T(8,128)(2,1)S(1)} %collective-permute-done.3.refs_1_), channel_id=1, source_target_pairs={{0,8},{1,57},{8,16},{9,1},{16,24},{17,9},{24,32},{25,17},{32,40},{... | collective-permute-start | bytes 1622024 | tf_op jit(solution)/shard_map/ppermute | solution.py:57
  74.4 0.1 collective-permute-done.4.refs_2_
  74.5 6.3 %collective-permute-start.6 = (bf16[4,3,64,352]{3,2,1,0:T(8,128)(2,1)}, bf16[4,3,64,352]{3,2,1,0:T(8,128)(2,1)}, u32[]{:S(2)}, u32[]{:S(2)}) collective-permute-start(bf16[4,3,64,352]{3,2,1,0:T(8,128)(2,1)} %collective-permute-done.4.refs_2_), channel_id=1, source_target_pairs={{0,56},{1,9},{8,0},{9,17},{16,8},{17,25},{24,16},{25,33},{32,24},{... | collective-permute-start | bytes 1622024 | tf_op jit(solution)/shard_map/ppermute | solution.py:57
  80.8 1.2 pad_maximum_fusion.1
  82.0 6.5 %collective-permute-done.5.refs_3_ = bf16[4,3,64,352]{3,2,1,0:T(8,128)(2,1)} collective-permute-done((bf16[4,3,64,352]{3,2,1,0:T(8,128)(2,1)S(1)}, bf16[4,3,64,352]{3,2,1,0:T(8,128)(2,1)}, u32[]{:S(2)}, u32[]{:S(2)}) %collective-permute-start.5) | collective-permute-done | bytes 540704 | tf_op jit(solution)/shard_map/ppermute | solution.py:57
  88.5 1.9 collective-permute-start.7
  90.5 5.3 %collective-permute-start.8 = (bf16[4,3,64,352]{3,2,1,0:T(8,128)(2,1)}, bf16[4,3,64,352]{3,2,1,0:T(8,128)(2,1)}, u32[]{:S(2)}, u32[]{:S(2)}) collective-permute-start(bf16[4,3,64,352]{3,2,1,0:T(8,128)(2,1)} %collective-permute-done.6.refs_4_), channel_id=1, source_target_pairs={{0,56},{1,9},{8,0},{9,17},{16,8},{17,25},{24,16},{25,33},{32,24},{... | collective-permute-start | bytes 1622024 | tf_op jit(solution)/shard_map/ppermute | solution.py:57
  95.8 1.1 broadcast_select_fusion
  96.8 6.3 %collective-permute-start.13 = (bf16[520,352]{1,0:T(8,128)(2,1)}, bf16[520,352]{1,0:T(8,128)(2,1)}, u32[]{:S(2)}, u32[]{:S(2)}) collective-permute-start(bf16[520,352]{1,0:T(8,128)(2,1)} %get-tuple-element.25), channel_id=1, source_target_pairs={{0,64},{64,0},{1,65},{65,1},{2,66},{66,2},{3,67},{67,3},{4,68},{68... | collective-permute-start | bytes 1098248 | tf_op jit(solution)/shard_map/ppermute | solution.py:33
  103.2 0.8 dynamic-slice_convert_fusion.refs_13_
  104.0 0.5 and_select_fusion.places
  104.5 0.1 collective-permute-done.7.refs_5_
  104.7 4.4 %collective-permute-start.9 = (bf16[2,3,64,352]{3,2,1,0:T(8,128)(2,1)S(1)}, bf16[2,3,64,352]{3,2,1,0:T(8,128)(2,1)S(1)}, u32[]{:S(2)}, u32[]{:S(2)}) collective-permute-start(bf16[2,3,64,352]{3,2,1,0:T(8,128)(2,1)S(1)} %slice.107), channel_id=1, source_target_pairs={{0,8},{1,57},{8,16},{9,1},{16,24},{17,9},{24,32},{25,17},{32,40},{... | collective-permute-start | bytes 811016 | tf_op jit(solution)/shard_map/ppermute | solution.py:57
  109.1 1.0 slice.108
  110.1 1.9 collective-permute-start.10
  112.1 1.2 select_bitcast_fusion.1
  113.3 0.2 maximum_convert_fusion
  113.5 0.1 fusion.13
  113.7 1.0 pad.22.refs_12_
  114.6 0.7 fusion.12
  115.3 0.9 pad.20.refs_10_
  116.2 1.0 pad.21.refs_11_
  117.2 1.6 collective-permute-done.10.refs_8_
  118.8 0.7 copy-done.7
  119.5 1.4 copy-done
  120.9 5.9 %shard_map.95 = (bf16[2,256,352]{2,1,0:T(8,128)(2,1)}, bf16[2,256,352]{2,1,0:T(8,128)(2,1)}, f32[3,352]{1,0:T(4,128)}) custom-call(s32[9]{0:T(128)} %and_select_fusion.places, bf16[4,3,64,352]{3,2,1,0:T(8,128)(2,1)} %copy-done.1, bf16[4,3,64,352]{3,2,1,0:T(8,128)(2,1)} %copy-done.3, bf16[4,3,64,352]{3,2,1,0:T(8,128)(2,1)} %collective-permute-done.4.refs_2_, ...), custom_call_target="tpu_custom_call" | custom-call | tf_op jit(solution)/shard_map/pallas_call | solution.py:150
  126.8 1.3 broadcast_in_dim.20
  128.1 22.0 %all-to-all-start.2 = ((f32[12,3,352]{2,1,0:T(4,128)}), f32[12,3,352]{2,1,0:T(4,128)S(1)}, u32[]{:S(2)}, u32[]{:S(2)}) async-start(f32[12,3,352]{2,1,0:T(4,128)} %broadcast_in_dim.20), calls=%async_computation.2 | async-start | bytes 147456 | tf_op jit(solution)/shard_map/all_to_all | solution.py:38
  150.1 7.0 %shard_map.96 = bf16[2,8,256,256]{3,2,1,0:T(8,128)(2,1)} custom-call(s32[9]{0:T(128)} %and_select_fusion.places, bf16[4,3,64,352]{3,2,1,0:T(8,128)(2,1)} %copy-done.1, bf16[4,3,64,352]{3,2,1,0:T(8,128)(2,1)} %copy-done.3, bf16[4,3,64,352]{3,2,1,0:T(8,128)(2,1)} %collective-permute-done.4.refs_2_, bf16[4,3,64,352]{3,2,1,0:T(8,128)(2,1)} %collective-permute-done.5.refs_3_, ...), custom_call_target="tpu_custom_call" | custom-call | tf_op jit(solution)/shard_map/pallas_call | solution.py:217
  157.1 2.7 %all-to-all-done.2 = f32[12,3,352]{2,1,0:T(4,128)S(1)} async-done(((f32[12,3,352]{2,1,0:T(4,128)}), f32[12,3,352]{2,1,0:T(4,128)S(1)}, u32[]{:S(2)}, u32[]{:S(2)}) %all-to-all-start.2) | async-done | bytes 50720 | tf_op jit(solution)/shard_map/all_to_all | solution.py:38
  159.8 8.7 %all-to-all-start.1 = ((bf16[16,256,256]{2,1,0:T(8,128)(2,1)}), bf16[16,256,256]{2,1,0:T(8,128)(2,1)S(1)}, u32[]{:S(2)}, u32[]{:S(2)}) async-start(bf16[16,256,256]{2,1,0:T(8,128)(2,1)} %bitcast.26), calls=%async_computation.1 | async-start | bytes 4194304 | tf_op jit(solution)/shard_map/all_to_all | solution.py:282
  168.7 1.9 collective-permute-start.14
  170.6 2.8 %collective-permute-done.14 = f32[3,704]{1,0:T(4,128)S(1)} collective-permute-done((f32[3,704]{1,0:T(4,128)S(1)}, f32[3,704]{1,0:T(4,128)S(1)}, u32[]{:S(2)}, u32[]{:S(2)}) %collective-permute-start.14) | collective-permute-done | bytes 8480 | tf_op jit(solution)/shard_map/ppermute | solution.py:33
  173.4 3.3 %collective-permute-start.15 = (f32[3,704]{1,0:T(4,128)S(1)}, f32[3,704]{1,0:T(4,128)S(1)}, u32[]{:S(2)}, u32[]{:S(2)}) collective-permute-start(f32[3,704]{1,0:T(4,128)S(1)} %add.87), channel_id=1, source_target_pairs={{0,16},{8,24},{16,0},{24,8},{32,48},{40,56},{48,32},{56,40},{1,17}... | collective-permute-start | bytes 25352 | tf_op jit(solution)/shard_map/ppermute | solution.py:33
  176.7 2.3 %collective-permute-done.15 = f32[3,704]{1,0:T(4,128)S(1)} collective-permute-done((f32[3,704]{1,0:T(4,128)S(1)}, f32[3,704]{1,0:T(4,128)S(1)}, u32[]{:S(2)}, u32[]{:S(2)}) %collective-permute-start.15) | collective-permute-done | bytes 8480 | tf_op jit(solution)/shard_map/ppermute | solution.py:33
  179.0 4.5 %collective-permute-start.16 = (f32[3,704]{1,0:T(4,128)S(1)}, f32[3,704]{1,0:T(4,128)S(1)}, u32[]{:S(2)}, u32[]{:S(2)}) collective-permute-start(f32[3,704]{1,0:T(4,128)S(1)} %add.88), channel_id=1, source_target_pairs={{0,32},{8,40},{16,48},{24,56},{32,0},{40,8},{48,16},{56,24},{1,33}... | collective-permute-start | bytes 25352 | tf_op jit(solution)/shard_map/ppermute | solution.py:33
  183.5 3.8 %collective-permute-done.16 = f32[3,704]{1,0:T(4,128)S(1)} collective-permute-done((f32[3,704]{1,0:T(4,128)S(1)}, f32[3,704]{1,0:T(4,128)S(1)}, u32[]{:S(2)}, u32[]{:S(2)}) %collective-permute-start.16) | collective-permute-done | bytes 8480 | tf_op jit(solution)/shard_map/ppermute | solution.py:33
  187.4 4.9 %collective-permute-start.17 = (f32[1,3,704]{2,1,0:T(4,128)S(1)}, f32[1,3,704]{2,1,0:T(4,128)S(1)}, u32[]{:S(2)}, u32[]{:S(2)}) collective-permute-start(f32[1,3,704]{2,1,0:T(4,128)S(1)} %add_bitcast_fusion), channel_id=1, source_target_pairs={{0,1},{1,0},{2,3},{3,2},{4,5},{5,4},{6,7},{7,6},{8,9},{9,8},{10,11... | collective-permute-start | bytes 25352 | tf_op jit(solution)/shard_map/ppermute | solution.py:33
  192.3 0.8 collective-permute-done.17
  193.1 3.9 %collective-permute-start.18 = (f32[2,3,704]{2,1,0:T(4,128)S(1)}, f32[2,3,704]{2,1,0:T(4,128)S(1)}, u32[]{:S(2)}, u32[]{:S(2)}) collective-permute-start(f32[2,3,704]{2,1,0:T(4,128)S(1)} %pad_maximum_fusion.5), channel_id=1, source_target_pairs={{0,2},{2,0},{4,6},{6,4},{1,3},{3,1},{5,7},{7,5},{8,10},{10,8},{12,... | collective-permute-start | bytes 50696 | tf_op jit(solution)/shard_map/ppermute | solution.py:33
  197.0 1.2 collective-permute-done.18
  198.3 4.6 %collective-permute-start.19 = (f32[4,3,704]{2,1,0:T(4,128)S(1)}, f32[4,3,704]{2,1,0:T(4,128)S(1)}, u32[]{:S(2)}, u32[]{:S(2)}) collective-permute-start(f32[4,3,704]{2,1,0:T(4,128)S(1)} %pad_maximum_fusion.4), channel_id=1, source_target_pairs={{0,4},{2,6},{4,0},{6,2},{1,5},{3,7},{5,1},{7,3},{8,12},{10,14},{12... | collective-permute-start | bytes 101384 | tf_op jit(solution)/shard_map/ppermute | solution.py:33
  202.8 1.8 collective-permute-done.19
  204.7 0.7 reshape.24
  205.4 1.0 reduce_sum.21
  (62 shorter events, 0.8 us)
Async XLA Ops:
  0.6 10.0 %copy-start.8 = (bf16[256,256]{1,0:T(8,128)(2,1)S(1)}, bf16[256,256]{1,0:T(8,128)(2,1)}, u32[]{:S(2)}) copy-start(bf16[256,256]{1,0:T(8,128)(2,1)} %param.8) | copy-start | bytes 393220
  2.6 9.7 %copy-start.4 = (bf16[256,704]{1,0:T(8,128)(2,1)}, bf16[256,704]{1,0:T(8,128)(2,1)S(1)}, u32[]{:S(2)}) copy-start(bf16[256,704]{1,0:T(8,128)(2,1)S(1)} %copy.32) | copy-start | bytes 1081348
  3.9 8.4 %copy-start.5 = (bf16[256,704]{1,0:T(8,128)(2,1)}, bf16[256,704]{1,0:T(8,128)(2,1)S(1)}, u32[]{:S(2)}) copy-start(bf16[256,704]{1,0:T(8,128)(2,1)S(1)} %copy.31) | copy-start | bytes 1081348
  3.9 6.1 %collective-permute-start.12 = (bf16[4,704]{1,0:T(4,128)(2,1)S(1)}, bf16[4,704]{1,0:T(4,128)(2,1)S(1)}, u32[]{:S(2)}, u32[]{:S(2)}) collective-permute-start(bf16[4,704]{1,0:T(4,128)(2,1)S(1)} %fusion.10), channel_id=1, source_target_pairs={{8,0},{16,8},{24,16},{32,24},{40,32},{48,40},{56,48},{64,56},{72,6... | collective-permute-start | bytes 16904 | tf_op jit(solution)/shard_map/ppermute | solution.py:29
  5.3 5.4 %collective-permute-start.11 = (bf16[4,704]{1,0:T(4,128)(2,1)S(1)}, bf16[4,704]{1,0:T(4,128)(2,1)S(1)}, u32[]{:S(2)}, u32[]{:S(2)}) collective-permute-start(bf16[4,704]{1,0:T(4,128)(2,1)S(1)} %fusion.9), channel_id=1, source_target_pairs={{0,8},{8,16},{16,24},{24,32},{32,40},{40,48},{48,56},{56,64},{64,7... | collective-permute-start | bytes 16904 | tf_op jit(solution)/shard_map/ppermute | solution.py:29
  12.3 14.6 %copy-start.9 = (bf16[704,64]{0,1:T(8,128)(2,1)S(1)}, bf16[704,64]{0,1:T(8,128)(2,1)}, u32[]{:S(2)}) copy-start(bf16[704,64]{0,1:T(8,128)(2,1)} %param.14) | copy-start | bytes 270340
  12.3 14.6 %copy-start.10 = (bf16[64,704]{1,0:T(8,128)(2,1)S(1)}, bf16[64,704]{1,0:T(8,128)(2,1)}, u32[]{:S(2)}) copy-start(bf16[64,704]{1,0:T(8,128)(2,1)} %param.13) | copy-start | bytes 270340
  12.3 14.6 %copy-start.11 = (bf16[64,704]{1,0:T(8,128)(2,1)S(1)}, bf16[64,704]{1,0:T(8,128)(2,1)}, u32[]{:S(2)}) copy-start(bf16[64,704]{1,0:T(8,128)(2,1)} %param.12) | copy-start | bytes 270340
  12.3 106.5 %all-to-all-start = ((bf16[16,264,256]{2,1,0:T(8,128)(2,1)}), bf16[16,264,256]{2,1,0:T(8,128)(2,1)S(1)}, u32[]{:S(2)}, u32[]{:S(2)}) async-start(bf16[16,264,256]{2,1,0:T(8,128)(2,1)} %broadcast_in_dim.9), calls=%async_computation | async-start | bytes 4325376 | tf_op jit(solution)/shard_map/all_to_all | solution.py:38
  27.1 19.4 %collective-permute-start.1 = (bf16[3,64,352]{2,1,0:T(8,128)(2,1)S(1)}, bf16[3,64,352]{2,1,0:T(8,128)(2,1)S(1)}, u32[]{:S(2)}, u32[]{:S(2)}) collective-permute-start(bf16[3,64,352]{2,1,0:T(8,128)(2,1)S(1)} %get-tuple-element.36), channel_id=1, source_target_pairs={{0,128},{1,641},{64,192},{65,705},{128,256},{129,1},{192,320},{193... | collective-permute-start | bytes 405512 | tf_op jit(solution)/shard_map/ppermute | solution.py:57
  40.0 16.3 %collective-permute-start.2 = (bf16[3,64,352]{2,1,0:T(8,128)(2,1)S(1)}, bf16[3,64,352]{2,1,0:T(8,128)(2,1)S(1)}, u32[]{:S(2)}, u32[]{:S(2)}) collective-permute-start(bf16[3,64,352]{2,1,0:T(8,128)(2,1)S(1)} %get-tuple-element.35), channel_id=1, source_target_pairs={{0,64},{64,128},{128,192},{192,256},{256,320},{320,384},{384,448},... | collective-permute-start | bytes 405512 | tf_op jit(solution)/shard_map/ppermute | solution.py:23
  43.2 17.1 %collective-permute-start = (bf16[3,64,352]{2,1,0:T(8,128)(2,1)S(1)}, bf16[3,64,352]{2,1,0:T(8,128)(2,1)S(1)}, u32[]{:S(2)}, u32[]{:S(2)}) collective-permute-start(bf16[3,64,352]{2,1,0:T(8,128)(2,1)S(1)} %get-tuple-element.35), channel_id=1, source_target_pairs={{0,704},{64,0},{128,64},{192,128},{256,192},{320,256},{384,320},{4... | collective-permute-start | bytes 405512 | tf_op jit(solution)/shard_map/ppermute | solution.py:23
  60.6 36.2 %copy-start.1 = (bf16[4,3,64,352]{3,2,1,0:T(8,128)(2,1)}, bf16[4,3,64,352]{3,2,1,0:T(8,128)(2,1)S(1)}, u32[]{:S(2)}) copy-start(bf16[4,3,64,352]{3,2,1,0:T(8,128)(2,1)S(1)} %pad_maximum_fusion.2.refs_0_) | copy-start | bytes 1622020
  60.6 11.2 %collective-permute-start.3 = (bf16[4,3,64,352]{3,2,1,0:T(8,128)(2,1)S(1)}, bf16[4,3,64,352]{3,2,1,0:T(8,128)(2,1)S(1)}, u32[]{:S(2)}, u32[]{:S(2)}) collective-permute-start(bf16[4,3,64,352]{3,2,1,0:T(8,128)(2,1)S(1)} %pad_maximum_fusion.2.refs_0_), channel_id=1, source_target_pairs={{0,8},{1,57},{8,16},{9,1},{16,24},{17,9},{24,32},{25,17},{32,40},{... | collective-permute-start | bytes 1622024 | tf_op jit(solution)/shard_map/ppermute | solution.py:57
  62.5 11.9 %collective-permute-start.4 = (bf16[4,3,64,352]{3,2,1,0:T(8,128)(2,1)S(1)}, bf16[4,3,64,352]{3,2,1,0:T(8,128)(2,1)}, u32[]{:S(2)}, u32[]{:S(2)}) collective-permute-start(bf16[4,3,64,352]{3,2,1,0:T(8,128)(2,1)S(1)} %pad_maximum_fusion.2.refs_0_), channel_id=1, source_target_pairs={{0,56},{1,9},{8,0},{9,17},{16,8},{17,25},{24,16},{25,33},{32,24},{... | collective-permute-start | bytes 1622024 | tf_op jit(solution)/shard_map/ppermute | solution.py:57
  71.8 10.2 %copy-start.3 = (bf16[4,3,64,352]{3,2,1,0:T(8,128)(2,1)}, bf16[4,3,64,352]{3,2,1,0:T(8,128)(2,1)S(1)}, u32[]{:S(2)}) copy-start(bf16[4,3,64,352]{3,2,1,0:T(8,128)(2,1)S(1)} %collective-permute-done.3.refs_1_) | copy-start | bytes 1622020
  71.8 16.7 %collective-permute-start.5 = (bf16[4,3,64,352]{3,2,1,0:T(8,128)(2,1)S(1)}, bf16[4,3,64,352]{3,2,1,0:T(8,128)(2,1)}, u32[]{:S(2)}, u32[]{:S(2)}) collective-permute-start(bf16[4,3,64,352]{3,2,1,0:T(8,128)(2,1)S(1)} %collective-permute-done.3.refs_1_), channel_id=1, source_target_pairs={{0,8},{1,57},{8,16},{9,1},{16,24},{17,9},{24,32},{25,17},{32,40},{... | collective-permute-start | bytes 1622024 | tf_op jit(solution)/shard_map/ppermute | solution.py:57
  74.5 16.0 %collective-permute-start.6 = (bf16[4,3,64,352]{3,2,1,0:T(8,128)(2,1)}, bf16[4,3,64,352]{3,2,1,0:T(8,128)(2,1)}, u32[]{:S(2)}, u32[]{:S(2)}) collective-permute-start(bf16[4,3,64,352]{3,2,1,0:T(8,128)(2,1)} %collective-permute-done.4.refs_2_), channel_id=1, source_target_pairs={{0,56},{1,9},{8,0},{9,17},{16,8},{17,25},{24,16},{25,33},{32,24},{... | collective-permute-start | bytes 1622024 | tf_op jit(solution)/shard_map/ppermute | solution.py:57
  80.8 23.1 %copy-start.13 = (s32[9]{0:T(128)S(1)}, s32[9]{0:T(128)}, u32[]{:S(2)}) copy-start(s32[9]{0:T(128)} %constant.89.clone) | copy-start | bytes 112
  88.5 16.1 %collective-permute-start.7 = (bf16[4,3,64,352]{3,2,1,0:T(8,128)(2,1)}, bf16[4,3,64,352]{3,2,1,0:T(8,128)(2,1)S(1)}, u32[]{:S(2)}, u32[]{:S(2)}) collective-permute-start(bf16[4,3,64,352]{3,2,1,0:T(8,128)(2,1)} %collective-permute-done.5.refs_3_), channel_id=1, source_target_pairs={{0,8},{1,57},{8,16},{9,1},{16,24},{17,9},{24,32},{25,17},{32,40},{... | collective-permute-start | bytes 1622024 | tf_op jit(solution)/shard_map/ppermute | solution.py:57
  90.5 18.6 %collective-permute-start.8 = (bf16[4,3,64,352]{3,2,1,0:T(8,128)(2,1)}, bf16[4,3,64,352]{3,2,1,0:T(8,128)(2,1)}, u32[]{:S(2)}, u32[]{:S(2)}) collective-permute-start(bf16[4,3,64,352]{3,2,1,0:T(8,128)(2,1)} %collective-permute-done.6.refs_4_), channel_id=1, source_target_pairs={{0,56},{1,9},{8,0},{9,17},{16,8},{17,25},{24,16},{25,33},{32,24},{... | collective-permute-start | bytes 1622024 | tf_op jit(solution)/shard_map/ppermute | solution.py:57
  96.8 15.2 %collective-permute-start.13 = (bf16[520,352]{1,0:T(8,128)(2,1)}, bf16[520,352]{1,0:T(8,128)(2,1)}, u32[]{:S(2)}, u32[]{:S(2)}) collective-permute-start(bf16[520,352]{1,0:T(8,128)(2,1)} %get-tuple-element.25), channel_id=1, source_target_pairs={{0,64},{64,0},{1,65},{65,1},{2,66},{66,2},{3,67},{67,3},{4,68},{68... | collective-permute-start | bytes 1098248 | tf_op jit(solution)/shard_map/ppermute | solution.py:33
  103.9 9.3 %copy-start.12 = (f32[3,352]{1,0:T(4,128)}, f32[3,352]{1,0:T(4,128)S(1)}, u32[]{:S(2)}) copy-start(f32[3,352]{1,0:T(4,128)S(1)} %dynamic-slice_convert_fusion.refs_13_) | copy-start | bytes 12676
  104.6 8.7 %copy-start.2 = (bf16[4,3,64,352]{3,2,1,0:T(8,128)(2,1)}, bf16[4,3,64,352]{3,2,1,0:T(8,128)(2,1)S(1)}, u32[]{:S(2)}) copy-start(bf16[4,3,64,352]{3,2,1,0:T(8,128)(2,1)S(1)} %collective-permute-done.7.refs_5_) | copy-start | bytes 1622020
  104.7 12.5 %collective-permute-start.9 = (bf16[2,3,64,352]{3,2,1,0:T(8,128)(2,1)S(1)}, bf16[2,3,64,352]{3,2,1,0:T(8,128)(2,1)S(1)}, u32[]{:S(2)}, u32[]{:S(2)}) collective-permute-start(bf16[2,3,64,352]{3,2,1,0:T(8,128)(2,1)S(1)} %slice.107), channel_id=1, source_target_pairs={{0,8},{1,57},{8,16},{9,1},{16,24},{17,9},{24,32},{25,17},{32,40},{... | collective-permute-start | bytes 811016 | tf_op jit(solution)/shard_map/ppermute | solution.py:57
  110.1 8.7 %collective-permute-start.10 = (bf16[2,3,64,352]{3,2,1,0:T(8,128)(2,1)S(1)}, bf16[2,3,64,352]{3,2,1,0:T(8,128)(2,1)S(1)}, u32[]{:S(2)}, u32[]{:S(2)}) collective-permute-start(bf16[2,3,64,352]{3,2,1,0:T(8,128)(2,1)S(1)} %slice.108), channel_id=1, source_target_pairs={{0,56},{1,9},{8,0},{9,17},{16,8},{17,25},{24,16},{25,33},{32,24},{... | collective-permute-start | bytes 811016 | tf_op jit(solution)/shard_map/ppermute | solution.py:57
  117.2 1.6 copy-start.6
  118.8 0.7 copy-start.7
  119.5 1.4 copy-start
  128.1 31.7 %all-to-all-start.2 = ((f32[12,3,352]{2,1,0:T(4,128)}), f32[12,3,352]{2,1,0:T(4,128)S(1)}, u32[]{:S(2)}, u32[]{:S(2)}) async-start(f32[12,3,352]{2,1,0:T(4,128)} %broadcast_in_dim.20), calls=%async_computation.2 | async-start | bytes 147456 | tf_op jit(solution)/shard_map/all_to_all | solution.py:38
  159.8 45.6 %all-to-all-start.1 = ((bf16[16,256,256]{2,1,0:T(8,128)(2,1)}), bf16[16,256,256]{2,1,0:T(8,128)(2,1)S(1)}, u32[]{:S(2)}, u32[]{:S(2)}) async-start(bf16[16,256,256]{2,1,0:T(8,128)(2,1)} %bitcast.26), calls=%async_computation.1 | async-start | bytes 4194304 | tf_op jit(solution)/shard_map/all_to_all | solution.py:282
  168.7 4.7 %collective-permute-start.14 = (f32[3,704]{1,0:T(4,128)S(1)}, f32[3,704]{1,0:T(4,128)S(1)}, u32[]{:S(2)}, u32[]{:S(2)}) collective-permute-start(f32[3,704]{1,0:T(4,128)S(1)} %reshape.23), channel_id=1, source_target_pairs={{0,8},{8,0},{16,24},{24,16},{32,40},{40,32},{48,56},{56,48},{1,9},... | collective-permute-start | bytes 25352 | tf_op jit(solution)/shard_map/ppermute | solution.py:33
  173.4 5.6 %collective-permute-start.15 = (f32[3,704]{1,0:T(4,128)S(1)}, f32[3,704]{1,0:T(4,128)S(1)}, u32[]{:S(2)}, u32[]{:S(2)}) collective-permute-start(f32[3,704]{1,0:T(4,128)S(1)} %add.87), channel_id=1, source_target_pairs={{0,16},{8,24},{16,0},{24,8},{32,48},{40,56},{48,32},{56,40},{1,17}... | collective-permute-start | bytes 25352 | tf_op jit(solution)/shard_map/ppermute | solution.py:33
  179.0 8.3 %collective-permute-start.16 = (f32[3,704]{1,0:T(4,128)S(1)}, f32[3,704]{1,0:T(4,128)S(1)}, u32[]{:S(2)}, u32[]{:S(2)}) collective-permute-start(f32[3,704]{1,0:T(4,128)S(1)} %add.88), channel_id=1, source_target_pairs={{0,32},{8,40},{16,48},{24,56},{32,0},{40,8},{48,16},{56,24},{1,33}... | collective-permute-start | bytes 25352 | tf_op jit(solution)/shard_map/ppermute | solution.py:33
  187.4 5.8 %collective-permute-start.17 = (f32[1,3,704]{2,1,0:T(4,128)S(1)}, f32[1,3,704]{2,1,0:T(4,128)S(1)}, u32[]{:S(2)}, u32[]{:S(2)}) collective-permute-start(f32[1,3,704]{2,1,0:T(4,128)S(1)} %add_bitcast_fusion), channel_id=1, source_target_pairs={{0,1},{1,0},{2,3},{3,2},{4,5},{5,4},{6,7},{7,6},{8,9},{9,8},{10,11... | collective-permute-start | bytes 25352 | tf_op jit(solution)/shard_map/ppermute | solution.py:33
  193.1 5.1 %collective-permute-start.18 = (f32[2,3,704]{2,1,0:T(4,128)S(1)}, f32[2,3,704]{2,1,0:T(4,128)S(1)}, u32[]{:S(2)}, u32[]{:S(2)}) collective-permute-start(f32[2,3,704]{2,1,0:T(4,128)S(1)} %pad_maximum_fusion.5), channel_id=1, source_target_pairs={{0,2},{2,0},{4,6},{6,4},{1,3},{3,1},{5,7},{7,5},{8,10},{10,8},{12,... | collective-permute-start | bytes 50696 | tf_op jit(solution)/shard_map/ppermute | solution.py:33
  198.3 6.3 %collective-permute-start.19 = (f32[4,3,704]{2,1,0:T(4,128)S(1)}, f32[4,3,704]{2,1,0:T(4,128)S(1)}, u32[]{:S(2)}, u32[]{:S(2)}) collective-permute-start(f32[4,3,704]{2,1,0:T(4,128)S(1)} %pad_maximum_fusion.4), channel_id=1, source_target_pairs={{0,4},{2,6},{4,0},{6,2},{1,5},{3,7},{5,1},{7,3},{8,12},{10,14},{12... | collective-permute-start | bytes 101384 | tf_op jit(solution)/shard_map/ppermute | solution.py:33

commit v5 on v4

--- a/solution.py
+++ b/solution.py
@@ -76,7 +76,8 @@
     sign = 1 - 2 * lax.axis_index("core")
     count = lax.axis_size("y")
     places = (lax.axis_index("y") + sign * jnp.array(steps + [4, 4], jnp.int32)) % count
-    return pieces, places.astype(jnp.int32), one
+    places = jnp.append(places, lax.axis_index("core"))
+    return pieces, places.astype(jnp.int32), pieces[3]
 
 
 def gelu_parts(gate):
@@ -175,9 +176,9 @@
 
 
 def output_kernel(places, *refs):
-    pieces, (linear_grad, up_grad, out, both) = refs[:PIECES], refs[PIECES:]
+    pieces, (linear_grad, up_grad, kept, sent, both) = refs[:PIECES], refs[PIECES:]
     _, _, share, half = both.shape
-    width = out.shape[3]
+    width = kept.shape[3]
     per_tp = width // share
     z = pl.program_id(0)
     split = pl.num_programs(0) // 2
@@ -190,9 +191,10 @@
     pl.when(z < split)(lambda: place(PIECES - 2))
     pl.when(z >= split)(lambda: place(PIECES - 1))
     contract = (((1,), (1,)), ((), ()))
-    for t in range(out.shape[1]):
+    core = places[PIECES]
+    for target, out in ((core, kept), (1 - core, sent)):
         gate, up = (
-            both[part, t * per_tp : (t + 1) * per_tp].reshape(width, half) for part in range(2)
+            both[part, pl.ds(target * per_tp, per_tp)].reshape(width, half) for part in range(2)
         )
         for b in range(2):
             part = lax.dot_general(
@@ -200,32 +202,32 @@
             ) + lax.dot_general(
                 up_grad[b], up, contract, preferred_element_type=jnp.float32
             )
-            out[b, t] = part.astype(jnp.bfloat16)
+            out[b, 0] = part.astype(jnp.bfloat16)
 
 
 def output_partials(pieces, places, linear_grad, up_grad, width):
     _, rows, half = linear_grad.shape
     z_count, _, share, _ = pieces[0].shape
     mid = pieces[-1].shape[0]
-    y_count = 8
-    peers = z_count * y_count * share // width
+    y_count = 2 * width // share
     whole = pl.BlockSpec((2, rows, half), lambda i, at: (0, 0, 0))
     maps = [lambda i, at: (i, 0, 0, 0)] * (PIECES - 2) + [
         lambda i, at: (jnp.minimum(i, mid - 1), 0, 0, 0),
         lambda i, at: (jnp.maximum(i - mid, 0), 0, 0, 0),
     ]
-    product = pl.pallas_call(
+    made = pl.BlockSpec((2, 1, rows, width), lambda i, at: (0, i, 0, 0))
+    shape = jax.ShapeDtypeStruct((2, z_count, rows, width), jnp.bfloat16)
+    return pl.pallas_call(
         output_kernel,
         grid_spec=pltpu.PrefetchScalarGridSpec(
             num_scalar_prefetch=1,
             grid=(z_count,),
             in_specs=[pl.BlockSpec((1, 2, share, half), m) for m in maps] + [whole, whole],
-            out_specs=pl.BlockSpec((2, peers // z_count, rows, width), lambda i, at: (0, i, 0, 0)),
+            out_specs=[made, made],
             scratch_shapes=[pltpu.VMEM((2, y_count, share, half), jnp.bfloat16)],
         ),
-        out_shape=jax.ShapeDtypeStruct((2, peers, rows, width), jnp.bfloat16),
+        out_shape=[shape, shape],
     )(places, *pieces, linear_grad, up_grad)
-    return product.reshape(2 * peers, rows, width)
 
 
 def block_gradients(out_grad, gate_lin, up_lin, conv_weight, gate_weight, up_weight, down_weight):
@@ -278,11 +280,15 @@
     )
     conv = sent_to_all(conv, Z_ALL)
     conv = conv.reshape(-1, 2, 3, half).sum(axis=0).transpose(1, 0, 2).reshape(3, columns)
-    product = output_partials(pieces, places, linear_grad, up_grad, width)
-    arrived = lax.all_to_all(product, GROUP, 0, 0, tiled=True)
+    kept, sent = output_partials(pieces, places, linear_grad, up_grad, width)
+    came = swapped(sent, "core", 1)
+    product = (kept.astype(jnp.float32) + came.astype(jnp.float32)).astype(jnp.bfloat16)
+    conv = sent_to_all(conv, "y")
+    conv = conv.sum(axis=0)
+    arrived = lax.all_to_all(
+        product.reshape(-1, rows, width), ("zp", "x"), 0, 0, tiled=True
+    )
     input_grad = arrived.astype(jnp.float32).sum(axis=0).astype(jnp.bfloat16)
-    for bit in (1, 2, 4):
-        conv = conv + swapped(conv, "y", bit)
     conv = conv[None]
     for axis, bit in (("core", 1), ("x", 1), ("x", 2)):
         low = lax.axis_index(axis) & bit == 0

time: 209 us -> 210 us (level)
  blocking collectives: 0 us -> 23 us
  starting transfers between devices: 128 us -> 106 us
  other arithmetic: 7.31 us -> 9.77 us
    all_to_all x0 -> x1, blocking collectives: none -> 23 us  [sent_to_all(): lax.all_to_all(jnp.broadcast_to(value[None], (peers, *value.shape)), axis...]
    all_to_all x2, starting transfers between devices: 36.6 us -> 19.3 us  [sent_to_all(): lax.all_to_all(jnp.broadcast_to(value[None], (peers, *value.shape)), axis...]
    ppermute x7 -> x5, waiting for transfers between devices: 12.7 us -> 7.35 us  [swapped(): lax.ppermute(value, axis, [(i, i ^ bit) for i in range(lax.axis_size(axis...]
    all_to_all x1, starting transfers between devices: 8.69 us -> 5.45 us  [block_gradients(): lax.all_to_all(product.reshape(-1, rows, width), ('zp', 'x'), 0, 0, tiled...]
    ppermute x9, waiting for transfers between devices: 13.7 us -> 16.5 us  [crossed(): return lax.ppermute(value, (*names, 'core'), pairs)]
    all_to_all x2, waiting for transfers between devices: 2.72 us -> 5.22 us  [sent_to_all(): lax.all_to_all(jnp.broadcast_to(value[None], (peers, *value.shape)), axis...]
    convert_element_type x0 -> x1, other arithmetic: none -> 2.45 us  [block_gradients(): (kept.astype(jnp.float32) + came.astype(jnp.float32)).astype(jnp.bfloat16)]
    ppermute x7 -> x5, starting transfers between devices: 29.4 us -> 28.9 us  [swapped(): lax.ppermute(value, axis, [(i, i ^ bit) for i in range(lax.axis_size(axis...]
  transfers between devices with their start and end apart: 23 -> 21, of which waited for: 15 -> 13; matrix products, arithmetic and copies ran while one was open for 5% -> 6% of each run, Pallas kernels for 3% -> 0%
where the time goes in v5:
time: 210 us; the launch traced here: 208 us
  starting transfers between devices  106 us (50%)
  waiting for transfers between devices  43.5 us (21%)
  blocking collectives  23 us (11%)
  Pallas kernels  12.9 us (6%)
  local copies, waits for them, and re-layouts  11.6 us (6%)
  other arithmetic  9.77 us (5%)
    ppermute x9, starting transfers between devices, crossed(): return lax.ppermute(value, (*names, 'core'), pairs)  40 us
    ppermute x5, starting transfers between devices, swapped(): lax.ppermute(value, axis, [(i, i ^ bit) for i in range(lax.axis_size(axis...  28.9 us
    all_to_all x1, blocking collectives, sent_to_all(): lax.all_to_all(jnp.broadcast_to(value[None], (peers, *value.shape)), axis...  23 us
    all_to_all x2, starting transfers between devices, sent_to_all(): lax.all_to_all(jnp.broadcast_to(value[None], (peers, *value.shape)), axis...  19.3 us
    ppermute x9, waiting for transfers between devices, crossed(): return lax.ppermute(value, (*names, 'core'), pairs)  16.5 us
    ppermute x2, waiting for transfers between devices, shifted(): lax.ppermute(value, axis, [(i, (i + by) % count) for i in range(count)])  13.8 us
    ppermute x5, waiting for transfers between devices, swapped(): lax.ppermute(value, axis, [(i, i ^ bit) for i in range(lax.axis_size(axis...  7.35 us
    pallas_call x1, Pallas kernels, output_partials(): pl.pallas_call(output_kernel, grid_spec=pltpu.PrefetchScalarGridSpec(num_...  7.02 us
  transfers between devices with their start and end apart: 21, of which 13 were waited for; matrix products, arithmetic and copies ran while one was open for 6% of the time, Pallas kernels for 0%

profile of v5, /device:TPU:1, one launch (start us, length us, event | category | flops | bytes accessed | tf_op | source)
XLA Modules:
  0.0 208.1 jit_solution(18027375995143014501)
XLA Ops:
  0.6 0.8 fusion.16
  1.4 1.2 copy.37
  2.6 1.3 copy.36
  3.9 1.3 collective-permute-start.12
  5.3 4.6 %collective-permute-start.11 = (bf16[4,704]{1,0:T(4,128)(2,1)S(1)}, bf16[4,704]{1,0:T(4,128)(2,1)S(1)}, u32[]{:S(2)}, u32[]{:S(2)}) collective-permute-start(bf16[4,704]{1,0:T(4,128)(2,1)S(1)} %fusion.9), channel_id=1, source_target_pairs={{0,8},{8,16},{16,24},{24,32},{32,40},{40,48},{48,56},{56,64},{64,7... | collective-permute-start | bytes 16904 | tf_op jit(solution)/shard_map/ppermute | solution.py:29
  9.9 0.1 pad.48.clone
  10.0 0.7 collective-permute-done.11
  10.7 0.1 maximum_maximum_fusion
  10.8 1.5 broadcast_in_dim.26
  12.3 14.6 %all-to-all-start = ((bf16[16,264,256]{2,1,0:T(8,128)(2,1)}), bf16[16,264,256]{2,1,0:T(8,128)(2,1)S(1)}, u32[]{:S(2)}, u32[]{:S(2)}) async-start(bf16[16,264,256]{2,1,0:T(8,128)(2,1)} %broadcast_in_dim.26), calls=%async_computation | async-start | bytes 4325376 | tf_op jit(solution)/shard_map/all_to_all | solution.py:38
  27.0 0.1 broadcast_select_fusion.2
  27.1 12.8 %collective-permute-start.1 = (bf16[3,64,352]{2,1,0:T(8,128)(2,1)S(1)}, bf16[3,64,352]{2,1,0:T(8,128)(2,1)S(1)}, u32[]{:S(2)}, u32[]{:S(2)}) collective-permute-start(bf16[3,64,352]{2,1,0:T(8,128)(2,1)S(1)} %get-tuple-element.40), channel_id=1, source_target_pairs={{0,128},{1,641},{64,192},{65,705},{128,256},{129,1},{192,320},{193... | collective-permute-start | bytes 405512 | tf_op jit(solution)/shard_map/ppermute | solution.py:57
  40.0 3.3 %collective-permute-start.2 = (bf16[3,64,352]{2,1,0:T(8,128)(2,1)S(1)}, bf16[3,64,352]{2,1,0:T(8,128)(2,1)S(1)}, u32[]{:S(2)}, u32[]{:S(2)}) collective-permute-start(bf16[3,64,352]{2,1,0:T(8,128)(2,1)S(1)} %get-tuple-element.39), channel_id=1, source_target_pairs={{0,64},{64,128},{128,192},{192,256},{256,320},{320,384},{384,448},... | collective-permute-start | bytes 405512 | tf_op jit(solution)/shard_map/ppermute | solution.py:23
  43.2 3.2 %collective-permute-start = (bf16[3,64,352]{2,1,0:T(8,128)(2,1)S(1)}, bf16[3,64,352]{2,1,0:T(8,128)(2,1)S(1)}, u32[]{:S(2)}, u32[]{:S(2)}) collective-permute-start(bf16[3,64,352]{2,1,0:T(8,128)(2,1)S(1)} %get-tuple-element.39), channel_id=1, source_target_pairs={{0,704},{64,0},{128,64},{192,128},{256,192},{320,256},{384,320},{4... | collective-permute-start | bytes 405512 | tf_op jit(solution)/shard_map/ppermute | solution.py:23
  46.6 9.7 %collective-permute-done.2 = bf16[3,64,352]{2,1,0:T(8,128)(2,1)S(1)} collective-permute-done((bf16[3,64,352]{2,1,0:T(8,128)(2,1)S(1)}, bf16[3,64,352]{2,1,0:T(8,128)(2,1)S(1)}, u32[]{:S(2)}, u32[]{:S(2)}) %collective-permute-start.2) | collective-permute-done | bytes 135200 | tf_op jit(solution)/shard_map/ppermute | solution.py:23
  56.3 4.1 %collective-permute-done = bf16[3,64,352]{2,1,0:T(8,128)(2,1)S(1)} collective-permute-done((bf16[3,64,352]{2,1,0:T(8,128)(2,1)S(1)}, bf16[3,64,352]{2,1,0:T(8,128)(2,1)S(1)}, u32[]{:S(2)}, u32[]{:S(2)}) %collective-permute-start) | collective-permute-done | bytes 135200 | tf_op jit(solution)/shard_map/ppermute | solution.py:23
  60.4 0.1 select_bitcast_fusion.5
  60.5 0.1 pad_maximum_fusion.2.refs_0_
  60.6 1.9 collective-permute-start.3
  62.6 3.9 %collective-permute-start.4 = (bf16[4,3,64,352]{3,2,1,0:T(8,128)(2,1)S(1)}, bf16[4,3,64,352]{3,2,1,0:T(8,128)(2,1)}, u32[]{:S(2)}, u32[]{:S(2)}) collective-permute-start(bf16[4,3,64,352]{3,2,1,0:T(8,128)(2,1)S(1)} %pad_maximum_fusion.2.refs_0_), channel_id=1, source_target_pairs={{0,56},{1,9},{8,0},{9,17},{16,8},{17,25},{24,16},{25,33},{32,24},{... | collective-permute-start | bytes 1622024 | tf_op jit(solution)/shard_map/ppermute | solution.py:57
  66.5 1.2 pad_maximum_fusion.1
  67.7 1.1 broadcast_select_fusion
  68.8 1.9 collective-permute-start.13
  70.7 1.1 collective-permute-done.3.refs_1_
  71.8 2.6 %collective-permute-start.5 = (bf16[4,3,64,352]{3,2,1,0:T(8,128)(2,1)S(1)}, bf16[4,3,64,352]{3,2,1,0:T(8,128)(2,1)}, u32[]{:S(2)}, u32[]{:S(2)}) collective-permute-start(bf16[4,3,64,352]{3,2,1,0:T(8,128)(2,1)S(1)} %collective-permute-done.3.refs_1_), channel_id=1, source_target_pairs={{0,8},{1,57},{8,16},{9,1},{16,24},{17,9},{24,32},{25,17},{32,40},{... | collective-permute-start | bytes 1622024 | tf_op jit(solution)/shard_map/ppermute | solution.py:57
  74.4 0.1 collective-permute-done.4.refs_2_
  74.5 6.3 %collective-permute-start.6 = (bf16[4,3,64,352]{3,2,1,0:T(8,128)(2,1)}, bf16[4,3,64,352]{3,2,1,0:T(8,128)(2,1)}, u32[]{:S(2)}, u32[]{:S(2)}) collective-permute-start(bf16[4,3,64,352]{3,2,1,0:T(8,128)(2,1)} %collective-permute-done.4.refs_2_), channel_id=1, source_target_pairs={{0,56},{1,9},{8,0},{9,17},{16,8},{17,25},{24,16},{25,33},{32,24},{... | collective-permute-start | bytes 1622024 | tf_op jit(solution)/shard_map/ppermute | solution.py:57
  80.9 0.6 pad_add_fusion.places
  81.5 0.8 dynamic-slice_convert_fusion.refs_13_
  82.3 6.3 %collective-permute-done.5.refs_3_ = bf16[4,3,64,352]{3,2,1,0:T(8,128)(2,1)} collective-permute-done((bf16[4,3,64,352]{3,2,1,0:T(8,128)(2,1)S(1)}, bf16[4,3,64,352]{3,2,1,0:T(8,128)(2,1)}, u32[]{:S(2)}, u32[]{:S(2)}) %collective-permute-start.5) | collective-permute-done | bytes 540704 | tf_op jit(solution)/shard_map/ppermute | solution.py:57
  88.5 1.9 collective-permute-start.7
  90.5 5.3 %collective-permute-start.8 = (bf16[4,3,64,352]{3,2,1,0:T(8,128)(2,1)}, bf16[4,3,64,352]{3,2,1,0:T(8,128)(2,1)S(1)}, u32[]{:S(2)}, u32[]{:S(2)}) collective-permute-start(bf16[4,3,64,352]{3,2,1,0:T(8,128)(2,1)} %collective-permute-done.6.refs_4_), channel_id=1, source_target_pairs={{0,56},{1,9},{8,0},{9,17},{16,8},{17,25},{24,16},{25,33},{32,24},{... | collective-permute-start | bytes 1622024 | tf_op jit(solution)/shard_map/ppermute | solution.py:57
  95.8 1.2 select_bitcast_fusion.1
  97.0 0.2 maximum_convert_fusion
  97.2 0.1 fusion.13
  97.4 1.0 pad.22.refs_12_
  98.3 6.3 %collective-permute-done.7.refs_5_ = bf16[4,3,64,352]{3,2,1,0:T(8,128)(2,1)S(1)} collective-permute-done((bf16[4,3,64,352]{3,2,1,0:T(8,128)(2,1)}, bf16[4,3,64,352]{3,2,1,0:T(8,128)(2,1)S(1)}, u32[]{:S(2)}, u32[]{:S(2)}) %collective-permute-start.7) | collective-permute-done | bytes 540704 | tf_op jit(solution)/shard_map/ppermute | solution.py:57
  104.7 1.9 collective-permute-start.9
  106.7 3.4 %collective-permute-start.10 = (bf16[2,3,64,352]{3,2,1,0:T(8,128)(2,1)S(1)}, bf16[2,3,64,352]{3,2,1,0:T(8,128)(2,1)S(1)}, u32[]{:S(2)}, u32[]{:S(2)}) collective-permute-start(bf16[2,3,64,352]{3,2,1,0:T(8,128)(2,1)S(1)} %slice.108), channel_id=1, source_target_pairs={{0,56},{1,9},{8,0},{9,17},{16,8},{17,25},{24,16},{25,33},{32,24},{... | collective-permute-start | bytes 811016 | tf_op jit(solution)/shard_map/ppermute | solution.py:57
  110.0 0.7 fusion.12
  110.7 1.0 pad.20.refs_10_
  111.7 0.9 pad.21.refs_11_
  112.6 0.5 collective-permute-done.9.refs_7_
  113.1 2.2 %collective-permute-done.10.refs_8_ = bf16[2,3,64,352]{3,2,1,0:T(8,128)(2,1)S(1)} collective-permute-done((bf16[2,3,64,352]{3,2,1,0:T(8,128)(2,1)S(1)}, bf16[2,3,64,352]{3,2,1,0:T(8,128)(2,1)S(1)}, u32[]{:S(2)}, u32[]{:S(2)}) %collective-permute-start.10) | collective-permute-done | bytes 270368 | tf_op jit(solution)/shard_map/ppermute | solution.py:57
  115.4 0.7 copy-done.8
  116.1 1.4 copy-done
  117.5 5.9 %shard_map.95 = (bf16[2,256,352]{2,1,0:T(8,128)(2,1)}, bf16[2,256,352]{2,1,0:T(8,128)(2,1)}, f32[3,352]{1,0:T(4,128)}) custom-call(s32[10]{0:T(128)} %pad_add_fusion.places, bf16[4,3,64,352]{3,2,1,0:T(8,128)(2,1)} %copy-done.1, bf16[4,3,64,352]{3,2,1,0:T(8,128)(2,1)} %copy-done.4, bf16[4,3,64,352]{3,2,1,0:T(8,128)(2,1)} %collective-permute-done.4.refs_2_, ...), custom_call_target="tpu_custom_call" | custom-call | tf_op jit(solution)/shard_map/pallas_call | solution.py:151
  123.3 7.0 %shard_map.96 = (bf16[2,4,256,256]{3,2,1,0:T(8,128)(2,1)}, bf16[2,4,256,256]{3,2,1,0:T(8,128)(2,1)}) custom-call(s32[10]{0:T(128)} %pad_add_fusion.places, bf16[4,3,64,352]{3,2,1,0:T(8,128)(2,1)} %copy-done.1, bf16[4,3,64,352]{3,2,1,0:T(8,128)(2,1)} %copy-done.4, bf16[4,3,64,352]{3,2,1,0:T(8,128)(2,1)} %collective-permute-done.4.refs_2_, ...), custom_call_target="tpu_custom_call" | custom-call | tf_op jit(solution)/shard_map/pallas_call | solution.py:220
  130.4 14.4 %collective-permute-start.14 = (bf16[2,4,256,256]{3,2,1,0:T(8,128)(2,1)}, bf16[2,4,256,256]{3,2,1,0:T(8,128)(2,1)S(1)}, u32[]{:S(2)}, u32[]{:S(2)}) collective-permute-start(bf16[2,4,256,256]{3,2,1,0:T(8,128)(2,1)} %get-tuple-element.14), channel_id=1, source_target_pairs={{0,1},{1,0},{2,3},{3,2},{4,5},{5,4},{6,7},{7,6},{8,9},{9,8},{10,11... | collective-permute-start | bytes 3145736 | tf_op jit(solution)/shard_map/ppermute | solution.py:33
  144.8 23.0 %all_to_all.20 = f32[12,3,352]{2,1,0:T(4,128)S(1)} all-to-all(f32[12,3,352]{2,1,0:T(4,128)S(1)} %broadcast_in_dim.27), channel_id=1, replica_groups=mesh['rep'=3,'zk'=2,'zp'=2,'y'=8,'x'=4,'core'=2] {'rep','zk','zp'}, dimensions={0} | all-to-all | bytes 101376 | tf_op jit(solution)/shard_map/all_to_all | solution.py:38
  167.8 0.1 broadcast_in_dim.28
  167.9 0.7 broadcast_in_dim.29
  168.6 4.7 %all-to-all-start.3 = ((f32[8,3,704]{2,1,0:T(4,128)}), f32[8,3,704]{2,1,0:T(4,128)S(1)}, u32[]{:S(2)}, u32[]{:S(2)}) async-start(f32[8,3,704]{2,1,0:T(4,128)} %broadcast_in_dim.29), calls=%async_computation.3 | async-start | bytes 196608 | tf_op jit(solution)/shard_map/all_to_all | solution.py:38
  173.3 2.5 %add_convert_fusion = bf16[2,4,256,256]{3,2,1,0:T(8,128)(2,1)} fusion(bf16[2,4,256,256]{3,2,1,0:T(8,128)(2,1)S(1)} %collective-permute-done.14, bf16[2,4,256,256]{3,2,1,0:T(8,128)(2,1)} %get-tuple-element.13), kind=kLoop, calls=%fused_computation | loop fusion | flops 2097152 | bytes 3145728 | tf_op jit(solution)/shard_map/convert_element_type | solution.py:285
  175.7 5.2 %all-to-all-done.3 = f32[8,3,704]{2,1,0:T(4,128)S(1)} async-done(((f32[8,3,704]{2,1,0:T(4,128)}), f32[8,3,704]{2,1,0:T(4,128)S(1)}, u32[]{:S(2)}, u32[]{:S(2)}) %all-to-all-start.3) | async-done | bytes 67616 | tf_op jit(solution)/shard_map/all_to_all | solution.py:38
  181.0 5.4 %all-to-all-start.1 = ((bf16[8,256,256]{2,1,0:T(8,128)(2,1)}), bf16[8,256,256]{2,1,0:T(8,128)(2,1)S(1)}, u32[]{:S(2)}, u32[]{:S(2)}) async-start(bf16[8,256,256]{2,1,0:T(8,128)(2,1)} %bitcast.11), calls=%async_computation.1 | async-start | bytes 2097152 | tf_op jit(solution)/shard_map/all_to_all | solution.py:288
  186.4 4.6 %collective-permute-start.15 = (f32[1,3,704]{2,1,0:T(4,128)S(1)}, f32[1,3,704]{2,1,0:T(4,128)S(1)}, u32[]{:S(2)}, u32[]{:S(2)}) collective-permute-start(f32[1,3,704]{2,1,0:T(4,128)S(1)} %bitcast.32), channel_id=1, source_target_pairs={{0,1},{1,0},{2,3},{3,2},{4,5},{5,4},{6,7},{7,6},{8,9},{9,8},{10,11... | collective-permute-start | bytes 25352 | tf_op jit(solution)/shard_map/ppermute | solution.py:33
  191.1 0.8 collective-permute-done.15
  191.9 3.6 %collective-permute-start.16 = (f32[2,3,704]{2,1,0:T(4,128)S(1)}, f32[2,3,704]{2,1,0:T(4,128)S(1)}, u32[]{:S(2)}, u32[]{:S(2)}) collective-permute-start(f32[2,3,704]{2,1,0:T(4,128)S(1)} %pad_maximum_fusion.5), channel_id=1, source_target_pairs={{0,2},{2,0},{4,6},{6,4},{1,3},{3,1},{5,7},{7,5},{8,10},{10,8},{12,... | collective-permute-start | bytes 50696 | tf_op jit(solution)/shard_map/ppermute | solution.py:33
  195.6 4.5 %collective-permute-done.16 = f32[2,3,704]{2,1,0:T(4,128)S(1)} collective-permute-done((f32[2,3,704]{2,1,0:T(4,128)S(1)}, f32[2,3,704]{2,1,0:T(4,128)S(1)}, u32[]{:S(2)}, u32[]{:S(2)}) %collective-permute-start.16) | collective-permute-done | bytes 16928 | tf_op jit(solution)/shard_map/ppermute | solution.py:33
  200.1 4.3 %collective-permute-start.17 = (f32[4,3,704]{2,1,0:T(4,128)S(1)}, f32[4,3,704]{2,1,0:T(4,128)S(1)}, u32[]{:S(2)}, u32[]{:S(2)}) collective-permute-start(f32[4,3,704]{2,1,0:T(4,128)S(1)} %pad_maximum_fusion.4), channel_id=1, source_target_pairs={{0,4},{2,6},{4,0},{6,2},{1,5},{3,7},{5,1},{7,3},{8,12},{10,14},{12... | collective-permute-start | bytes 101384 | tf_op jit(solution)/shard_map/ppermute | solution.py:33
  204.4 2.0 collective-permute-done.17
  206.5 0.7 reshape.26
  207.3 0.8 reduce_sum.30
  (64 shorter events, 0.6 us)
Async XLA Ops:
  0.6 10.0 %copy-start.9 = (bf16[256,256]{1,0:T(8,128)(2,1)S(1)}, bf16[256,256]{1,0:T(8,128)(2,1)}, u32[]{:S(2)}) copy-start(bf16[256,256]{1,0:T(8,128)(2,1)} %param.8) | copy-start | bytes 393220
  2.6 9.8 %copy-start.5 = (bf16[256,704]{1,0:T(8,128)(2,1)}, bf16[256,704]{1,0:T(8,128)(2,1)S(1)}, u32[]{:S(2)}) copy-start(bf16[256,704]{1,0:T(8,128)(2,1)S(1)} %copy.37) | copy-start | bytes 1081348
  3.9 8.4 %copy-start.6 = (bf16[256,704]{1,0:T(8,128)(2,1)}, bf16[256,704]{1,0:T(8,128)(2,1)S(1)}, u32[]{:S(2)}) copy-start(bf16[256,704]{1,0:T(8,128)(2,1)S(1)} %copy.36) | copy-start | bytes 1081348
  3.9 6.1 %collective-permute-start.12 = (bf16[4,704]{1,0:T(4,128)(2,1)S(1)}, bf16[4,704]{1,0:T(4,128)(2,1)S(1)}, u32[]{:S(2)}, u32[]{:S(2)}) collective-permute-start(bf16[4,704]{1,0:T(4,128)(2,1)S(1)} %fusion.10), channel_id=1, source_target_pairs={{8,0},{16,8},{24,16},{32,24},{40,32},{48,40},{56,48},{64,56},{72,6... | collective-permute-start | bytes 16904 | tf_op jit(solution)/shard_map/ppermute | solution.py:29
  5.3 5.4 %collective-permute-start.11 = (bf16[4,704]{1,0:T(4,128)(2,1)S(1)}, bf16[4,704]{1,0:T(4,128)(2,1)S(1)}, u32[]{:S(2)}, u32[]{:S(2)}) collective-permute-start(bf16[4,704]{1,0:T(4,128)(2,1)S(1)} %fusion.9), channel_id=1, source_target_pairs={{0,8},{8,16},{16,24},{24,32},{32,40},{40,48},{48,56},{56,64},{64,7... | collective-permute-start | bytes 16904 | tf_op jit(solution)/shard_map/ppermute | solution.py:29
  12.3 14.6 %copy-start.10 = (bf16[704,64]{0,1:T(8,128)(2,1)S(1)}, bf16[704,64]{0,1:T(8,128)(2,1)}, u32[]{:S(2)}) copy-start(bf16[704,64]{0,1:T(8,128)(2,1)} %param.14) | copy-start | bytes 270340
  12.3 14.6 %copy-start.11 = (bf16[64,704]{1,0:T(8,128)(2,1)S(1)}, bf16[64,704]{1,0:T(8,128)(2,1)}, u32[]{:S(2)}) copy-start(bf16[64,704]{1,0:T(8,128)(2,1)} %param.13) | copy-start | bytes 270340
  12.3 14.6 %copy-start.12 = (bf16[64,704]{1,0:T(8,128)(2,1)S(1)}, bf16[64,704]{1,0:T(8,128)(2,1)}, u32[]{:S(2)}) copy-start(bf16[64,704]{1,0:T(8,128)(2,1)} %param.12) | copy-start | bytes 270340
  12.3 103.0 %all-to-all-start = ((bf16[16,264,256]{2,1,0:T(8,128)(2,1)}), bf16[16,264,256]{2,1,0:T(8,128)(2,1)S(1)}, u32[]{:S(2)}, u32[]{:S(2)}) async-start(bf16[16,264,256]{2,1,0:T(8,128)(2,1)} %broadcast_in_dim.26), calls=%async_computation | async-start | bytes 4325376 | tf_op jit(solution)/shard_map/all_to_all | solution.py:38
  27.1 19.4 %collective-permute-start.1 = (bf16[3,64,352]{2,1,0:T(8,128)(2,1)S(1)}, bf16[3,64,352]{2,1,0:T(8,128)(2,1)S(1)}, u32[]{:S(2)}, u32[]{:S(2)}) collective-permute-start(bf16[3,64,352]{2,1,0:T(8,128)(2,1)S(1)} %get-tuple-element.40), channel_id=1, source_target_pairs={{0,128},{1,641},{64,192},{65,705},{128,256},{129,1},{192,320},{193... | collective-permute-start | bytes 405512 | tf_op jit(solution)/shard_map/ppermute | solution.py:57
  40.0 16.3 %collective-permute-start.2 = (bf16[3,64,352]{2,1,0:T(8,128)(2,1)S(1)}, bf16[3,64,352]{2,1,0:T(8,128)(2,1)S(1)}, u32[]{:S(2)}, u32[]{:S(2)}) collective-permute-start(bf16[3,64,352]{2,1,0:T(8,128)(2,1)S(1)} %get-tuple-element.39), channel_id=1, source_target_pairs={{0,64},{64,128},{128,192},{192,256},{256,320},{320,384},{384,448},... | collective-permute-start | bytes 405512 | tf_op jit(solution)/shard_map/ppermute | solution.py:23
  43.2 17.1 %collective-permute-start = (bf16[3,64,352]{2,1,0:T(8,128)(2,1)S(1)}, bf16[3,64,352]{2,1,0:T(8,128)(2,1)S(1)}, u32[]{:S(2)}, u32[]{:S(2)}) collective-permute-start(bf16[3,64,352]{2,1,0:T(8,128)(2,1)S(1)} %get-tuple-element.39), channel_id=1, source_target_pairs={{0,704},{64,0},{128,64},{192,128},{256,192},{320,256},{384,320},{4... | collective-permute-start | bytes 405512 | tf_op jit(solution)/shard_map/ppermute | solution.py:23
  60.6 8.2 %copy-start.1 = (bf16[4,3,64,352]{3,2,1,0:T(8,128)(2,1)}, bf16[4,3,64,352]{3,2,1,0:T(8,128)(2,1)S(1)}, u32[]{:S(2)}) copy-start(bf16[4,3,64,352]{3,2,1,0:T(8,128)(2,1)S(1)} %pad_maximum_fusion.2.refs_0_) | copy-start | bytes 1622020
  60.6 11.2 %collective-permute-start.3 = (bf16[4,3,64,352]{3,2,1,0:T(8,128)(2,1)S(1)}, bf16[4,3,64,352]{3,2,1,0:T(8,128)(2,1)S(1)}, u32[]{:S(2)}, u32[]{:S(2)}) collective-permute-start(bf16[4,3,64,352]{3,2,1,0:T(8,128)(2,1)S(1)} %pad_maximum_fusion.2.refs_0_), channel_id=1, source_target_pairs={{0,8},{1,57},{8,16},{9,1},{16,24},{17,9},{24,32},{25,17},{32,40},{... | collective-permute-start | bytes 1622024 | tf_op jit(solution)/shard_map/ppermute | solution.py:57
  62.6 11.9 %collective-permute-start.4 = (bf16[4,3,64,352]{3,2,1,0:T(8,128)(2,1)S(1)}, bf16[4,3,64,352]{3,2,1,0:T(8,128)(2,1)}, u32[]{:S(2)}, u32[]{:S(2)}) collective-permute-start(bf16[4,3,64,352]{3,2,1,0:T(8,128)(2,1)S(1)} %pad_maximum_fusion.2.refs_0_), channel_id=1, source_target_pairs={{0,56},{1,9},{8,0},{9,17},{16,8},{17,25},{24,16},{25,33},{32,24},{... | collective-permute-start | bytes 1622024 | tf_op jit(solution)/shard_map/ppermute | solution.py:57
  66.5 14.3 %copy-start.15 = (s32[9]{0:T(128)S(1)}, s32[9]{0:T(128)}, u32[]{:S(2)}) copy-start(s32[9]{0:T(128)} %constant.89.clone) | copy-start | bytes 112
  68.8 13.5 %collective-permute-start.13 = (bf16[520,352]{1,0:T(8,128)(2,1)}, bf16[520,352]{1,0:T(8,128)(2,1)}, u32[]{:S(2)}, u32[]{:S(2)}) collective-permute-start(bf16[520,352]{1,0:T(8,128)(2,1)} %get-tuple-element.29), channel_id=1, source_target_pairs={{0,64},{64,0},{1,65},{65,1},{2,66},{66,2},{3,67},{67,3},{4,68},{68... | collective-permute-start | bytes 1098248 | tf_op jit(solution)/shard_map/ppermute | solution.py:33
  71.8 18.7 %copy-start.4 = (bf16[4,3,64,352]{3,2,1,0:T(8,128)(2,1)}, bf16[4,3,64,352]{3,2,1,0:T(8,128)(2,1)S(1)}, u32[]{:S(2)}) copy-start(bf16[4,3,64,352]{3,2,1,0:T(8,128)(2,1)S(1)} %collective-permute-done.3.refs_1_) | copy-start | bytes 1622020
  71.8 16.7 %collective-permute-start.5 = (bf16[4,3,64,352]{3,2,1,0:T(8,128)(2,1)S(1)}, bf16[4,3,64,352]{3,2,1,0:T(8,128)(2,1)}, u32[]{:S(2)}, u32[]{:S(2)}) collective-permute-start(bf16[4,3,64,352]{3,2,1,0:T(8,128)(2,1)S(1)} %collective-permute-done.3.refs_1_), channel_id=1, source_target_pairs={{0,8},{1,57},{8,16},{9,1},{16,24},{17,9},{24,32},{25,17},{32,40},{... | collective-permute-start | bytes 1622024 | tf_op jit(solution)/shard_map/ppermute | solution.py:57
  74.5 16.0 %collective-permute-start.6 = (bf16[4,3,64,352]{3,2,1,0:T(8,128)(2,1)}, bf16[4,3,64,352]{3,2,1,0:T(8,128)(2,1)}, u32[]{:S(2)}, u32[]{:S(2)}) collective-permute-start(bf16[4,3,64,352]{3,2,1,0:T(8,128)(2,1)} %collective-permute-done.4.refs_2_), channel_id=1, source_target_pairs={{0,56},{1,9},{8,0},{9,17},{16,8},{17,25},{24,16},{25,33},{32,24},{... | collective-permute-start | bytes 1622024 | tf_op jit(solution)/shard_map/ppermute | solution.py:57
  82.3 14.9 %copy-start.13 = (f32[3,352]{1,0:T(4,128)}, f32[3,352]{1,0:T(4,128)S(1)}, u32[]{:S(2)}) copy-start(f32[3,352]{1,0:T(4,128)S(1)} %dynamic-slice_convert_fusion.refs_13_) | copy-start | bytes 12676
  88.5 16.1 %collective-permute-start.7 = (bf16[4,3,64,352]{3,2,1,0:T(8,128)(2,1)}, bf16[4,3,64,352]{3,2,1,0:T(8,128)(2,1)S(1)}, u32[]{:S(2)}, u32[]{:S(2)}) collective-permute-start(bf16[4,3,64,352]{3,2,1,0:T(8,128)(2,1)} %collective-permute-done.5.refs_3_), channel_id=1, source_target_pairs={{0,8},{1,57},{8,16},{9,1},{16,24},{17,9},{24,32},{25,17},{32,40},{... | collective-permute-start | bytes 1622024 | tf_op jit(solution)/shard_map/ppermute | solution.py:57
  90.5 16.1 %collective-permute-start.8 = (bf16[4,3,64,352]{3,2,1,0:T(8,128)(2,1)}, bf16[4,3,64,352]{3,2,1,0:T(8,128)(2,1)S(1)}, u32[]{:S(2)}, u32[]{:S(2)}) collective-permute-start(bf16[4,3,64,352]{3,2,1,0:T(8,128)(2,1)} %collective-permute-done.6.refs_4_), channel_id=1, source_target_pairs={{0,56},{1,9},{8,0},{9,17},{16,8},{17,25},{24,16},{25,33},{32,24},{... | collective-permute-start | bytes 1622024 | tf_op jit(solution)/shard_map/ppermute | solution.py:57
  104.6 6.1 %copy-start.2 = (bf16[4,3,64,352]{3,2,1,0:T(8,128)(2,1)}, bf16[4,3,64,352]{3,2,1,0:T(8,128)(2,1)S(1)}, u32[]{:S(2)}) copy-start(bf16[4,3,64,352]{3,2,1,0:T(8,128)(2,1)S(1)} %collective-permute-done.7.refs_5_) | copy-start | bytes 1622020
  104.7 8.4 %collective-permute-start.9 = (bf16[2,3,64,352]{3,2,1,0:T(8,128)(2,1)S(1)}, bf16[2,3,64,352]{3,2,1,0:T(8,128)(2,1)S(1)}, u32[]{:S(2)}, u32[]{:S(2)}) collective-permute-start(bf16[2,3,64,352]{3,2,1,0:T(8,128)(2,1)S(1)} %slice.107), channel_id=1, source_target_pairs={{0,8},{1,57},{8,16},{9,1},{16,24},{17,9},{24,32},{25,17},{32,40},{... | collective-permute-start | bytes 811016 | tf_op jit(solution)/shard_map/ppermute | solution.py:57
  106.6 4.1 %copy-start.3 = (bf16[4,3,64,352]{3,2,1,0:T(8,128)(2,1)}, bf16[4,3,64,352]{3,2,1,0:T(8,128)(2,1)S(1)}, u32[]{:S(2)}) copy-start(bf16[4,3,64,352]{3,2,1,0:T(8,128)(2,1)S(1)} %collective-permute-done.8.refs_6_) | copy-start | bytes 1622020
  106.7 8.7 %collective-permute-start.10 = (bf16[2,3,64,352]{3,2,1,0:T(8,128)(2,1)S(1)}, bf16[2,3,64,352]{3,2,1,0:T(8,128)(2,1)S(1)}, u32[]{:S(2)}, u32[]{:S(2)}) collective-permute-start(bf16[2,3,64,352]{3,2,1,0:T(8,128)(2,1)S(1)} %slice.108), channel_id=1, source_target_pairs={{0,56},{1,9},{8,0},{9,17},{16,8},{17,25},{24,16},{25,33},{32,24},{... | collective-permute-start | bytes 811016 | tf_op jit(solution)/shard_map/ppermute | solution.py:57
  113.1 2.2 %copy-start.7 = (bf16[2,3,64,352]{3,2,1,0:T(8,128)(2,1)}, bf16[2,3,64,352]{3,2,1,0:T(8,128)(2,1)S(1)}, u32[]{:S(2)}) copy-start(bf16[2,3,64,352]{3,2,1,0:T(8,128)(2,1)S(1)} %collective-permute-done.9.refs_7_) | copy-start | bytes 811012
  115.3 0.7 copy-start.8
  116.1 1.4 copy-start
  123.3 21.4 %copy-start.14 = (f32[3,352]{1,0:T(4,128)S(1)}, f32[3,352]{1,0:T(4,128)}, u32[]{:S(2)}) copy-start(f32[3,352]{1,0:T(4,128)} %get-tuple-element.15) | copy-start | bytes 12676
  130.4 42.9 %collective-permute-start.14 = (bf16[2,4,256,256]{3,2,1,0:T(8,128)(2,1)}, bf16[2,4,256,256]{3,2,1,0:T(8,128)(2,1)S(1)}, u32[]{:S(2)}, u32[]{:S(2)}) collective-permute-start(bf16[2,4,256,256]{3,2,1,0:T(8,128)(2,1)} %get-tuple-element.14), channel_id=1, source_target_pairs={{0,1},{1,0},{2,3},{3,2},{4,5},{5,4},{6,7},{7,6},{8,9},{9,8},{10,11... | collective-permute-start | bytes 3145736 | tf_op jit(solution)/shard_map/ppermute | solution.py:33
  168.6 12.4 %all-to-all-start.3 = ((f32[8,3,704]{2,1,0:T(4,128)}), f32[8,3,704]{2,1,0:T(4,128)S(1)}, u32[]{:S(2)}, u32[]{:S(2)}) async-start(f32[8,3,704]{2,1,0:T(4,128)} %broadcast_in_dim.29), calls=%async_computation.3 | async-start | bytes 196608 | tf_op jit(solution)/shard_map/all_to_all | solution.py:38
  181.0 26.3 %all-to-all-start.1 = ((bf16[8,256,256]{2,1,0:T(8,128)(2,1)}), bf16[8,256,256]{2,1,0:T(8,128)(2,1)S(1)}, u32[]{:S(2)}, u32[]{:S(2)}) async-start(bf16[8,256,256]{2,1,0:T(8,128)(2,1)} %bitcast.11), calls=%async_computation.1 | async-start | bytes 2097152 | tf_op jit(solution)/shard_map/all_to_all | solution.py:288
  186.4 5.4 %collective-permute-start.15 = (f32[1,3,704]{2,1,0:T(4,128)S(1)}, f32[1,3,704]{2,1,0:T(4,128)S(1)}, u32[]{:S(2)}, u32[]{:S(2)}) collective-permute-start(f32[1,3,704]{2,1,0:T(4,128)S(1)} %bitcast.32), channel_id=1, source_target_pairs={{0,1},{1,0},{2,3},{3,2},{4,5},{5,4},{6,7},{7,6},{8,9},{9,8},{10,11... | collective-permute-start | bytes 25352 | tf_op jit(solution)/shard_map/ppermute | solution.py:33
  191.9 8.2 %collective-permute-start.16 = (f32[2,3,704]{2,1,0:T(4,128)S(1)}, f32[2,3,704]{2,1,0:T(4,128)S(1)}, u32[]{:S(2)}, u32[]{:S(2)}) collective-permute-start(f32[2,3,704]{2,1,0:T(4,128)S(1)} %pad_maximum_fusion.5), channel_id=1, source_target_pairs={{0,2},{2,0},{4,6},{6,4},{1,3},{3,1},{5,7},{7,5},{8,10},{10,8},{12,... | collective-permute-start | bytes 50696 | tf_op jit(solution)/shard_map/ppermute | solution.py:33
  200.1 6.3 %collective-permute-start.17 = (f32[4,3,704]{2,1,0:T(4,128)S(1)}, f32[4,3,704]{2,1,0:T(4,128)S(1)}, u32[]{:S(2)}, u32[]{:S(2)}) collective-permute-start(f32[4,3,704]{2,1,0:T(4,128)S(1)} %pad_maximum_fusion.4), channel_id=1, source_target_pairs={{0,4},{2,6},{4,0},{6,2},{1,5},{3,7},{5,1},{7,3},{8,12},{10,14},{12... | collective-permute-start | bytes 101384 | tf_op jit(solution)/shard_map/ppermute | solution.py:33

commit v6 on v5

--- a/solution.py
+++ b/solution.py
@@ -69,13 +69,12 @@
     pieces, steps = [block], [0]
     one = two = block
     for k in range(1, 4):
-        one, two = crossed(one, "y", 1), crossed(two, "y", -1)
+        one, two = shifted(one, "y", 1), shifted(two, "y", -1)
         pieces += [one, two]
         steps += [-k, k]
-    pieces += [crossed(one[:mid], "y", 1), crossed(two[mid:], "y", -1)]
-    sign = 1 - 2 * lax.axis_index("core")
+    pieces += [shifted(one[:mid], "y", 1), shifted(two[mid:], "y", -1)]
     count = lax.axis_size("y")
-    places = (lax.axis_index("y") + sign * jnp.array(steps + [4, 4], jnp.int32)) % count
+    places = (lax.axis_index("y") + jnp.array(steps + [4, 4], jnp.int32)) % count
     places = jnp.append(places, lax.axis_index("core"))
     return pieces, places.astype(jnp.int32), pieces[3]
 
@@ -289,11 +288,7 @@
         product.reshape(-1, rows, width), ("zp", "x"), 0, 0, tiled=True
     )
     input_grad = arrived.astype(jnp.float32).sum(axis=0).astype(jnp.bfloat16)
-    conv = conv[None]
-    for axis, bit in (("core", 1), ("x", 1), ("x", 2)):
-        low = lax.axis_index(axis) & bit == 0
-        peer = swapped(conv, axis, bit)
-        conv = jnp.concatenate([jnp.where(low, conv, peer), jnp.where(low, peer, conv)])
+    conv = lax.all_gather(conv, TP)
     conv_grad = conv.transpose(1, 0, 2).reshape(3, -1)
     return (input_grad, conv_grad)
 

time: 210 us -> 212 us (level)
  blocking collectives: 23 us -> 39.2 us
  starting transfers between devices: 106 us -> 95.4 us
  waiting for transfers between devices: 43.5 us -> 40.6 us
    ppermute x9 -> x1, starting transfers between devices: 40 us -> 12.8 us  [crossed(): return lax.ppermute(value, (*names, 'core'), pairs)]
    ppermute x2 -> x10, starting transfers between devices: 6.49 us -> 33 us  [shifted(): lax.ppermute(value, axis, [(i, (i + by) % count) for i in range(count)])]
    all_gather x0 -> x1, blocking collectives: none -> 23.1 us  [block_gradients(): conv = lax.all_gather(conv, TP)]
    ppermute x2 -> x10, waiting for transfers between devices: 13.8 us -> 34.7 us  [shifted(): lax.ppermute(value, axis, [(i, (i + by) % count) for i in range(count)])]
    ppermute x9 -> x1, waiting for transfers between devices: 16.5 us -> 0.01 us  [crossed(): return lax.ppermute(value, (*names, 'core'), pairs)]
    ppermute x5 -> x2, starting transfers between devices: 28.9 us -> 18 us  [swapped(): lax.ppermute(value, axis, [(i, i ^ bit) for i in range(lax.axis_size(axis...]
    ppermute x5 -> x2, waiting for transfers between devices: 7.35 us -> 0.01 us  [swapped(): lax.ppermute(value, axis, [(i, i ^ bit) for i in range(lax.axis_size(axis...]
    all_to_all x1, blocking collectives: 23 us -> 16.1 us  [sent_to_all(): lax.all_to_all(jnp.broadcast_to(value[None], (peers, *value.shape)), axis...]
  transfers between devices with their start and end apart: 21 -> 18, of which waited for: 13 -> 11; matrix products, arithmetic and copies ran while one was open for 6% -> 6% of each run, Pallas kernels for 0% -> 0%
where the time goes in v6:
time: 212 us; the launch traced here: 210 us
  starting transfers between devices  95.4 us (45%)
  waiting for transfers between devices  40.6 us (19%)
  blocking collectives  39.2 us (18%)
  Pallas kernels  12.9 us (6%)
  local copies, waits for them, and re-layouts  11.6 us (5%)
  other arithmetic  9.59 us (5%)
    ppermute x10, waiting for transfers between devices, shifted(): lax.ppermute(value, axis, [(i, (i + by) % count) for i in range(count)])  34.7 us
    ppermute x10, starting transfers between devices, shifted(): lax.ppermute(value, axis, [(i, (i + by) % count) for i in range(count)])  33 us
    all_gather x1, blocking collectives, block_gradients(): conv = lax.all_gather(conv, TP)  23.1 us
    all_to_all x2, starting transfers between devices, sent_to_all(): lax.all_to_all(jnp.broadcast_to(value[None], (peers, *value.shape)), axis...  19.3 us
    ppermute x2, starting transfers between devices, swapped(): lax.ppermute(value, axis, [(i, i ^ bit) for i in range(lax.axis_size(axis...  18 us
    all_to_all x1, blocking collectives, sent_to_all(): lax.all_to_all(jnp.broadcast_to(value[None], (peers, *value.shape)), axis...  16.1 us
    ppermute x1, starting transfers between devices, crossed(): return lax.ppermute(value, (*names, 'core'), pairs)  12.8 us
    pallas_call x1, Pallas kernels, output_partials(): pl.pallas_call(output_kernel, grid_spec=pltpu.PrefetchScalarGridSpec(num_...  7.05 us
  transfers between devices with their start and end apart: 18, of which 11 were waited for; matrix products, arithmetic and copies ran while one was open for 6% of the time, Pallas kernels for 0%

profile of v6, /device:TPU:1, one launch (start us, length us, event | category | flops | bytes accessed | tf_op | source)
XLA Modules:
  0.0 210.4 jit_solution(7967133267262749303)
XLA Ops:
  0.6 0.8 fusion.16
  1.4 1.2 copy.51
  2.6 1.3 copy.50
  3.9 1.3 collective-permute-start.12
  5.3 4.6 %collective-permute-start.11 = (bf16[4,704]{1,0:T(4,128)(2,1)S(1)}, bf16[4,704]{1,0:T(4,128)(2,1)S(1)}, u32[]{:S(2)}, u32[]{:S(2)}) collective-permute-start(bf16[4,704]{1,0:T(4,128)(2,1)S(1)} %fusion.9), channel_id=1, source_target_pairs={{0,8},{8,16},{16,24},{24,32},{32,40},{40,48},{48,56},{56,64},{64,7... | collective-permute-start | bytes 16904 | tf_op jit(solution)/shard_map/ppermute | solution.py:29
  9.9 0.1 pad.42.clone
  10.0 0.0 collective-permute-done.12
  10.0 0.7 collective-permute-done.11
  10.7 0.1 maximum_maximum_fusion
  10.8 1.5 broadcast_in_dim.11
  12.3 14.6 %all-to-all-start = ((bf16[16,264,256]{2,1,0:T(8,128)(2,1)}), bf16[16,264,256]{2,1,0:T(8,128)(2,1)S(1)}, u32[]{:S(2)}, u32[]{:S(2)}) async-start(bf16[16,264,256]{2,1,0:T(8,128)(2,1)} %broadcast_in_dim.11), calls=%async_computation | async-start | bytes 4325376 | tf_op jit(solution)/shard_map/all_to_all | solution.py:38
  27.0 0.1 broadcast_select_fusion.2
  27.1 12.8 %collective-permute-start.1 = (bf16[3,64,352]{2,1,0:T(8,128)(2,1)S(1)}, bf16[3,64,352]{2,1,0:T(8,128)(2,1)S(1)}, u32[]{:S(2)}, u32[]{:S(2)}) collective-permute-start(bf16[3,64,352]{2,1,0:T(8,128)(2,1)S(1)} %get-tuple-element.40), channel_id=1, source_target_pairs={{0,128},{1,641},{64,192},{65,705},{128,256},{129,1},{192,320},{193... | collective-permute-start | bytes 405512 | tf_op jit(solution)/shard_map/ppermute | solution.py:57
  40.0 3.3 %collective-permute-start.2 = (bf16[3,64,352]{2,1,0:T(8,128)(2,1)S(1)}, bf16[3,64,352]{2,1,0:T(8,128)(2,1)S(1)}, u32[]{:S(2)}, u32[]{:S(2)}) collective-permute-start(bf16[3,64,352]{2,1,0:T(8,128)(2,1)S(1)} %get-tuple-element.39), channel_id=1, source_target_pairs={{0,64},{64,128},{128,192},{192,256},{256,320},{320,384},{384,448},... | collective-permute-start | bytes 405512 | tf_op jit(solution)/shard_map/ppermute | solution.py:23
  43.2 3.2 %collective-permute-start = (bf16[3,64,352]{2,1,0:T(8,128)(2,1)S(1)}, bf16[3,64,352]{2,1,0:T(8,128)(2,1)S(1)}, u32[]{:S(2)}, u32[]{:S(2)}) collective-permute-start(bf16[3,64,352]{2,1,0:T(8,128)(2,1)S(1)} %get-tuple-element.39), channel_id=1, source_target_pairs={{0,704},{64,0},{128,64},{192,128},{256,192},{320,256},{384,320},{4... | collective-permute-start | bytes 405512 | tf_op jit(solution)/shard_map/ppermute | solution.py:23
  46.6 9.7 %collective-permute-done.2 = bf16[3,64,352]{2,1,0:T(8,128)(2,1)S(1)} collective-permute-done((bf16[3,64,352]{2,1,0:T(8,128)(2,1)S(1)}, bf16[3,64,352]{2,1,0:T(8,128)(2,1)S(1)}, u32[]{:S(2)}, u32[]{:S(2)}) %collective-permute-start.2) | collective-permute-done | bytes 135200 | tf_op jit(solution)/shard_map/ppermute | solution.py:23
  56.3 4.1 %collective-permute-done = bf16[3,64,352]{2,1,0:T(8,128)(2,1)S(1)} collective-permute-done((bf16[3,64,352]{2,1,0:T(8,128)(2,1)S(1)}, bf16[3,64,352]{2,1,0:T(8,128)(2,1)S(1)}, u32[]{:S(2)}, u32[]{:S(2)}) %collective-permute-start) | collective-permute-done | bytes 135200 | tf_op jit(solution)/shard_map/ppermute | solution.py:23
  60.3 0.1 select_bitcast_fusion.5
  60.5 0.1 pad_maximum_fusion.2.refs_0_
  60.6 3.9 %collective-permute-start.3 = (bf16[4,3,64,352]{3,2,1,0:T(8,128)(2,1)S(1)}, bf16[4,3,64,352]{3,2,1,0:T(8,128)(2,1)S(1)}, u32[]{:S(2)}, u32[]{:S(2)}) collective-permute-start(bf16[4,3,64,352]{3,2,1,0:T(8,128)(2,1)S(1)} %pad_maximum_fusion.2.refs_0_), channel_id=1, source_target_pairs={{0,8},{8,16},{16,24},{24,32},{32,40},{40,48},{48,56},{56,0},{1,9},... | collective-permute-start | bytes 1622024 | tf_op jit(solution)/shard_map/ppermute | solution.py:23
  64.5 2.6 %collective-permute-start.4 = (bf16[4,3,64,352]{3,2,1,0:T(8,128)(2,1)S(1)}, bf16[4,3,64,352]{3,2,1,0:T(8,128)(2,1)}, u32[]{:S(2)}, u32[]{:S(2)}) collective-permute-start(bf16[4,3,64,352]{3,2,1,0:T(8,128)(2,1)S(1)} %pad_maximum_fusion.2.refs_0_), channel_id=1, source_target_pairs={{0,56},{8,0},{16,8},{24,16},{32,24},{40,32},{48,40},{56,48},{1,57}... | collective-permute-start | bytes 1622024 | tf_op jit(solution)/shard_map/ppermute | solution.py:23
  67.1 0.0 copy-start.15
  67.1 1.2 pad_maximum_fusion.1
  68.3 1.1 broadcast_select_fusion
  69.4 2.2 %collective-permute-start.13 = (bf16[520,352]{1,0:T(8,128)(2,1)}, bf16[520,352]{1,0:T(8,128)(2,1)}, u32[]{:S(2)}, u32[]{:S(2)}) collective-permute-start(bf16[520,352]{1,0:T(8,128)(2,1)} %get-tuple-element.29), channel_id=1, source_target_pairs={{0,64},{64,0},{1,65},{65,1},{2,66},{66,2},{3,67},{67,3},{4,68},{68... | collective-permute-start | bytes 1098248 | tf_op jit(solution)/shard_map/ppermute | solution.py:33
  71.6 0.8 collective-permute-done.3.refs_1_
  72.5 2.7 %collective-permute-start.5 = (bf16[4,3,64,352]{3,2,1,0:T(8,128)(2,1)S(1)}, bf16[4,3,64,352]{3,2,1,0:T(8,128)(2,1)}, u32[]{:S(2)}, u32[]{:S(2)}) collective-permute-start(bf16[4,3,64,352]{3,2,1,0:T(8,128)(2,1)S(1)} %collective-permute-done.3.refs_1_), channel_id=1, source_target_pairs={{0,8},{8,16},{16,24},{24,32},{32,40},{40,48},{48,56},{56,0},{1,9},... | collective-permute-start | bytes 1622024 | tf_op jit(solution)/shard_map/ppermute | solution.py:23
  75.2 0.1 collective-permute-done.4.refs_2_
  75.3 3.8 %collective-permute-start.6 = (bf16[4,3,64,352]{3,2,1,0:T(8,128)(2,1)}, bf16[4,3,64,352]{3,2,1,0:T(8,128)(2,1)}, u32[]{:S(2)}, u32[]{:S(2)}) collective-permute-start(bf16[4,3,64,352]{3,2,1,0:T(8,128)(2,1)} %collective-permute-done.4.refs_2_), channel_id=1, source_target_pairs={{0,56},{8,0},{16,8},{24,16},{32,24},{40,32},{48,40},{56,48},{1,57}... | collective-permute-start | bytes 1622024 | tf_op jit(solution)/shard_map/ppermute | solution.py:23
  79.1 0.6 pad_add_fusion.places
  79.7 0.8 dynamic-slice_convert_fusion.refs_13_
  80.5 8.3 %collective-permute-done.5.refs_3_ = bf16[4,3,64,352]{3,2,1,0:T(8,128)(2,1)} collective-permute-done((bf16[4,3,64,352]{3,2,1,0:T(8,128)(2,1)S(1)}, bf16[4,3,64,352]{3,2,1,0:T(8,128)(2,1)}, u32[]{:S(2)}, u32[]{:S(2)}) %collective-permute-start.5) | collective-permute-done | bytes 540704 | tf_op jit(solution)/shard_map/ppermute | solution.py:23
  88.7 1.9 collective-permute-start.7
  90.6 4.8 %collective-permute-start.8 = (bf16[4,3,64,352]{3,2,1,0:T(8,128)(2,1)}, bf16[4,3,64,352]{3,2,1,0:T(8,128)(2,1)S(1)}, u32[]{:S(2)}, u32[]{:S(2)}) collective-permute-start(bf16[4,3,64,352]{3,2,1,0:T(8,128)(2,1)} %collective-permute-done.6.refs_4_), channel_id=1, source_target_pairs={{0,56},{8,0},{16,8},{24,16},{32,24},{40,32},{48,40},{56,48},{1,57}... | collective-permute-start | bytes 1622024 | tf_op jit(solution)/shard_map/ppermute | solution.py:23
  95.5 1.2 select_bitcast_fusion.1
  96.7 0.2 maximum_convert_fusion
  96.9 0.1 fusion.13
  97.0 0.1 pad_maximum_fusion
  97.1 1.0 pad.22.refs_12_
  98.0 7.8 %collective-permute-done.7.refs_5_ = bf16[4,3,64,352]{3,2,1,0:T(8,128)(2,1)S(1)} collective-permute-done((bf16[4,3,64,352]{3,2,1,0:T(8,128)(2,1)}, bf16[4,3,64,352]{3,2,1,0:T(8,128)(2,1)S(1)}, u32[]{:S(2)}, u32[]{:S(2)}) %collective-permute-start.7) | collective-permute-done | bytes 540704 | tf_op jit(solution)/shard_map/ppermute | solution.py:23
  105.9 1.9 collective-permute-start.9
  107.9 0.2 collective-permute-done.8.refs_6_
  108.1 4.9 %collective-permute-start.10 = (bf16[2,3,64,352]{3,2,1,0:T(8,128)(2,1)S(1)}, bf16[2,3,64,352]{3,2,1,0:T(8,128)(2,1)S(1)}, u32[]{:S(2)}, u32[]{:S(2)}) collective-permute-start(bf16[2,3,64,352]{3,2,1,0:T(8,128)(2,1)S(1)} %slice.108), channel_id=1, source_target_pairs={{0,56},{8,0},{16,8},{24,16},{32,24},{40,32},{48,40},{56,48},{1,57}... | collective-permute-start | bytes 811016 | tf_op jit(solution)/shard_map/ppermute | solution.py:23
  113.0 0.7 fusion.12
  113.7 1.0 pad.20.refs_10_
  114.7 0.9 pad.21.refs_11_
  115.6 2.2 %collective-permute-done.9.refs_7_ = bf16[2,3,64,352]{3,2,1,0:T(8,128)(2,1)S(1)} collective-permute-done((bf16[2,3,64,352]{3,2,1,0:T(8,128)(2,1)S(1)}, bf16[2,3,64,352]{3,2,1,0:T(8,128)(2,1)S(1)}, u32[]{:S(2)}, u32[]{:S(2)}) %collective-permute-start.9) | collective-permute-done | bytes 270368 | tf_op jit(solution)/shard_map/ppermute | solution.py:23
  117.8 1.5 collective-permute-done.10.refs_8_
  119.3 0.7 copy-done.8
  120.0 1.4 copy-done
  121.4 5.9 %shard_map.95 = (bf16[2,256,352]{2,1,0:T(8,128)(2,1)}, bf16[2,256,352]{2,1,0:T(8,128)(2,1)}, f32[3,352]{1,0:T(4,128)}) custom-call(s32[10]{0:T(128)} %pad_add_fusion.places, bf16[4,3,64,352]{3,2,1,0:T(8,128)(2,1)} %copy-done.1, bf16[4,3,64,352]{3,2,1,0:T(8,128)(2,1)} %copy-done.4, bf16[4,3,64,352]{3,2,1,0:T(8,128)(2,1)} %collective-permute-done.4.refs_2_, ...), custom_call_target="tpu_custom_call" | custom-call | tf_op jit(solution)/shard_map/pallas_call | solution.py:150
  127.2 0.0 copy-start.14
  127.3 7.1 %shard_map.96 = (bf16[2,4,256,256]{3,2,1,0:T(8,128)(2,1)}, bf16[2,4,256,256]{3,2,1,0:T(8,128)(2,1)}) custom-call(s32[10]{0:T(128)} %pad_add_fusion.places, bf16[4,3,64,352]{3,2,1,0:T(8,128)(2,1)} %copy-done.1, bf16[4,3,64,352]{3,2,1,0:T(8,128)(2,1)} %copy-done.4, bf16[4,3,64,352]{3,2,1,0:T(8,128)(2,1)} %collective-permute-done.4.refs_2_, ...), custom_call_target="tpu_custom_call" | custom-call | tf_op jit(solution)/shard_map/pallas_call | solution.py:219
  134.3 15.8 %collective-permute-start.14 = (bf16[2,4,256,256]{3,2,1,0:T(8,128)(2,1)}, bf16[2,4,256,256]{3,2,1,0:T(8,128)(2,1)S(1)}, u32[]{:S(2)}, u32[]{:S(2)}) collective-permute-start(bf16[2,4,256,256]{3,2,1,0:T(8,128)(2,1)} %get-tuple-element.14), channel_id=1, source_target_pairs={{0,1},{1,0},{2,3},{3,2},{4,5},{5,4},{6,7},{7,6},{8,9},{9,8},{10,11... | collective-permute-start | bytes 3145736 | tf_op jit(solution)/shard_map/ppermute | solution.py:33
  150.2 16.1 %all_to_all.20 = f32[12,3,352]{2,1,0:T(4,128)S(1)} all-to-all(f32[12,3,352]{2,1,0:T(4,128)S(1)} %broadcast_in_dim.24), channel_id=1, replica_groups=mesh['rep'=3,'zk'=2,'zp'=2,'y'=8,'x'=4,'core'=2] {'rep','zk','zp'}, dimensions={0} | all-to-all | bytes 101376 | tf_op jit(solution)/shard_map/all_to_all | solution.py:38
  166.4 0.1 broadcast_in_dim.25
  166.5 0.7 broadcast_in_dim.26
  167.1 4.7 %all-to-all-start.3 = ((f32[8,3,704]{2,1,0:T(4,128)}), f32[8,3,704]{2,1,0:T(4,128)S(1)}, u32[]{:S(2)}, u32[]{:S(2)}) async-start(f32[8,3,704]{2,1,0:T(4,128)} %broadcast_in_dim.26), calls=%async_computation.3 | async-start | bytes 196608 | tf_op jit(solution)/shard_map/all_to_all | solution.py:38
  171.8 2.4 %add_convert_fusion = bf16[2,4,256,256]{3,2,1,0:T(8,128)(2,1)} fusion(bf16[2,4,256,256]{3,2,1,0:T(8,128)(2,1)S(1)} %collective-permute-done.14, bf16[2,4,256,256]{3,2,1,0:T(8,128)(2,1)} %get-tuple-element.13), kind=kLoop, calls=%fused_computation | loop fusion | flops 2097152 | bytes 3145728 | tf_op jit(solution)/shard_map/convert_element_type | solution.py:284
  174.3 5.2 %all-to-all-done.3 = f32[8,3,704]{2,1,0:T(4,128)S(1)} async-done(((f32[8,3,704]{2,1,0:T(4,128)}), f32[8,3,704]{2,1,0:T(4,128)S(1)}, u32[]{:S(2)}, u32[]{:S(2)}) %all-to-all-start.3) | async-done | bytes 67616 | tf_op jit(solution)/shard_map/all_to_all | solution.py:38
  179.5 6.2 %all-to-all-start.1 = ((bf16[8,256,256]{2,1,0:T(8,128)(2,1)}), bf16[8,256,256]{2,1,0:T(8,128)(2,1)S(1)}, u32[]{:S(2)}, u32[]{:S(2)}) async-start(bf16[8,256,256]{2,1,0:T(8,128)(2,1)} %bitcast.11), calls=%async_computation.1 | async-start | bytes 2097152 | tf_op jit(solution)/shard_map/all_to_all | solution.py:287
  185.7 23.1 %all-gather.1 = f32[8,3,704]{2,1,0:T(4,128)S(1)} all-gather(f32[1,3,704]{2,1,0:T(4,128)S(1)} %bitcast.30), channel_id=2, replica_groups=mesh['rep'=3,'zk'=2,'zp'=2,'y'=8,'x'=4,'core'=2] {'x','core'}, dimensions={0}, use_global_device_ids=true | all-gather | bytes 76032 | tf_op jit(solution)/shard_map/all_gather | solution.py:291
  208.8 0.7 reshape.26
  209.5 0.8 reduce_sum.30
  (53 shorter events, 0.4 us)
Async XLA Ops:
  0.6 10.0 %copy-start.9 = (bf16[256,256]{1,0:T(8,128)(2,1)S(1)}, bf16[256,256]{1,0:T(8,128)(2,1)}, u32[]{:S(2)}) copy-start(bf16[256,256]{1,0:T(8,128)(2,1)} %param.8) | copy-start | bytes 393220
  2.6 9.7 %copy-start.5 = (bf16[256,704]{1,0:T(8,128)(2,1)}, bf16[256,704]{1,0:T(8,128)(2,1)S(1)}, u32[]{:S(2)}) copy-start(bf16[256,704]{1,0:T(8,128)(2,1)S(1)} %copy.51) | copy-start | bytes 1081348
  3.9 8.4 %copy-start.6 = (bf16[256,704]{1,0:T(8,128)(2,1)}, bf16[256,704]{1,0:T(8,128)(2,1)S(1)}, u32[]{:S(2)}) copy-start(bf16[256,704]{1,0:T(8,128)(2,1)S(1)} %copy.50) | copy-start | bytes 1081348
  3.9 6.1 %collective-permute-start.12 = (bf16[4,704]{1,0:T(4,128)(2,1)S(1)}, bf16[4,704]{1,0:T(4,128)(2,1)S(1)}, u32[]{:S(2)}, u32[]{:S(2)}) collective-permute-start(bf16[4,704]{1,0:T(4,128)(2,1)S(1)} %fusion.10), channel_id=1, source_target_pairs={{8,0},{16,8},{24,16},{32,24},{40,32},{48,40},{56,48},{64,56},{72,6... | collective-permute-start | bytes 16904 | tf_op jit(solution)/shard_map/ppermute | solution.py:29
  5.3 5.4 %collective-permute-start.11 = (bf16[4,704]{1,0:T(4,128)(2,1)S(1)}, bf16[4,704]{1,0:T(4,128)(2,1)S(1)}, u32[]{:S(2)}, u32[]{:S(2)}) collective-permute-start(bf16[4,704]{1,0:T(4,128)(2,1)S(1)} %fusion.9), channel_id=1, source_target_pairs={{0,8},{8,16},{16,24},{24,32},{32,40},{40,48},{48,56},{56,64},{64,7... | collective-permute-start | bytes 16904 | tf_op jit(solution)/shard_map/ppermute | solution.py:29
  12.3 14.6 %copy-start.10 = (bf16[704,64]{0,1:T(8,128)(2,1)S(1)}, bf16[704,64]{0,1:T(8,128)(2,1)}, u32[]{:S(2)}) copy-start(bf16[704,64]{0,1:T(8,128)(2,1)} %param.14) | copy-start | bytes 270340
  12.3 14.6 %copy-start.11 = (bf16[64,704]{1,0:T(8,128)(2,1)S(1)}, bf16[64,704]{1,0:T(8,128)(2,1)}, u32[]{:S(2)}) copy-start(bf16[64,704]{1,0:T(8,128)(2,1)} %param.13) | copy-start | bytes 270340
  12.3 14.6 %copy-start.12 = (bf16[64,704]{1,0:T(8,128)(2,1)S(1)}, bf16[64,704]{1,0:T(8,128)(2,1)}, u32[]{:S(2)}) copy-start(bf16[64,704]{1,0:T(8,128)(2,1)} %param.12) | copy-start | bytes 270340
  12.3 107.0 %all-to-all-start = ((bf16[16,264,256]{2,1,0:T(8,128)(2,1)}), bf16[16,264,256]{2,1,0:T(8,128)(2,1)S(1)}, u32[]{:S(2)}, u32[]{:S(2)}) async-start(bf16[16,264,256]{2,1,0:T(8,128)(2,1)} %broadcast_in_dim.11), calls=%async_computation | async-start | bytes 4325376 | tf_op jit(solution)/shard_map/all_to_all | solution.py:38
  27.1 19.5 %collective-permute-start.1 = (bf16[3,64,352]{2,1,0:T(8,128)(2,1)S(1)}, bf16[3,64,352]{2,1,0:T(8,128)(2,1)S(1)}, u32[]{:S(2)}, u32[]{:S(2)}) collective-permute-start(bf16[3,64,352]{2,1,0:T(8,128)(2,1)S(1)} %get-tuple-element.40), channel_id=1, source_target_pairs={{0,128},{1,641},{64,192},{65,705},{128,256},{129,1},{192,320},{193... | collective-permute-start | bytes 405512 | tf_op jit(solution)/shard_map/ppermute | solution.py:57
  40.0 16.3 %collective-permute-start.2 = (bf16[3,64,352]{2,1,0:T(8,128)(2,1)S(1)}, bf16[3,64,352]{2,1,0:T(8,128)(2,1)S(1)}, u32[]{:S(2)}, u32[]{:S(2)}) collective-permute-start(bf16[3,64,352]{2,1,0:T(8,128)(2,1)S(1)} %get-tuple-element.39), channel_id=1, source_target_pairs={{0,64},{64,128},{128,192},{192,256},{256,320},{320,384},{384,448},... | collective-permute-start | bytes 405512 | tf_op jit(solution)/shard_map/ppermute | solution.py:23
  43.2 17.1 %collective-permute-start = (bf16[3,64,352]{2,1,0:T(8,128)(2,1)S(1)}, bf16[3,64,352]{2,1,0:T(8,128)(2,1)S(1)}, u32[]{:S(2)}, u32[]{:S(2)}) collective-permute-start(bf16[3,64,352]{2,1,0:T(8,128)(2,1)S(1)} %get-tuple-element.39), channel_id=1, source_target_pairs={{0,704},{64,0},{128,64},{192,128},{256,192},{320,256},{384,320},{4... | collective-permute-start | bytes 405512 | tf_op jit(solution)/shard_map/ppermute | solution.py:23
  60.6 8.8 %copy-start.1 = (bf16[4,3,64,352]{3,2,1,0:T(8,128)(2,1)}, bf16[4,3,64,352]{3,2,1,0:T(8,128)(2,1)S(1)}, u32[]{:S(2)}) copy-start(bf16[4,3,64,352]{3,2,1,0:T(8,128)(2,1)S(1)} %pad_maximum_fusion.2.refs_0_) | copy-start | bytes 1622020
  60.6 11.8 %collective-permute-start.3 = (bf16[4,3,64,352]{3,2,1,0:T(8,128)(2,1)S(1)}, bf16[4,3,64,352]{3,2,1,0:T(8,128)(2,1)S(1)}, u32[]{:S(2)}, u32[]{:S(2)}) collective-permute-start(bf16[4,3,64,352]{3,2,1,0:T(8,128)(2,1)S(1)} %pad_maximum_fusion.2.refs_0_), channel_id=1, source_target_pairs={{0,8},{8,16},{16,24},{24,32},{32,40},{40,48},{48,56},{56,0},{1,9},... | collective-permute-start | bytes 1622024 | tf_op jit(solution)/shard_map/ppermute | solution.py:23
  64.5 10.7 %collective-permute-start.4 = (bf16[4,3,64,352]{3,2,1,0:T(8,128)(2,1)S(1)}, bf16[4,3,64,352]{3,2,1,0:T(8,128)(2,1)}, u32[]{:S(2)}, u32[]{:S(2)}) collective-permute-start(bf16[4,3,64,352]{3,2,1,0:T(8,128)(2,1)S(1)} %pad_maximum_fusion.2.refs_0_), channel_id=1, source_target_pairs={{0,56},{8,0},{16,8},{24,16},{32,24},{40,32},{48,40},{56,48},{1,57}... | collective-permute-start | bytes 1622024 | tf_op jit(solution)/shard_map/ppermute | solution.py:23
  67.1 11.9 %copy-start.15 = (s32[9]{0:T(128)S(1)}, s32[9]{0:T(128)}, u32[]{:S(2)}) copy-start(s32[9]{0:T(128)} %constant.89.clone) | copy-start | bytes 112
  69.4 11.0 %collective-permute-start.13 = (bf16[520,352]{1,0:T(8,128)(2,1)}, bf16[520,352]{1,0:T(8,128)(2,1)}, u32[]{:S(2)}, u32[]{:S(2)}) collective-permute-start(bf16[520,352]{1,0:T(8,128)(2,1)} %get-tuple-element.29), channel_id=1, source_target_pairs={{0,64},{64,0},{1,65},{65,1},{2,66},{66,2},{3,67},{67,3},{4,68},{68... | collective-permute-start | bytes 1098248 | tf_op jit(solution)/shard_map/ppermute | solution.py:33
  72.5 18.2 %copy-start.4 = (bf16[4,3,64,352]{3,2,1,0:T(8,128)(2,1)}, bf16[4,3,64,352]{3,2,1,0:T(8,128)(2,1)S(1)}, u32[]{:S(2)}) copy-start(bf16[4,3,64,352]{3,2,1,0:T(8,128)(2,1)S(1)} %collective-permute-done.3.refs_1_) | copy-start | bytes 1622020
  72.5 16.2 %collective-permute-start.5 = (bf16[4,3,64,352]{3,2,1,0:T(8,128)(2,1)S(1)}, bf16[4,3,64,352]{3,2,1,0:T(8,128)(2,1)}, u32[]{:S(2)}, u32[]{:S(2)}) collective-permute-start(bf16[4,3,64,352]{3,2,1,0:T(8,128)(2,1)S(1)} %collective-permute-done.3.refs_1_), channel_id=1, source_target_pairs={{0,8},{8,16},{16,24},{24,32},{32,40},{40,48},{48,56},{56,0},{1,9},... | collective-permute-start | bytes 1622024 | tf_op jit(solution)/shard_map/ppermute | solution.py:23
  75.3 15.4 %collective-permute-start.6 = (bf16[4,3,64,352]{3,2,1,0:T(8,128)(2,1)}, bf16[4,3,64,352]{3,2,1,0:T(8,128)(2,1)}, u32[]{:S(2)}, u32[]{:S(2)}) collective-permute-start(bf16[4,3,64,352]{3,2,1,0:T(8,128)(2,1)} %collective-permute-done.4.refs_2_), channel_id=1, source_target_pairs={{0,56},{8,0},{16,8},{24,16},{32,24},{40,32},{48,40},{56,48},{1,57}... | collective-permute-start | bytes 1622024 | tf_op jit(solution)/shard_map/ppermute | solution.py:23
  80.4 16.4 %copy-start.13 = (f32[3,352]{1,0:T(4,128)}, f32[3,352]{1,0:T(4,128)S(1)}, u32[]{:S(2)}) copy-start(f32[3,352]{1,0:T(4,128)S(1)} %dynamic-slice_convert_fusion.refs_13_) | copy-start | bytes 12676
  88.7 17.2 %collective-permute-start.7 = (bf16[4,3,64,352]{3,2,1,0:T(8,128)(2,1)}, bf16[4,3,64,352]{3,2,1,0:T(8,128)(2,1)S(1)}, u32[]{:S(2)}, u32[]{:S(2)}) collective-permute-start(bf16[4,3,64,352]{3,2,1,0:T(8,128)(2,1)} %collective-permute-done.5.refs_3_), channel_id=1, source_target_pairs={{0,8},{8,16},{16,24},{24,32},{32,40},{40,48},{48,56},{56,0},{1,9},... | collective-permute-start | bytes 1622024 | tf_op jit(solution)/shard_map/ppermute | solution.py:23
  90.6 17.4 %collective-permute-start.8 = (bf16[4,3,64,352]{3,2,1,0:T(8,128)(2,1)}, bf16[4,3,64,352]{3,2,1,0:T(8,128)(2,1)S(1)}, u32[]{:S(2)}, u32[]{:S(2)}) collective-permute-start(bf16[4,3,64,352]{3,2,1,0:T(8,128)(2,1)} %collective-permute-done.6.refs_4_), channel_id=1, source_target_pairs={{0,56},{8,0},{16,8},{24,16},{32,24},{40,32},{48,40},{56,48},{1,57}... | collective-permute-start | bytes 1622024 | tf_op jit(solution)/shard_map/ppermute | solution.py:23
  105.9 7.8 %copy-start.2 = (bf16[4,3,64,352]{3,2,1,0:T(8,128)(2,1)}, bf16[4,3,64,352]{3,2,1,0:T(8,128)(2,1)S(1)}, u32[]{:S(2)}) copy-start(bf16[4,3,64,352]{3,2,1,0:T(8,128)(2,1)S(1)} %collective-permute-done.7.refs_5_) | copy-start | bytes 1622020
  105.9 11.9 %collective-permute-start.9 = (bf16[2,3,64,352]{3,2,1,0:T(8,128)(2,1)S(1)}, bf16[2,3,64,352]{3,2,1,0:T(8,128)(2,1)S(1)}, u32[]{:S(2)}, u32[]{:S(2)}) collective-permute-start(bf16[2,3,64,352]{3,2,1,0:T(8,128)(2,1)S(1)} %slice.107), channel_id=1, source_target_pairs={{0,8},{8,16},{16,24},{24,32},{32,40},{40,48},{48,56},{56,0},{1,9},... | collective-permute-start | bytes 811016 | tf_op jit(solution)/shard_map/ppermute | solution.py:23
  108.0 5.6 %copy-start.3 = (bf16[4,3,64,352]{3,2,1,0:T(8,128)(2,1)}, bf16[4,3,64,352]{3,2,1,0:T(8,128)(2,1)S(1)}, u32[]{:S(2)}) copy-start(bf16[4,3,64,352]{3,2,1,0:T(8,128)(2,1)S(1)} %collective-permute-done.8.refs_6_) | copy-start | bytes 1622020
  108.1 11.2 %collective-permute-start.10 = (bf16[2,3,64,352]{3,2,1,0:T(8,128)(2,1)S(1)}, bf16[2,3,64,352]{3,2,1,0:T(8,128)(2,1)S(1)}, u32[]{:S(2)}, u32[]{:S(2)}) collective-permute-start(bf16[2,3,64,352]{3,2,1,0:T(8,128)(2,1)S(1)} %slice.108), channel_id=1, source_target_pairs={{0,56},{8,0},{16,8},{24,16},{32,24},{40,32},{48,40},{56,48},{1,57}... | collective-permute-start | bytes 811016 | tf_op jit(solution)/shard_map/ppermute | solution.py:23
  117.8 1.5 copy-start.7
  119.3 0.7 copy-start.8
  120.0 1.4 copy-start
  127.2 22.9 %copy-start.14 = (f32[3,352]{1,0:T(4,128)S(1)}, f32[3,352]{1,0:T(4,128)}, u32[]{:S(2)}) copy-start(f32[3,352]{1,0:T(4,128)} %get-tuple-element.15) | copy-start | bytes 12676
  134.3 37.5 %collective-permute-start.14 = (bf16[2,4,256,256]{3,2,1,0:T(8,128)(2,1)}, bf16[2,4,256,256]{3,2,1,0:T(8,128)(2,1)S(1)}, u32[]{:S(2)}, u32[]{:S(2)}) collective-permute-start(bf16[2,4,256,256]{3,2,1,0:T(8,128)(2,1)} %get-tuple-element.14), channel_id=1, source_target_pairs={{0,1},{1,0},{2,3},{3,2},{4,5},{5,4},{6,7},{7,6},{8,9},{9,8},{10,11... | collective-permute-start | bytes 3145736 | tf_op jit(solution)/shard_map/ppermute | solution.py:33
  167.1 12.4 %all-to-all-start.3 = ((f32[8,3,704]{2,1,0:T(4,128)}), f32[8,3,704]{2,1,0:T(4,128)S(1)}, u32[]{:S(2)}, u32[]{:S(2)}) async-start(f32[8,3,704]{2,1,0:T(4,128)} %broadcast_in_dim.26), calls=%async_computation.3 | async-start | bytes 196608 | tf_op jit(solution)/shard_map/all_to_all | solution.py:38
  179.5 30.0 %all-to-all-start.1 = ((bf16[8,256,256]{2,1,0:T(8,128)(2,1)}), bf16[8,256,256]{2,1,0:T(8,128)(2,1)S(1)}, u32[]{:S(2)}, u32[]{:S(2)}) async-start(bf16[8,256,256]{2,1,0:T(8,128)(2,1)} %bitcast.11), calls=%async_computation.1 | async-start | bytes 2097152 | tf_op jit(solution)/shard_map/all_to_all | solution.py:287

commit v7 on v6

--- a/solution.py
+++ b/solution.py
@@ -12,7 +12,6 @@
 Z_ALL = ("rep", "zk", "zp")
 SEQ_AXES = ("zk", "zp", "y")
 TP = ("x", "core")
-GROUP = ("zp", "x", "core")
 ROWS = ("rep", "zk", "zp", "y")
 PAD = 264
 PIECES = 9
@@ -87,10 +86,10 @@
 
 def hidden_kernel(places, *refs):
     pieces, refs = refs[:PIECES], refs[PIECES:]
-    grads, slope, value, linear, taps, linear_out, up_out, conv_out, down = refs
-    peers, padded, width = grads.shape
+    grads, shared, slope, value, linear, taps, linear_out, up_out, conv_out, down = refs
+    _, padded, width = grads.shape
     rows = linear_out.shape[1]
-    z_count, y_count, share, half = down.shape
+    z_count, _, share, half = down.shape
     first = pl.program_id(0) == 0
 
     @pl.when(first)
@@ -103,13 +102,14 @@
 
     per_tp = width // share
     act = jnp.zeros(slope.shape[1:], jnp.float32)
-    for t in range(peers):
-        z, y = divmod(t * per_tp, y_count)
-        act += jnp.dot(
-            grads[t],
-            down[z, y : y + per_tp].reshape(width, half),
-            preferred_element_type=jnp.float32,
-        )
+    core = places[PIECES]
+    for z in range(z_count):
+        for part, owner in ((grads, core), (shared, 1 - core)):
+            act += jnp.dot(
+                part[z],
+                down[z, pl.ds(owner * per_tp, per_tp)].reshape(width, half),
+                preferred_element_type=jnp.float32,
+            )
     grad = act * slope[0]
 
     def ahead(value, by):
@@ -139,10 +139,10 @@
         conv_out[...] += sums
 
 
-def hidden_gradients(pieces, places, grads, slope, value, linear, taps):
+def hidden_gradients(pieces, places, grads, shared, slope, value, linear, taps):
     peers, padded, width = grads.shape
     z_count, _, share, half = pieces[0].shape
-    y_count = peers // 2 * width // share // z_count
+    y_count = 2 * width // share
     rows = width
     saved = pl.BlockSpec((1, padded, half), lambda b, at: (b, 0, 0))
     made = pl.BlockSpec((1, rows, half), lambda b, at: (b, 0, 0))
@@ -158,6 +158,7 @@
             ]
             + [
                 pl.BlockSpec((peers // 2, padded, width), lambda b, at: (b, 0, 0)),
+                pl.BlockSpec((peers // 2, padded, width), lambda b, at: (b, 0, 0)),
                 saved,
                 saved,
                 saved,
@@ -171,7 +172,7 @@
             jax.ShapeDtypeStruct((2, rows, half), jnp.bfloat16),
             jax.ShapeDtypeStruct((3, half), jnp.float32),
         ],
-    )(places, *pieces, grads, slope, value, linear, taps)
+    )(places, *pieces, grads, shared, slope, value, linear, taps)
 
 
 def output_kernel(places, *refs):
@@ -251,7 +252,8 @@
             jnp.zeros((PAD - rows - 2, width), out_grad.dtype),
         ]
     )
-    grads = sent_to_all(grads, GROUP)
+    grads = sent_to_all(grads, ("zp", "x"))
+    shared = swapped(grads, "core", 1)
 
     kept, sent = halves_of(jnp.concatenate([gate_lin, up_lin, before, after]), second)
     came = swapped(sent, "zp", 1)
@@ -272,6 +274,7 @@
         pieces,
         places,
         grads,
+        shared,
         jnp.pad(up_ext * gelu_slope, tail),
         jnp.pad(gelu_value, tail),
         jnp.pad(linear, ((0, 0), (0, PAD - rows - 4), (0, 0))),

time: 212 us -> 202 us (0.953)
  starting transfers between devices: 95.4 us -> 89 us
  waiting for transfers between devices: 40.6 us -> 35.3 us
  blocking collectives: 39.2 us -> 43.2 us
    ppermute x10, waiting for transfers between devices: 34.7 us -> 24.4 us  [shifted(): lax.ppermute(value, axis, [(i, (i + by) % count) for i in range(count)])]
    ppermute x10, starting transfers between devices: 33 us -> 43.1 us  [shifted(): lax.ppermute(value, axis, [(i, (i + by) % count) for i in range(count)])]
    ppermute x1, starting transfers between devices: 12.8 us -> 3.09 us  [crossed(): return lax.ppermute(value, (*names, 'core'), pairs)]
    all_to_all x2, starting transfers between devices: 19.3 us -> 14.2 us  [sent_to_all(): lax.all_to_all(jnp.broadcast_to(value[None], (peers, *value.shape)), axis...]
    ppermute x1, waiting for transfers between devices: 0.01 us -> 4.95 us  [crossed(): return lax.ppermute(value, (*names, 'core'), pairs)]
    all_to_all x1, blocking collectives: 16.1 us -> 20.1 us  [sent_to_all(): lax.all_to_all(jnp.broadcast_to(value[None], (peers, *value.shape)), axis...]
    ppermute x2 -> x3, starting transfers between devices: 18 us -> 17.6 us  [swapped(): lax.ppermute(value, axis, [(i, i ^ bit) for i in range(lax.axis_size(axis...]
  transfers between devices with their start and end apart: 18 -> 19, of which waited for: 11 -> 8; matrix products, arithmetic and copies ran while one was open for 6% -> 7% of each run, Pallas kernels for 0% -> 0%
where the time goes in v7:
time: 202 us; the launch traced here: 201 us
  starting transfers between devices  89 us (44%)
  blocking collectives  43.2 us (21%)
  waiting for transfers between devices  35.3 us (17%)
  Pallas kernels  12.9 us (6%)
  local copies, waits for them, and re-layouts  9.61 us (5%)
  other arithmetic  9.55 us (5%)
    ppermute x10, starting transfers between devices, shifted(): lax.ppermute(value, axis, [(i, (i + by) % count) for i in range(count)])  43.1 us
    ppermute x10, waiting for transfers between devices, shifted(): lax.ppermute(value, axis, [(i, (i + by) % count) for i in range(count)])  24.4 us
    all_gather x1, blocking collectives, block_gradients(): conv = lax.all_gather(conv, TP)  23.1 us
    all_to_all x1, blocking collectives, sent_to_all(): lax.all_to_all(jnp.broadcast_to(value[None], (peers, *value.shape)), axis...  20.1 us
    ppermute x3, starting transfers between devices, swapped(): lax.ppermute(value, axis, [(i, i ^ bit) for i in range(lax.axis_size(axis...  17.6 us
    all_to_all x2, starting transfers between devices, sent_to_all(): lax.all_to_all(jnp.broadcast_to(value[None], (peers, *value.shape)), axis...  14.2 us
    pallas_call x1, Pallas kernels, output_partials(): pl.pallas_call(output_kernel, grid_spec=pltpu.PrefetchScalarGridSpec(num_...  7.03 us
    ppermute x2, starting transfers between devices, to_next(): return lax.ppermute(value, axis, pairs)  5.94 us
  transfers between devices with their start and end apart: 19, of which 8 were waited for; matrix products, arithmetic and copies ran while one was open for 7% of the time, Pallas kernels for 0%

profile of v7, /device:TPU:1, one launch (start us, length us, event | category | flops | bytes accessed | tf_op | source)
XLA Modules:
  0.0 200.9 jit_solution(3302138704162045471)
XLA Ops:
  0.6 0.8 fusion.16
  1.4 1.2 copy.50
  2.6 1.2 copy.51
  3.8 1.3 collective-permute-start.12
  5.1 4.6 %collective-permute-start.11 = (bf16[4,704]{1,0:T(4,128)(2,1)S(1)}, bf16[4,704]{1,0:T(4,128)(2,1)S(1)}, u32[]{:S(2)}, u32[]{:S(2)}) collective-permute-start(bf16[4,704]{1,0:T(4,128)(2,1)S(1)} %fusion.9), channel_id=1, source_target_pairs={{0,8},{8,16},{16,24},{24,32},{32,40},{40,48},{48,56},{56,64},{64,7... | collective-permute-start | bytes 16904 | tf_op jit(solution)/shard_map/ppermute | solution.py:28
  9.8 0.1 pad.42.clone
  9.9 0.7 collective-permute-done.11
  10.5 0.1 maximum_maximum_fusion
  10.6 0.0 copy-start.10
  10.7 0.0 copy-start.11
  10.7 0.0 copy-start.12
  10.7 1.1 broadcast_in_dim.11
  11.7 10.6 %all-to-all-start = ((bf16[8,264,256]{2,1,0:T(8,128)(2,1)}), bf16[8,264,256]{2,1,0:T(8,128)(2,1)S(1)}, u32[]{:S(2)}, u32[]{:S(2)}) async-start(bf16[8,264,256]{2,1,0:T(8,128)(2,1)} %broadcast_in_dim.11), calls=%async_computation | async-start | bytes 2162688 | tf_op jit(solution)/shard_map/all_to_all | solution.py:37
  22.4 0.1 broadcast_select_fusion.2
  22.5 3.4 %collective-permute-start.2 = (bf16[3,64,352]{2,1,0:T(8,128)(2,1)S(1)}, bf16[3,64,352]{2,1,0:T(8,128)(2,1)S(1)}, u32[]{:S(2)}, u32[]{:S(2)}) collective-permute-start(bf16[3,64,352]{2,1,0:T(8,128)(2,1)S(1)} %get-tuple-element.39), channel_id=1, source_target_pairs={{0,64},{64,128},{128,192},{192,256},{256,320},{320,384},{384,448},... | collective-permute-start | bytes 405512 | tf_op jit(solution)/shard_map/ppermute | solution.py:22
  25.9 13.1 %collective-permute-start = (bf16[3,64,352]{2,1,0:T(8,128)(2,1)S(1)}, bf16[3,64,352]{2,1,0:T(8,128)(2,1)S(1)}, u32[]{:S(2)}, u32[]{:S(2)}) collective-permute-start(bf16[3,64,352]{2,1,0:T(8,128)(2,1)S(1)} %get-tuple-element.39), channel_id=1, source_target_pairs={{0,704},{64,0},{128,64},{192,128},{256,192},{320,256},{384,320},{4... | collective-permute-start | bytes 405512 | tf_op jit(solution)/shard_map/ppermute | solution.py:22
  39.1 3.1 %collective-permute-start.1 = (bf16[3,64,352]{2,1,0:T(8,128)(2,1)S(1)}, bf16[3,64,352]{2,1,0:T(8,128)(2,1)S(1)}, u32[]{:S(2)}, u32[]{:S(2)}) collective-permute-start(bf16[3,64,352]{2,1,0:T(8,128)(2,1)S(1)} %get-tuple-element.40), channel_id=1, source_target_pairs={{0,128},{1,641},{64,192},{65,705},{128,256},{129,1},{192,320},{193... | collective-permute-start | bytes 405512 | tf_op jit(solution)/shard_map/ppermute | solution.py:56
  42.2 0.0 collective-permute-done.2
  42.3 5.0 %collective-permute-done.1 = bf16[3,64,352]{2,1,0:T(8,128)(2,1)S(1)} collective-permute-done((bf16[3,64,352]{2,1,0:T(8,128)(2,1)S(1)}, bf16[3,64,352]{2,1,0:T(8,128)(2,1)S(1)}, u32[]{:S(2)}, u32[]{:S(2)}) %collective-permute-start.1) | collective-permute-done | bytes 135200 | tf_op jit(solution)/shard_map/ppermute | solution.py:56
  47.2 0.1 select_bitcast_fusion.5
  47.3 0.1 pad_maximum_fusion.2.refs_0_
  47.5 1.9 collective-permute-start.3
  49.4 0.0 copy-start.15
  49.4 4.6 %collective-permute-start.4 = (bf16[4,3,64,352]{3,2,1,0:T(8,128)(2,1)S(1)}, bf16[4,3,64,352]{3,2,1,0:T(8,128)(2,1)S(1)}, u32[]{:S(2)}, u32[]{:S(2)}) collective-permute-start(bf16[4,3,64,352]{3,2,1,0:T(8,128)(2,1)S(1)} %pad_maximum_fusion.2.refs_0_), channel_id=1, source_target_pairs={{0,56},{8,0},{16,8},{24,16},{32,24},{40,32},{48,40},{56,48},{1,57}... | collective-permute-start | bytes 1622024 | tf_op jit(solution)/shard_map/ppermute | solution.py:22
  54.0 1.1 pad_maximum_fusion.1
  55.1 1.1 broadcast_select_fusion
  56.2 1.9 collective-permute-start.14
  58.1 1.2 collective-permute-done.3.refs_1_
  59.3 1.9 collective-permute-start.5
  61.3 4.6 %collective-permute-start.6 = (bf16[4,3,64,352]{3,2,1,0:T(8,128)(2,1)S(1)}, bf16[4,3,64,352]{3,2,1,0:T(8,128)(2,1)}, u32[]{:S(2)}, u32[]{:S(2)}) collective-permute-start(bf16[4,3,64,352]{3,2,1,0:T(8,128)(2,1)S(1)} %collective-permute-done.4.refs_2_), channel_id=1, source_target_pairs={{0,56},{8,0},{16,8},{24,16},{32,24},{40,32},{48,40},{56,48},{1,57}... | collective-permute-start | bytes 1622024 | tf_op jit(solution)/shard_map/ppermute | solution.py:22
  65.9 0.6 pad_add_fusion.places
  66.5 0.8 dynamic-slice_convert_fusion.refs_14_
  67.3 6.3 %collective-permute-done.5.refs_3_ = bf16[4,3,64,352]{3,2,1,0:T(8,128)(2,1)} collective-permute-done((bf16[4,3,64,352]{3,2,1,0:T(8,128)(2,1)S(1)}, bf16[4,3,64,352]{3,2,1,0:T(8,128)(2,1)}, u32[]{:S(2)}, u32[]{:S(2)}) %collective-permute-start.5) | collective-permute-done | bytes 540704 | tf_op jit(solution)/shard_map/ppermute | solution.py:22
  73.5 11.5 %collective-permute-start.13 = (bf16[8,264,256]{2,1,0:T(8,128)(2,1)S(1)}, bf16[8,264,256]{2,1,0:T(8,128)(2,1)}, u32[]{:S(2)}, u32[]{:S(2)}) collective-permute-start(bf16[8,264,256]{2,1,0:T(8,128)(2,1)S(1)} %all-to-all-done.refs_9_), channel_id=1, source_target_pairs={{0,1},{1,0},{2,3},{3,2},{4,5},{5,4},{6,7},{7,6},{8,9},{9,8},{10,11... | collective-permute-start | bytes 3244040 | tf_op jit(solution)/shard_map/ppermute | solution.py:32
  85.1 1.2 select_bitcast_fusion.1
  86.3 1.9 collective-permute-start.7
  88.2 4.6 %collective-permute-start.8 = (bf16[4,3,64,352]{3,2,1,0:T(8,128)(2,1)}, bf16[4,3,64,352]{3,2,1,0:T(8,128)(2,1)S(1)}, u32[]{:S(2)}, u32[]{:S(2)}) collective-permute-start(bf16[4,3,64,352]{3,2,1,0:T(8,128)(2,1)} %collective-permute-done.6.refs_4_), channel_id=1, source_target_pairs={{0,56},{8,0},{16,8},{24,16},{32,24},{40,32},{48,40},{56,48},{1,57}... | collective-permute-start | bytes 1622024 | tf_op jit(solution)/shard_map/ppermute | solution.py:22
  92.8 0.2 maximum_convert_fusion
  93.0 0.1 fusion.13
  93.1 0.1 pad_maximum_fusion
  93.2 1.0 pad.22.refs_13_
  94.2 11.3 %collective-permute-done.8.refs_6_ = bf16[4,3,64,352]{3,2,1,0:T(8,128)(2,1)S(1)} collective-permute-done((bf16[4,3,64,352]{3,2,1,0:T(8,128)(2,1)}, bf16[4,3,64,352]{3,2,1,0:T(8,128)(2,1)S(1)}, u32[]{:S(2)}, u32[]{:S(2)}) %collective-permute-start.8) | collective-permute-done | bytes 540704 | tf_op jit(solution)/shard_map/ppermute | solution.py:22
  105.5 5.2 %collective-permute-start.10 = (bf16[2,3,64,352]{3,2,1,0:T(8,128)(2,1)S(1)}, bf16[2,3,64,352]{3,2,1,0:T(8,128)(2,1)S(1)}, u32[]{:S(2)}, u32[]{:S(2)}) collective-permute-start(bf16[2,3,64,352]{3,2,1,0:T(8,128)(2,1)S(1)} %slice.108), channel_id=1, source_target_pairs={{0,56},{8,0},{16,8},{24,16},{32,24},{40,32},{48,40},{56,48},{1,57}... | collective-permute-start | bytes 811016 | tf_op jit(solution)/shard_map/ppermute | solution.py:22
  110.8 1.9 collective-permute-start.9
  112.7 0.7 fusion.12
  113.4 1.0 pad.21.refs_12_
  114.4 1.0 pad.20.refs_11_
  115.3 0.6 collective-permute-done.10.refs_8_
  115.9 5.1 %collective-permute-done.9.refs_7_ = bf16[2,3,64,352]{3,2,1,0:T(8,128)(2,1)S(1)} collective-permute-done((bf16[2,3,64,352]{3,2,1,0:T(8,128)(2,1)S(1)}, bf16[2,3,64,352]{3,2,1,0:T(8,128)(2,1)S(1)}, u32[]{:S(2)}, u32[]{:S(2)}) %collective-permute-start.9) | collective-permute-done | bytes 270368 | tf_op jit(solution)/shard_map/ppermute | solution.py:22
  121.0 0.7 copy-done.8
  121.7 5.9 %shard_map.95 = (bf16[2,256,352]{2,1,0:T(8,128)(2,1)}, bf16[2,256,352]{2,1,0:T(8,128)(2,1)}, f32[3,352]{1,0:T(4,128)}) custom-call(s32[10]{0:T(128)} %pad_add_fusion.places, bf16[4,3,64,352]{3,2,1,0:T(8,128)(2,1)} %copy-done, bf16[4,3,64,352]{3,2,1,0:T(8,128)(2,1)} %copy-done.4, bf16[4,3,64,352]{3,2,1,0:T(8,128)(2,1)} %copy-done.5, ...), custom_call_target="tpu_custom_call" | custom-call | tf_op jit(solution)/shard_map/pallas_call | solution.py:150
  127.6 0.0 copy-start.14
  127.7 7.0 %shard_map.96 = (bf16[2,4,256,256]{3,2,1,0:T(8,128)(2,1)}, bf16[2,4,256,256]{3,2,1,0:T(8,128)(2,1)}) custom-call(s32[10]{0:T(128)} %pad_add_fusion.places, bf16[4,3,64,352]{3,2,1,0:T(8,128)(2,1)} %copy-done, bf16[4,3,64,352]{3,2,1,0:T(8,128)(2,1)} %copy-done.4, bf16[4,3,64,352]{3,2,1,0:T(8,128)(2,1)} %copy-done.5, ...), custom_call_target="tpu_custom_call" | custom-call | tf_op jit(solution)/shard_map/pallas_call | solution.py:220
  134.7 4.2 %collective-permute-start.15 = (bf16[2,4,256,256]{3,2,1,0:T(8,128)(2,1)}, bf16[2,4,256,256]{3,2,1,0:T(8,128)(2,1)S(1)}, u32[]{:S(2)}, u32[]{:S(2)}) collective-permute-start(bf16[2,4,256,256]{3,2,1,0:T(8,128)(2,1)} %get-tuple-element.14), channel_id=1, source_target_pairs={{0,1},{1,0},{2,3},{3,2},{4,5},{5,4},{6,7},{7,6},{8,9},{9,8},{10,11... | collective-permute-start | bytes 3145736 | tf_op jit(solution)/shard_map/ppermute | solution.py:32
  138.9 20.1 %all_to_all.20 = f32[12,3,352]{2,1,0:T(4,128)S(1)} all-to-all(f32[12,3,352]{2,1,0:T(4,128)S(1)} %broadcast_in_dim.24), channel_id=1, replica_groups=mesh['rep'=3,'zk'=2,'zp'=2,'y'=8,'x'=4,'core'=2] {'rep','zk','zp'}, dimensions={0} | all-to-all | bytes 101376 | tf_op jit(solution)/shard_map/all_to_all | solution.py:37
  159.1 0.1 broadcast_in_dim.25
  159.2 0.7 broadcast_in_dim.26
  159.8 3.6 %all-to-all-start.3 = ((f32[8,3,704]{2,1,0:T(4,128)}), f32[8,3,704]{2,1,0:T(4,128)S(1)}, u32[]{:S(2)}, u32[]{:S(2)}) async-start(f32[8,3,704]{2,1,0:T(4,128)} %broadcast_in_dim.26), calls=%async_computation.3 | async-start | bytes 196608 | tf_op jit(solution)/shard_map/all_to_all | solution.py:37
  163.4 2.4 %add_convert_fusion = bf16[2,4,256,256]{3,2,1,0:T(8,128)(2,1)} fusion(bf16[2,4,256,256]{3,2,1,0:T(8,128)(2,1)S(1)} %collective-permute-done.15, bf16[2,4,256,256]{3,2,1,0:T(8,128)(2,1)} %get-tuple-element.13), kind=kLoop, calls=%fused_computation | loop fusion | flops 2097152 | bytes 3145728 | tf_op jit(solution)/shard_map/convert_element_type | solution.py:287
  165.9 5.2 %all-to-all-done.3 = f32[8,3,704]{2,1,0:T(4,128)S(1)} async-done(((f32[8,3,704]{2,1,0:T(4,128)}), f32[8,3,704]{2,1,0:T(4,128)S(1)}, u32[]{:S(2)}, u32[]{:S(2)}) %all-to-all-start.3) | async-done | bytes 67616 | tf_op jit(solution)/shard_map/all_to_all | solution.py:37
  171.1 5.1 %all-to-all-start.1 = ((bf16[8,256,256]{2,1,0:T(8,128)(2,1)}), bf16[8,256,256]{2,1,0:T(8,128)(2,1)S(1)}, u32[]{:S(2)}, u32[]{:S(2)}) async-start(bf16[8,256,256]{2,1,0:T(8,128)(2,1)} %bitcast.11), calls=%async_computation.1 | async-start | bytes 2097152 | tf_op jit(solution)/shard_map/all_to_all | solution.py:290
  176.2 23.1 %all-gather.1 = f32[8,3,704]{2,1,0:T(4,128)S(1)} all-gather(f32[1,3,704]{2,1,0:T(4,128)S(1)} %bitcast.30), channel_id=2, replica_groups=mesh['rep'=3,'zk'=2,'zp'=2,'y'=8,'x'=4,'core'=2] {'x','core'}, dimensions={0}, use_global_device_ids=true | all-gather | bytes 76032 | tf_op jit(solution)/shard_map/all_gather | solution.py:294
  199.3 0.7 reshape.26
  200.1 0.8 reduce_sum.30
  (55 shorter events, 0.4 us)
Async XLA Ops:
  0.6 9.9 %copy-start.9 = (bf16[256,256]{1,0:T(8,128)(2,1)S(1)}, bf16[256,256]{1,0:T(8,128)(2,1)}, u32[]{:S(2)}) copy-start(bf16[256,256]{1,0:T(8,128)(2,1)} %param.8) | copy-start | bytes 393220
  3.7 8.0 %copy-start.6 = (bf16[256,704]{1,0:T(8,128)(2,1)}, bf16[256,704]{1,0:T(8,128)(2,1)S(1)}, u32[]{:S(2)}) copy-start(bf16[256,704]{1,0:T(8,128)(2,1)S(1)} %copy.51) | copy-start | bytes 1081348
  3.8 6.1 %collective-permute-start.12 = (bf16[4,704]{1,0:T(4,128)(2,1)S(1)}, bf16[4,704]{1,0:T(4,128)(2,1)S(1)}, u32[]{:S(2)}, u32[]{:S(2)}) collective-permute-start(bf16[4,704]{1,0:T(4,128)(2,1)S(1)} %fusion.10), channel_id=1, source_target_pairs={{8,0},{16,8},{24,16},{32,24},{40,32},{48,40},{56,48},{64,56},{72,6... | collective-permute-start | bytes 16904 | tf_op jit(solution)/shard_map/ppermute | solution.py:28
  5.1 5.4 %collective-permute-start.11 = (bf16[4,704]{1,0:T(4,128)(2,1)S(1)}, bf16[4,704]{1,0:T(4,128)(2,1)S(1)}, u32[]{:S(2)}, u32[]{:S(2)}) collective-permute-start(bf16[4,704]{1,0:T(4,128)(2,1)S(1)} %fusion.9), channel_id=1, source_target_pairs={{0,8},{8,16},{16,24},{24,32},{32,40},{40,48},{48,56},{56,64},{64,7... | collective-permute-start | bytes 16904 | tf_op jit(solution)/shard_map/ppermute | solution.py:28
  10.6 11.7 %copy-start.10 = (bf16[704,64]{0,1:T(8,128)(2,1)S(1)}, bf16[704,64]{0,1:T(8,128)(2,1)}, u32[]{:S(2)}) copy-start(bf16[704,64]{0,1:T(8,128)(2,1)} %param.14) | copy-start | bytes 270340
  10.7 11.7 %copy-start.11 = (bf16[64,704]{1,0:T(8,128)(2,1)S(1)}, bf16[64,704]{1,0:T(8,128)(2,1)}, u32[]{:S(2)}) copy-start(bf16[64,704]{1,0:T(8,128)(2,1)} %param.13) | copy-start | bytes 270340
  10.7 11.7 %copy-start.12 = (bf16[64,704]{1,0:T(8,128)(2,1)S(1)}, bf16[64,704]{1,0:T(8,128)(2,1)}, u32[]{:S(2)}) copy-start(bf16[64,704]{1,0:T(8,128)(2,1)} %param.12) | copy-start | bytes 270340
  11.7 61.8 %all-to-all-start = ((bf16[8,264,256]{2,1,0:T(8,128)(2,1)}), bf16[8,264,256]{2,1,0:T(8,128)(2,1)S(1)}, u32[]{:S(2)}, u32[]{:S(2)}) async-start(bf16[8,264,256]{2,1,0:T(8,128)(2,1)} %broadcast_in_dim.11), calls=%async_computation | async-start | bytes 2162688 | tf_op jit(solution)/shard_map/all_to_all | solution.py:37
  22.5 19.7 %collective-permute-start.2 = (bf16[3,64,352]{2,1,0:T(8,128)(2,1)S(1)}, bf16[3,64,352]{2,1,0:T(8,128)(2,1)S(1)}, u32[]{:S(2)}, u32[]{:S(2)}) collective-permute-start(bf16[3,64,352]{2,1,0:T(8,128)(2,1)S(1)} %get-tuple-element.39), channel_id=1, source_target_pairs={{0,64},{64,128},{128,192},{192,256},{256,320},{320,384},{384,448},... | collective-permute-start | bytes 405512 | tf_op jit(solution)/shard_map/ppermute | solution.py:22
  25.9 16.3 %collective-permute-start = (bf16[3,64,352]{2,1,0:T(8,128)(2,1)S(1)}, bf16[3,64,352]{2,1,0:T(8,128)(2,1)S(1)}, u32[]{:S(2)}, u32[]{:S(2)}) collective-permute-start(bf16[3,64,352]{2,1,0:T(8,128)(2,1)S(1)} %get-tuple-element.39), channel_id=1, source_target_pairs={{0,704},{64,0},{128,64},{192,128},{256,192},{320,256},{384,320},{4... | collective-permute-start | bytes 405512 | tf_op jit(solution)/shard_map/ppermute | solution.py:22
  39.1 8.2 %collective-permute-start.1 = (bf16[3,64,352]{2,1,0:T(8,128)(2,1)S(1)}, bf16[3,64,352]{2,1,0:T(8,128)(2,1)S(1)}, u32[]{:S(2)}, u32[]{:S(2)}) collective-permute-start(bf16[3,64,352]{2,1,0:T(8,128)(2,1)S(1)} %get-tuple-element.40), channel_id=1, source_target_pairs={{0,128},{1,641},{64,192},{65,705},{128,256},{129,1},{192,320},{193... | collective-permute-start | bytes 405512 | tf_op jit(solution)/shard_map/ppermute | solution.py:56
  47.5 8.7 %copy-start = (bf16[4,3,64,352]{3,2,1,0:T(8,128)(2,1)}, bf16[4,3,64,352]{3,2,1,0:T(8,128)(2,1)S(1)}, u32[]{:S(2)}) copy-start(bf16[4,3,64,352]{3,2,1,0:T(8,128)(2,1)S(1)} %pad_maximum_fusion.2.refs_0_) | copy-start | bytes 1622020
  47.5 11.8 %collective-permute-start.3 = (bf16[4,3,64,352]{3,2,1,0:T(8,128)(2,1)S(1)}, bf16[4,3,64,352]{3,2,1,0:T(8,128)(2,1)S(1)}, u32[]{:S(2)}, u32[]{:S(2)}) collective-permute-start(bf16[4,3,64,352]{3,2,1,0:T(8,128)(2,1)S(1)} %pad_maximum_fusion.2.refs_0_), channel_id=1, source_target_pairs={{0,8},{8,16},{16,24},{24,32},{32,40},{40,48},{48,56},{56,0},{1,9},... | collective-permute-start | bytes 1622024 | tf_op jit(solution)/shard_map/ppermute | solution.py:22
  49.4 11.8 %copy-start.15 = (s32[9]{0:T(128)S(1)}, s32[9]{0:T(128)}, u32[]{:S(2)}) copy-start(s32[9]{0:T(128)} %constant.89.clone) | copy-start | bytes 112
  49.4 11.8 %collective-permute-start.4 = (bf16[4,3,64,352]{3,2,1,0:T(8,128)(2,1)S(1)}, bf16[4,3,64,352]{3,2,1,0:T(8,128)(2,1)S(1)}, u32[]{:S(2)}, u32[]{:S(2)}) collective-permute-start(bf16[4,3,64,352]{3,2,1,0:T(8,128)(2,1)S(1)} %pad_maximum_fusion.2.refs_0_), channel_id=1, source_target_pairs={{0,56},{8,0},{16,8},{24,16},{32,24},{40,32},{48,40},{56,48},{1,57}... | collective-permute-start | bytes 1622024 | tf_op jit(solution)/shard_map/ppermute | solution.py:22
  56.2 11.1 %collective-permute-start.14 = (bf16[520,352]{1,0:T(8,128)(2,1)}, bf16[520,352]{1,0:T(8,128)(2,1)}, u32[]{:S(2)}, u32[]{:S(2)}) collective-permute-start(bf16[520,352]{1,0:T(8,128)(2,1)} %get-tuple-element.29), channel_id=1, source_target_pairs={{0,64},{64,0},{1,65},{65,1},{2,66},{66,2},{3,67},{67,3},{4,68},{68... | collective-permute-start | bytes 1098248 | tf_op jit(solution)/shard_map/ppermute | solution.py:32
  59.3 33.7 %copy-start.4 = (bf16[4,3,64,352]{3,2,1,0:T(8,128)(2,1)}, bf16[4,3,64,352]{3,2,1,0:T(8,128)(2,1)S(1)}, u32[]{:S(2)}) copy-start(bf16[4,3,64,352]{3,2,1,0:T(8,128)(2,1)S(1)} %collective-permute-done.3.refs_1_) | copy-start | bytes 1622020
  59.3 14.2 %collective-permute-start.5 = (bf16[4,3,64,352]{3,2,1,0:T(8,128)(2,1)S(1)}, bf16[4,3,64,352]{3,2,1,0:T(8,128)(2,1)}, u32[]{:S(2)}, u32[]{:S(2)}) collective-permute-start(bf16[4,3,64,352]{3,2,1,0:T(8,128)(2,1)S(1)} %collective-permute-done.3.refs_1_), channel_id=1, source_target_pairs={{0,8},{8,16},{16,24},{24,32},{32,40},{40,48},{48,56},{56,0},{1,9},... | collective-permute-start | bytes 1622024 | tf_op jit(solution)/shard_map/ppermute | solution.py:22
  61.3 31.7 %copy-start.5 = (bf16[4,3,64,352]{3,2,1,0:T(8,128)(2,1)}, bf16[4,3,64,352]{3,2,1,0:T(8,128)(2,1)S(1)}, u32[]{:S(2)}) copy-start(bf16[4,3,64,352]{3,2,1,0:T(8,128)(2,1)S(1)} %collective-permute-done.4.refs_2_) | copy-start | bytes 1622020
  61.3 26.9 %collective-permute-start.6 = (bf16[4,3,64,352]{3,2,1,0:T(8,128)(2,1)S(1)}, bf16[4,3,64,352]{3,2,1,0:T(8,128)(2,1)}, u32[]{:S(2)}, u32[]{:S(2)}) collective-permute-start(bf16[4,3,64,352]{3,2,1,0:T(8,128)(2,1)S(1)} %collective-permute-done.4.refs_2_), channel_id=1, source_target_pairs={{0,56},{8,0},{16,8},{24,16},{32,24},{40,32},{48,40},{56,48},{1,57}... | collective-permute-start | bytes 1622024 | tf_op jit(solution)/shard_map/ppermute | solution.py:22
  67.2 25.7 %copy-start.13 = (f32[3,352]{1,0:T(4,128)}, f32[3,352]{1,0:T(4,128)S(1)}, u32[]{:S(2)}) copy-start(f32[3,352]{1,0:T(4,128)S(1)} %dynamic-slice_convert_fusion.refs_14_) | copy-start | bytes 12676
  73.5 19.5 %copy-start.1 = (bf16[8,264,256]{2,1,0:T(8,128)(2,1)}, bf16[8,264,256]{2,1,0:T(8,128)(2,1)S(1)}, u32[]{:S(2)}) copy-start(bf16[8,264,256]{2,1,0:T(8,128)(2,1)S(1)} %all-to-all-done.refs_9_) | copy-start | bytes 3244036
  73.5 47.5 %collective-permute-start.13 = (bf16[8,264,256]{2,1,0:T(8,128)(2,1)S(1)}, bf16[8,264,256]{2,1,0:T(8,128)(2,1)}, u32[]{:S(2)}, u32[]{:S(2)}) collective-permute-start(bf16[8,264,256]{2,1,0:T(8,128)(2,1)S(1)} %all-to-all-done.refs_9_), channel_id=1, source_target_pairs={{0,1},{1,0},{2,3},{3,2},{4,5},{5,4},{6,7},{7,6},{8,9},{9,8},{10,11... | collective-permute-start | bytes 3244040 | tf_op jit(solution)/shard_map/ppermute | solution.py:32
  86.3 24.5 %collective-permute-start.7 = (bf16[4,3,64,352]{3,2,1,0:T(8,128)(2,1)}, bf16[4,3,64,352]{3,2,1,0:T(8,128)(2,1)S(1)}, u32[]{:S(2)}, u32[]{:S(2)}) collective-permute-start(bf16[4,3,64,352]{3,2,1,0:T(8,128)(2,1)} %collective-permute-done.5.refs_3_), channel_id=1, source_target_pairs={{0,8},{8,16},{16,24},{24,32},{32,40},{40,48},{48,56},{56,0},{1,9},... | collective-permute-start | bytes 1622024 | tf_op jit(solution)/shard_map/ppermute | solution.py:22
  88.2 17.3 %collective-permute-start.8 = (bf16[4,3,64,352]{3,2,1,0:T(8,128)(2,1)}, bf16[4,3,64,352]{3,2,1,0:T(8,128)(2,1)S(1)}, u32[]{:S(2)}, u32[]{:S(2)}) collective-permute-start(bf16[4,3,64,352]{3,2,1,0:T(8,128)(2,1)} %collective-permute-done.6.refs_4_), channel_id=1, source_target_pairs={{0,56},{8,0},{16,8},{24,16},{32,24},{40,32},{48,40},{56,48},{1,57}... | collective-permute-start | bytes 1622024 | tf_op jit(solution)/shard_map/ppermute | solution.py:22
  105.5 7.9 %copy-start.3 = (bf16[4,3,64,352]{3,2,1,0:T(8,128)(2,1)}, bf16[4,3,64,352]{3,2,1,0:T(8,128)(2,1)S(1)}, u32[]{:S(2)}) copy-start(bf16[4,3,64,352]{3,2,1,0:T(8,128)(2,1)S(1)} %collective-permute-done.8.refs_6_) | copy-start | bytes 1622020
  105.5 10.4 %collective-permute-start.10 = (bf16[2,3,64,352]{3,2,1,0:T(8,128)(2,1)S(1)}, bf16[2,3,64,352]{3,2,1,0:T(8,128)(2,1)S(1)}, u32[]{:S(2)}, u32[]{:S(2)}) collective-permute-start(bf16[2,3,64,352]{3,2,1,0:T(8,128)(2,1)S(1)} %slice.108), channel_id=1, source_target_pairs={{0,56},{8,0},{16,8},{24,16},{32,24},{40,32},{48,40},{56,48},{1,57}... | collective-permute-start | bytes 811016 | tf_op jit(solution)/shard_map/ppermute | solution.py:22
  110.7 2.7 %copy-start.2 = (bf16[4,3,64,352]{3,2,1,0:T(8,128)(2,1)}, bf16[4,3,64,352]{3,2,1,0:T(8,128)(2,1)S(1)}, u32[]{:S(2)}) copy-start(bf16[4,3,64,352]{3,2,1,0:T(8,128)(2,1)S(1)} %collective-permute-done.7.refs_5_) | copy-start | bytes 1622020
  110.8 10.2 %collective-permute-start.9 = (bf16[2,3,64,352]{3,2,1,0:T(8,128)(2,1)S(1)}, bf16[2,3,64,352]{3,2,1,0:T(8,128)(2,1)S(1)}, u32[]{:S(2)}, u32[]{:S(2)}) collective-permute-start(bf16[2,3,64,352]{3,2,1,0:T(8,128)(2,1)S(1)} %slice.107), channel_id=1, source_target_pairs={{0,8},{8,16},{16,24},{24,32},{32,40},{40,48},{48,56},{56,0},{1,9},... | collective-permute-start | bytes 811016 | tf_op jit(solution)/shard_map/ppermute | solution.py:22
  115.9 5.1 %copy-start.7 = (bf16[2,3,64,352]{3,2,1,0:T(8,128)(2,1)}, bf16[2,3,64,352]{3,2,1,0:T(8,128)(2,1)S(1)}, u32[]{:S(2)}) copy-start(bf16[2,3,64,352]{3,2,1,0:T(8,128)(2,1)S(1)} %collective-permute-done.10.refs_8_) | copy-start | bytes 811012
  121.0 0.7 copy-start.8
  127.6 11.2 %copy-start.14 = (f32[3,352]{1,0:T(4,128)S(1)}, f32[3,352]{1,0:T(4,128)}, u32[]{:S(2)}) copy-start(f32[3,352]{1,0:T(4,128)} %get-tuple-element.15) | copy-start | bytes 12676
  134.7 28.8 %collective-permute-start.15 = (bf16[2,4,256,256]{3,2,1,0:T(8,128)(2,1)}, bf16[2,4,256,256]{3,2,1,0:T(8,128)(2,1)S(1)}, u32[]{:S(2)}, u32[]{:S(2)}) collective-permute-start(bf16[2,4,256,256]{3,2,1,0:T(8,128)(2,1)} %get-tuple-element.14), channel_id=1, source_target_pairs={{0,1},{1,0},{2,3},{3,2},{4,5},{5,4},{6,7},{7,6},{8,9},{9,8},{10,11... | collective-permute-start | bytes 3145736 | tf_op jit(solution)/shard_map/ppermute | solution.py:32
  159.8 11.3 %all-to-all-start.3 = ((f32[8,3,704]{2,1,0:T(4,128)}), f32[8,3,704]{2,1,0:T(4,128)S(1)}, u32[]{:S(2)}, u32[]{:S(2)}) async-start(f32[8,3,704]{2,1,0:T(4,128)} %broadcast_in_dim.26), calls=%async_computation.3 | async-start | bytes 196608 | tf_op jit(solution)/shard_map/all_to_all | solution.py:37
  171.1 29.0 %all-to-all-start.1 = ((bf16[8,256,256]{2,1,0:T(8,128)(2,1)}), bf16[8,256,256]{2,1,0:T(8,128)(2,1)S(1)}, u32[]{:S(2)}, u32[]{:S(2)}) async-start(bf16[8,256,256]{2,1,0:T(8,128)(2,1)} %bitcast.11), calls=%async_computation.1 | async-start | bytes 2097152 | tf_op jit(solution)/shard_map/all_to_all | solution.py:290

commit v8 on v7

--- a/solution.py
+++ b/solution.py
@@ -86,7 +86,7 @@
 
 def hidden_kernel(places, *refs):
     pieces, refs = refs[:PIECES], refs[PIECES:]
-    grads, shared, slope, value, linear, taps, linear_out, up_out, conv_out, down = refs
+    grads, shared, slope, value, linear, taps, linear_out, up_out, conv_out, down, total = refs
     _, padded, width = grads.shape
     rows = linear_out.shape[1]
     z_count, _, share, half = down.shape
@@ -132,14 +132,15 @@
 
     @pl.when(first)
     def _():
-        conv_out[...] = sums
+        total[...] = sums
 
     @pl.when(jnp.logical_not(first))
     def _():
-        conv_out[...] += sums
+        conv_out[...] = jnp.broadcast_to((total[...] + sums)[None], conv_out.shape)
 
 
 def hidden_gradients(pieces, places, grads, shared, slope, value, linear, taps):
+    copies = lax.axis_size(Z_ALL)
     peers, padded, width = grads.shape
     z_count, _, share, half = pieces[0].shape
     y_count = 2 * width // share
@@ -164,13 +165,16 @@
                 saved,
                 small,
             ],
-            out_specs=[made, made, small],
-            scratch_shapes=[pltpu.VMEM((z_count, y_count, share, half), jnp.bfloat16)],
+            out_specs=[made, made, pl.BlockSpec((copies, 3, half), lambda b, at: (0, 0, 0))],
+            scratch_shapes=[
+                pltpu.VMEM((z_count, y_count, share, half), jnp.bfloat16),
+                pltpu.VMEM((3, half), jnp.float32),
+            ],
         ),
         out_shape=[
             jax.ShapeDtypeStruct((2, rows, half), jnp.bfloat16),
             jax.ShapeDtypeStruct((2, rows, half), jnp.bfloat16),
-            jax.ShapeDtypeStruct((3, half), jnp.float32),
+            jax.ShapeDtypeStruct((copies, 3, half), jnp.float32),
         ],
     )(places, *pieces, grads, shared, slope, value, linear, taps)
 
@@ -280,7 +284,7 @@
         jnp.pad(linear, ((0, 0), (0, PAD - rows - 4), (0, 0))),
         taps,
     )
-    conv = sent_to_all(conv, Z_ALL)
+    conv = lax.all_to_all(conv, Z_ALL, 0, 0, tiled=True)
     conv = conv.reshape(-1, 2, 3, half).sum(axis=0).transpose(1, 0, 2).reshape(3, columns)
     kept, sent = output_partials(pieces, places, linear_grad, up_grad, width)
     came = swapped(sent, "core", 1)

time: 202 us -> 202 us (level)
  no operation moved by 1% of the time
where the time goes in v8:
time: 202 us; the launch traced here: 201 us
  starting transfers between devices  89.1 us (44%)
  blocking collectives  43.2 us (21%)
  waiting for transfers between devices  35.3 us (17%)
  Pallas kernels  13.1 us (6%)
  local copies, waits for them, and re-layouts  9.6 us (5%)
  other arithmetic  9.55 us (5%)
    ppermute x10, starting transfers between devices, shifted(): lax.ppermute(value, axis, [(i, (i + by) % count) for i in range(count)])  43.1 us
    ppermute x10, waiting for transfers between devices, shifted(): lax.ppermute(value, axis, [(i, (i + by) % count) for i in range(count)])  24.4 us
    all_gather x1, blocking collectives, block_gradients(): conv = lax.all_gather(conv, TP)  23.1 us
    all_to_all x1, blocking collectives, block_gradients(): conv = lax.all_to_all(conv, Z_ALL, 0, 0, tiled=True)  20.1 us
    ppermute x3, starting transfers between devices, swapped(): lax.ppermute(value, axis, [(i, i ^ bit) for i in range(lax.axis_size(axis...  17.6 us
    all_to_all x2, starting transfers between devices, sent_to_all(): lax.all_to_all(jnp.broadcast_to(value[None], (peers, *value.shape)), axis...  14.2 us
    pallas_call x1, Pallas kernels, output_partials(): pl.pallas_call(output_kernel, grid_spec=pltpu.PrefetchScalarGridSpec(num_...  7.17 us
    ppermute x2, starting transfers between devices, to_next(): return lax.ppermute(value, axis, pairs)  5.94 us
  transfers between devices with their start and end apart: 19, of which 8 were waited for; matrix products, arithmetic and copies ran while one was open for 7% of the time, Pallas kernels for 0%

profile of v8, /device:TPU:1, one launch (start us, length us, event | category | flops | bytes accessed | tf_op | source)
XLA Modules:
  0.0 201.0 jit_solution(11836896033244074895)
XLA Ops:
  0.6 0.8 fusion.16
  1.4 1.2 copy.45
  2.6 1.2 copy.46
  3.8 1.3 collective-permute-start.12
  5.1 4.6 %collective-permute-start.11 = (bf16[4,704]{1,0:T(4,128)(2,1)S(1)}, bf16[4,704]{1,0:T(4,128)(2,1)S(1)}, u32[]{:S(2)}, u32[]{:S(2)}) collective-permute-start(bf16[4,704]{1,0:T(4,128)(2,1)S(1)} %fusion.9), channel_id=1, source_target_pairs={{0,8},{8,16},{16,24},{24,32},{32,40},{40,48},{48,56},{56,64},{64,7... | collective-permute-start | bytes 16904 | tf_op jit(solution)/shard_map/ppermute | solution.py:28
  9.8 0.1 pad.42.clone
  9.9 0.7 collective-permute-done.11
  10.5 0.1 maximum_maximum_fusion
  10.6 0.0 copy-start.10
  10.7 0.0 copy-start.11
  10.7 0.0 copy-start.12
  10.7 1.1 broadcast_in_dim.17
  11.7 10.6 %all-to-all-start = ((bf16[8,264,256]{2,1,0:T(8,128)(2,1)}), bf16[8,264,256]{2,1,0:T(8,128)(2,1)S(1)}, u32[]{:S(2)}, u32[]{:S(2)}) async-start(bf16[8,264,256]{2,1,0:T(8,128)(2,1)} %broadcast_in_dim.17), calls=%async_computation | async-start | bytes 2162688 | tf_op jit(solution)/shard_map/all_to_all | solution.py:37
  22.4 0.1 broadcast_select_fusion.2
  22.5 3.4 %collective-permute-start.2 = (bf16[3,64,352]{2,1,0:T(8,128)(2,1)S(1)}, bf16[3,64,352]{2,1,0:T(8,128)(2,1)S(1)}, u32[]{:S(2)}, u32[]{:S(2)}) collective-permute-start(bf16[3,64,352]{2,1,0:T(8,128)(2,1)S(1)} %get-tuple-element.39), channel_id=1, source_target_pairs={{0,64},{64,128},{128,192},{192,256},{256,320},{320,384},{384,448},... | collective-permute-start | bytes 405512 | tf_op jit(solution)/shard_map/ppermute | solution.py:22
  25.9 13.1 %collective-permute-start = (bf16[3,64,352]{2,1,0:T(8,128)(2,1)S(1)}, bf16[3,64,352]{2,1,0:T(8,128)(2,1)S(1)}, u32[]{:S(2)}, u32[]{:S(2)}) collective-permute-start(bf16[3,64,352]{2,1,0:T(8,128)(2,1)S(1)} %get-tuple-element.39), channel_id=1, source_target_pairs={{0,704},{64,0},{128,64},{192,128},{256,192},{320,256},{384,320},{4... | collective-permute-start | bytes 405512 | tf_op jit(solution)/shard_map/ppermute | solution.py:22
  39.1 3.1 %collective-permute-start.1 = (bf16[3,64,352]{2,1,0:T(8,128)(2,1)S(1)}, bf16[3,64,352]{2,1,0:T(8,128)(2,1)S(1)}, u32[]{:S(2)}, u32[]{:S(2)}) collective-permute-start(bf16[3,64,352]{2,1,0:T(8,128)(2,1)S(1)} %get-tuple-element.40), channel_id=1, source_target_pairs={{0,128},{1,641},{64,192},{65,705},{128,256},{129,1},{192,320},{193... | collective-permute-start | bytes 405512 | tf_op jit(solution)/shard_map/ppermute | solution.py:56
  42.2 0.0 collective-permute-done.2
  42.3 5.0 %collective-permute-done.1 = bf16[3,64,352]{2,1,0:T(8,128)(2,1)S(1)} collective-permute-done((bf16[3,64,352]{2,1,0:T(8,128)(2,1)S(1)}, bf16[3,64,352]{2,1,0:T(8,128)(2,1)S(1)}, u32[]{:S(2)}, u32[]{:S(2)}) %collective-permute-start.1) | collective-permute-done | bytes 135200 | tf_op jit(solution)/shard_map/ppermute | solution.py:56
  47.2 0.1 select_bitcast_fusion.5
  47.3 0.1 pad_maximum_fusion.2.refs_0_
  47.5 1.9 collective-permute-start.3
  49.4 0.0 copy-start.15
  49.4 4.6 %collective-permute-start.4 = (bf16[4,3,64,352]{3,2,1,0:T(8,128)(2,1)S(1)}, bf16[4,3,64,352]{3,2,1,0:T(8,128)(2,1)S(1)}, u32[]{:S(2)}, u32[]{:S(2)}) collective-permute-start(bf16[4,3,64,352]{3,2,1,0:T(8,128)(2,1)S(1)} %pad_maximum_fusion.2.refs_0_), channel_id=1, source_target_pairs={{0,56},{8,0},{16,8},{24,16},{32,24},{40,32},{48,40},{56,48},{1,57}... | collective-permute-start | bytes 1622024 | tf_op jit(solution)/shard_map/ppermute | solution.py:22
  54.0 1.1 pad_maximum_fusion.1
  55.1 1.1 broadcast_select_fusion
  56.2 1.9 collective-permute-start.14
  58.1 1.2 collective-permute-done.3.refs_1_
  59.3 1.9 collective-permute-start.5
  61.3 4.6 %collective-permute-start.6 = (bf16[4,3,64,352]{3,2,1,0:T(8,128)(2,1)S(1)}, bf16[4,3,64,352]{3,2,1,0:T(8,128)(2,1)}, u32[]{:S(2)}, u32[]{:S(2)}) collective-permute-start(bf16[4,3,64,352]{3,2,1,0:T(8,128)(2,1)S(1)} %collective-permute-done.4.refs_2_), channel_id=1, source_target_pairs={{0,56},{8,0},{16,8},{24,16},{32,24},{40,32},{48,40},{56,48},{1,57}... | collective-permute-start | bytes 1622024 | tf_op jit(solution)/shard_map/ppermute | solution.py:22
  65.9 0.6 pad_add_fusion.places
  66.5 0.8 dynamic-slice_convert_fusion.refs_14_
  67.3 6.3 %collective-permute-done.5.refs_3_ = bf16[4,3,64,352]{3,2,1,0:T(8,128)(2,1)} collective-permute-done((bf16[4,3,64,352]{3,2,1,0:T(8,128)(2,1)S(1)}, bf16[4,3,64,352]{3,2,1,0:T(8,128)(2,1)}, u32[]{:S(2)}, u32[]{:S(2)}) %collective-permute-start.5) | collective-permute-done | bytes 540704 | tf_op jit(solution)/shard_map/ppermute | solution.py:22
  73.5 11.5 %collective-permute-start.13 = (bf16[8,264,256]{2,1,0:T(8,128)(2,1)S(1)}, bf16[8,264,256]{2,1,0:T(8,128)(2,1)}, u32[]{:S(2)}, u32[]{:S(2)}) collective-permute-start(bf16[8,264,256]{2,1,0:T(8,128)(2,1)S(1)} %all-to-all-done.refs_9_), channel_id=1, source_target_pairs={{0,1},{1,0},{2,3},{3,2},{4,5},{5,4},{6,7},{7,6},{8,9},{9,8},{10,11... | collective-permute-start | bytes 3244040 | tf_op jit(solution)/shard_map/ppermute | solution.py:32
  85.1 1.2 select_bitcast_fusion.1
  86.3 1.9 collective-permute-start.7
  88.2 4.6 %collective-permute-start.8 = (bf16[4,3,64,352]{3,2,1,0:T(8,128)(2,1)}, bf16[4,3,64,352]{3,2,1,0:T(8,128)(2,1)S(1)}, u32[]{:S(2)}, u32[]{:S(2)}) collective-permute-start(bf16[4,3,64,352]{3,2,1,0:T(8,128)(2,1)} %collective-permute-done.6.refs_4_), channel_id=1, source_target_pairs={{0,56},{8,0},{16,8},{24,16},{32,24},{40,32},{48,40},{56,48},{1,57}... | collective-permute-start | bytes 1622024 | tf_op jit(solution)/shard_map/ppermute | solution.py:22
  92.8 0.2 maximum_convert_fusion
  93.0 0.1 fusion.13
  93.1 0.1 pad_maximum_fusion
  93.2 1.0 pad.22.refs_13_
  94.2 11.3 %collective-permute-done.8.refs_6_ = bf16[4,3,64,352]{3,2,1,0:T(8,128)(2,1)S(1)} collective-permute-done((bf16[4,3,64,352]{3,2,1,0:T(8,128)(2,1)}, bf16[4,3,64,352]{3,2,1,0:T(8,128)(2,1)S(1)}, u32[]{:S(2)}, u32[]{:S(2)}) %collective-permute-start.8) | collective-permute-done | bytes 540704 | tf_op jit(solution)/shard_map/ppermute | solution.py:22
  105.5 5.2 %collective-permute-start.10 = (bf16[2,3,64,352]{3,2,1,0:T(8,128)(2,1)S(1)}, bf16[2,3,64,352]{3,2,1,0:T(8,128)(2,1)S(1)}, u32[]{:S(2)}, u32[]{:S(2)}) collective-permute-start(bf16[2,3,64,352]{3,2,1,0:T(8,128)(2,1)S(1)} %slice.108), channel_id=1, source_target_pairs={{0,56},{8,0},{16,8},{24,16},{32,24},{40,32},{48,40},{56,48},{1,57}... | collective-permute-start | bytes 811016 | tf_op jit(solution)/shard_map/ppermute | solution.py:22
  110.8 1.9 collective-permute-start.9
  112.7 0.7 fusion.12
  113.4 1.0 pad.21.refs_12_
  114.4 1.0 pad.20.refs_11_
  115.3 0.6 collective-permute-done.10.refs_8_
  115.9 5.1 %collective-permute-done.9.refs_7_ = bf16[2,3,64,352]{3,2,1,0:T(8,128)(2,1)S(1)} collective-permute-done((bf16[2,3,64,352]{3,2,1,0:T(8,128)(2,1)S(1)}, bf16[2,3,64,352]{3,2,1,0:T(8,128)(2,1)S(1)}, u32[]{:S(2)}, u32[]{:S(2)}) %collective-permute-start.9) | collective-permute-done | bytes 270368 | tf_op jit(solution)/shard_map/ppermute | solution.py:22
  121.0 0.7 copy-done.8
  121.7 5.9 %shard_map.95 = (bf16[2,256,352]{2,1,0:T(8,128)(2,1)}, bf16[2,256,352]{2,1,0:T(8,128)(2,1)}, f32[12,3,352]{2,1,0:T(4,128)}) custom-call(s32[10]{0:T(128)} %pad_add_fusion.places, bf16[4,3,64,352]{3,2,1,0:T(8,128)(2,1)} %copy-done, bf16[4,3,64,352]{3,2,1,0:T(8,128)(2,1)} %copy-done.4, bf16[4,3,64,352]{3,2,1,0:T(8,128)(2,1)} %copy-done.5, ...), custom_call_target="tpu_custom_call" | custom-call | tf_op jit(solution)/shard_map/pallas_call | solution.py:151
  127.7 0.0 copy-start.13
  127.7 7.2 %shard_map.96 = (bf16[2,4,256,256]{3,2,1,0:T(8,128)(2,1)}, bf16[2,4,256,256]{3,2,1,0:T(8,128)(2,1)}) custom-call(s32[10]{0:T(128)} %pad_add_fusion.places, bf16[4,3,64,352]{3,2,1,0:T(8,128)(2,1)} %copy-done, bf16[4,3,64,352]{3,2,1,0:T(8,128)(2,1)} %copy-done.4, bf16[4,3,64,352]{3,2,1,0:T(8,128)(2,1)} %copy-done.5, ...), custom_call_target="tpu_custom_call" | custom-call | tf_op jit(solution)/shard_map/pallas_call | solution.py:224
  134.8 4.2 %collective-permute-start.15 = (bf16[2,4,256,256]{3,2,1,0:T(8,128)(2,1)}, bf16[2,4,256,256]{3,2,1,0:T(8,128)(2,1)S(1)}, u32[]{:S(2)}, u32[]{:S(2)}) collective-permute-start(bf16[2,4,256,256]{3,2,1,0:T(8,128)(2,1)} %get-tuple-element.14), channel_id=1, source_target_pairs={{0,1},{1,0},{2,3},{3,2},{4,5},{5,4},{6,7},{7,6},{8,9},{9,8},{10,11... | collective-permute-start | bytes 3145736 | tf_op jit(solution)/shard_map/ppermute | solution.py:32
  139.1 20.1 %all_to_all.20 = f32[12,3,352]{2,1,0:T(4,128)S(1)} all-to-all(f32[12,3,352]{2,1,0:T(4,128)S(1)} %copy-done.13), channel_id=1, replica_groups=mesh['rep'=3,'zk'=2,'zp'=2,'y'=8,'x'=4,'core'=2] {'rep','zk','zp'}, dimensions={0} | all-to-all | bytes 101376 | tf_op jit(solution)/shard_map/all_to_all | solution.py:287
  159.2 0.1 broadcast_in_dim.18
  159.3 0.7 broadcast_in_dim.19
  160.0 3.6 %all-to-all-start.3 = ((f32[8,3,704]{2,1,0:T(4,128)}), f32[8,3,704]{2,1,0:T(4,128)S(1)}, u32[]{:S(2)}, u32[]{:S(2)}) async-start(f32[8,3,704]{2,1,0:T(4,128)} %broadcast_in_dim.19), calls=%async_computation.3 | async-start | bytes 196608 | tf_op jit(solution)/shard_map/all_to_all | solution.py:37
  163.6 2.4 %add_convert_fusion = bf16[2,4,256,256]{3,2,1,0:T(8,128)(2,1)} fusion(bf16[2,4,256,256]{3,2,1,0:T(8,128)(2,1)S(1)} %collective-permute-done.15, bf16[2,4,256,256]{3,2,1,0:T(8,128)(2,1)} %get-tuple-element.13), kind=kLoop, calls=%fused_computation | loop fusion | flops 2097152 | bytes 3145728 | tf_op jit(solution)/shard_map/convert_element_type | solution.py:291
  166.0 5.2 %all-to-all-done.3 = f32[8,3,704]{2,1,0:T(4,128)S(1)} async-done(((f32[8,3,704]{2,1,0:T(4,128)}), f32[8,3,704]{2,1,0:T(4,128)S(1)}, u32[]{:S(2)}, u32[]{:S(2)}) %all-to-all-start.3) | async-done | bytes 67616 | tf_op jit(solution)/shard_map/all_to_all | solution.py:37
  171.2 5.1 %all-to-all-start.1 = ((bf16[8,256,256]{2,1,0:T(8,128)(2,1)}), bf16[8,256,256]{2,1,0:T(8,128)(2,1)S(1)}, u32[]{:S(2)}, u32[]{:S(2)}) async-start(bf16[8,256,256]{2,1,0:T(8,128)(2,1)} %bitcast.11), calls=%async_computation.1 | async-start | bytes 2097152 | tf_op jit(solution)/shard_map/all_to_all | solution.py:294
  176.4 23.1 %all-gather.1 = f32[8,3,704]{2,1,0:T(4,128)S(1)} all-gather(f32[1,3,704]{2,1,0:T(4,128)S(1)} %bitcast.28), channel_id=2, replica_groups=mesh['rep'=3,'zk'=2,'zp'=2,'y'=8,'x'=4,'core'=2] {'x','core'}, dimensions={0}, use_global_device_ids=true | all-gather | bytes 76032 | tf_op jit(solution)/shard_map/all_gather | solution.py:298
  199.4 0.7 reshape.25
  200.2 0.8 reduce_sum.30
  (54 shorter events, 0.4 us)
Async XLA Ops:
  0.6 9.9 %copy-start.9 = (bf16[256,256]{1,0:T(8,128)(2,1)S(1)}, bf16[256,256]{1,0:T(8,128)(2,1)}, u32[]{:S(2)}) copy-start(bf16[256,256]{1,0:T(8,128)(2,1)} %param.8) | copy-start | bytes 393220
  3.7 8.0 %copy-start.6 = (bf16[256,704]{1,0:T(8,128)(2,1)}, bf16[256,704]{1,0:T(8,128)(2,1)S(1)}, u32[]{:S(2)}) copy-start(bf16[256,704]{1,0:T(8,128)(2,1)S(1)} %copy.46) | copy-start | bytes 1081348
  3.8 6.1 %collective-permute-start.12 = (bf16[4,704]{1,0:T(4,128)(2,1)S(1)}, bf16[4,704]{1,0:T(4,128)(2,1)S(1)}, u32[]{:S(2)}, u32[]{:S(2)}) collective-permute-start(bf16[4,704]{1,0:T(4,128)(2,1)S(1)} %fusion.10), channel_id=1, source_target_pairs={{8,0},{16,8},{24,16},{32,24},{40,32},{48,40},{56,48},{64,56},{72,6... | collective-permute-start | bytes 16904 | tf_op jit(solution)/shard_map/ppermute | solution.py:28
  5.1 5.4 %collective-permute-start.11 = (bf16[4,704]{1,0:T(4,128)(2,1)S(1)}, bf16[4,704]{1,0:T(4,128)(2,1)S(1)}, u32[]{:S(2)}, u32[]{:S(2)}) collective-permute-start(bf16[4,704]{1,0:T(4,128)(2,1)S(1)} %fusion.9), channel_id=1, source_target_pairs={{0,8},{8,16},{16,24},{24,32},{32,40},{40,48},{48,56},{56,64},{64,7... | collective-permute-start | bytes 16904 | tf_op jit(solution)/shard_map/ppermute | solution.py:28
  10.6 11.7 %copy-start.10 = (bf16[704,64]{0,1:T(8,128)(2,1)S(1)}, bf16[704,64]{0,1:T(8,128)(2,1)}, u32[]{:S(2)}) copy-start(bf16[704,64]{0,1:T(8,128)(2,1)} %param.14) | copy-start | bytes 270340
  10.7 11.7 %copy-start.11 = (bf16[64,704]{1,0:T(8,128)(2,1)S(1)}, bf16[64,704]{1,0:T(8,128)(2,1)}, u32[]{:S(2)}) copy-start(bf16[64,704]{1,0:T(8,128)(2,1)} %param.13) | copy-start | bytes 270340
  10.7 11.7 %copy-start.12 = (bf16[64,704]{1,0:T(8,128)(2,1)S(1)}, bf16[64,704]{1,0:T(8,128)(2,1)}, u32[]{:S(2)}) copy-start(bf16[64,704]{1,0:T(8,128)(2,1)} %param.12) | copy-start | bytes 270340
  11.7 61.8 %all-to-all-start = ((bf16[8,264,256]{2,1,0:T(8,128)(2,1)}), bf16[8,264,256]{2,1,0:T(8,128)(2,1)S(1)}, u32[]{:S(2)}, u32[]{:S(2)}) async-start(bf16[8,264,256]{2,1,0:T(8,128)(2,1)} %broadcast_in_dim.17), calls=%async_computation | async-start | bytes 2162688 | tf_op jit(solution)/shard_map/all_to_all | solution.py:37
  22.5 19.7 %collective-permute-start.2 = (bf16[3,64,352]{2,1,0:T(8,128)(2,1)S(1)}, bf16[3,64,352]{2,1,0:T(8,128)(2,1)S(1)}, u32[]{:S(2)}, u32[]{:S(2)}) collective-permute-start(bf16[3,64,352]{2,1,0:T(8,128)(2,1)S(1)} %get-tuple-element.39), channel_id=1, source_target_pairs={{0,64},{64,128},{128,192},{192,256},{256,320},{320,384},{384,448},... | collective-permute-start | bytes 405512 | tf_op jit(solution)/shard_map/ppermute | solution.py:22
  25.9 16.3 %collective-permute-start = (bf16[3,64,352]{2,1,0:T(8,128)(2,1)S(1)}, bf16[3,64,352]{2,1,0:T(8,128)(2,1)S(1)}, u32[]{:S(2)}, u32[]{:S(2)}) collective-permute-start(bf16[3,64,352]{2,1,0:T(8,128)(2,1)S(1)} %get-tuple-element.39), channel_id=1, source_target_pairs={{0,704},{64,0},{128,64},{192,128},{256,192},{320,256},{384,320},{4... | collective-permute-start | bytes 405512 | tf_op jit(solution)/shard_map/ppermute | solution.py:22
  39.1 8.2 %collective-permute-start.1 = (bf16[3,64,352]{2,1,0:T(8,128)(2,1)S(1)}, bf16[3,64,352]{2,1,0:T(8,128)(2,1)S(1)}, u32[]{:S(2)}, u32[]{:S(2)}) collective-permute-start(bf16[3,64,352]{2,1,0:T(8,128)(2,1)S(1)} %get-tuple-element.40), channel_id=1, source_target_pairs={{0,128},{1,641},{64,192},{65,705},{128,256},{129,1},{192,320},{193... | collective-permute-start | bytes 405512 | tf_op jit(solution)/shard_map/ppermute | solution.py:56
  47.5 8.7 %copy-start = (bf16[4,3,64,352]{3,2,1,0:T(8,128)(2,1)}, bf16[4,3,64,352]{3,2,1,0:T(8,128)(2,1)S(1)}, u32[]{:S(2)}) copy-start(bf16[4,3,64,352]{3,2,1,0:T(8,128)(2,1)S(1)} %pad_maximum_fusion.2.refs_0_) | copy-start | bytes 1622020
  47.5 11.8 %collective-permute-start.3 = (bf16[4,3,64,352]{3,2,1,0:T(8,128)(2,1)S(1)}, bf16[4,3,64,352]{3,2,1,0:T(8,128)(2,1)S(1)}, u32[]{:S(2)}, u32[]{:S(2)}) collective-permute-start(bf16[4,3,64,352]{3,2,1,0:T(8,128)(2,1)S(1)} %pad_maximum_fusion.2.refs_0_), channel_id=1, source_target_pairs={{0,8},{8,16},{16,24},{24,32},{32,40},{40,48},{48,56},{56,0},{1,9},... | collective-permute-start | bytes 1622024 | tf_op jit(solution)/shard_map/ppermute | solution.py:22
  49.4 11.8 %copy-start.15 = (s32[9]{0:T(128)S(1)}, s32[9]{0:T(128)}, u32[]{:S(2)}) copy-start(s32[9]{0:T(128)} %constant.89.clone) | copy-start | bytes 112
  49.4 11.8 %collective-permute-start.4 = (bf16[4,3,64,352]{3,2,1,0:T(8,128)(2,1)S(1)}, bf16[4,3,64,352]{3,2,1,0:T(8,128)(2,1)S(1)}, u32[]{:S(2)}, u32[]{:S(2)}) collective-permute-start(bf16[4,3,64,352]{3,2,1,0:T(8,128)(2,1)S(1)} %pad_maximum_fusion.2.refs_0_), channel_id=1, source_target_pairs={{0,56},{8,0},{16,8},{24,16},{32,24},{40,32},{48,40},{56,48},{1,57}... | collective-permute-start | bytes 1622024 | tf_op jit(solution)/shard_map/ppermute | solution.py:22
  56.2 11.1 %collective-permute-start.14 = (bf16[520,352]{1,0:T(8,128)(2,1)}, bf16[520,352]{1,0:T(8,128)(2,1)}, u32[]{:S(2)}, u32[]{:S(2)}) collective-permute-start(bf16[520,352]{1,0:T(8,128)(2,1)} %get-tuple-element.29), channel_id=1, source_target_pairs={{0,64},{64,0},{1,65},{65,1},{2,66},{66,2},{3,67},{67,3},{4,68},{68... | collective-permute-start | bytes 1098248 | tf_op jit(solution)/shard_map/ppermute | solution.py:32
  59.3 33.7 %copy-start.4 = (bf16[4,3,64,352]{3,2,1,0:T(8,128)(2,1)}, bf16[4,3,64,352]{3,2,1,0:T(8,128)(2,1)S(1)}, u32[]{:S(2)}) copy-start(bf16[4,3,64,352]{3,2,1,0:T(8,128)(2,1)S(1)} %collective-permute-done.3.refs_1_) | copy-start | bytes 1622020
  59.3 14.2 %collective-permute-start.5 = (bf16[4,3,64,352]{3,2,1,0:T(8,128)(2,1)S(1)}, bf16[4,3,64,352]{3,2,1,0:T(8,128)(2,1)}, u32[]{:S(2)}, u32[]{:S(2)}) collective-permute-start(bf16[4,3,64,352]{3,2,1,0:T(8,128)(2,1)S(1)} %collective-permute-done.3.refs_1_), channel_id=1, source_target_pairs={{0,8},{8,16},{16,24},{24,32},{32,40},{40,48},{48,56},{56,0},{1,9},... | collective-permute-start | bytes 1622024 | tf_op jit(solution)/shard_map/ppermute | solution.py:22
  61.3 31.7 %copy-start.5 = (bf16[4,3,64,352]{3,2,1,0:T(8,128)(2,1)}, bf16[4,3,64,352]{3,2,1,0:T(8,128)(2,1)S(1)}, u32[]{:S(2)}) copy-start(bf16[4,3,64,352]{3,2,1,0:T(8,128)(2,1)S(1)} %collective-permute-done.4.refs_2_) | copy-start | bytes 1622020
  61.3 26.9 %collective-permute-start.6 = (bf16[4,3,64,352]{3,2,1,0:T(8,128)(2,1)S(1)}, bf16[4,3,64,352]{3,2,1,0:T(8,128)(2,1)}, u32[]{:S(2)}, u32[]{:S(2)}) collective-permute-start(bf16[4,3,64,352]{3,2,1,0:T(8,128)(2,1)S(1)} %collective-permute-done.4.refs_2_), channel_id=1, source_target_pairs={{0,56},{8,0},{16,8},{24,16},{32,24},{40,32},{48,40},{56,48},{1,57}... | collective-permute-start | bytes 1622024 | tf_op jit(solution)/shard_map/ppermute | solution.py:22
  67.2 25.7 %copy-start.14 = (f32[3,352]{1,0:T(4,128)}, f32[3,352]{1,0:T(4,128)S(1)}, u32[]{:S(2)}) copy-start(f32[3,352]{1,0:T(4,128)S(1)} %dynamic-slice_convert_fusion.refs_14_) | copy-start | bytes 12676
  73.5 19.5 %copy-start.1 = (bf16[8,264,256]{2,1,0:T(8,128)(2,1)}, bf16[8,264,256]{2,1,0:T(8,128)(2,1)S(1)}, u32[]{:S(2)}) copy-start(bf16[8,264,256]{2,1,0:T(8,128)(2,1)S(1)} %all-to-all-done.refs_9_) | copy-start | bytes 3244036
  73.5 47.5 %collective-permute-start.13 = (bf16[8,264,256]{2,1,0:T(8,128)(2,1)S(1)}, bf16[8,264,256]{2,1,0:T(8,128)(2,1)}, u32[]{:S(2)}, u32[]{:S(2)}) collective-permute-start(bf16[8,264,256]{2,1,0:T(8,128)(2,1)S(1)} %all-to-all-done.refs_9_), channel_id=1, source_target_pairs={{0,1},{1,0},{2,3},{3,2},{4,5},{5,4},{6,7},{7,6},{8,9},{9,8},{10,11... | collective-permute-start | bytes 3244040 | tf_op jit(solution)/shard_map/ppermute | solution.py:32
  86.3 24.5 %collective-permute-start.7 = (bf16[4,3,64,352]{3,2,1,0:T(8,128)(2,1)}, bf16[4,3,64,352]{3,2,1,0:T(8,128)(2,1)S(1)}, u32[]{:S(2)}, u32[]{:S(2)}) collective-permute-start(bf16[4,3,64,352]{3,2,1,0:T(8,128)(2,1)} %collective-permute-done.5.refs_3_), channel_id=1, source_target_pairs={{0,8},{8,16},{16,24},{24,32},{32,40},{40,48},{48,56},{56,0},{1,9},... | collective-permute-start | bytes 1622024 | tf_op jit(solution)/shard_map/ppermute | solution.py:22
  88.2 17.3 %collective-permute-start.8 = (bf16[4,3,64,352]{3,2,1,0:T(8,128)(2,1)}, bf16[4,3,64,352]{3,2,1,0:T(8,128)(2,1)S(1)}, u32[]{:S(2)}, u32[]{:S(2)}) collective-permute-start(bf16[4,3,64,352]{3,2,1,0:T(8,128)(2,1)} %collective-permute-done.6.refs_4_), channel_id=1, source_target_pairs={{0,56},{8,0},{16,8},{24,16},{32,24},{40,32},{48,40},{56,48},{1,57}... | collective-permute-start | bytes 1622024 | tf_op jit(solution)/shard_map/ppermute | solution.py:22
  105.5 7.9 %copy-start.3 = (bf16[4,3,64,352]{3,2,1,0:T(8,128)(2,1)}, bf16[4,3,64,352]{3,2,1,0:T(8,128)(2,1)S(1)}, u32[]{:S(2)}) copy-start(bf16[4,3,64,352]{3,2,1,0:T(8,128)(2,1)S(1)} %collective-permute-done.8.refs_6_) | copy-start | bytes 1622020
  105.5 10.4 %collective-permute-start.10 = (bf16[2,3,64,352]{3,2,1,0:T(8,128)(2,1)S(1)}, bf16[2,3,64,352]{3,2,1,0:T(8,128)(2,1)S(1)}, u32[]{:S(2)}, u32[]{:S(2)}) collective-permute-start(bf16[2,3,64,352]{3,2,1,0:T(8,128)(2,1)S(1)} %slice.108), channel_id=1, source_target_pairs={{0,56},{8,0},{16,8},{24,16},{32,24},{40,32},{48,40},{56,48},{1,57}... | collective-permute-start | bytes 811016 | tf_op jit(solution)/shard_map/ppermute | solution.py:22
  110.7 2.7 %copy-start.2 = (bf16[4,3,64,352]{3,2,1,0:T(8,128)(2,1)}, bf16[4,3,64,352]{3,2,1,0:T(8,128)(2,1)S(1)}, u32[]{:S(2)}) copy-start(bf16[4,3,64,352]{3,2,1,0:T(8,128)(2,1)S(1)} %collective-permute-done.7.refs_5_) | copy-start | bytes 1622020
  110.8 10.2 %collective-permute-start.9 = (bf16[2,3,64,352]{3,2,1,0:T(8,128)(2,1)S(1)}, bf16[2,3,64,352]{3,2,1,0:T(8,128)(2,1)S(1)}, u32[]{:S(2)}, u32[]{:S(2)}) collective-permute-start(bf16[2,3,64,352]{3,2,1,0:T(8,128)(2,1)S(1)} %slice.107), channel_id=1, source_target_pairs={{0,8},{8,16},{16,24},{24,32},{32,40},{40,48},{48,56},{56,0},{1,9},... | collective-permute-start | bytes 811016 | tf_op jit(solution)/shard_map/ppermute | solution.py:22
  115.9 5.1 %copy-start.7 = (bf16[2,3,64,352]{3,2,1,0:T(8,128)(2,1)}, bf16[2,3,64,352]{3,2,1,0:T(8,128)(2,1)S(1)}, u32[]{:S(2)}) copy-start(bf16[2,3,64,352]{3,2,1,0:T(8,128)(2,1)S(1)} %collective-permute-done.10.refs_8_) | copy-start | bytes 811012
  121.0 0.7 copy-start.8
  127.7 11.4 %copy-start.13 = (f32[12,3,352]{2,1,0:T(4,128)S(1)}, f32[12,3,352]{2,1,0:T(4,128)}, u32[]{:S(2)}) copy-start(f32[12,3,352]{2,1,0:T(4,128)} %get-tuple-element.15) | copy-start | bytes 152068
  134.8 28.7 %collective-permute-start.15 = (bf16[2,4,256,256]{3,2,1,0:T(8,128)(2,1)}, bf16[2,4,256,256]{3,2,1,0:T(8,128)(2,1)S(1)}, u32[]{:S(2)}, u32[]{:S(2)}) collective-permute-start(bf16[2,4,256,256]{3,2,1,0:T(8,128)(2,1)} %get-tuple-element.14), channel_id=1, source_target_pairs={{0,1},{1,0},{2,3},{3,2},{4,5},{5,4},{6,7},{7,6},{8,9},{9,8},{10,11... | collective-permute-start | bytes 3145736 | tf_op jit(solution)/shard_map/ppermute | solution.py:32
  160.0 11.3 %all-to-all-start.3 = ((f32[8,3,704]{2,1,0:T(4,128)}), f32[8,3,704]{2,1,0:T(4,128)S(1)}, u32[]{:S(2)}, u32[]{:S(2)}) async-start(f32[8,3,704]{2,1,0:T(4,128)} %broadcast_in_dim.19), calls=%async_computation.3 | async-start | bytes 196608 | tf_op jit(solution)/shard_map/all_to_all | solution.py:37
  171.2 28.9 %all-to-all-start.1 = ((bf16[8,256,256]{2,1,0:T(8,128)(2,1)}), bf16[8,256,256]{2,1,0:T(8,128)(2,1)S(1)}, u32[]{:S(2)}, u32[]{:S(2)}) async-start(bf16[8,256,256]{2,1,0:T(8,128)(2,1)} %bitcast.11), calls=%async_computation.1 | async-start | bytes 2097152 | tf_op jit(solution)/shard_map/all_to_all | solution.py:294

commit v9 on v8

--- a/solution.py
+++ b/solution.py
@@ -57,7 +57,9 @@
 
 
 def gathered_z(own, other):
-    relative = [own, shifted(other, Z_ALL, -1), crossed(own, Z_ALL, 2), shifted(other, Z_ALL, 1)]
+    two_away = crossed(own, Z_ALL, 2)
+    above, below = shifted(other, Z_ALL, -1), shifted(other, Z_ALL, 1)
+    relative = [own, above, two_away, below]
     count = len(relative)
     at = lax.axis_index(("zk", "zp"))
     return jnp.stack([lax.select_n((place - at) % count, *relative) for place in range(count)])
@@ -75,7 +77,7 @@
     count = lax.axis_size("y")
     places = (lax.axis_index("y") + jnp.array(steps + [4, 4], jnp.int32)) % count
     places = jnp.append(places, lax.axis_index("core"))
-    return pieces, places.astype(jnp.int32), pieces[3]
+    return pieces, places.astype(jnp.int32), pieces[5]
 
 
 def gelu_parts(gate):
@@ -122,7 +124,7 @@
     up_out[0] = ahead(act * value[0], 1)[:rows].astype(jnp.bfloat16)
     at = lax.broadcasted_iota(jnp.int32, grad.shape, 0)
     own = jnp.where((at >= 1) & (at <= rows), grad, 0.0)
-    near = linear[0]
+    near = linear[0].astype(jnp.float32)
     sums = jnp.concatenate(
         [
             jnp.sum(own * (near if k == 0 else ahead(near, k)), axis=0, keepdims=True)
@@ -269,7 +271,6 @@
     up_ext = jnp.concatenate([edge[:, 2:3], pair[:, rows : 2 * rows], edge[:, 6:7]], axis=1)
     start = lax.axis_index(TP) * columns + jnp.where(second, half, 0)
     taps = lax.dynamic_slice_in_dim(conv_weight, start, half, 1).astype(jnp.float32)
-
     gate = taps[0] * linear[:, :-2] + taps[1] * linear[:, 1:-1] + taps[2] * linear[:, 2:]
     gelu_value, gelu_slope = gelu_parts(gate)
 
@@ -281,7 +282,7 @@
         shared,
         jnp.pad(up_ext * gelu_slope, tail),
         jnp.pad(gelu_value, tail),
-        jnp.pad(linear, ((0, 0), (0, PAD - rows - 4), (0, 0))),
+        jnp.pad(linear, ((0, 0), (0, PAD - rows - 4), (0, 0))).astype(jnp.bfloat16),
         taps,
     )
     conv = lax.all_to_all(conv, Z_ALL, 0, 0, tiled=True)

time: 202 us -> 194 us (0.960)
  waiting for transfers between devices: 35.3 us -> 26.7 us
    ppermute x10, waiting for transfers between devices: 24.4 us -> 15.8 us  [shifted(): lax.ppermute(value, axis, [(i, (i + by) % count) for i in range(count)])]
    ppermute x10, starting transfers between devices: 43.1 us -> 38.1 us  [shifted(): lax.ppermute(value, axis, [(i, (i + by) % count) for i in range(count)])]
    ppermute x3, starting transfers between devices: 17.6 us -> 22.5 us  [swapped(): lax.ppermute(value, axis, [(i, i ^ bit) for i in range(lax.axis_size(axis...]
  transfers between devices with their start and end apart: 19 -> 19, of which waited for: 8 -> 7; matrix products, arithmetic and copies ran while one was open for 7% -> 8% of each run, Pallas kernels for 0% -> 0%
where the time goes in v9:
time: 194 us; the launch traced here: 193 us
  starting transfers between devices  88.8 us (46%)
  blocking collectives  42.6 us (22%)
  waiting for transfers between devices  26.7 us (14%)
  Pallas kernels  13 us (7%)
  local copies, waits for them, and re-layouts  11.1 us (6%)
  other arithmetic  9.55 us (5%)
    ppermute x10, starting transfers between devices, shifted(): lax.ppermute(value, axis, [(i, (i + by) % count) for i in range(count)])  38.1 us
    all_gather x1, blocking collectives, block_gradients(): conv = lax.all_gather(conv, TP)  23.1 us
    ppermute x3, starting transfers between devices, swapped(): lax.ppermute(value, axis, [(i, i ^ bit) for i in range(lax.axis_size(axis...  22.5 us
    all_to_all x1, blocking collectives, block_gradients(): conv = lax.all_to_all(conv, Z_ALL, 0, 0, tiled=True)  19.5 us
    ppermute x10, waiting for transfers between devices, shifted(): lax.ppermute(value, axis, [(i, (i + by) % count) for i in range(count)])  15.8 us
    all_to_all x2, starting transfers between devices, sent_to_all(): lax.all_to_all(jnp.broadcast_to(value[None], (peers, *value.shape)), axis...  14.1 us
    pallas_call x1, Pallas kernels, output_partials(): pl.pallas_call(output_kernel, grid_spec=pltpu.PrefetchScalarGridSpec(num_...  7.18 us
    ppermute x2, starting transfers between devices, to_next(): return lax.ppermute(value, axis, pairs)  5.94 us
  transfers between devices with their start and end apart: 19, of which 7 were waited for; matrix products, arithmetic and copies ran while one was open for 8% of the time, Pallas kernels for 0%

profile of v9, /device:TPU:1, one launch (start us, length us, event | category | flops | bytes accessed | tf_op | source)
XLA Modules:
  0.0 193.0 jit_solution(10635772057734138353)
XLA Ops:
  0.6 0.8 fusion.17
  1.4 1.2 copy.45
  2.6 1.2 copy.46
  3.8 1.3 collective-permute-start.12
  5.1 4.6 %collective-permute-start.11 = (bf16[4,704]{1,0:T(4,128)(2,1)S(1)}, bf16[4,704]{1,0:T(4,128)(2,1)S(1)}, u32[]{:S(2)}, u32[]{:S(2)}) collective-permute-start(bf16[4,704]{1,0:T(4,128)(2,1)S(1)} %fusion.9), channel_id=1, source_target_pairs={{0,8},{8,16},{16,24},{24,32},{32,40},{40,48},{48,56},{56,64},{64,7... | collective-permute-start | bytes 16904 | tf_op jit(solution)/shard_map/ppermute | solution.py:28
  9.8 0.1 pad.43.clone
  9.9 0.7 collective-permute-done.11
  10.5 0.1 maximum_maximum_fusion
  10.6 0.0 copy-start.10
  10.7 0.0 copy-start.11
  10.7 1.1 broadcast_in_dim.17
  11.7 10.6 %all-to-all-start = ((bf16[8,264,256]{2,1,0:T(8,128)(2,1)}), bf16[8,264,256]{2,1,0:T(8,128)(2,1)S(1)}, u32[]{:S(2)}, u32[]{:S(2)}) async-start(bf16[8,264,256]{2,1,0:T(8,128)(2,1)} %broadcast_in_dim.17), calls=%async_computation | async-start | bytes 2162688 | tf_op jit(solution)/shard_map/all_to_all | solution.py:37
  22.4 0.1 broadcast_select_fusion.2
  22.5 3.4 %collective-permute-start.2 = (bf16[3,64,352]{2,1,0:T(8,128)(2,1)S(1)}, bf16[3,64,352]{2,1,0:T(8,128)(2,1)S(1)}, u32[]{:S(2)}, u32[]{:S(2)}) collective-permute-start(bf16[3,64,352]{2,1,0:T(8,128)(2,1)S(1)} %get-tuple-element.39), channel_id=1, source_target_pairs={{0,64},{64,128},{128,192},{192,256},{256,320},{320,384},{384,448},... | collective-permute-start | bytes 405512 | tf_op jit(solution)/shard_map/ppermute | solution.py:22
  25.9 13.1 %collective-permute-start = (bf16[3,64,352]{2,1,0:T(8,128)(2,1)S(1)}, bf16[3,64,352]{2,1,0:T(8,128)(2,1)S(1)}, u32[]{:S(2)}, u32[]{:S(2)}) collective-permute-start(bf16[3,64,352]{2,1,0:T(8,128)(2,1)S(1)} %get-tuple-element.39), channel_id=1, source_target_pairs={{0,704},{64,0},{128,64},{192,128},{256,192},{320,256},{384,320},{4... | collective-permute-start | bytes 405512 | tf_op jit(solution)/shard_map/ppermute | solution.py:22
  39.1 3.1 %collective-permute-start.1 = (bf16[3,64,352]{2,1,0:T(8,128)(2,1)S(1)}, bf16[3,64,352]{2,1,0:T(8,128)(2,1)S(1)}, u32[]{:S(2)}, u32[]{:S(2)}) collective-permute-start(bf16[3,64,352]{2,1,0:T(8,128)(2,1)S(1)} %get-tuple-element.40), channel_id=1, source_target_pairs={{0,128},{1,641},{64,192},{65,705},{128,256},{129,1},{192,320},{193... | collective-permute-start | bytes 405512 | tf_op jit(solution)/shard_map/ppermute | solution.py:56
  42.3 5.0 %collective-permute-done.1 = bf16[3,64,352]{2,1,0:T(8,128)(2,1)S(1)} collective-permute-done((bf16[3,64,352]{2,1,0:T(8,128)(2,1)S(1)}, bf16[3,64,352]{2,1,0:T(8,128)(2,1)S(1)}, u32[]{:S(2)}, u32[]{:S(2)}) %collective-permute-start.1) | collective-permute-done | bytes 135200 | tf_op jit(solution)/shard_map/ppermute | solution.py:56
  47.2 0.1 select_bitcast_fusion.5
  47.3 0.1 pad_maximum_fusion.2.refs_0_
  47.5 1.9 collective-permute-start.4
  49.4 3.4 %collective-permute-start.3 = (bf16[4,3,64,352]{3,2,1,0:T(8,128)(2,1)S(1)}, bf16[4,3,64,352]{3,2,1,0:T(8,128)(2,1)S(1)}, u32[]{:S(2)}, u32[]{:S(2)}) collective-permute-start(bf16[4,3,64,352]{3,2,1,0:T(8,128)(2,1)S(1)} %pad_maximum_fusion.2.refs_0_), channel_id=1, source_target_pairs={{0,8},{8,16},{16,24},{24,32},{32,40},{40,48},{48,56},{56,0},{1,9},... | collective-permute-start | bytes 1622024 | tf_op jit(solution)/shard_map/ppermute | solution.py:22
  52.8 5.3 %collective-permute-done.4.refs_2_ = bf16[4,3,64,352]{3,2,1,0:T(8,128)(2,1)S(1)} collective-permute-done((bf16[4,3,64,352]{3,2,1,0:T(8,128)(2,1)S(1)}, bf16[4,3,64,352]{3,2,1,0:T(8,128)(2,1)S(1)}, u32[]{:S(2)}, u32[]{:S(2)}) %collective-permute-start.4) | collective-permute-done | bytes 540704 | tf_op jit(solution)/shard_map/ppermute | solution.py:22
  58.1 3.1 %collective-permute-start.6 = (bf16[4,3,64,352]{3,2,1,0:T(8,128)(2,1)S(1)}, bf16[4,3,64,352]{3,2,1,0:T(8,128)(2,1)}, u32[]{:S(2)}, u32[]{:S(2)}) collective-permute-start(bf16[4,3,64,352]{3,2,1,0:T(8,128)(2,1)S(1)} %collective-permute-done.4.refs_2_), channel_id=1, source_target_pairs={{0,56},{8,0},{16,8},{24,16},{32,24},{40,32},{48,40},{56,48},{1,57}... | collective-permute-start | bytes 1622024 | tf_op jit(solution)/shard_map/ppermute | solution.py:22
  61.2 0.0 collective-permute-done.3.refs_1_
  61.3 2.4 %collective-permute-start.5 = (bf16[4,3,64,352]{3,2,1,0:T(8,128)(2,1)S(1)}, bf16[4,3,64,352]{3,2,1,0:T(8,128)(2,1)}, u32[]{:S(2)}, u32[]{:S(2)}) collective-permute-start(bf16[4,3,64,352]{3,2,1,0:T(8,128)(2,1)S(1)} %collective-permute-done.3.refs_1_), channel_id=1, source_target_pairs={{0,8},{8,16},{16,24},{24,32},{32,40},{40,48},{48,56},{56,0},{1,9},... | collective-permute-start | bytes 1622024 | tf_op jit(solution)/shard_map/ppermute | solution.py:22
  63.7 0.0 copy-start.15
  63.7 1.1 pad_maximum_fusion.1
  64.8 1.1 broadcast_select_fusion
  65.9 4.5 %collective-permute-start.14 = (bf16[520,352]{1,0:T(8,128)(2,1)}, bf16[520,352]{1,0:T(8,128)(2,1)S(1)}, u32[]{:S(2)}, u32[]{:S(2)}) collective-permute-start(bf16[520,352]{1,0:T(8,128)(2,1)} %get-tuple-element.29), channel_id=1, source_target_pairs={{0,64},{64,0},{1,65},{65,1},{2,66},{66,2},{3,67},{67,3},{4,68},{68... | collective-permute-start | bytes 1098248 | tf_op jit(solution)/shard_map/ppermute | solution.py:32
  70.4 1.9 collective-permute-done.6.refs_4_
  72.3 2.8 %collective-permute-start.8 = (bf16[4,3,64,352]{3,2,1,0:T(8,128)(2,1)}, bf16[4,3,64,352]{3,2,1,0:T(8,128)(2,1)S(1)}, u32[]{:S(2)}, u32[]{:S(2)}) collective-permute-start(bf16[4,3,64,352]{3,2,1,0:T(8,128)(2,1)} %collective-permute-done.6.refs_4_), channel_id=1, source_target_pairs={{0,56},{8,0},{16,8},{24,16},{32,24},{40,32},{48,40},{56,48},{1,57}... | collective-permute-start | bytes 1622024 | tf_op jit(solution)/shard_map/ppermute | solution.py:22
  75.2 0.3 collective-permute-done.5.refs_3_
  75.5 2.7 %collective-permute-start.7 = (bf16[4,3,64,352]{3,2,1,0:T(8,128)(2,1)}, bf16[4,3,64,352]{3,2,1,0:T(8,128)(2,1)S(1)}, u32[]{:S(2)}, u32[]{:S(2)}) collective-permute-start(bf16[4,3,64,352]{3,2,1,0:T(8,128)(2,1)} %collective-permute-done.5.refs_3_), channel_id=1, source_target_pairs={{0,8},{8,16},{16,24},{24,32},{32,40},{40,48},{48,56},{56,0},{1,9},... | collective-permute-start | bytes 1622024 | tf_op jit(solution)/shard_map/ppermute | solution.py:22
  78.2 0.6 pad_add_fusion.places
  78.8 0.8 dynamic-slice_convert_fusion.refs_14_
  79.6 8.3 %collective-permute-done.8.refs_6_ = bf16[4,3,64,352]{3,2,1,0:T(8,128)(2,1)S(1)} collective-permute-done((bf16[4,3,64,352]{3,2,1,0:T(8,128)(2,1)}, bf16[4,3,64,352]{3,2,1,0:T(8,128)(2,1)S(1)}, u32[]{:S(2)}, u32[]{:S(2)}) %collective-permute-start.8) | collective-permute-done | bytes 540704 | tf_op jit(solution)/shard_map/ppermute | solution.py:22
  87.9 0.8 slice.108
  88.7 2.5 %collective-permute-start.10 = (bf16[2,3,64,352]{3,2,1,0:T(8,128)(2,1)}, bf16[2,3,64,352]{3,2,1,0:T(8,128)(2,1)S(1)}, u32[]{:S(2)}, u32[]{:S(2)}) collective-permute-start(bf16[2,3,64,352]{3,2,1,0:T(8,128)(2,1)} %slice.108), channel_id=1, source_target_pairs={{0,56},{8,0},{16,8},{24,16},{32,24},{40,32},{48,40},{56,48},{1,57}... | collective-permute-start | bytes 811016 | tf_op jit(solution)/shard_map/ppermute | solution.py:22
  91.2 0.8 slice.107
  92.0 2.8 %collective-permute-start.9 = (bf16[2,3,64,352]{3,2,1,0:T(8,128)(2,1)}, bf16[2,3,64,352]{3,2,1,0:T(8,128)(2,1)}, u32[]{:S(2)}, u32[]{:S(2)}) collective-permute-start(bf16[2,3,64,352]{3,2,1,0:T(8,128)(2,1)} %slice.107), channel_id=1, source_target_pairs={{0,8},{8,16},{16,24},{24,32},{32,40},{40,48},{48,56},{56,0},{1,9},... | collective-permute-start | bytes 811016 | tf_op jit(solution)/shard_map/ppermute | solution.py:22
  94.8 1.2 select_bitcast_fusion.1
  96.1 16.0 %collective-permute-start.13 = (bf16[8,264,256]{2,1,0:T(8,128)(2,1)S(1)}, bf16[8,264,256]{2,1,0:T(8,128)(2,1)}, u32[]{:S(2)}, u32[]{:S(2)}) collective-permute-start(bf16[8,264,256]{2,1,0:T(8,128)(2,1)S(1)} %all-to-all-done.refs_9_), channel_id=1, source_target_pairs={{0,1},{1,0},{2,3},{3,2},{4,5},{5,4},{6,7},{7,6},{8,9},{9,8},{10,11... | collective-permute-start | bytes 3244040 | tf_op jit(solution)/shard_map/ppermute | solution.py:32
  112.1 0.2 maximum_convert_fusion
  112.3 0.1 fusion.14
  112.4 0.1 fusion.12
  112.5 0.8 pad.23.refs_13_
  113.4 0.1 pad_maximum_fusion
  113.5 0.7 fusion.13
  114.1 1.0 pad.22.refs_12_
  115.1 1.0 pad.21.refs_11_
  116.1 0.7 copy-done.7
  116.8 5.9 %shard_map.95 = (bf16[2,256,352]{2,1,0:T(8,128)(2,1)}, bf16[2,256,352]{2,1,0:T(8,128)(2,1)}, f32[12,3,352]{2,1,0:T(4,128)}) custom-call(s32[10]{0:T(128)} %pad_add_fusion.places, bf16[4,3,64,352]{3,2,1,0:T(8,128)(2,1)} %copy-done, bf16[4,3,64,352]{3,2,1,0:T(8,128)(2,1)} %copy-done.5, bf16[4,3,64,352]{3,2,1,0:T(8,128)(2,1)} %copy-done.4, ...), custom_call_target="tpu_custom_call" | custom-call | tf_op jit(solution)/shard_map/pallas_call | solution.py:153
  122.7 7.2 %shard_map.96 = (bf16[2,4,256,256]{3,2,1,0:T(8,128)(2,1)}, bf16[2,4,256,256]{3,2,1,0:T(8,128)(2,1)}) custom-call(s32[10]{0:T(128)} %pad_add_fusion.places, bf16[4,3,64,352]{3,2,1,0:T(8,128)(2,1)} %copy-done, bf16[4,3,64,352]{3,2,1,0:T(8,128)(2,1)} %copy-done.5, bf16[4,3,64,352]{3,2,1,0:T(8,128)(2,1)} %copy-done.4, ...), custom_call_target="tpu_custom_call" | custom-call | tf_op jit(solution)/shard_map/pallas_call | solution.py:226
  129.9 1.9 collective-permute-start.15
  131.8 19.5 %all_to_all.20 = f32[12,3,352]{2,1,0:T(4,128)S(1)} all-to-all(f32[12,3,352]{2,1,0:T(4,128)S(1)} %copy-done.13), channel_id=1, replica_groups=mesh['rep'=3,'zk'=2,'zp'=2,'y'=8,'x'=4,'core'=2] {'rep','zk','zp'}, dimensions={0} | all-to-all | bytes 101376 | tf_op jit(solution)/shard_map/all_to_all | solution.py:288
  151.4 0.1 broadcast_in_dim.18
  151.5 0.7 broadcast_in_dim.19
  152.1 3.5 %all-to-all-start.3 = ((f32[8,3,704]{2,1,0:T(4,128)}), f32[8,3,704]{2,1,0:T(4,128)S(1)}, u32[]{:S(2)}, u32[]{:S(2)}) async-start(f32[8,3,704]{2,1,0:T(4,128)} %broadcast_in_dim.19), calls=%async_computation.3 | async-start | bytes 196608 | tf_op jit(solution)/shard_map/all_to_all | solution.py:37
  155.6 2.4 %add_convert_fusion = bf16[2,4,256,256]{3,2,1,0:T(8,128)(2,1)} fusion(bf16[2,4,256,256]{3,2,1,0:T(8,128)(2,1)S(1)} %collective-permute-done.15, bf16[2,4,256,256]{3,2,1,0:T(8,128)(2,1)} %get-tuple-element.13), kind=kLoop, calls=%fused_computation | loop fusion | flops 2097152 | bytes 3145728 | tf_op jit(solution)/shard_map/convert_element_type | solution.py:292
  158.0 5.2 %all-to-all-done.3 = f32[8,3,704]{2,1,0:T(4,128)S(1)} async-done(((f32[8,3,704]{2,1,0:T(4,128)}), f32[8,3,704]{2,1,0:T(4,128)S(1)}, u32[]{:S(2)}, u32[]{:S(2)}) %all-to-all-start.3) | async-done | bytes 67616 | tf_op jit(solution)/shard_map/all_to_all | solution.py:37
  163.2 5.1 %all-to-all-start.1 = ((bf16[8,256,256]{2,1,0:T(8,128)(2,1)}), bf16[8,256,256]{2,1,0:T(8,128)(2,1)S(1)}, u32[]{:S(2)}, u32[]{:S(2)}) async-start(bf16[8,256,256]{2,1,0:T(8,128)(2,1)} %bitcast.11), calls=%async_computation.1 | async-start | bytes 2097152 | tf_op jit(solution)/shard_map/all_to_all | solution.py:295
  168.4 23.1 %all-gather.1 = f32[8,3,704]{2,1,0:T(4,128)S(1)} all-gather(f32[1,3,704]{2,1,0:T(4,128)S(1)} %bitcast.28), channel_id=2, replica_groups=mesh['rep'=3,'zk'=2,'zp'=2,'y'=8,'x'=4,'core'=2] {'x','core'}, dimensions={0}, use_global_device_ids=true | all-gather | bytes 76032 | tf_op jit(solution)/shard_map/all_gather | solution.py:299
  191.5 0.7 reshape.25
  192.2 0.8 reduce_sum.30
  (55 shorter events, 0.3 us)
Async XLA Ops:
  0.6 9.9 %copy-start.9 = (bf16[256,256]{1,0:T(8,128)(2,1)S(1)}, bf16[256,256]{1,0:T(8,128)(2,1)}, u32[]{:S(2)}) copy-start(bf16[256,256]{1,0:T(8,128)(2,1)} %param.8) | copy-start | bytes 393220
  3.7 8.0 %copy-start.6 = (bf16[256,704]{1,0:T(8,128)(2,1)}, bf16[256,704]{1,0:T(8,128)(2,1)S(1)}, u32[]{:S(2)}) copy-start(bf16[256,704]{1,0:T(8,128)(2,1)S(1)} %copy.46) | copy-start | bytes 1081348
  3.8 6.1 %collective-permute-start.12 = (bf16[4,704]{1,0:T(4,128)(2,1)S(1)}, bf16[4,704]{1,0:T(4,128)(2,1)S(1)}, u32[]{:S(2)}, u32[]{:S(2)}) collective-permute-start(bf16[4,704]{1,0:T(4,128)(2,1)S(1)} %fusion.10), channel_id=1, source_target_pairs={{8,0},{16,8},{24,16},{32,24},{40,32},{48,40},{56,48},{64,56},{72,6... | collective-permute-start | bytes 16904 | tf_op jit(solution)/shard_map/ppermute | solution.py:28
  5.1 5.4 %collective-permute-start.11 = (bf16[4,704]{1,0:T(4,128)(2,1)S(1)}, bf16[4,704]{1,0:T(4,128)(2,1)S(1)}, u32[]{:S(2)}, u32[]{:S(2)}) collective-permute-start(bf16[4,704]{1,0:T(4,128)(2,1)S(1)} %fusion.9), channel_id=1, source_target_pairs={{0,8},{8,16},{16,24},{24,32},{32,40},{40,48},{48,56},{56,64},{64,7... | collective-permute-start | bytes 16904 | tf_op jit(solution)/shard_map/ppermute | solution.py:28
  10.6 11.7 %copy-start.10 = (bf16[704,64]{0,1:T(8,128)(2,1)S(1)}, bf16[704,64]{0,1:T(8,128)(2,1)}, u32[]{:S(2)}) copy-start(bf16[704,64]{0,1:T(8,128)(2,1)} %param.14) | copy-start | bytes 270340
  10.7 11.7 %copy-start.11 = (bf16[64,704]{1,0:T(8,128)(2,1)S(1)}, bf16[64,704]{1,0:T(8,128)(2,1)}, u32[]{:S(2)}) copy-start(bf16[64,704]{1,0:T(8,128)(2,1)} %param.13) | copy-start | bytes 270340
  10.7 11.7 %copy-start.12 = (bf16[64,704]{1,0:T(8,128)(2,1)S(1)}, bf16[64,704]{1,0:T(8,128)(2,1)}, u32[]{:S(2)}) copy-start(bf16[64,704]{1,0:T(8,128)(2,1)} %param.12) | copy-start | bytes 270340
  11.7 84.3 %all-to-all-start = ((bf16[8,264,256]{2,1,0:T(8,128)(2,1)}), bf16[8,264,256]{2,1,0:T(8,128)(2,1)S(1)}, u32[]{:S(2)}, u32[]{:S(2)}) async-start(bf16[8,264,256]{2,1,0:T(8,128)(2,1)} %broadcast_in_dim.17), calls=%async_computation | async-start | bytes 2162688 | tf_op jit(solution)/shard_map/all_to_all | solution.py:37
  22.5 19.7 %collective-permute-start.2 = (bf16[3,64,352]{2,1,0:T(8,128)(2,1)S(1)}, bf16[3,64,352]{2,1,0:T(8,128)(2,1)S(1)}, u32[]{:S(2)}, u32[]{:S(2)}) collective-permute-start(bf16[3,64,352]{2,1,0:T(8,128)(2,1)S(1)} %get-tuple-element.39), channel_id=1, source_target_pairs={{0,64},{64,128},{128,192},{192,256},{256,320},{320,384},{384,448},... | collective-permute-start | bytes 405512 | tf_op jit(solution)/shard_map/ppermute | solution.py:22
  25.9 16.3 %collective-permute-start = (bf16[3,64,352]{2,1,0:T(8,128)(2,1)S(1)}, bf16[3,64,352]{2,1,0:T(8,128)(2,1)S(1)}, u32[]{:S(2)}, u32[]{:S(2)}) collective-permute-start(bf16[3,64,352]{2,1,0:T(8,128)(2,1)S(1)} %get-tuple-element.39), channel_id=1, source_target_pairs={{0,704},{64,0},{128,64},{192,128},{256,192},{320,256},{384,320},{4... | collective-permute-start | bytes 405512 | tf_op jit(solution)/shard_map/ppermute | solution.py:22
  39.1 8.2 %collective-permute-start.1 = (bf16[3,64,352]{2,1,0:T(8,128)(2,1)S(1)}, bf16[3,64,352]{2,1,0:T(8,128)(2,1)S(1)}, u32[]{:S(2)}, u32[]{:S(2)}) collective-permute-start(bf16[3,64,352]{2,1,0:T(8,128)(2,1)S(1)} %get-tuple-element.40), channel_id=1, source_target_pairs={{0,128},{1,641},{64,192},{65,705},{128,256},{129,1},{192,320},{193... | collective-permute-start | bytes 405512 | tf_op jit(solution)/shard_map/ppermute | solution.py:56
  47.5 18.4 %copy-start = (bf16[4,3,64,352]{3,2,1,0:T(8,128)(2,1)}, bf16[4,3,64,352]{3,2,1,0:T(8,128)(2,1)S(1)}, u32[]{:S(2)}) copy-start(bf16[4,3,64,352]{3,2,1,0:T(8,128)(2,1)S(1)} %pad_maximum_fusion.2.refs_0_) | copy-start | bytes 1622020
  47.5 10.6 %collective-permute-start.4 = (bf16[4,3,64,352]{3,2,1,0:T(8,128)(2,1)S(1)}, bf16[4,3,64,352]{3,2,1,0:T(8,128)(2,1)S(1)}, u32[]{:S(2)}, u32[]{:S(2)}) collective-permute-start(bf16[4,3,64,352]{3,2,1,0:T(8,128)(2,1)S(1)} %pad_maximum_fusion.2.refs_0_), channel_id=1, source_target_pairs={{0,56},{8,0},{16,8},{24,16},{32,24},{40,32},{48,40},{56,48},{1,57}... | collective-permute-start | bytes 1622024 | tf_op jit(solution)/shard_map/ppermute | solution.py:22
  49.4 11.8 %collective-permute-start.3 = (bf16[4,3,64,352]{3,2,1,0:T(8,128)(2,1)S(1)}, bf16[4,3,64,352]{3,2,1,0:T(8,128)(2,1)S(1)}, u32[]{:S(2)}, u32[]{:S(2)}) collective-permute-start(bf16[4,3,64,352]{3,2,1,0:T(8,128)(2,1)S(1)} %pad_maximum_fusion.2.refs_0_), channel_id=1, source_target_pairs={{0,8},{8,16},{16,24},{24,32},{32,40},{40,48},{48,56},{56,0},{1,9},... | collective-permute-start | bytes 1622024 | tf_op jit(solution)/shard_map/ppermute | solution.py:22
  58.1 7.7 %copy-start.4 = (bf16[4,3,64,352]{3,2,1,0:T(8,128)(2,1)}, bf16[4,3,64,352]{3,2,1,0:T(8,128)(2,1)S(1)}, u32[]{:S(2)}) copy-start(bf16[4,3,64,352]{3,2,1,0:T(8,128)(2,1)S(1)} %collective-permute-done.4.refs_2_) | copy-start | bytes 1622020
  58.1 14.2 %collective-permute-start.6 = (bf16[4,3,64,352]{3,2,1,0:T(8,128)(2,1)S(1)}, bf16[4,3,64,352]{3,2,1,0:T(8,128)(2,1)}, u32[]{:S(2)}, u32[]{:S(2)}) collective-permute-start(bf16[4,3,64,352]{3,2,1,0:T(8,128)(2,1)S(1)} %collective-permute-done.4.refs_2_), channel_id=1, source_target_pairs={{0,56},{8,0},{16,8},{24,16},{32,24},{40,32},{48,40},{56,48},{1,57}... | collective-permute-start | bytes 1622024 | tf_op jit(solution)/shard_map/ppermute | solution.py:22
  61.2 4.6 %copy-start.5 = (bf16[4,3,64,352]{3,2,1,0:T(8,128)(2,1)}, bf16[4,3,64,352]{3,2,1,0:T(8,128)(2,1)S(1)}, u32[]{:S(2)}) copy-start(bf16[4,3,64,352]{3,2,1,0:T(8,128)(2,1)S(1)} %collective-permute-done.3.refs_1_) | copy-start | bytes 1622020
  61.3 14.2 %collective-permute-start.5 = (bf16[4,3,64,352]{3,2,1,0:T(8,128)(2,1)S(1)}, bf16[4,3,64,352]{3,2,1,0:T(8,128)(2,1)}, u32[]{:S(2)}, u32[]{:S(2)}) collective-permute-start(bf16[4,3,64,352]{3,2,1,0:T(8,128)(2,1)S(1)} %collective-permute-done.3.refs_1_), channel_id=1, source_target_pairs={{0,8},{8,16},{16,24},{24,32},{32,40},{40,48},{48,56},{56,0},{1,9},... | collective-permute-start | bytes 1622024 | tf_op jit(solution)/shard_map/ppermute | solution.py:22
  63.7 14.5 %copy-start.15 = (s32[9]{0:T(128)S(1)}, s32[9]{0:T(128)}, u32[]{:S(2)}) copy-start(s32[9]{0:T(128)} %constant.90.clone) | copy-start | bytes 112
  65.9 25.3 %collective-permute-start.14 = (bf16[520,352]{1,0:T(8,128)(2,1)}, bf16[520,352]{1,0:T(8,128)(2,1)S(1)}, u32[]{:S(2)}, u32[]{:S(2)}) collective-permute-start(bf16[520,352]{1,0:T(8,128)(2,1)} %get-tuple-element.29), channel_id=1, source_target_pairs={{0,64},{64,0},{1,65},{65,1},{2,66},{66,2},{3,67},{67,3},{4,68},{68... | collective-permute-start | bytes 1098248 | tf_op jit(solution)/shard_map/ppermute | solution.py:32
  72.3 15.5 %collective-permute-start.8 = (bf16[4,3,64,352]{3,2,1,0:T(8,128)(2,1)}, bf16[4,3,64,352]{3,2,1,0:T(8,128)(2,1)S(1)}, u32[]{:S(2)}, u32[]{:S(2)}) collective-permute-start(bf16[4,3,64,352]{3,2,1,0:T(8,128)(2,1)} %collective-permute-done.6.refs_4_), channel_id=1, source_target_pairs={{0,56},{8,0},{16,8},{24,16},{32,24},{40,32},{48,40},{56,48},{1,57}... | collective-permute-start | bytes 1622024 | tf_op jit(solution)/shard_map/ppermute | solution.py:22
  75.5 15.7 %collective-permute-start.7 = (bf16[4,3,64,352]{3,2,1,0:T(8,128)(2,1)}, bf16[4,3,64,352]{3,2,1,0:T(8,128)(2,1)S(1)}, u32[]{:S(2)}, u32[]{:S(2)}) collective-permute-start(bf16[4,3,64,352]{3,2,1,0:T(8,128)(2,1)} %collective-permute-done.5.refs_3_), channel_id=1, source_target_pairs={{0,8},{8,16},{16,24},{24,32},{32,40},{40,48},{48,56},{56,0},{1,9},... | collective-permute-start | bytes 1622024 | tf_op jit(solution)/shard_map/ppermute | solution.py:22
  79.6 16.5 %copy-start.14 = (f32[3,352]{1,0:T(4,128)}, f32[3,352]{1,0:T(4,128)S(1)}, u32[]{:S(2)}) copy-start(f32[3,352]{1,0:T(4,128)S(1)} %dynamic-slice_convert_fusion.refs_14_) | copy-start | bytes 12676
  87.8 8.2 %copy-start.2 = (bf16[4,3,64,352]{3,2,1,0:T(8,128)(2,1)}, bf16[4,3,64,352]{3,2,1,0:T(8,128)(2,1)S(1)}, u32[]{:S(2)}) copy-start(bf16[4,3,64,352]{3,2,1,0:T(8,128)(2,1)S(1)} %collective-permute-done.8.refs_6_) | copy-start | bytes 1622020
  88.7 27.4 %collective-permute-start.10 = (bf16[2,3,64,352]{3,2,1,0:T(8,128)(2,1)}, bf16[2,3,64,352]{3,2,1,0:T(8,128)(2,1)S(1)}, u32[]{:S(2)}, u32[]{:S(2)}) collective-permute-start(bf16[2,3,64,352]{3,2,1,0:T(8,128)(2,1)} %slice.108), channel_id=1, source_target_pairs={{0,56},{8,0},{16,8},{24,16},{32,24},{40,32},{48,40},{56,48},{1,57}... | collective-permute-start | bytes 811016 | tf_op jit(solution)/shard_map/ppermute | solution.py:22
  91.2 0.9 copy-start.8
  91.2 21.1 %copy-start.3 = (bf16[4,3,64,352]{3,2,1,0:T(8,128)(2,1)}, bf16[4,3,64,352]{3,2,1,0:T(8,128)(2,1)S(1)}, u32[]{:S(2)}) copy-start(bf16[4,3,64,352]{3,2,1,0:T(8,128)(2,1)S(1)} %collective-permute-done.7.refs_5_) | copy-start | bytes 1622020
  92.0 24.0 %collective-permute-start.9 = (bf16[2,3,64,352]{3,2,1,0:T(8,128)(2,1)}, bf16[2,3,64,352]{3,2,1,0:T(8,128)(2,1)}, u32[]{:S(2)}, u32[]{:S(2)}) collective-permute-start(bf16[2,3,64,352]{3,2,1,0:T(8,128)(2,1)} %slice.107), channel_id=1, source_target_pairs={{0,8},{8,16},{16,24},{24,32},{32,40},{40,48},{48,56},{56,0},{1,9},... | collective-permute-start | bytes 811016 | tf_op jit(solution)/shard_map/ppermute | solution.py:22
  96.1 16.3 %copy-start.1 = (bf16[8,264,256]{2,1,0:T(8,128)(2,1)}, bf16[8,264,256]{2,1,0:T(8,128)(2,1)S(1)}, u32[]{:S(2)}) copy-start(bf16[8,264,256]{2,1,0:T(8,128)(2,1)S(1)} %all-to-all-done.refs_9_) | copy-start | bytes 3244036
  96.1 20.0 %collective-permute-start.13 = (bf16[8,264,256]{2,1,0:T(8,128)(2,1)S(1)}, bf16[8,264,256]{2,1,0:T(8,128)(2,1)}, u32[]{:S(2)}, u32[]{:S(2)}) collective-permute-start(bf16[8,264,256]{2,1,0:T(8,128)(2,1)S(1)} %all-to-all-done.refs_9_), channel_id=1, source_target_pairs={{0,1},{1,0},{2,3},{3,2},{4,5},{5,4},{6,7},{7,6},{8,9},{9,8},{10,11... | collective-permute-start | bytes 3244040 | tf_op jit(solution)/shard_map/ppermute | solution.py:32
  116.1 0.7 copy-start.7
  122.7 9.1 %copy-start.13 = (f32[12,3,352]{2,1,0:T(4,128)S(1)}, f32[12,3,352]{2,1,0:T(4,128)}, u32[]{:S(2)}) copy-start(f32[12,3,352]{2,1,0:T(4,128)} %get-tuple-element.15) | copy-start | bytes 152068
  129.9 25.7 %collective-permute-start.15 = (bf16[2,4,256,256]{3,2,1,0:T(8,128)(2,1)}, bf16[2,4,256,256]{3,2,1,0:T(8,128)(2,1)S(1)}, u32[]{:S(2)}, u32[]{:S(2)}) collective-permute-start(bf16[2,4,256,256]{3,2,1,0:T(8,128)(2,1)} %get-tuple-element.14), channel_id=1, source_target_pairs={{0,1},{1,0},{2,3},{3,2},{4,5},{5,4},{6,7},{7,6},{8,9},{9,8},{10,11... | collective-permute-start | bytes 3145736 | tf_op jit(solution)/shard_map/ppermute | solution.py:32
  152.1 11.1 %all-to-all-start.3 = ((f32[8,3,704]{2,1,0:T(4,128)}), f32[8,3,704]{2,1,0:T(4,128)S(1)}, u32[]{:S(2)}, u32[]{:S(2)}) async-start(f32[8,3,704]{2,1,0:T(4,128)} %broadcast_in_dim.19), calls=%async_computation.3 | async-start | bytes 196608 | tf_op jit(solution)/shard_map/all_to_all | solution.py:37
  163.2 29.0 %all-to-all-start.1 = ((bf16[8,256,256]{2,1,0:T(8,128)(2,1)}), bf16[8,256,256]{2,1,0:T(8,128)(2,1)S(1)}, u32[]{:S(2)}, u32[]{:S(2)}) async-start(bf16[8,256,256]{2,1,0:T(8,128)(2,1)} %bitcast.11), calls=%async_computation.1 | async-start | bytes 2097152 | tf_op jit(solution)/shard_map/all_to_all | solution.py:295
